TPU v7x, 32 devices: a whole 2x2x4 slice. The times are simulated.
32 devices in a mesh: ep: 4 (over z), tp: 8 (over y, x, core).
Axes of the slice: x: 2, y: 2, z: 4, core: 2. Of those that a mesh axis runs over, the one named last changes fastest.
Arguments:
- tokens: bfloat16 [256, 4096], P('ep', 'tp'), may hold values from -24 to 24, as said below
- state_real: float32 [256, 128, 64], P('ep', 'tp'), may hold values from -3 to 3
- state_imag: float32 [256, 128, 64], P('ep', 'tp'), may hold values from -3 to 3
- mix_gain: bfloat16 [4096], replicated, may hold values from 0.099609375 to 1.8984375
- in_weight: bfloat16 [2048, 4096], P('tp'), may hold values from -0.09375 to 0.09375
- eig_real: float32 [128, 64], P('tp'), may hold values from -1 to -0.1
- eig_imag: float32 [128, 64], P('tp'), may hold values from 0 to 200
- log_step: float32 [128], P('tp'), may hold values from -4 to 0
- input_real: float32 [128, 64, 16], P('tp'), may hold values from -1 to 1
- input_imag: float32 [128, 64, 16], P('tp'), may hold values from -1 to 1
- output_matrix_real: float32 [128, 16, 64], P('tp'), may hold values from -0.5 to 0.5
- output_matrix_imag: float32 [128, 16, 64], P('tp'), may hold values from -0.5 to 0.5
- skip_weight: float32 [2048], P('tp'), may hold values from -3 to 3
- glu_weight: bfloat16 [2048, 2048], P('tp'), may hold values from -0.375 to 0.375
- glu_bias: float32 [2048], P('tp'), may hold values from -3 to 3
- out_weight: bfloat16 [2048, 4096], P('tp'), may hold values from -0.25 to 0.25
- moe_gain: bfloat16 [4096], replicated, may hold values from 0.099609375 to 1.8984375
- routes: int32 [256, 2], P('ep'), may hold values from 0 to 7, all different within a row; in each aligned block of 64 rows (0 to 63, 64 to 127, ...) at most 24 rows name the same one
- route_weight: float32 [256, 2], P('ep'), may hold values from 0.2 to 1
- gate_weight: bfloat16 [8, 2048, 4096], P('ep', 'tp'), may hold values from -0.09375 to 0.09375
- up_weight: bfloat16 [8, 2048, 4096], P('ep', 'tp'), may hold values from -0.09375 to 0.09375
- down_weight: bfloat16 [8, 2048, 4096], P('ep', 'tp'), may hold values from -0.125 to 0.125
Outputs:
- result: bfloat16 [256, 4096], P('ep', 'tp')
- updated_state_real: float32 [256, 128, 64], P('ep', 'tp')
- updated_state_imag: float32 [256, 128, 64], P('ep', 'tp')
Inputs may be any that keep to these rules, and one draw needn't show every extreme that they name: `routes`: each row names 2 different experts. Among the rows of one index of ep, no expert is named by more than 24 rows, a bound that some expert reaches in some such blocks. `tokens`: feature blocks of the stream have scales that differ by up to a factor of ten.
All inputs are finite; a program needn't handle non-finite values.
Results may differ from a plain program's by a relative error of at most 0.013.
Values may be sent and summed in bfloat16 or wider, within the bound.
No kernel may reach another device: no remote copies, remote signals or barrier semaphores. Data moves between devices by JAX's collectives and lax.ppermute only.
A program may use at most 64 MiB of HBM per device.

v0:
```python
import functools
import jax
import jax.numpy as jnp
from jax import lax
from jax.experimental import pallas as pl
from jax.experimental.pallas import tpu as pltpu
from jax.sharding import PartitionSpec as P


norm_eps = 1e-06
f32 = jnp.float32
bf16 = jnp.bfloat16
NT = (((1,), (1,)), ((), ()))
NN = (((1,), (0,)), ((), ()))
TN = (((0,), (0,)), ((), ()))
WHOLE = pl.BlockSpec(memory_space=pltpu.VMEM)
FAR = pl.BlockSpec(memory_space=pltpu.HBM)
LANES = 128


def stay(x):
    return pltpu.with_memory_space_constraint(x, pltpu.HBM)


def dot(a, b, dims):
    return lax.dot_general(a, b, dims, preferred_element_type=f32)


def swap(x, axis, k):
    return lax.ppermute(x, axis, [(i, i ^ k) for i in range(lax.axis_size(axis))])


def gather_swaps(x, n):
    pieces = [None] * n
    pieces[0] = x
    for k in range(2, n, 2):
        pieces[k] = swap(x, "tp", k)
    for k in range(0, n, 2):
        pieces[k ^ 1] = swap(pieces[k], "tp", 1)
    return pieces


def pair_swaps(own, partner, n):
    other = swap(partner, "tp", 1)
    shape = own.shape[1:]
    return call(
        pair_body,
        [jax.ShapeDtypeStruct(shape, f32)] + [jax.ShapeDtypeStruct(shape, bf16)] * (n // 2 - 1),
        [WHOLE] * 2,
        limit=8 * 2**20,
    )(own, other)


def reduce_swaps(own, partner, n):
    first, *rest = pair_swaps(own, partner, n)
    return [first] + [swap(x, "tp", k) for x, k in zip(rest, range(2, n, 2))]


def pair_body(own, other, *outs):
    for i, out in enumerate(outs):
        out[...] = (own[i].astype(f32) + other[i].astype(f32)).astype(out.dtype)


def block_of(own, partner, k):
    return (partner if k % 2 else own), k // 2


def call(body, out_shape, in_specs, scratch=(), limit=None, flops=10**7):
    single = not isinstance(out_shape, (list, tuple))
    return pl.pallas_call(
        body,
        out_shape=out_shape,
        in_specs=in_specs,
        out_specs=WHOLE if single else [WHOLE] * len(out_shape),
        scratch_shapes=list(scratch),
        compiler_params=pltpu.CompilerParams(vmem_limit_bytes=limit),
        cost_estimate=pl.CostEstimate(flops=flops, bytes_accessed=10**6, transcendentals=0),
    )


def column(row):
    n = row.shape[1]
    at = lax.broadcasted_iota(jnp.int32, (n, n), 0)
    to = lax.broadcasted_iota(jnp.int32, (n, n), 1)
    return jnp.sum(jnp.where(at == to, jnp.broadcast_to(row, (n, n)), 0.0), axis=1, keepdims=True)


def place(k, width):
    return pl.ds(pl.multiple_of((lax.axis_index("tp") ^ k) * width, width), width)


def prep_body(n, cap, *refs):
    weight_hbm = refs[0]
    far = refs[1:16]
    dec_r, dec_i, bt_r, bt_i, cm_r, cm_i, fac, choose, table = refs[16:25]
    flat = refs[25:29]
    weight, tokens = refs[29:31]
    held = refs[31:45]
    sems, weight_sems = refs[45:]
    held = (*held, tokens)
    copies = [pltpu.make_async_copy(a, b, sems.at[i]) for i, (a, b) in enumerate(zip(far, held))]
    for copy in copies:
        copy.start()
    weights = load(weight_hbm, weight, weight_sems, n, weight.shape[2])
    copies[13].wait()
    routes = held[13]
    slots, count = table.shape
    top = routes.shape[0]
    names = lax.broadcasted_iota(jnp.int32, (16, count), 0)
    marks = [(routes[r : r + 1, :] == names).astype(f32) for r in range(top)]
    total = marks[0]
    for r in range(1, top):
        total = total + marks[r]
    row = lax.broadcasted_iota(jnp.int32, (count, count), 0)
    col = lax.broadcasted_iota(jnp.int32, (count, count), 1)
    before = dot(total.astype(bf16), (row < col).astype(bf16), NN)
    places = lax.broadcasted_iota(jnp.int32, (slots, count), 0).astype(f32)
    used = jnp.zeros((slots, count), f32)
    for r in range(top):
        rank = jnp.sum(before * marks[r], axis=0, keepdims=True)
        slot = routes[r : r + 1, :].astype(f32) * cap + rank
        hit = (places == slot).astype(f32)
        choose[r] = hit.astype(bf16)
        used = used + hit
    table[...] = used.astype(bf16)
    st_r, st_i, in_r, _, _, _ = held[:6]
    groups, inner, entries = in_r.shape
    pack = LANES // inner
    for i, dst in ((2, bt_r), (3, bt_i), (4, cm_r), (5, cm_i)):
        copies[i].wait()
        spread(held[i][...].reshape(groups * inner, entries), dst, inner, pack)
    for i in (0, 1, 10, 11, 12):
        copies[i].wait()
    real, imag, log_step = held[10][...], held[11][...], held[12][...]
    step = column(jnp.exp(log_step))
    size = jnp.exp(real * step)
    angle = imag * step
    bar_r = size * jnp.cos(angle)
    bar_i = size * jnp.sin(angle)
    modulus = real * real + imag * imag
    fac_r = ((bar_r - 1.0) * real + bar_i * imag) / modulus
    fac_i = (bar_i * real - (bar_r - 1.0) * imag) / modulus
    for g in range(groups):
        cols = slice(g * entries, (g + 1) * entries)
        s_r, s_i = st_r[:, g, :], st_i[:, g, :]
        b_r, b_i = bar_r[g : g + 1, :], bar_i[g : g + 1, :]
        dec_r[:, cols] = b_r * s_r - b_i * s_i
        dec_i[:, cols] = b_r * s_i + b_i * s_r
        fac[0:1, cols] = fac_r[g : g + 1, :]
        fac[1:2, cols] = fac_i[g : g + 1, :]
    for i in range(len(flat)):
        copies[6 + i].wait()
        rows = held[6 + i][...].astype(f32)
        for r in range(rows.shape[0]):
            flat[i][0:1, r * LANES : (r + 1) * LANES] = rows[r : r + 1, :]
    copies[14].wait()
    for copy in weights:
        copy.wait()


def spread(blocks, out, height, pack):
    rows, inner = blocks.shape
    columns = pack * inner
    at = lax.broadcasted_iota(jnp.int32, (inner, columns), 0)
    to = lax.broadcasted_iota(jnp.int32, (inner, columns), 1)
    wide = dot(blocks.astype(bf16), (to % inner == at).astype(bf16), NN)
    row = lax.broadcasted_iota(jnp.int32, (rows, columns), 0)
    col = lax.broadcasted_iota(jnp.int32, (rows, columns), 1)
    own = (row // height) % pack == col // inner
    out[...] = jnp.where(own, wide, 0.0).astype(bf16)


def load(src, dst, sems, n, width):
    copies = []
    for k in range(n):
        part = src.at[:, place(k, width)] if len(src.shape) == 2 else src.at[:, :, place(k, width)]
        copies.append(pltpu.make_async_copy(part, dst.at[k], sems.at[k]))
    for copy in copies:
        copy.start()
    return copies


def mixer_body(n, *refs):
    pieces = refs[:n]
    gain, weight, bt_r, bt_i, fac, dec_r, dec_i, cm_r, cm_i, skip = refs[n : n + 10]
    new_r_ref, new_i_ref, act_ref = refs[n + 10 :]
    width = pieces[0].shape[1]
    square = 0.0
    for k in range(n):
        x = pieces[k][...].astype(f32)
        square = square + jnp.sum(x * x, axis=1, keepdims=True)
    scale = lax.rsqrt(square / (n * width) + norm_eps)
    total = 0.0
    for k in range(n):
        part = gain[:, place(k, width)]
        normed = (pieces[k][...].astype(f32) * scale * part).astype(bf16)
        total = total + dot(normed, weight[k], NT)
    driven = total.astype(bf16)
    high = cm_r.shape[1]
    for b in range(driven.shape[1] // LANES):
        rows = slice(b * high, (b + 1) * high)
        lanes = slice(b * LANES, (b + 1) * LANES)
        u_r = dot(driven[:, lanes], bt_r[lanes, :], NN)
        u_i = dot(driven[:, lanes], bt_i[lanes, :], NN)
        f_r, f_i = fac[0:1, rows], fac[1:2, rows]
        new_r = dec_r[:, rows] + f_r * u_r - f_i * u_i
        new_i = dec_i[:, rows] + f_r * u_i + f_i * u_r
        new_r_ref[:, rows] = new_r
        new_i_ref[:, rows] = new_i
        out = dot(new_r.astype(bf16), cm_r[lanes, :], NT) - dot(new_i.astype(bf16), cm_i[lanes, :], NT)
        out = out + skip[:, lanes] * driven[:, lanes].astype(f32)
        act_ref[:, lanes] = jax.nn.gelu(out).astype(bf16)


def unpack_body(new_r, new_i, out_r, out_i):
    for src, dst in ((new_r, out_r), (new_i, out_i)):
        entries = dst.shape[2]
        for g in range(dst.shape[1]):
            dst[:, g, :] = src[:, g * entries : (g + 1) * entries]


def fetch_body(n, count, *refs):
    copies = []
    for i in range(count):
        src, dst, sems = refs[i], refs[count + i], refs[2 * count + i]
        copies += load(src, dst, sems, n, dst.shape[-1])
    for copy in copies:
        copy.wait()


def fetch(n, *sources):
    shapes = [(n, *x.shape[:-1], x.shape[-1] // n) for x in sources]
    return call(
        functools.partial(fetch_body, n, len(sources)),
        [pltpu.VMEM(x, bf16) for x in shapes],
        [FAR] * len(sources),
        [pltpu.SemaphoreType.DMA((n,))] * len(sources),
        limit=2**20,
    )(*[stay(x) for x in sources])


def glu_body(n, *refs):
    pieces = refs[:n]
    glu, bias, out_w = refs[n : n + 3]
    own, partner = refs[n + 3 :]
    gate = bias[...]
    for k in range(n):
        gate = gate + dot(pieces[k][...], glu[k], NT)
    glued = (pieces[0][...].astype(f32) * jax.nn.sigmoid(gate)).astype(bf16)
    for k in range(n):
        to, at = block_of(own, partner, k)
        to[at] = dot(glued, out_w[k], NN).astype(bf16)


def merge_body(*refs):
    out = refs[-1]
    cap = refs[0].shape[1]
    for j, x in enumerate(refs[:-1]):
        out[:, j * cap : (j + 1) * cap, :] = x[...]


def dispatch_body(m, terms, *refs):
    tokens = refs[0]
    sums = refs[1 : 1 + terms]
    table = refs[1 + terms]
    resid_ref = refs[2 + terms]
    outs = refs[3 + terms :]
    mixed = sums[0][...]
    for s in sums[1:]:
        mixed = mixed + s[...].astype(f32)
    resid = (tokens[...].astype(f32) + mixed).astype(bf16)
    resid_ref[...] = resid
    experts, cap, wide = outs[0].shape
    count = experts * cap
    for j in range(m):
        at = pl.multiple_of((lax.axis_index("ep") ^ j) * count, count)
        picked = dot(table[pl.ds(at, count), :], resid, NN).astype(bf16)
        outs[j][...] = picked.reshape(experts, cap, wide)


def up_body(n, *refs):
    near, far = refs[:n], refs[n : 2 * n]
    gain, gate_w, up_w, down_w = refs[2 * n : 2 * n + 4]
    later, own, partner = refs[2 * n + 4 :]
    experts, count, width = near[0].shape
    g, u, square = [0.0] * experts, [0.0] * experts, [0.0] * experts
    for k in range(n):
        part = gain[:, place(k, width)]
        for i in range(experts):
            x = jnp.concatenate([near[k][i], far[k][i]], axis=0).astype(f32)
            square[i] = square[i] + jnp.sum(x * x, axis=1, keepdims=True)
            x = (x * part).astype(bf16)
            g[i] = g[i] + dot(x, gate_w[k, i], NT)
            u[i] = u[i] + dot(x, up_w[k, i], NT)
    for i in range(experts):
        scale = lax.rsqrt(square[i] / (n * width) + norm_eps)
        hidden = (jax.nn.silu(g[i] * scale) * (u[i] * scale)).astype(bf16)
        later[i] = hidden[:count]
        for k in range(n):
            to, at = block_of(own, partner, k)
            to[at, i] = dot(hidden[count:], down_w[k, i], NN).astype(bf16)


def down_body(n, hidden, down_w, own, partner):
    for i in range(hidden.shape[0]):
        for k in range(n):
            to, at = block_of(own, partner, k)
            to[at, i] = dot(hidden[i], down_w[k, i], NN).astype(bf16)


def total_body(m, terms, *refs):
    sums = refs[:terms]
    outs = refs[terms:]
    total = sums[0][...]
    for s in sums[1:]:
        total = total + s[...].astype(f32)
    total = total.astype(bf16)
    cap = outs[0].shape[1]
    for j in range(m):
        outs[j][...] = total[:, j * cap : (j + 1) * cap, :]


def combine_body(m, *refs):
    resid, choose, weight = refs[:3]
    back = refs[3 : 3 + m]
    out, rows = refs[3 + m :]
    experts, cap, wide = back[0].shape
    count = experts * cap
    for j in range(m):
        at = pl.multiple_of((lax.axis_index("ep") ^ j) * count, count)
        rows[pl.ds(at, count), :] = back[j][...].reshape(count, wide)
    total = resid[...].astype(f32)
    for r in range(weight.shape[0]):
        picked = dot(choose[r], rows[...], TN)
        total = total + column(weight[r : r + 1, :]) * picked
    out[...] = total.astype(bf16)


def local_swaps(
    tokens,
    state_real,
    state_imag,
    mix_gain,
    in_weight,
    eig_real,
    eig_imag,
    log_step,
    input_real,
    input_imag,
    output_matrix_real,
    output_matrix_imag,
    skip_weight,
    glu_weight,
    glu_bias,
    out_weight,
    moe_gain,
    routes,
    route_weight,
    gate_weight,
    up_weight,
    down_weight,
):
    count, wide = tokens.shape
    n = lax.axis_size("tp")
    m = lax.axis_size("ep")
    groups, entries = eig_real.shape
    inner = input_real.shape[2]
    states = groups * entries
    channels = groups * inner
    full = wide * n
    exp_dev = gate_weight.shape[0]
    experts = exp_dev * m
    top = routes.shape[1]
    cap = max(2, (3 * top * count + 2 * experts - 1) // (2 * experts))
    slots = experts * cap

    pieces = gather_swaps(tokens, n)
    pack = LANES // inner
    far = [
        state_real,
        state_imag,
        input_real.transpose(0, 2, 1),
        input_imag.transpose(0, 2, 1),
        output_matrix_real,
        output_matrix_imag,
        skip_weight.reshape(-1, LANES),
        glu_bias.reshape(-1, LANES),
        mix_gain.reshape(-1, LANES),
        moe_gain.reshape(-1, LANES),
        eig_real,
        eig_imag,
        log_step.reshape(1, groups),
        routes.T,
        tokens,
    ]
    dec_r, dec_i, bt_r, bt_i, cm_r, cm_i, fac, choose, table, skip, bias, gain1, gain2, in_w, own = call(
        functools.partial(prep_body, n, cap),
        [jax.ShapeDtypeStruct((count, states), f32)] * 2
        + [jax.ShapeDtypeStruct((channels, pack * entries), bf16)] * 4
        + [
            jax.ShapeDtypeStruct((2, states), f32),
            jax.ShapeDtypeStruct((top, slots, count), bf16),
            jax.ShapeDtypeStruct((slots, count), bf16),
        ]
        + [jax.ShapeDtypeStruct((1, channels), f32)] * 2
        + [jax.ShapeDtypeStruct((1, full), f32)] * 2
        + [pltpu.VMEM((n, channels, wide), bf16), pltpu.VMEM((count, wide), bf16)],
        [FAR] * 16,
        [pltpu.VMEM(x.shape, x.dtype) for x in far[:-1]]
        + [pltpu.SemaphoreType.DMA((15,)), pltpu.SemaphoreType.DMA((n,))],
        limit=12 * 2**20,
    )(*[stay(x) for x in [in_weight] + far])
    pieces[0] = own

    new_r, new_i, activated = call(
        functools.partial(mixer_body, n),
        [
            jax.ShapeDtypeStruct((count, states), f32),
            jax.ShapeDtypeStruct((count, states), f32),
            jax.ShapeDtypeStruct((count, channels), bf16),
        ],
        [WHOLE] * (n + 10),
        limit=12 * 2**20,
    )(
        *pieces,
        gain1,
        in_w,
        bt_r,
        bt_i,
        fac,
        dec_r,
        dec_i,
        cm_r,
        cm_i,
        skip,
    )

    acts = gather_swaps(activated, n)
    glu_w, out_w = fetch(n, glu_weight, out_weight)
    parts = call(
        functools.partial(glu_body, n),
        [jax.ShapeDtypeStruct((n // 2, count, wide), bf16)] * 2,
        [WHOLE] * (n + 3),
        limit=12 * 2**20,
    )(*acts, glu_w, bias, out_w)

    terms = reduce_swaps(*parts, n)
    hidden = gate_weight.shape[1]
    gate_w, up_w, down_w = fetch(n, gate_weight, up_weight, down_weight)
    resid, *packed = call(
        functools.partial(dispatch_body, m, len(terms)),
        [jax.ShapeDtypeStruct((count, wide), bf16)]
        + [jax.ShapeDtypeStruct((exp_dev, cap, wide), bf16)] * m,
        [WHOLE] * (2 + len(terms)),
        limit=8 * 2**20,
    )(own, *terms, table)

    arrived = [packed[0]] + [swap(packed[j], "ep", j) for j in range(1, m)]
    half = m // 2
    fragments = []
    for group in (arrived[:half], arrived[half:]):
        merged = call(
            merge_body,
            jax.ShapeDtypeStruct((exp_dev, half * cap, wide), bf16),
            [WHOLE] * half,
            limit=2**20,
        )(*group)
        fragments += gather_swaps(merged, n)
    part = jax.ShapeDtypeStruct((n // 2, exp_dev, half * cap, wide), bf16)
    later, *far_outs = call(
        functools.partial(up_body, n),
        [jax.ShapeDtypeStruct((exp_dev, half * cap, hidden), bf16)] + [part] * 2,
        [WHOLE] * (2 * n + 4),
        limit=16 * 2**20,
    )(*fragments, gain2, gate_w, up_w, down_w)
    near_outs = call(
        functools.partial(down_body, n), [part] * 2, [WHOLE] * 2, limit=8 * 2**20
    )(later, down_w)
    back = [None] * m
    for outs, first in ((far_outs, half), (near_outs, 0)):
        terms = reduce_swaps(*outs, n)
        totals = call(
            functools.partial(total_body, half, len(terms)),
            [jax.ShapeDtypeStruct((exp_dev, cap, wide), bf16)] * half,
            [WHOLE] * len(terms),
            limit=4 * 2**20,
        )(*terms)
        for j in range(first, first + half):
            back[j] = swap(totals[j - first], "ep", j) if j else totals[0]
    new_r, new_i = call(
        unpack_body,
        [jax.ShapeDtypeStruct((count, groups, entries), f32)] * 2,
        [WHOLE] * 2,
        limit=4 * 2**20,
    )(new_r, new_i)
    result = call(
        functools.partial(combine_body, m),
        jax.ShapeDtypeStruct((count, wide), bf16),
        [WHOLE] * (3 + m),
        [pltpu.VMEM((slots, wide), bf16)],
        limit=8 * 2**20,
    )(resid, choose, route_weight.T, *back)
    return (
        result,
        new_r,
        new_i,
    )


def ssm_step(
    driven,
    state_real,
    state_imag,
    eig_real,
    eig_imag,
    log_step,
    input_real,
    input_imag,
    output_matrix_real,
    output_matrix_imag,
    skip_weight,
):
    highest_precision = lax.Precision.HIGHEST
    count_of_rows = driven.shape[0]
    groups = eig_real.shape[0]
    group_width = input_real.shape[2]
    time_step = jnp.exp(log_step)[:, None]
    magnitude = jnp.exp(eig_real * time_step)
    angle_now = eig_imag * time_step
    bar_real = magnitude * jnp.cos(angle_now)
    bar_imag = magnitude * jnp.sin(angle_now)
    modulus = eig_real * eig_real + eig_imag * eig_imag
    fac_real = ((bar_real - 1.0) * eig_real + bar_imag * eig_imag) / modulus
    fac_imag = (bar_imag * eig_real - (bar_real - 1.0) * eig_imag) / modulus
    ib_real = fac_real[..., None] * input_real - fac_imag[..., None] * input_imag
    ib_imag = fac_real[..., None] * input_imag + fac_imag[..., None] * input_real
    grouped = driven.astype(jnp.float32).reshape(count_of_rows, groups, group_width)
    push_real = jnp.einsum("gpc,ngc->ngp", ib_real, grouped, precision=highest_precision)
    push_imag = jnp.einsum("gpc,ngc->ngp", ib_imag, grouped, precision=highest_precision)
    updated_state_real = bar_real[None] * state_real - bar_imag[None] * state_imag + push_real
    updated_state_imag = bar_real[None] * state_imag + bar_imag[None] * state_real + push_imag
    state_readout = jnp.einsum(
        "jiy,sjy->sji", output_matrix_real, updated_state_real, precision=highest_precision
    ) - jnp.einsum(
        "jiy,sjy->sji", output_matrix_imag, updated_state_imag, precision=highest_precision
    )
    state_readout = state_readout.reshape(count_of_rows, groups * group_width) + skip_weight[
        None, :
    ] * driven.astype(jnp.float32)
    activated = jax.nn.gelu(state_readout).astype(jnp.bfloat16)
    return (updated_state_real, updated_state_imag, activated)


def local(
    tokens,
    state_real,
    state_imag,
    mix_gain,
    in_weight,
    eig_real,
    eig_imag,
    log_step,
    input_real,
    input_imag,
    output_matrix_real,
    output_matrix_imag,
    skip_weight,
    glu_weight,
    glu_bias,
    out_weight,
    moe_gain,
    routes,
    route_weight,
    gate_weight,
    up_weight,
    down_weight,
):
    count_of_rows = tokens.shape[0]
    n_ep = lax.axis_size("ep")
    width_tp = lax.axis_size("tp")
    whole_rows = lax.all_gather(tokens, "tp", axis=1, tiled=True)
    whole_float = whole_rows.astype(jnp.float32)
    first_scale = lax.rsqrt(jnp.mean(whole_float * whole_float, axis=1, keepdims=True) + norm_eps)
    normed = (whole_float * first_scale * mix_gain.astype(jnp.float32)).astype(jnp.bfloat16)
    driven = jnp.einsum("rd,cd->rc", normed, in_weight, preferred_element_type=jnp.float32).astype(
        jnp.bfloat16
    )
    updated_state_real, updated_state_imag, activated = ssm_step(
        driven,
        state_real,
        state_imag,
        eig_real,
        eig_imag,
        log_step,
        input_real,
        input_imag,
        output_matrix_real,
        output_matrix_imag,
        skip_weight,
    )
    gate_pre = (
        jnp.einsum(
            "rc,oc->ro",
            lax.all_gather(activated, "tp", axis=1, tiled=True),
            glu_weight,
            preferred_element_type=jnp.float32,
        )
        + glu_bias
    )
    glued = (activated.astype(jnp.float32) * jax.nn.sigmoid(gate_pre)).astype(jnp.bfloat16)
    partial_value = jnp.dot(glued, out_weight, preferred_element_type=jnp.float32)
    mixed = lax.psum_scatter(
        partial_value.astype(jnp.bfloat16), "tp", scatter_dimension=1, tiled=True
    ).astype(jnp.float32)
    residual = (tokens.astype(jnp.float32) + mixed).astype(jnp.bfloat16)
    resid_float = residual.astype(jnp.float32)
    exp_dev = gate_weight.shape[0]
    experts = exp_dev * n_ep
    top_count = routes.shape[1]
    capacity = max(2, (3 * top_count * count_of_rows + 2 * experts - 1) // (2 * experts))
    chosen = routes.reshape(-1)
    onehot = (chosen[:, None] == jnp.arange(experts, dtype=jnp.int32)[None, :]).astype(jnp.int32)
    rank_index = jnp.sum((jnp.cumsum(onehot, axis=0) - onehot) * onehot, axis=1)
    slot_index = (chosen * capacity + rank_index).reshape(count_of_rows, top_count)
    slots_all = experts * capacity
    choose = slot_index[:, :, None] == jnp.arange(slots_all, dtype=jnp.int32)[None, None, :]
    dispatch = jnp.sum(choose.astype(jnp.float32), axis=1).astype(jnp.bfloat16)
    local_sq = jnp.sum(resid_float * resid_float, axis=1)
    total_sq = lax.psum(local_sq, "tp")
    dim_full = residual.shape[1] * width_tp
    second_scale = lax.rsqrt(total_sq[:, None] / dim_full + norm_eps)
    gain_part = lax.dynamic_slice_in_dim(
        moe_gain, lax.axis_index("tp") * residual.shape[1], residual.shape[1], 0
    )
    expert_in = (resid_float * second_scale * gain_part.astype(jnp.float32)).astype(jnp.bfloat16)
    packed = jnp.einsum(
        "rs,rd->sd", dispatch, expert_in, preferred_element_type=jnp.float32
    ).astype(jnp.bfloat16)
    packed = packed.reshape(n_ep, exp_dev * capacity, residual.shape[1])
    arrived = lax.all_to_all(packed, "ep", split_axis=0, concat_axis=0, tiled=True)
    arrived = arrived.reshape(n_ep, exp_dev, capacity, residual.shape[1])
    fragment = lax.all_gather(arrived, "tp", axis=3, tiled=True)
    gate_part = jnp.einsum(
        "necd,efd->necf", fragment, gate_weight, preferred_element_type=jnp.float32
    )
    up_part = jnp.einsum("necd,efd->necf", fragment, up_weight, preferred_element_type=jnp.float32)
    hidden_width = (jax.nn.silu(gate_part) * up_part).astype(jnp.bfloat16)
    partial_out = jnp.einsum(
        "necf,efd->necd", hidden_width, down_weight, preferred_element_type=jnp.float32
    )
    summed = lax.psum_scatter(
        partial_out.astype(jnp.bfloat16), "tp", scatter_dimension=3, tiled=True
    )
    summed = summed.reshape(n_ep, exp_dev * capacity, summed.shape[3])
    returned = lax.all_to_all(summed, "ep", split_axis=0, concat_axis=0, tiled=True)
    returned = returned.reshape(slots_all, returned.shape[2])
    gathered_k = jnp.einsum(
        "rks,sd->rkd", choose.astype(jnp.bfloat16), returned, preferred_element_type=jnp.float32
    )
    result = (resid_float + jnp.sum(route_weight[..., None] * gathered_k, axis=1)).astype(
        jnp.bfloat16
    )
    return (result, updated_state_real, updated_state_imag)


def solution(mesh):
    n, m = mesh.shape["tp"], mesh.shape["ep"]
    small = n in (4, 8) and m in (2, 4)

    def whole(*args):
        if not small:
            return local(*args)
        return local_swaps(*args)

    return jax.shard_map(
        whole,
        mesh=mesh,
        in_specs=(
            P("ep", "tp"),
            P("ep", "tp", None),
            P("ep", "tp", None),
            P(),
            P("tp", None),
            P("tp", None),
            P("tp", None),
            P("tp"),
            P("tp", None, None),
            P("tp", None, None),
            P("tp", None, None),
            P("tp", None, None),
            P("tp"),
            P("tp", None),
            P("tp"),
            P("tp", None),
            P(),
            P("ep", None),
            P("ep", None),
            P("ep", "tp", None),
            P("ep", "tp", None),
            P("ep", "tp", None),
        ),
        out_specs=(P("ep", "tp"), P("ep", "tp", None), P("ep", "tp", None)),
        check_vma=False,
    )
```

profile of v0, /device:TPU:0, one launch (start us, length us, event | category | flops | bytes accessed | tf_op | source)
XLA Modules:
  0.0 89.5 jit_solution(1152584166715055835)
XLA Ops:
  0.6 3.0 %collective-permute-start.1 = (bf16[64,512]{1,0:T(8,128)(2,1)}, bf16[64,512]{1,0:T(8,128)(2,1)S(1)}, u32[]{:S(2)}, u32[]{:S(2)}) collective-permute-start(bf16[64,512]{1,0:T(8,128)(2,1)} %refs_15_.1), channel_id=1, source_target_pairs={{0,2},{1,3},{2,0},{3,1},{4,6},{5,7},{6,4},{7,5},{8,10},{9,11},{10,... | collective-permute-start | bytes 196616 | tf_op jit(solution)/shard_map/ppermute | solution.py:30
  3.7 1.5 %collective-permute-start.3 = (bf16[64,512]{1,0:T(8,128)(2,1)}, bf16[64,512]{1,0:T(8,128)(2,1)S(1)}, u32[]{:S(2)}, u32[]{:S(2)}) collective-permute-start(bf16[64,512]{1,0:T(8,128)(2,1)} %refs_15_.1), channel_id=1, source_target_pairs={{0,4},{1,5},{2,6},{3,7},{4,0},{5,1},{6,2},{7,3},{8,12},{9,13},{10,... | collective-permute-start | bytes 196616 | tf_op jit(solution)/shard_map/ppermute | solution.py:30
  5.2 1.1 %collective-permute-done.1.refs_2_ = bf16[64,512]{1,0:T(8,128)(2,1)S(1)} collective-permute-done((bf16[64,512]{1,0:T(8,128)(2,1)}, bf16[64,512]{1,0:T(8,128)(2,1)S(1)}, u32[]{:S(2)}, u32[]{:S(2)}) %collective-permute-start.1) | collective-permute-done | bytes 65568 | tf_op jit(solution)/shard_map/ppermute | solution.py:30
  6.3 1.8 %collective-permute-done.3.refs_4_ = bf16[64,512]{1,0:T(8,128)(2,1)S(1)} collective-permute-done((bf16[64,512]{1,0:T(8,128)(2,1)}, bf16[64,512]{1,0:T(8,128)(2,1)S(1)}, u32[]{:S(2)}, u32[]{:S(2)}) %collective-permute-start.3) | collective-permute-done | bytes 65568 | tf_op jit(solution)/shard_map/ppermute | solution.py:30
  8.1 2.4 %collective-permute-done.5.refs_6_ = bf16[64,512]{1,0:T(8,128)(2,1)S(1)} collective-permute-done((bf16[64,512]{1,0:T(8,128)(2,1)}, bf16[64,512]{1,0:T(8,128)(2,1)S(1)}, u32[]{:S(2)}, u32[]{:S(2)}) %collective-permute-start.5) | collective-permute-done | bytes 65568 | tf_op jit(solution)/shard_map/ppermute | solution.py:30
  10.6 3.7 %shard_map.229 = (f32[64,1024]{1,0:T(8,128)S(1)}, f32[64,1024]{1,0:T(8,128)S(1)}, bf16[256,512]{1,0:T(8,128)(2,1)S(1)}, bf16[256,512]{1,0:T(8,128)(2,1)S(1)}, bf...) custom-call(bf16[256,4096]{1,0:T(8,128)(2,1)} %refs_0_.3, ...), custom_call_target="tpu_custom_call" | custom-call | flops 10000000 | bytes 1000000 | tf_op jit(solution)/shard_map/pallas_call | solution.py:396
  14.3 1.7 %shard_map.230 = (f32[64,1024]{1,0:T(8,128)S(1)}, f32[64,1024]{1,0:T(8,128)S(1)}, bf16[64,256]{1,0:T(8,128)(2,1)S(1)}) custom-call(bf16[64,512]{1,0:T(8,128)(2,1)S(1)} %get-tuple-element.56.refs_0_, bf16[64,512]{1,0:T(8,128)(2,1)S(1)} %collective-permute-done.refs_1_, bf16[64,512]{1,0:T(8,128)(2,1)S(1)} %collective-permute-done.1.refs_2_, ...), custom_call_target="tpu_custom_call" | custom-call | flops 10000000 | bytes 1000000 | tf_op jit(solution)/shard_map/pallas_call | solution.py:415
  16.0 0.6 collective-permute-start.8
  16.6 0.8 collective-permute-start.10
  17.4 2.1 %collective-permute-start.12 = (bf16[64,256]{1,0:T(8,128)(2,1)S(1)}, bf16[64,256]{1,0:T(8,128)(2,1)S(1)}, u32[]{:S(2)}, u32[]{:S(2)}) collective-permute-start(bf16[64,256]{1,0:T(8,128)(2,1)S(1)} %get-tuple-element.67.refs_0_), channel_id=1, source_target_pairs={{0,6},{1,7},{2,4},{3,5},{4,2},{5,3},{6,0},{7,1},{8,14},{9,15},{10,... | collective-permute-start | bytes 98312 | tf_op jit(solution)/shard_map/ppermute | solution.py:30
  19.5 0.4 collective-permute-done.8.refs_2_
  19.9 0.1 collective-permute-start.9
  20.0 0.8 collective-permute-done.10.refs_4_
  20.8 1.3 %collective-permute-done.12.refs_6_ = bf16[64,256]{1,0:T(8,128)(2,1)S(1)} collective-permute-done((bf16[64,256]{1,0:T(8,128)(2,1)S(1)}, bf16[64,256]{1,0:T(8,128)(2,1)S(1)}, u32[]{:S(2)}, u32[]{:S(2)}) %collective-permute-start.12) | collective-permute-done | bytes 32800 | tf_op jit(solution)/shard_map/ppermute | solution.py:30
  22.2 2.0 %shard_map.231 = (bf16[8,256,256]{2,1,0:T(8,128)(2,1)S(1)}, bf16[8,256,512]{2,1,0:T(8,128)(2,1)S(1)}) custom-call(bf16[256,2048]{1,0:T(8,128)(2,1)} %refs_0_.4, bf16[256,4096]{1,0:T(8,128)(2,1)} %refs_1_.4), custom_call_target="tpu_custom_call" | custom-call | flops 10000000 | bytes 1000000 | tf_op jit(solution)/shard_map/pallas_call | solution.py:233
  24.3 1.4 %shard_map.232 = (bf16[4,64,512]{2,1,0:T(8,128)(2,1)S(1)}, bf16[4,64,512]{2,1,0:T(8,128)(2,1)S(1)}) custom-call(bf16[64,256]{1,0:T(8,128)(2,1)S(1)} %get-tuple-element.67.refs_0_, bf16[64,256]{1,0:T(8,128)(2,1)S(1)} %collective-permute-done.7.refs_1_, bf16[64,256]{1,0:T(8,128)(2,1)S(1)} %collective-permute-done.8.refs_2_, ...), custom_call_target="tpu_custom_call" | custom-call | flops 10000000 | bytes 1000000 | tf_op jit(solution)/shard_map/pallas_call | solution.py:440
  25.7 0.6 collective-permute-start.14
  26.2 1.2 %collective-permute-done.14.other = bf16[4,64,512]{2,1,0:T(8,128)(2,1)S(1)} collective-permute-done((bf16[4,64,512]{2,1,0:T(8,128)(2,1)S(1)}, bf16[4,64,512]{2,1,0:T(8,128)(2,1)S(1)}, u32[]{:S(2)}, u32[]{:S(2)}) %collective-permute-start.14) | collective-permute-done | bytes 262176 | tf_op jit(solution)/shard_map/ppermute | solution.py:30
  27.4 1.3 %collective-permute-start.15 = (bf16[64,512]{1,0:T(8,128)(2,1)S(1)}, bf16[64,512]{1,0:T(8,128)(2,1)S(1)}, u32[]{:S(2)}, u32[]{:S(2)}) collective-permute-start(bf16[64,512]{1,0:T(8,128)(2,1)S(1)} %get-tuple-element.74), channel_id=1, source_target_pairs={{0,2},{1,3},{2,0},{3,1},{4,6},{5,7},{6,4},{7,5},{8,10},{9,11},{10,... | collective-permute-start | bytes 196616 | tf_op jit(solution)/shard_map/ppermute | solution.py:30
  28.7 1.5 %collective-permute-start.16 = (bf16[64,512]{1,0:T(8,128)(2,1)S(1)}, bf16[64,512]{1,0:T(8,128)(2,1)S(1)}, u32[]{:S(2)}, u32[]{:S(2)}) collective-permute-start(bf16[64,512]{1,0:T(8,128)(2,1)S(1)} %get-tuple-element.75), channel_id=1, source_target_pairs={{0,4},{1,5},{2,6},{3,7},{4,0},{5,1},{6,2},{7,3},{8,12},{9,13},{10,... | collective-permute-start | bytes 196616 | tf_op jit(solution)/shard_map/ppermute | solution.py:30
  30.2 0.8 collective-permute-start.17
  31.0 0.9 collective-permute-done.15.refs_2_
  31.9 1.1 %collective-permute-done.16.refs_3_ = bf16[64,512]{1,0:T(8,128)(2,1)S(1)} collective-permute-done((bf16[64,512]{1,0:T(8,128)(2,1)S(1)}, bf16[64,512]{1,0:T(8,128)(2,1)S(1)}, u32[]{:S(2)}, u32[]{:S(2)}) %collective-permute-start.16) | collective-permute-done | bytes 65568 | tf_op jit(solution)/shard_map/ppermute | solution.py:30
  33.0 2.4 %collective-permute-done.17.refs_4_ = bf16[64,512]{1,0:T(8,128)(2,1)S(1)} collective-permute-done((bf16[64,512]{1,0:T(8,128)(2,1)S(1)}, bf16[64,512]{1,0:T(8,128)(2,1)S(1)}, u32[]{:S(2)}, u32[]{:S(2)}) %collective-permute-start.17) | collective-permute-done | bytes 65568 | tf_op jit(solution)/shard_map/ppermute | solution.py:30
  35.4 0.2 shard_map.234
  35.6 1.7 %collective-permute-start.18 = (bf16[2,24,512]{2,1,0:T(8,128)(2,1)S(1)}, bf16[2,24,512]{2,1,0:T(8,128)(2,1)S(1)}, u32[]{:S(2)}, u32[]{:S(2)}) collective-permute-start(bf16[2,24,512]{2,1,0:T(8,128)(2,1)S(1)} %get-tuple-element.81), channel_id=1, source_target_pairs={{0,8},{8,0},{16,24},{24,16},{1,9},{9,1},{17,25},{25,17},{2,10},{10... | collective-permute-start | bytes 147464 | tf_op jit(solution)/shard_map/ppermute | solution.py:30
  37.3 2.6 %collective-permute-start.26 = (bf16[2,24,512]{2,1,0:T(8,128)(2,1)S(1)}, bf16[2,24,512]{2,1,0:T(8,128)(2,1)S(1)}, u32[]{:S(2)}, u32[]{:S(2)}) collective-permute-start(bf16[2,24,512]{2,1,0:T(8,128)(2,1)S(1)} %get-tuple-element.82), channel_id=1, source_target_pairs={{0,16},{8,24},{16,0},{24,8},{1,17},{9,25},{17,1},{25,9},{2,18},{10... | collective-permute-start | bytes 147464 | tf_op jit(solution)/shard_map/ppermute | solution.py:30
  39.9 0.3 collective-permute-done.18.refs_1_
  40.1 0.1 collective-permute-start.19
  40.2 0.6 collective-permute-start.20
  40.8 0.6 collective-permute-start.22
  41.4 2.3 %collective-permute-start.24 = (bf16[2,48,512]{2,1,0:T(8,128)(2,1)S(1)}, bf16[2,48,512]{2,1,0:T(8,128)(2,1)S(1)}, u32[]{:S(2)}, u32[]{:S(2)}) collective-permute-start(bf16[2,48,512]{2,1,0:T(8,128)(2,1)S(1)} %shard_map.235.refs_0_), channel_id=1, source_target_pairs={{0,6},{1,7},{2,4},{3,5},{4,2},{5,3},{6,0},{7,1},{8,14},{9,15},{10,... | collective-permute-start | bytes 294920 | tf_op jit(solution)/shard_map/ppermute | solution.py:30
  43.8 3.3 %collective-permute-start.27 = (bf16[2,24,512]{2,1,0:T(8,128)(2,1)S(1)}, bf16[2,24,512]{2,1,0:T(8,128)(2,1)S(1)}, u32[]{:S(2)}, u32[]{:S(2)}) collective-permute-start(bf16[2,24,512]{2,1,0:T(8,128)(2,1)S(1)} %get-tuple-element.83), channel_id=1, source_target_pairs={{0,24},{8,16},{16,8},{24,0},{1,25},{9,17},{17,9},{25,1},{2,26},{10... | collective-permute-start | bytes 147464 | tf_op jit(solution)/shard_map/ppermute | solution.py:30
  47.0 2.6 %collective-permute-done.27.refs_1_ = bf16[2,24,512]{2,1,0:T(8,128)(2,1)S(1)} collective-permute-done((bf16[2,24,512]{2,1,0:T(8,128)(2,1)S(1)}, bf16[2,24,512]{2,1,0:T(8,128)(2,1)S(1)}, u32[]{:S(2)}, u32[]{:S(2)}) %collective-permute-start.27) | collective-permute-done | bytes 49184 | tf_op jit(solution)/shard_map/ppermute | solution.py:30
  49.8 0.6 collective-permute-start.29
  50.4 0.6 collective-permute-start.31
  51.0 2.3 %collective-permute-start.33 = (bf16[2,48,512]{2,1,0:T(8,128)(2,1)S(1)}, bf16[2,48,512]{2,1,0:T(8,128)(2,1)S(1)}, u32[]{:S(2)}, u32[]{:S(2)}) collective-permute-start(bf16[2,48,512]{2,1,0:T(8,128)(2,1)S(1)} %shard_map.236.refs_8_), channel_id=1, source_target_pairs={{0,6},{1,7},{2,4},{3,5},{4,2},{5,3},{6,0},{7,1},{8,14},{9,15},{10,... | collective-permute-start | bytes 294920 | tf_op jit(solution)/shard_map/ppermute | solution.py:30
  53.3 0.5 collective-permute-start.23
  53.9 1.7 %collective-permute-done.29.refs_10_ = bf16[2,48,512]{2,1,0:T(8,128)(2,1)S(1)} collective-permute-done((bf16[2,48,512]{2,1,0:T(8,128)(2,1)S(1)}, bf16[2,48,512]{2,1,0:T(8,128)(2,1)S(1)}, u32[]{:S(2)}, u32[]{:S(2)}) %collective-permute-start.29) | collective-permute-done | bytes 98336 | tf_op jit(solution)/shard_map/ppermute | solution.py:30
  55.5 1.8 %collective-permute-done.31.refs_12_ = bf16[2,48,512]{2,1,0:T(8,128)(2,1)S(1)} collective-permute-done((bf16[2,48,512]{2,1,0:T(8,128)(2,1)S(1)}, bf16[2,48,512]{2,1,0:T(8,128)(2,1)S(1)}, u32[]{:S(2)}, u32[]{:S(2)}) %collective-permute-start.31) | collective-permute-done | bytes 98336 | tf_op jit(solution)/shard_map/ppermute | solution.py:30
  57.3 0.5 collective-permute-start.32
  57.9 4.9 %shard_map.237 = (bf16[8,2,256,512]{3,2,1,0:T(8,128)(2,1)S(1)}, bf16[8,2,256,512]{3,2,1,0:T(8,128)(2,1)S(1)}, bf16[8,2,256,512]{3,2,1,0:T(8,128)(2,1)S(1)}) custom-call(bf16[2,256,4096]{2,1,0:T(8,128)(2,1)} %refs_0_.5, bf16[2,256,4096]{2,1,0:T(8,128)(2,1)} %refs_1_.5, bf16[2,256,4096]{2,1,0:T(8,128)(2,1)} %refs_2_.3), custom_call_target="tpu_custom_call" | custom-call | flops 10000000 | bytes 1000000 | tf_op jit(solution)/shard_map/pallas_call | solution.py:233
  62.8 3.4 %shard_map.238 = (bf16[2,48,256]{2,1,0:T(8,128)(2,1)S(1)}, bf16[4,2,48,512]{3,2,1,0:T(8,128)(2,1)S(1)}, bf16[4,2,48,512]{3,2,1,0:T(8,128)(2,1)S(1)}) custom-call(bf16[2,48,512]{2,1,0:T(8,128)(2,1)S(1)} %shard_map.235.refs_0_, bf16[2,48,512]{2,1,0:T(8,128)(2,1)S(1)} %collective-permute-done.19.refs_1_, ...), custom_call_target="tpu_custom_call" | custom-call | flops 10000000 | bytes 1000000 | tf_op jit(solution)/shard_map/pallas_call | solution.py:470
  66.2 0.8 shard_map.239
  67.1 0.5 collective-permute-start.35
  67.6 0.1 collective-permute-start.40
  67.7 1.3 %collective-permute-done.35.other = bf16[4,2,48,512]{3,2,1,0:T(8,128)(2,1)S(1)} collective-permute-done((bf16[4,2,48,512]{3,2,1,0:T(8,128)(2,1)S(1)}, bf16[4,2,48,512]{3,2,1,0:T(8,128)(2,1)S(1)}, u32[]{:S(2)}, u32[]{:S(2)}) %collective-permute-start.35) | collective-permute-done | bytes 393248 | tf_op jit(solution)/shard_map/ppermute | solution.py:30
  68.9 0.1 shard_map.240
  69.0 1.6 %collective-permute-start.36 = (bf16[2,48,512]{2,1,0:T(8,128)(2,1)S(1)}, bf16[2,48,512]{2,1,0:T(8,128)(2,1)S(1)}, u32[]{:S(2)}, u32[]{:S(2)}) collective-permute-start(bf16[2,48,512]{2,1,0:T(8,128)(2,1)S(1)} %get-tuple-element.92), channel_id=1, source_target_pairs={{0,2},{1,3},{2,0},{3,1},{4,6},{5,7},{6,4},{7,5},{8,10},{9,11},{10,... | collective-permute-start | bytes 294920 | tf_op jit(solution)/shard_map/ppermute | solution.py:30
  70.6 0.5 collective-permute-start.37
  71.1 1.5 %collective-permute-start.38 = (bf16[2,48,512]{2,1,0:T(8,128)(2,1)S(1)}, bf16[2,48,512]{2,1,0:T(8,128)(2,1)S(1)}, u32[]{:S(2)}, u32[]{:S(2)}) collective-permute-start(bf16[2,48,512]{2,1,0:T(8,128)(2,1)S(1)} %get-tuple-element.94), channel_id=1, source_target_pairs={{0,6},{1,7},{2,4},{3,5},{4,2},{5,3},{6,0},{7,1},{8,14},{9,15},{10,... | collective-permute-start | bytes 294920 | tf_op jit(solution)/shard_map/ppermute | solution.py:30
  72.6 0.1 shard_map.242
  72.7 1.6 %collective-permute-start.41 = (bf16[2,48,512]{2,1,0:T(8,128)(2,1)S(1)}, bf16[2,48,512]{2,1,0:T(8,128)(2,1)S(1)}, u32[]{:S(2)}, u32[]{:S(2)}) collective-permute-start(bf16[2,48,512]{2,1,0:T(8,128)(2,1)S(1)} %get-tuple-element.100), channel_id=1, source_target_pairs={{0,2},{1,3},{2,0},{3,1},{4,6},{5,7},{6,4},{7,5},{8,10},{9,11},{10,... | collective-permute-start | bytes 294920 | tf_op jit(solution)/shard_map/ppermute | solution.py:30
  74.2 0.5 collective-permute-start.42
  74.7 1.5 %collective-permute-start.43 = (bf16[2,48,512]{2,1,0:T(8,128)(2,1)S(1)}, bf16[2,48,512]{2,1,0:T(8,128)(2,1)S(1)}, u32[]{:S(2)}, u32[]{:S(2)}) collective-permute-start(bf16[2,48,512]{2,1,0:T(8,128)(2,1)S(1)} %get-tuple-element.102), channel_id=1, source_target_pairs={{0,6},{1,7},{2,4},{3,5},{4,2},{5,3},{6,0},{7,1},{8,14},{9,15},{10,... | collective-permute-start | bytes 294920 | tf_op jit(solution)/shard_map/ppermute | solution.py:30
  76.2 2.4 %collective-permute-done.37.refs_2_ = bf16[2,48,512]{2,1,0:T(8,128)(2,1)S(1)} collective-permute-done((bf16[2,48,512]{2,1,0:T(8,128)(2,1)S(1)}, bf16[2,48,512]{2,1,0:T(8,128)(2,1)S(1)}, u32[]{:S(2)}, u32[]{:S(2)}) %collective-permute-start.37) | collective-permute-done | bytes 98336 | tf_op jit(solution)/shard_map/ppermute | solution.py:30
  78.8 0.9 %collective-permute-done.41.refs_1_ = bf16[2,48,512]{2,1,0:T(8,128)(2,1)S(1)} collective-permute-done((bf16[2,48,512]{2,1,0:T(8,128)(2,1)S(1)}, bf16[2,48,512]{2,1,0:T(8,128)(2,1)S(1)}, u32[]{:S(2)}, u32[]{:S(2)}) %collective-permute-start.41) | collective-permute-done | bytes 98336 | tf_op jit(solution)/shard_map/ppermute | solution.py:30
  79.7 2.0 %collective-permute-done.42.refs_2_ = bf16[2,48,512]{2,1,0:T(8,128)(2,1)S(1)} collective-permute-done((bf16[2,48,512]{2,1,0:T(8,128)(2,1)S(1)}, bf16[2,48,512]{2,1,0:T(8,128)(2,1)S(1)}, u32[]{:S(2)}, u32[]{:S(2)}) %collective-permute-start.42) | collective-permute-done | bytes 98336 | tf_op jit(solution)/shard_map/ppermute | solution.py:30
  81.8 1.0 %collective-permute-start.44 = (bf16[2,24,512]{2,1,0:T(8,128)(2,1)S(1)}, bf16[2,24,512]{2,1,0:T(8,128)(2,1)S(1)}, u32[]{:S(2)}, u32[]{:S(2)}) collective-permute-start(bf16[2,24,512]{2,1,0:T(8,128)(2,1)S(1)} %get-tuple-element.103), channel_id=1, source_target_pairs={{0,16},{8,24},{16,0},{24,8},{1,17},{9,25},{17,1},{25,9},{2,18},{10... | collective-permute-start | bytes 147464 | tf_op jit(solution)/shard_map/ppermute | solution.py:30
  82.7 2.4 %collective-permute-start.45 = (bf16[2,24,512]{2,1,0:T(8,128)(2,1)S(1)}, bf16[2,24,512]{2,1,0:T(8,128)(2,1)S(1)}, u32[]{:S(2)}, u32[]{:S(2)}) collective-permute-start(bf16[2,24,512]{2,1,0:T(8,128)(2,1)S(1)} %get-tuple-element.104), channel_id=1, source_target_pairs={{0,24},{8,16},{16,8},{24,0},{1,25},{9,17},{17,9},{25,1},{2,26},{10... | collective-permute-start | bytes 147464 | tf_op jit(solution)/shard_map/ppermute | solution.py:30
  85.2 2.2 %shard_map.245 = (f32[64,16,64]{2,1,0:T(8,128)}, f32[64,16,64]{2,1,0:T(8,128)}) custom-call(f32[64,1024]{1,0:T(8,128)S(1)} %get-tuple-element.105.new_r, f32[64,1024]{1,0:T(8,128)S(1)} %get-tuple-element.106.new_i), custom_call_target="tpu_custom_call" | custom-call | flops 10000000 | bytes 1000000 | tf_op jit(solution)/shard_map/pallas_call | solution.py:490
  87.4 0.5 collective-permute-done.44.refs_5_
  87.9 0.7 collective-permute-done.45.refs_6_
  88.6 0.9 shard_map.244
  (47 shorter events, 0.5 us)
Async XLA Ops:
  0.6 5.7 %collective-permute-start.1 = (bf16[64,512]{1,0:T(8,128)(2,1)}, bf16[64,512]{1,0:T(8,128)(2,1)S(1)}, u32[]{:S(2)}, u32[]{:S(2)}) collective-permute-start(bf16[64,512]{1,0:T(8,128)(2,1)} %refs_15_.1), channel_id=1, source_target_pairs={{0,2},{1,3},{2,0},{3,1},{4,6},{5,7},{6,4},{7,5},{8,10},{9,11},{10,... | collective-permute-start | bytes 196616 | tf_op jit(solution)/shard_map/ppermute | solution.py:30
  3.7 4.5 %collective-permute-start.3 = (bf16[64,512]{1,0:T(8,128)(2,1)}, bf16[64,512]{1,0:T(8,128)(2,1)S(1)}, u32[]{:S(2)}, u32[]{:S(2)}) collective-permute-start(bf16[64,512]{1,0:T(8,128)(2,1)} %refs_15_.1), channel_id=1, source_target_pairs={{0,4},{1,5},{2,6},{3,7},{4,0},{5,1},{6,2},{7,3},{8,12},{9,13},{10,... | collective-permute-start | bytes 196616 | tf_op jit(solution)/shard_map/ppermute | solution.py:30
  5.2 5.4 %collective-permute-start.5 = (bf16[64,512]{1,0:T(8,128)(2,1)}, bf16[64,512]{1,0:T(8,128)(2,1)S(1)}, u32[]{:S(2)}, u32[]{:S(2)}) collective-permute-start(bf16[64,512]{1,0:T(8,128)(2,1)} %refs_15_.1), channel_id=1, source_target_pairs={{0,6},{1,7},{2,4},{3,5},{4,2},{5,3},{6,0},{7,1},{8,14},{9,15},{10,... | collective-permute-start | bytes 196616 | tf_op jit(solution)/shard_map/ppermute | solution.py:30
  5.2 9.0 %collective-permute-start = (bf16[64,512]{1,0:T(8,128)(2,1)}, bf16[64,512]{1,0:T(8,128)(2,1)S(1)}, u32[]{:S(2)}, u32[]{:S(2)}) collective-permute-start(bf16[64,512]{1,0:T(8,128)(2,1)} %refs_15_.1), channel_id=1, source_target_pairs={{0,1},{1,0},{2,3},{3,2},{4,5},{5,4},{6,7},{7,6},{8,9},{9,8},{10,11... | collective-permute-start | bytes 196616 | tf_op jit(solution)/shard_map/ppermute | solution.py:30
  6.3 7.9 %collective-permute-start.2 = (bf16[64,512]{1,0:T(8,128)(2,1)S(1)}, bf16[64,512]{1,0:T(8,128)(2,1)S(1)}, u32[]{:S(2)}, u32[]{:S(2)}) collective-permute-start(bf16[64,512]{1,0:T(8,128)(2,1)S(1)} %collective-permute-done.1.refs_2_), channel_id=1, source_target_pairs={{0,1},{1,0},{2,3},{3,2},{4,5},{5,4},{6,7},{7,6},{8,9},{9,8},{10,11... | collective-permute-start | bytes 196616 | tf_op jit(solution)/shard_map/ppermute | solution.py:30
  8.1 6.1 %collective-permute-start.4 = (bf16[64,512]{1,0:T(8,128)(2,1)S(1)}, bf16[64,512]{1,0:T(8,128)(2,1)S(1)}, u32[]{:S(2)}, u32[]{:S(2)}) collective-permute-start(bf16[64,512]{1,0:T(8,128)(2,1)S(1)} %collective-permute-done.3.refs_4_), channel_id=1, source_target_pairs={{0,1},{1,0},{2,3},{3,2},{4,5},{5,4},{6,7},{7,6},{8,9},{9,8},{10,11... | collective-permute-start | bytes 196616 | tf_op jit(solution)/shard_map/ppermute | solution.py:30
  10.6 3.7 %collective-permute-start.6 = (bf16[64,512]{1,0:T(8,128)(2,1)S(1)}, bf16[64,512]{1,0:T(8,128)(2,1)S(1)}, u32[]{:S(2)}, u32[]{:S(2)}) collective-permute-start(bf16[64,512]{1,0:T(8,128)(2,1)S(1)} %collective-permute-done.5.refs_6_), channel_id=1, source_target_pairs={{0,1},{1,0},{2,3},{3,2},{4,5},{5,4},{6,7},{7,6},{8,9},{9,8},{10,11... | collective-permute-start | bytes 196616 | tf_op jit(solution)/shard_map/ppermute | solution.py:30
  16.0 4.0 %collective-permute-start.8 = (bf16[64,256]{1,0:T(8,128)(2,1)S(1)}, bf16[64,256]{1,0:T(8,128)(2,1)S(1)}, u32[]{:S(2)}, u32[]{:S(2)}) collective-permute-start(bf16[64,256]{1,0:T(8,128)(2,1)S(1)} %get-tuple-element.67.refs_0_), channel_id=1, source_target_pairs={{0,2},{1,3},{2,0},{3,1},{4,6},{5,7},{6,4},{7,5},{8,10},{9,11},{10,... | collective-permute-start | bytes 98312 | tf_op jit(solution)/shard_map/ppermute | solution.py:30
  16.6 4.3 %collective-permute-start.10 = (bf16[64,256]{1,0:T(8,128)(2,1)S(1)}, bf16[64,256]{1,0:T(8,128)(2,1)S(1)}, u32[]{:S(2)}, u32[]{:S(2)}) collective-permute-start(bf16[64,256]{1,0:T(8,128)(2,1)S(1)} %get-tuple-element.67.refs_0_), channel_id=1, source_target_pairs={{0,4},{1,5},{2,6},{3,7},{4,0},{5,1},{6,2},{7,3},{8,12},{9,13},{10,... | collective-permute-start | bytes 98312 | tf_op jit(solution)/shard_map/ppermute | solution.py:30
  17.4 4.8 %collective-permute-start.12 = (bf16[64,256]{1,0:T(8,128)(2,1)S(1)}, bf16[64,256]{1,0:T(8,128)(2,1)S(1)}, u32[]{:S(2)}, u32[]{:S(2)}) collective-permute-start(bf16[64,256]{1,0:T(8,128)(2,1)S(1)} %get-tuple-element.67.refs_0_), channel_id=1, source_target_pairs={{0,6},{1,7},{2,4},{3,5},{4,2},{5,3},{6,0},{7,1},{8,14},{9,15},{10,... | collective-permute-start | bytes 98312 | tf_op jit(solution)/shard_map/ppermute | solution.py:30
  19.5 4.7 %collective-permute-start.7 = (bf16[64,256]{1,0:T(8,128)(2,1)S(1)}, bf16[64,256]{1,0:T(8,128)(2,1)S(1)}, u32[]{:S(2)}, u32[]{:S(2)}) collective-permute-start(bf16[64,256]{1,0:T(8,128)(2,1)S(1)} %get-tuple-element.67.refs_0_), channel_id=1, source_target_pairs={{0,1},{1,0},{2,3},{3,2},{4,5},{5,4},{6,7},{7,6},{8,9},{9,8},{10,11... | collective-permute-start | bytes 98312 | tf_op jit(solution)/shard_map/ppermute | solution.py:30
  19.9 4.3 %collective-permute-start.9 = (bf16[64,256]{1,0:T(8,128)(2,1)S(1)}, bf16[64,256]{1,0:T(8,128)(2,1)S(1)}, u32[]{:S(2)}, u32[]{:S(2)}) collective-permute-start(bf16[64,256]{1,0:T(8,128)(2,1)S(1)} %collective-permute-done.8.refs_2_), channel_id=1, source_target_pairs={{0,1},{1,0},{2,3},{3,2},{4,5},{5,4},{6,7},{7,6},{8,9},{9,8},{10,11... | collective-permute-start | bytes 98312 | tf_op jit(solution)/shard_map/ppermute | solution.py:30
  20.8 3.4 %collective-permute-start.11 = (bf16[64,256]{1,0:T(8,128)(2,1)S(1)}, bf16[64,256]{1,0:T(8,128)(2,1)S(1)}, u32[]{:S(2)}, u32[]{:S(2)}) collective-permute-start(bf16[64,256]{1,0:T(8,128)(2,1)S(1)} %collective-permute-done.10.refs_4_), channel_id=1, source_target_pairs={{0,1},{1,0},{2,3},{3,2},{4,5},{5,4},{6,7},{7,6},{8,9},{9,8},{10,11... | collective-permute-start | bytes 98312 | tf_op jit(solution)/shard_map/ppermute | solution.py:30
  22.2 2.1 %collective-permute-start.13 = (bf16[64,256]{1,0:T(8,128)(2,1)S(1)}, bf16[64,256]{1,0:T(8,128)(2,1)S(1)}, u32[]{:S(2)}, u32[]{:S(2)}) collective-permute-start(bf16[64,256]{1,0:T(8,128)(2,1)S(1)} %collective-permute-done.12.refs_6_), channel_id=1, source_target_pairs={{0,1},{1,0},{2,3},{3,2},{4,5},{5,4},{6,7},{7,6},{8,9},{9,8},{10,11... | collective-permute-start | bytes 98312 | tf_op jit(solution)/shard_map/ppermute | solution.py:30
  25.7 1.7 %collective-permute-start.14 = (bf16[4,64,512]{2,1,0:T(8,128)(2,1)S(1)}, bf16[4,64,512]{2,1,0:T(8,128)(2,1)S(1)}, u32[]{:S(2)}, u32[]{:S(2)}) collective-permute-start(bf16[4,64,512]{2,1,0:T(8,128)(2,1)S(1)} %get-tuple-element.72), channel_id=1, source_target_pairs={{0,1},{1,0},{2,3},{3,2},{4,5},{5,4},{6,7},{7,6},{8,9},{9,8},{10,11... | collective-permute-start | bytes 786440 | tf_op jit(solution)/shard_map/ppermute | solution.py:30
  27.4 4.4 %collective-permute-start.15 = (bf16[64,512]{1,0:T(8,128)(2,1)S(1)}, bf16[64,512]{1,0:T(8,128)(2,1)S(1)}, u32[]{:S(2)}, u32[]{:S(2)}) collective-permute-start(bf16[64,512]{1,0:T(8,128)(2,1)S(1)} %get-tuple-element.74), channel_id=1, source_target_pairs={{0,2},{1,3},{2,0},{3,1},{4,6},{5,7},{6,4},{7,5},{8,10},{9,11},{10,... | collective-permute-start | bytes 196616 | tf_op jit(solution)/shard_map/ppermute | solution.py:30
  28.7 4.3 %collective-permute-start.16 = (bf16[64,512]{1,0:T(8,128)(2,1)S(1)}, bf16[64,512]{1,0:T(8,128)(2,1)S(1)}, u32[]{:S(2)}, u32[]{:S(2)}) collective-permute-start(bf16[64,512]{1,0:T(8,128)(2,1)S(1)} %get-tuple-element.75), channel_id=1, source_target_pairs={{0,4},{1,5},{2,6},{3,7},{4,0},{5,1},{6,2},{7,3},{8,12},{9,13},{10,... | collective-permute-start | bytes 196616 | tf_op jit(solution)/shard_map/ppermute | solution.py:30
  30.2 5.2 %collective-permute-start.17 = (bf16[64,512]{1,0:T(8,128)(2,1)S(1)}, bf16[64,512]{1,0:T(8,128)(2,1)S(1)}, u32[]{:S(2)}, u32[]{:S(2)}) collective-permute-start(bf16[64,512]{1,0:T(8,128)(2,1)S(1)} %get-tuple-element.76), channel_id=1, source_target_pairs={{0,6},{1,7},{2,4},{3,5},{4,2},{5,3},{6,0},{7,1},{8,14},{9,15},{10,... | collective-permute-start | bytes 196616 | tf_op jit(solution)/shard_map/ppermute | solution.py:30
  35.6 4.5 %collective-permute-start.18 = (bf16[2,24,512]{2,1,0:T(8,128)(2,1)S(1)}, bf16[2,24,512]{2,1,0:T(8,128)(2,1)S(1)}, u32[]{:S(2)}, u32[]{:S(2)}) collective-permute-start(bf16[2,24,512]{2,1,0:T(8,128)(2,1)S(1)} %get-tuple-element.81), channel_id=1, source_target_pairs={{0,8},{8,0},{16,24},{24,16},{1,9},{9,1},{17,25},{25,17},{2,10},{10... | collective-permute-start | bytes 147464 | tf_op jit(solution)/shard_map/ppermute | solution.py:30
  37.3 6.5 %collective-permute-start.26 = (bf16[2,24,512]{2,1,0:T(8,128)(2,1)S(1)}, bf16[2,24,512]{2,1,0:T(8,128)(2,1)S(1)}, u32[]{:S(2)}, u32[]{:S(2)}) collective-permute-start(bf16[2,24,512]{2,1,0:T(8,128)(2,1)S(1)} %get-tuple-element.82), channel_id=1, source_target_pairs={{0,16},{8,24},{16,0},{24,8},{1,17},{9,25},{17,1},{25,9},{2,18},{10... | collective-permute-start | bytes 147464 | tf_op jit(solution)/shard_map/ppermute | solution.py:30
  40.1 9.6 %collective-permute-start.19 = (bf16[2,48,512]{2,1,0:T(8,128)(2,1)S(1)}, bf16[2,48,512]{2,1,0:T(8,128)(2,1)S(1)}, u32[]{:S(2)}, u32[]{:S(2)}) collective-permute-start(bf16[2,48,512]{2,1,0:T(8,128)(2,1)S(1)} %shard_map.235.refs_0_), channel_id=1, source_target_pairs={{0,1},{1,0},{2,3},{3,2},{4,5},{5,4},{6,7},{7,6},{8,9},{9,8},{10,11... | collective-permute-start | bytes 294920 | tf_op jit(solution)/shard_map/ppermute | solution.py:30
  40.2 10.1 %collective-permute-start.20 = (bf16[2,48,512]{2,1,0:T(8,128)(2,1)S(1)}, bf16[2,48,512]{2,1,0:T(8,128)(2,1)S(1)}, u32[]{:S(2)}, u32[]{:S(2)}) collective-permute-start(bf16[2,48,512]{2,1,0:T(8,128)(2,1)S(1)} %shard_map.235.refs_0_), channel_id=1, source_target_pairs={{0,2},{1,3},{2,0},{3,1},{4,6},{5,7},{6,4},{7,5},{8,10},{9,11},{10,... | collective-permute-start | bytes 294920 | tf_op jit(solution)/shard_map/ppermute | solution.py:30
  40.8 10.2 %collective-permute-start.22 = (bf16[2,48,512]{2,1,0:T(8,128)(2,1)S(1)}, bf16[2,48,512]{2,1,0:T(8,128)(2,1)S(1)}, u32[]{:S(2)}, u32[]{:S(2)}) collective-permute-start(bf16[2,48,512]{2,1,0:T(8,128)(2,1)S(1)} %shard_map.235.refs_0_), channel_id=1, source_target_pairs={{0,4},{1,5},{2,6},{3,7},{4,0},{5,1},{6,2},{7,3},{8,12},{9,13},{10,... | collective-permute-start | bytes 294920 | tf_op jit(solution)/shard_map/ppermute | solution.py:30
  41.4 11.9 %collective-permute-start.24 = (bf16[2,48,512]{2,1,0:T(8,128)(2,1)S(1)}, bf16[2,48,512]{2,1,0:T(8,128)(2,1)S(1)}, u32[]{:S(2)}, u32[]{:S(2)}) collective-permute-start(bf16[2,48,512]{2,1,0:T(8,128)(2,1)S(1)} %shard_map.235.refs_0_), channel_id=1, source_target_pairs={{0,6},{1,7},{2,4},{3,5},{4,2},{5,3},{6,0},{7,1},{8,14},{9,15},{10,... | collective-permute-start | bytes 294920 | tf_op jit(solution)/shard_map/ppermute | solution.py:30
  43.8 5.9 %collective-permute-start.27 = (bf16[2,24,512]{2,1,0:T(8,128)(2,1)S(1)}, bf16[2,24,512]{2,1,0:T(8,128)(2,1)S(1)}, u32[]{:S(2)}, u32[]{:S(2)}) collective-permute-start(bf16[2,24,512]{2,1,0:T(8,128)(2,1)S(1)} %get-tuple-element.83), channel_id=1, source_target_pairs={{0,24},{8,16},{16,8},{24,0},{1,25},{9,17},{17,9},{25,1},{2,26},{10... | collective-permute-start | bytes 147464 | tf_op jit(solution)/shard_map/ppermute | solution.py:30
  49.7 3.7 %collective-permute-start.28 = (bf16[2,48,512]{2,1,0:T(8,128)(2,1)S(1)}, bf16[2,48,512]{2,1,0:T(8,128)(2,1)S(1)}, u32[]{:S(2)}, u32[]{:S(2)}) collective-permute-start(bf16[2,48,512]{2,1,0:T(8,128)(2,1)S(1)} %shard_map.236.refs_8_), channel_id=1, source_target_pairs={{0,1},{1,0},{2,3},{3,2},{4,5},{5,4},{6,7},{7,6},{8,9},{9,8},{10,11... | collective-permute-start | bytes 294920 | tf_op jit(solution)/shard_map/ppermute | solution.py:30
  49.8 5.7 %collective-permute-start.29 = (bf16[2,48,512]{2,1,0:T(8,128)(2,1)S(1)}, bf16[2,48,512]{2,1,0:T(8,128)(2,1)S(1)}, u32[]{:S(2)}, u32[]{:S(2)}) collective-permute-start(bf16[2,48,512]{2,1,0:T(8,128)(2,1)S(1)} %shard_map.236.refs_8_), channel_id=1, source_target_pairs={{0,2},{1,3},{2,0},{3,1},{4,6},{5,7},{6,4},{7,5},{8,10},{9,11},{10,... | collective-permute-start | bytes 294920 | tf_op jit(solution)/shard_map/ppermute | solution.py:30
  50.4 7.0 %collective-permute-start.31 = (bf16[2,48,512]{2,1,0:T(8,128)(2,1)S(1)}, bf16[2,48,512]{2,1,0:T(8,128)(2,1)S(1)}, u32[]{:S(2)}, u32[]{:S(2)}) collective-permute-start(bf16[2,48,512]{2,1,0:T(8,128)(2,1)S(1)} %shard_map.236.refs_8_), channel_id=1, source_target_pairs={{0,4},{1,5},{2,6},{3,7},{4,0},{5,1},{6,2},{7,3},{8,12},{9,13},{10,... | collective-permute-start | bytes 294920 | tf_op jit(solution)/shard_map/ppermute | solution.py:30
  51.0 6.3 %collective-permute-start.33 = (bf16[2,48,512]{2,1,0:T(8,128)(2,1)S(1)}, bf16[2,48,512]{2,1,0:T(8,128)(2,1)S(1)}, u32[]{:S(2)}, u32[]{:S(2)}) collective-permute-start(bf16[2,48,512]{2,1,0:T(8,128)(2,1)S(1)} %shard_map.236.refs_8_), channel_id=1, source_target_pairs={{0,6},{1,7},{2,4},{3,5},{4,2},{5,3},{6,0},{7,1},{8,14},{9,15},{10,... | collective-permute-start | bytes 294920 | tf_op jit(solution)/shard_map/ppermute | solution.py:30
  53.3 4.5 %collective-permute-start.21 = (bf16[2,48,512]{2,1,0:T(8,128)(2,1)S(1)}, bf16[2,48,512]{2,1,0:T(8,128)(2,1)S(1)}, u32[]{:S(2)}, u32[]{:S(2)}) collective-permute-start(bf16[2,48,512]{2,1,0:T(8,128)(2,1)S(1)} %collective-permute-done.20.refs_2_), channel_id=1, source_target_pairs={{0,1},{1,0},{2,3},{3,2},{4,5},{5,4},{6,7},{7,6},{8,9},{9,8},{10,11... | collective-permute-start | bytes 294920 | tf_op jit(solution)/shard_map/ppermute | solution.py:30
  53.3 9.4 %collective-permute-start.23 = (bf16[2,48,512]{2,1,0:T(8,128)(2,1)S(1)}, bf16[2,48,512]{2,1,0:T(8,128)(2,1)S(1)}, u32[]{:S(2)}, u32[]{:S(2)}) collective-permute-start(bf16[2,48,512]{2,1,0:T(8,128)(2,1)S(1)} %collective-permute-done.22.refs_4_), channel_id=1, source_target_pairs={{0,1},{1,0},{2,3},{3,2},{4,5},{5,4},{6,7},{7,6},{8,9},{9,8},{10,11... | collective-permute-start | bytes 294920 | tf_op jit(solution)/shard_map/ppermute | solution.py:30
  55.5 7.3 %collective-permute-start.25 = (bf16[2,48,512]{2,1,0:T(8,128)(2,1)S(1)}, bf16[2,48,512]{2,1,0:T(8,128)(2,1)S(1)}, u32[]{:S(2)}, u32[]{:S(2)}) collective-permute-start(bf16[2,48,512]{2,1,0:T(8,128)(2,1)S(1)} %collective-permute-done.24.refs_6_), channel_id=1, source_target_pairs={{0,1},{1,0},{2,3},{3,2},{4,5},{5,4},{6,7},{7,6},{8,9},{9,8},{10,11... | collective-permute-start | bytes 294920 | tf_op jit(solution)/shard_map/ppermute | solution.py:30
  57.3 5.5 %collective-permute-start.30 = (bf16[2,48,512]{2,1,0:T(8,128)(2,1)S(1)}, bf16[2,48,512]{2,1,0:T(8,128)(2,1)S(1)}, u32[]{:S(2)}, u32[]{:S(2)}) collective-permute-start(bf16[2,48,512]{2,1,0:T(8,128)(2,1)S(1)} %collective-permute-done.29.refs_10_), channel_id=1, source_target_pairs={{0,1},{1,0},{2,3},{3,2},{4,5},{5,4},{6,7},{7,6},{8,9},{9,8},{10,11... | collective-permute-start | bytes 294920 | tf_op jit(solution)/shard_map/ppermute | solution.py:30
  57.3 5.5 %collective-permute-start.32 = (bf16[2,48,512]{2,1,0:T(8,128)(2,1)S(1)}, bf16[2,48,512]{2,1,0:T(8,128)(2,1)S(1)}, u32[]{:S(2)}, u32[]{:S(2)}) collective-permute-start(bf16[2,48,512]{2,1,0:T(8,128)(2,1)S(1)} %collective-permute-done.31.refs_12_), channel_id=1, source_target_pairs={{0,1},{1,0},{2,3},{3,2},{4,5},{5,4},{6,7},{7,6},{8,9},{9,8},{10,11... | collective-permute-start | bytes 294920 | tf_op jit(solution)/shard_map/ppermute | solution.py:30
  57.8 5.0 %collective-permute-start.34 = (bf16[2,48,512]{2,1,0:T(8,128)(2,1)S(1)}, bf16[2,48,512]{2,1,0:T(8,128)(2,1)S(1)}, u32[]{:S(2)}, u32[]{:S(2)}) collective-permute-start(bf16[2,48,512]{2,1,0:T(8,128)(2,1)S(1)} %collective-permute-done.33.refs_14_), channel_id=1, source_target_pairs={{0,1},{1,0},{2,3},{3,2},{4,5},{5,4},{6,7},{7,6},{8,9},{9,8},{10,11... | collective-permute-start | bytes 294920 | tf_op jit(solution)/shard_map/ppermute | solution.py:30
  66.2 22.4 %copy-start = (f32[64,2]{0,1:T(2,128)S(1)}, f32[64,2]{0,1:T(2,128)}, u32[]{:S(2)}) copy-start(f32[64,2]{0,1:T(2,128)} %param.40) | copy-start | bytes 1540
  67.1 1.9 %collective-permute-start.35 = (bf16[4,2,48,512]{3,2,1,0:T(8,128)(2,1)S(1)}, bf16[4,2,48,512]{3,2,1,0:T(8,128)(2,1)S(1)}, u32[]{:S(2)}, u32[]{:S(2)}) collective-permute-start(bf16[4,2,48,512]{3,2,1,0:T(8,128)(2,1)S(1)} %get-tuple-element.90), channel_id=1, source_target_pairs={{0,1},{1,0},{2,3},{3,2},{4,5},{5,4},{6,7},{7,6},{8,9},{9,8},{10,11... | collective-permute-start | bytes 1179656 | tf_op jit(solution)/shard_map/ppermute | solution.py:30
  67.6 5.0 %collective-permute-start.40 = (bf16[4,2,48,512]{3,2,1,0:T(8,128)(2,1)S(1)}, bf16[4,2,48,512]{3,2,1,0:T(8,128)(2,1)S(1)}, u32[]{:S(2)}, u32[]{:S(2)}) collective-permute-start(bf16[4,2,48,512]{3,2,1,0:T(8,128)(2,1)S(1)} %get-tuple-element.98), channel_id=1, source_target_pairs={{0,1},{1,0},{2,3},{3,2},{4,5},{5,4},{6,7},{7,6},{8,9},{9,8},{10,11... | collective-permute-start | bytes 1179656 | tf_op jit(solution)/shard_map/ppermute | solution.py:30
  69.0 5.7 %collective-permute-start.36 = (bf16[2,48,512]{2,1,0:T(8,128)(2,1)S(1)}, bf16[2,48,512]{2,1,0:T(8,128)(2,1)S(1)}, u32[]{:S(2)}, u32[]{:S(2)}) collective-permute-start(bf16[2,48,512]{2,1,0:T(8,128)(2,1)S(1)} %get-tuple-element.92), channel_id=1, source_target_pairs={{0,2},{1,3},{2,0},{3,1},{4,6},{5,7},{6,4},{7,5},{8,10},{9,11},{10,... | collective-permute-start | bytes 294920 | tf_op jit(solution)/shard_map/ppermute | solution.py:30
  70.6 8.1 %collective-permute-start.37 = (bf16[2,48,512]{2,1,0:T(8,128)(2,1)S(1)}, bf16[2,48,512]{2,1,0:T(8,128)(2,1)S(1)}, u32[]{:S(2)}, u32[]{:S(2)}) collective-permute-start(bf16[2,48,512]{2,1,0:T(8,128)(2,1)S(1)} %get-tuple-element.93), channel_id=1, source_target_pairs={{0,4},{1,5},{2,6},{3,7},{4,0},{5,1},{6,2},{7,3},{8,12},{9,13},{10,... | collective-permute-start | bytes 294920 | tf_op jit(solution)/shard_map/ppermute | solution.py:30
  71.1 7.6 %collective-permute-start.38 = (bf16[2,48,512]{2,1,0:T(8,128)(2,1)S(1)}, bf16[2,48,512]{2,1,0:T(8,128)(2,1)S(1)}, u32[]{:S(2)}, u32[]{:S(2)}) collective-permute-start(bf16[2,48,512]{2,1,0:T(8,128)(2,1)S(1)} %get-tuple-element.94), channel_id=1, source_target_pairs={{0,6},{1,7},{2,4},{3,5},{4,2},{5,3},{6,0},{7,1},{8,14},{9,15},{10,... | collective-permute-start | bytes 294920 | tf_op jit(solution)/shard_map/ppermute | solution.py:30
  72.7 7.0 %collective-permute-start.41 = (bf16[2,48,512]{2,1,0:T(8,128)(2,1)S(1)}, bf16[2,48,512]{2,1,0:T(8,128)(2,1)S(1)}, u32[]{:S(2)}, u32[]{:S(2)}) collective-permute-start(bf16[2,48,512]{2,1,0:T(8,128)(2,1)S(1)} %get-tuple-element.100), channel_id=1, source_target_pairs={{0,2},{1,3},{2,0},{3,1},{4,6},{5,7},{6,4},{7,5},{8,10},{9,11},{10,... | collective-permute-start | bytes 294920 | tf_op jit(solution)/shard_map/ppermute | solution.py:30
  74.2 7.5 %collective-permute-start.42 = (bf16[2,48,512]{2,1,0:T(8,128)(2,1)S(1)}, bf16[2,48,512]{2,1,0:T(8,128)(2,1)S(1)}, u32[]{:S(2)}, u32[]{:S(2)}) collective-permute-start(bf16[2,48,512]{2,1,0:T(8,128)(2,1)S(1)} %get-tuple-element.101), channel_id=1, source_target_pairs={{0,4},{1,5},{2,6},{3,7},{4,0},{5,1},{6,2},{7,3},{8,12},{9,13},{10,... | collective-permute-start | bytes 294920 | tf_op jit(solution)/shard_map/ppermute | solution.py:30
  74.7 7.0 %collective-permute-start.43 = (bf16[2,48,512]{2,1,0:T(8,128)(2,1)S(1)}, bf16[2,48,512]{2,1,0:T(8,128)(2,1)S(1)}, u32[]{:S(2)}, u32[]{:S(2)}) collective-permute-start(bf16[2,48,512]{2,1,0:T(8,128)(2,1)S(1)} %get-tuple-element.102), channel_id=1, source_target_pairs={{0,6},{1,7},{2,4},{3,5},{4,2},{5,3},{6,0},{7,1},{8,14},{9,15},{10,... | collective-permute-start | bytes 294920 | tf_op jit(solution)/shard_map/ppermute | solution.py:30
  78.7 8.6 %collective-permute-start.39 = (bf16[2,24,512]{2,1,0:T(8,128)(2,1)S(1)}, bf16[2,24,512]{2,1,0:T(8,128)(2,1)S(1)}, u32[]{:S(2)}, u32[]{:S(2)}) collective-permute-start(bf16[2,24,512]{2,1,0:T(8,128)(2,1)S(1)} %get-tuple-element.96), channel_id=1, source_target_pairs={{0,8},{8,0},{16,24},{24,16},{1,9},{9,1},{17,25},{25,17},{2,10},{10... | collective-permute-start | bytes 147464 | tf_op jit(solution)/shard_map/ppermute | solution.py:30
  81.8 6.1 %collective-permute-start.44 = (bf16[2,24,512]{2,1,0:T(8,128)(2,1)S(1)}, bf16[2,24,512]{2,1,0:T(8,128)(2,1)S(1)}, u32[]{:S(2)}, u32[]{:S(2)}) collective-permute-start(bf16[2,24,512]{2,1,0:T(8,128)(2,1)S(1)} %get-tuple-element.103), channel_id=1, source_target_pairs={{0,16},{8,24},{16,0},{24,8},{1,17},{9,25},{17,1},{25,9},{2,18},{10... | collective-permute-start | bytes 147464 | tf_op jit(solution)/shard_map/ppermute | solution.py:30
  82.7 5.9 %collective-permute-start.45 = (bf16[2,24,512]{2,1,0:T(8,128)(2,1)S(1)}, bf16[2,24,512]{2,1,0:T(8,128)(2,1)S(1)}, u32[]{:S(2)}, u32[]{:S(2)}) collective-permute-start(bf16[2,24,512]{2,1,0:T(8,128)(2,1)S(1)} %get-tuple-element.104), channel_id=1, source_target_pairs={{0,24},{8,16},{16,8},{24,0},{1,25},{9,17},{17,9},{25,1},{2,26},{10... | collective-permute-start | bytes 147464 | tf_op jit(solution)/shard_map/ppermute | solution.py:30
where the time goes:
time: 89.6 us; the launch traced here: 89.5 us
  starting transfers between devices  39.3 us (44%)
  waiting for transfers between devices  27.8 us (31%)
  Pallas kernels  21.5 us (24%)
    ppermute x46, starting transfers between devices, swap(): lax.ppermute(x, axis, [(i, i ^ k) for i in range(lax.axis_size(axis))])  39.3 us
    ppermute x46, waiting for transfers between devices, swap(): lax.ppermute(x, axis, [(i, i ^ k) for i in range(lax.axis_size(axis))])  27.8 us
    pallas_call x2, Pallas kernels, fetch(): call(functools.partial(fetch_body, n, len(sources)), [pltpu.VMEM(x, bf16)...  6.91 us
    pallas_call x1, Pallas kernels, local_swaps(): call(functools.partial(prep_body, n, cap), [jax.ShapeDtypeStruct((count,...  3.67 us
    pallas_call x1, Pallas kernels, local_swaps(): call(functools.partial(up_body, n), [jax.ShapeDtypeStruct((exp_dev, half...  3.39 us
    pallas_call x1, Pallas kernels, local_swaps(): call(unpack_body, [jax.ShapeDtypeStruct((count, groups, entries), f32)] *...  2.2 us
  transfers between devices with their start and end apart: 46, of which 20 were waited for; matrix products, arithmetic and copies ran while one was open for 0% of the time, Pallas kernels for 15%

commit v1 on v0

--- a/solution.py
+++ b/solution.py
@@ -12,7 +12,6 @@
 bf16 = jnp.bfloat16
 NT = (((1,), (1,)), ((), ()))
 NN = (((1,), (0,)), ((), ()))
-TN = (((0,), (0,)), ((), ()))
 WHOLE = pl.BlockSpec(memory_space=pltpu.VMEM)
 FAR = pl.BlockSpec(memory_space=pltpu.HBM)
 LANES = 128
@@ -59,10 +58,6 @@
 def pair_body(own, other, *outs):
     for i, out in enumerate(outs):
         out[...] = (own[i].astype(f32) + other[i].astype(f32)).astype(out.dtype)
-
-
-def block_of(own, partner, k):
-    return (partner if k % 2 else own), k // 2
 
 
 def call(body, out_shape, in_specs, scratch=(), limit=None, flops=10**7):
@@ -92,11 +87,11 @@
 def prep_body(n, cap, *refs):
     weight_hbm = refs[0]
     far = refs[1:16]
-    dec_r, dec_i, bt_r, bt_i, cm_r, cm_i, fac, choose, table = refs[16:25]
-    flat = refs[25:29]
-    weight, tokens = refs[29:31]
-    held = refs[31:45]
-    sems, weight_sems = refs[45:]
+    dec_r, dec_i, bt_r, bt_i, base, mix, choose, table = refs[16:24]
+    flat = refs[24:28]
+    weight, tokens = refs[28:30]
+    held = refs[30:44]
+    sems, weight_sems, fac = refs[44:]
     held = (*held, tokens)
     copies = [pltpu.make_async_copy(a, b, sems.at[i]) for i, (a, b) in enumerate(zip(far, held))]
     for copy in copies:
@@ -114,21 +109,22 @@
     row = lax.broadcasted_iota(jnp.int32, (count, count), 0)
     col = lax.broadcasted_iota(jnp.int32, (count, count), 1)
     before = dot(total.astype(bf16), (row < col).astype(bf16), NN)
+    same = (row == col).astype(bf16)
     places = lax.broadcasted_iota(jnp.int32, (slots, count), 0).astype(f32)
     used = jnp.zeros((slots, count), f32)
     for r in range(top):
         rank = jnp.sum(before * marks[r], axis=0, keepdims=True)
         slot = routes[r : r + 1, :].astype(f32) * cap + rank
         hit = (places == slot).astype(f32)
-        choose[r] = hit.astype(bf16)
+        choose[r] = dot(same, hit.astype(bf16), NT).astype(bf16)
         used = used + hit
     table[...] = used.astype(bf16)
-    st_r, st_i, in_r, _, _, _ = held[:6]
+    st_r, st_i, in_r, in_i, om_r, om_i = held[:6]
     groups, inner, entries = in_r.shape
     pack = LANES // inner
-    for i, dst in ((2, bt_r), (3, bt_i), (4, cm_r), (5, cm_i)):
+    in_r, in_i, om_r, om_i = (x for x in held[2:6])
+    for i in range(2, 6):
         copies[i].wait()
-        spread(held[i][...].reshape(groups * inner, entries), dst, inner, pack)
     for i in (0, 1, 10, 11, 12):
         copies[i].wait()
     real, imag, log_step = held[10][...], held[11][...], held[12][...]
@@ -148,6 +144,24 @@
         dec_i[:, cols] = b_r * s_i + b_i * s_r
         fac[0:1, cols] = fac_r[g : g + 1, :]
         fac[1:2, cols] = fac_i[g : g + 1, :]
+    high = pack * entries
+    for b in range(groups // pack):
+        each = slice(b * pack, (b + 1) * pack)
+        lanes = slice(b * LANES, (b + 1) * LANES)
+        rows = slice(b * high, (b + 1) * high)
+        b_r, b_i, c_r, c_i = (
+            spread(x[each].reshape(LANES, entries), inner, pack) for x in (in_r, in_i, om_r, om_i)
+        )
+        f_r, f_i = fac[0:1, rows], fac[1:2, rows]
+        i_r = (f_r * b_r - f_i * b_i).astype(bf16)
+        i_i = (f_r * b_i + f_i * b_r).astype(bf16)
+        c_r, c_i = c_r.astype(bf16), c_i.astype(bf16)
+        bt_r[lanes, :] = i_r
+        bt_i[lanes, :] = i_i
+        mix[lanes, :] = (dot(i_r, c_r, NT) - dot(i_i, c_i, NT)).astype(bf16)
+        base[:, lanes] = dot(dec_r[:, rows].astype(bf16), c_r, NT) - dot(
+            dec_i[:, rows].astype(bf16), c_i, NT
+        )
     for i in range(len(flat)):
         copies[6 + i].wait()
         rows = held[6 + i][...].astype(f32)
@@ -158,7 +172,7 @@
         copy.wait()
 
 
-def spread(blocks, out, height, pack):
+def spread(blocks, height, pack):
     rows, inner = blocks.shape
     columns = pack * inner
     at = lax.broadcasted_iota(jnp.int32, (inner, columns), 0)
@@ -166,8 +180,7 @@
     wide = dot(blocks.astype(bf16), (to % inner == at).astype(bf16), NN)
     row = lax.broadcasted_iota(jnp.int32, (rows, columns), 0)
     col = lax.broadcasted_iota(jnp.int32, (rows, columns), 1)
-    own = (row // height) % pack == col // inner
-    out[...] = jnp.where(own, wide, 0.0).astype(bf16)
+    return jnp.where(row // height == col // inner, wide, 0.0)
 
 
 def load(src, dst, sems, n, width):
@@ -182,8 +195,8 @@
 
 def mixer_body(n, *refs):
     pieces = refs[:n]
-    gain, weight, bt_r, bt_i, fac, dec_r, dec_i, cm_r, cm_i, skip = refs[n : n + 10]
-    new_r_ref, new_i_ref, act_ref = refs[n + 10 :]
+    gain, weight, base, mix, skip = refs[n : n + 5]
+    driven_ref, act_ref = refs[n + 5 :]
     width = pieces[0].shape[1]
     square = 0.0
     for k in range(n):
@@ -196,27 +209,24 @@
         normed = (pieces[k][...].astype(f32) * scale * part).astype(bf16)
         total = total + dot(normed, weight[k], NT)
     driven = total.astype(bf16)
-    high = cm_r.shape[1]
+    driven_ref[...] = driven
     for b in range(driven.shape[1] // LANES):
-        rows = slice(b * high, (b + 1) * high)
         lanes = slice(b * LANES, (b + 1) * LANES)
-        u_r = dot(driven[:, lanes], bt_r[lanes, :], NN)
-        u_i = dot(driven[:, lanes], bt_i[lanes, :], NN)
-        f_r, f_i = fac[0:1, rows], fac[1:2, rows]
-        new_r = dec_r[:, rows] + f_r * u_r - f_i * u_i
-        new_i = dec_i[:, rows] + f_r * u_i + f_i * u_r
-        new_r_ref[:, rows] = new_r
-        new_i_ref[:, rows] = new_i
-        out = dot(new_r.astype(bf16), cm_r[lanes, :], NT) - dot(new_i.astype(bf16), cm_i[lanes, :], NT)
+        out = base[:, lanes] + dot(driven[:, lanes], mix[lanes, :], NN)
         out = out + skip[:, lanes] * driven[:, lanes].astype(f32)
         act_ref[:, lanes] = jax.nn.gelu(out).astype(bf16)
 
 
-def unpack_body(new_r, new_i, out_r, out_i):
-    for src, dst in ((new_r, out_r), (new_i, out_i)):
-        entries = dst.shape[2]
-        for g in range(dst.shape[1]):
-            dst[:, g, :] = src[:, g * entries : (g + 1) * entries]
+def state_body(driven, dec_r, dec_i, bt_r, bt_i, out_r, out_i):
+    groups, entries = out_r.shape[1:]
+    high = bt_r.shape[1]
+    pack = high // entries
+    for dec, bt, out in ((dec_r, bt_r, out_r), (dec_i, bt_i, out_i)):
+        for b in range(groups // pack):
+            lanes = slice(b * LANES, (b + 1) * LANES)
+            new = dec[:, b * high : (b + 1) * high] + dot(driven[:, lanes], bt[lanes, :], NN)
+            for g in range(pack):
+                out[:, b * pack + g, :] = new[:, g * entries : (g + 1) * entries]
 
 
 def fetch_body(n, count, *refs):
@@ -242,14 +252,19 @@
 def glu_body(n, *refs):
     pieces = refs[:n]
     glu, bias, out_w = refs[n : n + 3]
-    own, partner = refs[n + 3 :]
+    glued_ref, partner = refs[n + 3 :]
     gate = bias[...]
     for k in range(n):
         gate = gate + dot(pieces[k][...], glu[k], NT)
     glued = (pieces[0][...].astype(f32) * jax.nn.sigmoid(gate)).astype(bf16)
-    for k in range(n):
-        to, at = block_of(own, partner, k)
-        to[at] = dot(glued, out_w[k], NN).astype(bf16)
+    glued_ref[...] = glued
+    for k in range(1, n, 2):
+        partner[k // 2] = dot(glued, out_w[k], NN).astype(bf16)
+
+
+def out_body(n, glued, out_w, own):
+    for k in range(0, n, 2):
+        own[k // 2] = dot(glued[...], out_w[k], NN).astype(bf16)
 
 
 def merge_body(*refs):
@@ -281,7 +296,7 @@
 def up_body(n, *refs):
     near, far = refs[:n], refs[n : 2 * n]
     gain, gate_w, up_w, down_w = refs[2 * n : 2 * n + 4]
-    later, own, partner = refs[2 * n + 4 :]
+    later, partner = refs[2 * n + 4 :]
     experts, count, width = near[0].shape
     g, u, square = [0.0] * experts, [0.0] * experts, [0.0] * experts
     for k in range(n):
@@ -290,22 +305,26 @@
             x = jnp.concatenate([near[k][i], far[k][i]], axis=0).astype(f32)
             square[i] = square[i] + jnp.sum(x * x, axis=1, keepdims=True)
             x = (x * part).astype(bf16)
-            g[i] = g[i] + dot(x, gate_w[k, i], NT)
-            u[i] = u[i] + dot(x, up_w[k, i], NT)
+            g[i] = g[i] + dot(gate_w[k, i], x, NT)
+            u[i] = u[i] + dot(up_w[k, i], x, NT)
     for i in range(experts):
         scale = lax.rsqrt(square[i] / (n * width) + norm_eps)
-        hidden = (jax.nn.silu(g[i] * scale) * (u[i] * scale)).astype(bf16)
-        later[i] = hidden[:count]
-        for k in range(n):
-            to, at = block_of(own, partner, k)
-            to[at, i] = dot(hidden[count:], down_w[k, i], NN).astype(bf16)
-
-
-def down_body(n, hidden, down_w, own, partner):
+        hidden = (jax.nn.silu(g[i].T * scale) * (u[i].T * scale)).astype(bf16)
+        later[i] = hidden
+        for k in range(1, n, 2):
+            partner[k // 2, i] = dot(hidden[count:], down_w[k, i], NN).astype(bf16)
+
+
+def down_body(n, hidden, down_w, far_own, own, partner):
+    count = own.shape[2]
     for i in range(hidden.shape[0]):
-        for k in range(n):
-            to, at = block_of(own, partner, k)
-            to[at, i] = dot(hidden[i], down_w[k, i], NN).astype(bf16)
+        near, far = hidden[i, :count], hidden[i, count:]
+        for k in range(0, n, 2):
+            far_own[k // 2, i] = dot(far, down_w[k, i], NN).astype(bf16)
+        for k in range(1, n, 2):
+            partner[k // 2, i] = dot(near, down_w[k, i], NN).astype(bf16)
+        for k in range(0, n, 2):
+            own[k // 2, i] = dot(near, down_w[k, i], NN).astype(bf16)
 
 
 def total_body(m, terms, *refs):
@@ -331,7 +350,7 @@
         rows[pl.ds(at, count), :] = back[j][...].reshape(count, wide)
     total = resid[...].astype(f32)
     for r in range(weight.shape[0]):
-        picked = dot(choose[r], rows[...], TN)
+        picked = dot(choose[r], rows[...], NN)
         total = total + column(weight[r : r + 1, :]) * picked
     out[...] = total.astype(bf16)
 
@@ -393,13 +412,14 @@
         routes.T,
         tokens,
     ]
-    dec_r, dec_i, bt_r, bt_i, cm_r, cm_i, fac, choose, table, skip, bias, gain1, gain2, in_w, own = call(
+    dec_r, dec_i, bt_r, bt_i, base, mix, choose, table, skip, bias, gain1, gain2, in_w, own = call(
         functools.partial(prep_body, n, cap),
         [jax.ShapeDtypeStruct((count, states), f32)] * 2
-        + [jax.ShapeDtypeStruct((channels, pack * entries), bf16)] * 4
+        + [jax.ShapeDtypeStruct((channels, pack * entries), bf16)] * 2
         + [
-            jax.ShapeDtypeStruct((2, states), f32),
-            jax.ShapeDtypeStruct((top, slots, count), bf16),
+            jax.ShapeDtypeStruct((count, channels), f32),
+            jax.ShapeDtypeStruct((channels, LANES), bf16),
+            jax.ShapeDtypeStruct((top, count, slots), bf16),
             jax.ShapeDtypeStruct((slots, count), bf16),
         ]
         + [jax.ShapeDtypeStruct((1, channels), f32)] * 2
@@ -407,46 +427,34 @@
         + [pltpu.VMEM((n, channels, wide), bf16), pltpu.VMEM((count, wide), bf16)],
         [FAR] * 16,
         [pltpu.VMEM(x.shape, x.dtype) for x in far[:-1]]
-        + [pltpu.SemaphoreType.DMA((15,)), pltpu.SemaphoreType.DMA((n,))],
+        + [pltpu.SemaphoreType.DMA((15,)), pltpu.SemaphoreType.DMA((n,))]
+        + [pltpu.VMEM((2, states), f32)],
         limit=12 * 2**20,
     )(*[stay(x) for x in [in_weight] + far])
     pieces[0] = own
 
-    new_r, new_i, activated = call(
+    driven, activated = call(
         functools.partial(mixer_body, n),
-        [
-            jax.ShapeDtypeStruct((count, states), f32),
-            jax.ShapeDtypeStruct((count, states), f32),
-            jax.ShapeDtypeStruct((count, channels), bf16),
-        ],
-        [WHOLE] * (n + 10),
+        [jax.ShapeDtypeStruct((count, channels), bf16)] * 2,
+        [WHOLE] * (n + 5),
         limit=12 * 2**20,
-    )(
-        *pieces,
-        gain1,
-        in_w,
-        bt_r,
-        bt_i,
-        fac,
-        dec_r,
-        dec_i,
-        cm_r,
-        cm_i,
-        skip,
-    )
+    )(*pieces, gain1, in_w, base, mix, skip)
 
     acts = gather_swaps(activated, n)
     glu_w, out_w = fetch(n, glu_weight, out_weight)
-    parts = call(
+    block = jax.ShapeDtypeStruct((n // 2, count, wide), bf16)
+    glued, partner = call(
         functools.partial(glu_body, n),
-        [jax.ShapeDtypeStruct((n // 2, count, wide), bf16)] * 2,
+        [jax.ShapeDtypeStruct((count, channels), bf16), block],
         [WHOLE] * (n + 3),
         limit=12 * 2**20,
     )(*acts, glu_w, bias, out_w)
-
-    terms = reduce_swaps(*parts, n)
+    sums = call(functools.partial(out_body, n), block, [WHOLE] * 2, limit=8 * 2**20)(glued, out_w)
+
+    terms = reduce_swaps(sums, partner, n)
     hidden = gate_weight.shape[1]
-    gate_w, up_w, down_w = fetch(n, gate_weight, up_weight, down_weight)
+    gate_w, up_w = fetch(n, gate_weight, up_weight)
+    (down_w,) = fetch(n, down_weight)
     resid, *packed = call(
         functools.partial(dispatch_body, m, len(terms)),
         [jax.ShapeDtypeStruct((count, wide), bf16)]
@@ -467,15 +475,16 @@
         )(*group)
         fragments += gather_swaps(merged, n)
     part = jax.ShapeDtypeStruct((n // 2, exp_dev, half * cap, wide), bf16)
-    later, *far_outs = call(
+    later, far_partner = call(
         functools.partial(up_body, n),
-        [jax.ShapeDtypeStruct((exp_dev, half * cap, hidden), bf16)] + [part] * 2,
+        [jax.ShapeDtypeStruct((exp_dev, 2 * half * cap, hidden), bf16), part],
         [WHOLE] * (2 * n + 4),
         limit=16 * 2**20,
     )(*fragments, gain2, gate_w, up_w, down_w)
-    near_outs = call(
-        functools.partial(down_body, n), [part] * 2, [WHOLE] * 2, limit=8 * 2**20
+    far_own, *near_outs = call(
+        functools.partial(down_body, n), [part] * 3, [WHOLE] * 2, limit=8 * 2**20
     )(later, down_w)
+    far_outs = [far_own, far_partner]
     back = [None] * m
     for outs, first in ((far_outs, half), (near_outs, 0)):
         terms = reduce_swaps(*outs, n)
@@ -488,11 +497,11 @@
         for j in range(first, first + half):
             back[j] = swap(totals[j - first], "ep", j) if j else totals[0]
     new_r, new_i = call(
-        unpack_body,
+        state_body,
         [jax.ShapeDtypeStruct((count, groups, entries), f32)] * 2,
-        [WHOLE] * 2,
+        [WHOLE] * 5,
         limit=4 * 2**20,
-    )(new_r, new_i)
+    )(driven, dec_r, dec_i, bt_r, bt_i)
     result = call(
         functools.partial(combine_body, m),
         jax.ShapeDtypeStruct((count, wide), bf16),

time: 89.6 us -> 89.6 us (level)
  waiting for transfers between devices: 27.8 us -> 31 us
  starting transfers between devices: 39.3 us -> 36.3 us
    ppermute x46, waiting for transfers between devices: 27.8 us -> 31 us  [swap(): lax.ppermute(x, axis, [(i, i ^ k) for i in range(lax.axis_size(axis))])]
    ppermute x46, starting transfers between devices: 39.3 us -> 36.3 us  [swap(): lax.ppermute(x, axis, [(i, i ^ k) for i in range(lax.axis_size(axis))])]
    pallas_call x5 -> x6, Pallas kernels: 9.45 us -> 8.25 us  [the longest x1 2.73 us: local_swaps(): call(functools.partial(up_body, n), [jax.ShapeDtypeStruct((exp_dev, 2 * h...]
    pallas_call x2 -> x3, Pallas kernels: 6.91 us -> 7.87 us  [fetch(): call(functools.partial(fetch_body, n, len(sources)), [pltpu.VMEM(x, bf16)...]
  transfers between devices with their start and end apart: 46 -> 46, of which waited for: 20 -> 21; matrix products, arithmetic and copies ran while one was open for 0% -> 0% of each run, Pallas kernels for 15% -> 16%
where the time goes in v1:
time: 89.6 us; the launch traced here: 89.4 us
  starting transfers between devices  36.3 us (41%)
  waiting for transfers between devices  31 us (35%)
  Pallas kernels  21.3 us (24%)
    ppermute x46, starting transfers between devices, swap(): lax.ppermute(x, axis, [(i, i ^ k) for i in range(lax.axis_size(axis))])  36.3 us
    ppermute x46, waiting for transfers between devices, swap(): lax.ppermute(x, axis, [(i, i ^ k) for i in range(lax.axis_size(axis))])  31 us
    pallas_call x3, Pallas kernels, fetch(): call(functools.partial(fetch_body, n, len(sources)), [pltpu.VMEM(x, bf16)...  7.87 us
    pallas_call x1, Pallas kernels, local_swaps(): call(functools.partial(prep_body, n, cap), [jax.ShapeDtypeStruct((count,...  3.73 us
    pallas_call x1, Pallas kernels, local_swaps(): call(functools.partial(up_body, n), [jax.ShapeDtypeStruct((exp_dev, 2 * h...  2.73 us
    pallas_call x1, Pallas kernels, local_swaps(): call(state_body, [jax.ShapeDtypeStruct((count, groups, entries), f32)] *...  2.13 us
  transfers between devices with their start and end apart: 46, of which 21 were waited for; matrix products, arithmetic and copies ran while one was open for 0% of the time, Pallas kernels for 16%

profile of v1, /device:TPU:0, one launch (start us, length us, event | category | flops | bytes accessed | tf_op | source)
XLA Modules:
  0.0 89.4 jit_solution(13239163063158814388)
XLA Ops:
  0.6 3.0 %collective-permute-start.1 = (bf16[64,512]{1,0:T(8,128)(2,1)}, bf16[64,512]{1,0:T(8,128)(2,1)S(1)}, u32[]{:S(2)}, u32[]{:S(2)}) collective-permute-start(bf16[64,512]{1,0:T(8,128)(2,1)} %refs_15_.1), channel_id=1, source_target_pairs={{0,2},{1,3},{2,0},{3,1},{4,6},{5,7},{6,4},{7,5},{8,10},{9,11},{10,... | collective-permute-start | bytes 196616 | tf_op jit(solution)/shard_map/ppermute | solution.py:29
  3.7 1.5 %collective-permute-start.5 = (bf16[64,512]{1,0:T(8,128)(2,1)}, bf16[64,512]{1,0:T(8,128)(2,1)S(1)}, u32[]{:S(2)}, u32[]{:S(2)}) collective-permute-start(bf16[64,512]{1,0:T(8,128)(2,1)} %refs_15_.1), channel_id=1, source_target_pairs={{0,6},{1,7},{2,4},{3,5},{4,2},{5,3},{6,0},{7,1},{8,14},{9,15},{10,... | collective-permute-start | bytes 196616 | tf_op jit(solution)/shard_map/ppermute | solution.py:29
  5.2 1.2 %collective-permute-done.1.refs_2_ = bf16[64,512]{1,0:T(8,128)(2,1)S(1)} collective-permute-done((bf16[64,512]{1,0:T(8,128)(2,1)}, bf16[64,512]{1,0:T(8,128)(2,1)S(1)}, u32[]{:S(2)}, u32[]{:S(2)}) %collective-permute-start.1) | collective-permute-done | bytes 65568 | tf_op jit(solution)/shard_map/ppermute | solution.py:29
  6.4 2.7 %collective-permute-done.5.refs_6_ = bf16[64,512]{1,0:T(8,128)(2,1)S(1)} collective-permute-done((bf16[64,512]{1,0:T(8,128)(2,1)}, bf16[64,512]{1,0:T(8,128)(2,1)S(1)}, u32[]{:S(2)}, u32[]{:S(2)}) %collective-permute-start.5) | collective-permute-done | bytes 65568 | tf_op jit(solution)/shard_map/ppermute | solution.py:29
  9.1 0.8 collective-permute-done.3.refs_4_
  9.9 3.7 %shard_map.229 = (f32[64,1024]{1,0:T(8,128)S(1)}, f32[64,1024]{1,0:T(8,128)S(1)}, bf16[256,512]{1,0:T(8,128)(2,1)S(1)}, bf16[256,512]{1,0:T(8,128)(2,1)S(1)}, f3...) custom-call(bf16[256,4096]{1,0:T(8,128)(2,1)} %refs_0_.4, ...), custom_call_target="tpu_custom_call" | custom-call | flops 10000000 | bytes 1000000 | tf_op jit(solution)/shard_map/pallas_call | solution.py:415
  13.7 1.0 %shard_map.230 = (bf16[64,256]{1,0:T(8,128)(2,1)S(1)}, bf16[64,256]{1,0:T(8,128)(2,1)S(1)}) custom-call(bf16[64,512]{1,0:T(8,128)(2,1)S(1)} %get-tuple-element.53.refs_0_, bf16[64,512]{1,0:T(8,128)(2,1)S(1)} %collective-permute-done.refs_1_, bf16[64,512]{1,0:T(8,128)(2,1)S(1)} %collective-permute-done.1.refs_2_, ...), custom_call_target="tpu_custom_call" | custom-call | flops 10000000 | bytes 1000000 | tf_op jit(solution)/shard_map/pallas_call | solution.py:436
  14.6 1.5 %collective-permute-start.12 = (bf16[64,256]{1,0:T(8,128)(2,1)S(1)}, bf16[64,256]{1,0:T(8,128)(2,1)S(1)}, u32[]{:S(2)}, u32[]{:S(2)}) collective-permute-start(bf16[64,256]{1,0:T(8,128)(2,1)S(1)} %get-tuple-element.59.refs_0_), channel_id=1, source_target_pairs={{0,6},{1,7},{2,4},{3,5},{4,2},{5,3},{6,0},{7,1},{8,14},{9,15},{10,... | collective-permute-start | bytes 98312 | tf_op jit(solution)/shard_map/ppermute | solution.py:29
  16.2 1.2 %collective-permute-start.10 = (bf16[64,256]{1,0:T(8,128)(2,1)S(1)}, bf16[64,256]{1,0:T(8,128)(2,1)S(1)}, u32[]{:S(2)}, u32[]{:S(2)}) collective-permute-start(bf16[64,256]{1,0:T(8,128)(2,1)S(1)} %get-tuple-element.59.refs_0_), channel_id=1, source_target_pairs={{0,4},{1,5},{2,6},{3,7},{4,0},{5,1},{6,2},{7,3},{8,12},{9,13},{10,... | collective-permute-start | bytes 98312 | tf_op jit(solution)/shard_map/ppermute | solution.py:29
  17.4 0.8 collective-permute-start.8
  18.2 1.3 %collective-permute-done.12.refs_6_ = bf16[64,256]{1,0:T(8,128)(2,1)S(1)} collective-permute-done((bf16[64,256]{1,0:T(8,128)(2,1)S(1)}, bf16[64,256]{1,0:T(8,128)(2,1)S(1)}, u32[]{:S(2)}, u32[]{:S(2)}) %collective-permute-start.12) | collective-permute-done | bytes 32800 | tf_op jit(solution)/shard_map/ppermute | solution.py:29
  19.5 0.6 collective-permute-done.10.refs_4_
  20.1 1.2 %collective-permute-done.8.refs_2_ = bf16[64,256]{1,0:T(8,128)(2,1)S(1)} collective-permute-done((bf16[64,256]{1,0:T(8,128)(2,1)S(1)}, bf16[64,256]{1,0:T(8,128)(2,1)S(1)}, u32[]{:S(2)}, u32[]{:S(2)}) %collective-permute-start.8) | collective-permute-done | bytes 32800 | tf_op jit(solution)/shard_map/ppermute | solution.py:29
  21.3 2.0 %shard_map.231 = (bf16[8,256,256]{2,1,0:T(8,128)(2,1)S(1)}, bf16[8,256,512]{2,1,0:T(8,128)(2,1)S(1)}) custom-call(bf16[256,2048]{1,0:T(8,128)(2,1)} %refs_0_.5, bf16[256,4096]{1,0:T(8,128)(2,1)} %refs_1_.4), custom_call_target="tpu_custom_call" | custom-call | flops 10000000 | bytes 1000000 | tf_op jit(solution)/shard_map/pallas_call | solution.py:243
  23.4 0.9 %shard_map.232 = (bf16[64,256]{1,0:T(8,128)(2,1)S(1)}, bf16[4,64,512]{2,1,0:T(8,128)(2,1)S(1)}) custom-call(bf16[64,256]{1,0:T(8,128)(2,1)S(1)} %get-tuple-element.59.refs_0_, bf16[64,256]{1,0:T(8,128)(2,1)S(1)} %collective-permute-done.7.refs_1_, bf16[64,256]{1,0:T(8,128)(2,1)S(1)} %collective-permute-done.8.refs_2_, ...), custom_call_target="tpu_custom_call" | custom-call | flops 10000000 | bytes 1000000 | tf_op jit(solution)/shard_map/pallas_call | solution.py:446
  24.4 0.6 collective-permute-start.14
  24.9 0.3 shard_map.233.own
  25.2 0.9 collective-permute-done.14.other
  26.2 0.9 collective-permute-start.15
  27.0 1.2 %collective-permute-start.16 = (bf16[64,512]{1,0:T(8,128)(2,1)S(1)}, bf16[64,512]{1,0:T(8,128)(2,1)S(1)}, u32[]{:S(2)}, u32[]{:S(2)}) collective-permute-start(bf16[64,512]{1,0:T(8,128)(2,1)S(1)} %get-tuple-element.67), channel_id=1, source_target_pairs={{0,4},{1,5},{2,6},{3,7},{4,0},{5,1},{6,2},{7,3},{8,12},{9,13},{10,... | collective-permute-start | bytes 196616 | tf_op jit(solution)/shard_map/ppermute | solution.py:29
  28.2 1.5 %collective-permute-start.17 = (bf16[64,512]{1,0:T(8,128)(2,1)S(1)}, bf16[64,512]{1,0:T(8,128)(2,1)S(1)}, u32[]{:S(2)}, u32[]{:S(2)}) collective-permute-start(bf16[64,512]{1,0:T(8,128)(2,1)S(1)} %get-tuple-element.68), channel_id=1, source_target_pairs={{0,6},{1,7},{2,4},{3,5},{4,2},{5,3},{6,0},{7,1},{8,14},{9,15},{10,... | collective-permute-start | bytes 196616 | tf_op jit(solution)/shard_map/ppermute | solution.py:29
  29.7 0.9 collective-permute-done.15.refs_2_
  30.6 0.7 collective-permute-done.16.refs_3_
  31.3 2.1 %collective-permute-done.17.refs_4_ = bf16[64,512]{1,0:T(8,128)(2,1)S(1)} collective-permute-done((bf16[64,512]{1,0:T(8,128)(2,1)S(1)}, bf16[64,512]{1,0:T(8,128)(2,1)S(1)}, u32[]{:S(2)}, u32[]{:S(2)}) %collective-permute-start.17) | collective-permute-done | bytes 65568 | tf_op jit(solution)/shard_map/ppermute | solution.py:29
  33.4 0.2 shard_map.235
  33.6 2.7 %collective-permute-start.26 = (bf16[2,24,512]{2,1,0:T(8,128)(2,1)S(1)}, bf16[2,24,512]{2,1,0:T(8,128)(2,1)S(1)}, u32[]{:S(2)}, u32[]{:S(2)}) collective-permute-start(bf16[2,24,512]{2,1,0:T(8,128)(2,1)S(1)} %get-tuple-element.74), channel_id=1, source_target_pairs={{0,16},{8,24},{16,0},{24,8},{1,17},{9,25},{17,1},{25,9},{2,18},{10... | collective-permute-start | bytes 147464 | tf_op jit(solution)/shard_map/ppermute | solution.py:29
  36.3 1.3 %collective-permute-start.27 = (bf16[2,24,512]{2,1,0:T(8,128)(2,1)S(1)}, bf16[2,24,512]{2,1,0:T(8,128)(2,1)S(1)}, u32[]{:S(2)}, u32[]{:S(2)}) collective-permute-start(bf16[2,24,512]{2,1,0:T(8,128)(2,1)S(1)} %get-tuple-element.75), channel_id=1, source_target_pairs={{0,24},{8,16},{16,8},{24,0},{1,25},{9,17},{17,9},{25,1},{2,26},{10... | collective-permute-start | bytes 147464 | tf_op jit(solution)/shard_map/ppermute | solution.py:29
  37.7 1.3 %collective-permute-done.26.refs_0_ = bf16[2,24,512]{2,1,0:T(8,128)(2,1)S(1)} collective-permute-done((bf16[2,24,512]{2,1,0:T(8,128)(2,1)S(1)}, bf16[2,24,512]{2,1,0:T(8,128)(2,1)S(1)}, u32[]{:S(2)}, u32[]{:S(2)}) %collective-permute-start.26) | collective-permute-done | bytes 49184 | tf_op jit(solution)/shard_map/ppermute | solution.py:29
  39.0 3.3 %collective-permute-done.27.refs_1_ = bf16[2,24,512]{2,1,0:T(8,128)(2,1)S(1)} collective-permute-done((bf16[2,24,512]{2,1,0:T(8,128)(2,1)S(1)}, bf16[2,24,512]{2,1,0:T(8,128)(2,1)S(1)}, u32[]{:S(2)}, u32[]{:S(2)}) %collective-permute-start.27) | collective-permute-done | bytes 49184 | tf_op jit(solution)/shard_map/ppermute | solution.py:29
  42.2 1.5 %collective-permute-start.33 = (bf16[2,48,512]{2,1,0:T(8,128)(2,1)S(1)}, bf16[2,48,512]{2,1,0:T(8,128)(2,1)S(1)}, u32[]{:S(2)}, u32[]{:S(2)}) collective-permute-start(bf16[2,48,512]{2,1,0:T(8,128)(2,1)S(1)} %shard_map.237.refs_8_), channel_id=1, source_target_pairs={{0,6},{1,7},{2,4},{3,5},{4,2},{5,3},{6,0},{7,1},{8,14},{9,15},{10,... | collective-permute-start | bytes 294920 | tf_op jit(solution)/shard_map/ppermute | solution.py:29
  43.7 0.8 collective-permute-start.31
  44.5 1.3 %collective-permute-start.29 = (bf16[2,48,512]{2,1,0:T(8,128)(2,1)S(1)}, bf16[2,48,512]{2,1,0:T(8,128)(2,1)S(1)}, u32[]{:S(2)}, u32[]{:S(2)}) collective-permute-start(bf16[2,48,512]{2,1,0:T(8,128)(2,1)S(1)} %shard_map.237.refs_8_), channel_id=1, source_target_pairs={{0,2},{1,3},{2,0},{3,1},{4,6},{5,7},{6,4},{7,5},{8,10},{9,11},{10,... | collective-permute-start | bytes 294920 | tf_op jit(solution)/shard_map/ppermute | solution.py:29
  45.8 4.2 %collective-permute-done.18.refs_1_ = bf16[2,24,512]{2,1,0:T(8,128)(2,1)S(1)} collective-permute-done((bf16[2,24,512]{2,1,0:T(8,128)(2,1)S(1)}, bf16[2,24,512]{2,1,0:T(8,128)(2,1)S(1)}, u32[]{:S(2)}, u32[]{:S(2)}) %collective-permute-start.18) | collective-permute-done | bytes 49184 | tf_op jit(solution)/shard_map/ppermute | solution.py:29
  50.0 1.5 %collective-permute-start.24 = (bf16[2,48,512]{2,1,0:T(8,128)(2,1)S(1)}, bf16[2,48,512]{2,1,0:T(8,128)(2,1)S(1)}, u32[]{:S(2)}, u32[]{:S(2)}) collective-permute-start(bf16[2,48,512]{2,1,0:T(8,128)(2,1)S(1)} %shard_map.236.refs_0_), channel_id=1, source_target_pairs={{0,6},{1,7},{2,4},{3,5},{4,2},{5,3},{6,0},{7,1},{8,14},{9,15},{10,... | collective-permute-start | bytes 294920 | tf_op jit(solution)/shard_map/ppermute | solution.py:29
  51.4 0.8 collective-permute-start.22
  52.2 1.3 %collective-permute-start.20 = (bf16[2,48,512]{2,1,0:T(8,128)(2,1)S(1)}, bf16[2,48,512]{2,1,0:T(8,128)(2,1)S(1)}, u32[]{:S(2)}, u32[]{:S(2)}) collective-permute-start(bf16[2,48,512]{2,1,0:T(8,128)(2,1)S(1)} %shard_map.236.refs_0_), channel_id=1, source_target_pairs={{0,2},{1,3},{2,0},{3,1},{4,6},{5,7},{6,4},{7,5},{8,10},{9,11},{10,... | collective-permute-start | bytes 294920 | tf_op jit(solution)/shard_map/ppermute | solution.py:29
  53.5 0.5 collective-permute-start.34
  54.0 2.5 %collective-permute-done.24.refs_6_ = bf16[2,48,512]{2,1,0:T(8,128)(2,1)S(1)} collective-permute-done((bf16[2,48,512]{2,1,0:T(8,128)(2,1)S(1)}, bf16[2,48,512]{2,1,0:T(8,128)(2,1)S(1)}, u32[]{:S(2)}, u32[]{:S(2)}) %collective-permute-start.24) | collective-permute-done | bytes 98336 | tf_op jit(solution)/shard_map/ppermute | solution.py:29
  56.5 0.9 collective-permute-done.22.refs_4_
  57.4 0.5 collective-permute-start.25
  58.0 0.4 collective-permute-start.21
  58.4 2.2 %shard_map.239.refs_19_.down_w = bf16[8,2,256,512]{3,2,1,0:T(8,128)(2,1)S(1)} custom-call(bf16[2,256,4096]{2,1,0:T(8,128)(2,1)} %refs_0_.7), custom_call_target="tpu_custom_call" | custom-call | flops 10000000 | bytes 1000000 | tf_op jit(solution)/shard_map/pallas_call | solution.py:243
  60.7 3.6 %shard_map.238 = (bf16[8,2,256,512]{3,2,1,0:T(8,128)(2,1)S(1)}, bf16[8,2,256,512]{3,2,1,0:T(8,128)(2,1)S(1)}) custom-call(bf16[2,256,4096]{2,1,0:T(8,128)(2,1)} %refs_0_.6, bf16[2,256,4096]{2,1,0:T(8,128)(2,1)} %refs_1_.5), custom_call_target="tpu_custom_call" | custom-call | flops 10000000 | bytes 1000000 | tf_op jit(solution)/shard_map/pallas_call | solution.py:243
  64.3 2.7 %shard_map.240 = (bf16[2,96,256]{2,1,0:T(8,128)(2,1)S(1)}, bf16[4,2,48,512]{3,2,1,0:T(8,128)(2,1)S(1)}) custom-call(bf16[2,48,512]{2,1,0:T(8,128)(2,1)S(1)} %shard_map.236.refs_0_, bf16[2,48,512]{2,1,0:T(8,128)(2,1)S(1)} %collective-permute-done.19.refs_1_, bf16[2,48,512]{2,1,0:T(8,128)(2,1)S(1)} %collective-permute-done.20.refs_2_, ...), custom_call_target="tpu_custom_call" | custom-call | flops 10000000 | bytes 1000000 | tf_op jit(solution)/shard_map/pallas_call | solution.py:478
  67.1 1.2 %shard_map.241 = (bf16[4,2,48,512]{3,2,1,0:T(8,128)(2,1)S(1)}, bf16[4,2,48,512]{3,2,1,0:T(8,128)(2,1)S(1)}, bf16[4,2,48,512]{3,2,1,0:T(8,128)(2,1)S(1)}) custom-call(bf16[2,96,256]{2,1,0:T(8,128)(2,1)S(1)} %get-tuple-element.79.hidden, bf16[8,2,256,512]{3,2,1,0:T(8,128)(2,1)S(1)} %shard_map.239.refs_19_.down_w), custom_call_target="tpu_custom_call" | custom-call | flops 10000000 | bytes 1000000 | tf_op jit(solution)/shard_map/pallas_call | solution.py:484
  68.3 0.1 collective-permute-start.35
  68.4 0.4 collective-permute-start.40
  68.8 1.2 %collective-permute-done.35.other = bf16[4,2,48,512]{3,2,1,0:T(8,128)(2,1)S(1)} collective-permute-done((bf16[4,2,48,512]{3,2,1,0:T(8,128)(2,1)S(1)}, bf16[4,2,48,512]{3,2,1,0:T(8,128)(2,1)S(1)}, u32[]{:S(2)}, u32[]{:S(2)}) %collective-permute-start.35) | collective-permute-done | bytes 393248 | tf_op jit(solution)/shard_map/ppermute | solution.py:29
  70.1 0.8 collective-permute-start.36
  71.0 1.2 %collective-permute-start.37 = (bf16[2,48,512]{2,1,0:T(8,128)(2,1)S(1)}, bf16[2,48,512]{2,1,0:T(8,128)(2,1)S(1)}, u32[]{:S(2)}, u32[]{:S(2)}) collective-permute-start(bf16[2,48,512]{2,1,0:T(8,128)(2,1)S(1)} %get-tuple-element.84), channel_id=1, source_target_pairs={{0,4},{1,5},{2,6},{3,7},{4,0},{5,1},{6,2},{7,3},{8,12},{9,13},{10,... | collective-permute-start | bytes 294920 | tf_op jit(solution)/shard_map/ppermute | solution.py:29
  72.2 1.5 %collective-permute-start.38 = (bf16[2,48,512]{2,1,0:T(8,128)(2,1)S(1)}, bf16[2,48,512]{2,1,0:T(8,128)(2,1)S(1)}, u32[]{:S(2)}, u32[]{:S(2)}) collective-permute-start(bf16[2,48,512]{2,1,0:T(8,128)(2,1)S(1)} %get-tuple-element.85), channel_id=1, source_target_pairs={{0,6},{1,7},{2,4},{3,5},{4,2},{5,3},{6,0},{7,1},{8,14},{9,15},{10,... | collective-permute-start | bytes 294920 | tf_op jit(solution)/shard_map/ppermute | solution.py:29
  73.8 0.8 collective-permute-start.41
  74.6 1.2 %collective-permute-start.42 = (bf16[2,48,512]{2,1,0:T(8,128)(2,1)S(1)}, bf16[2,48,512]{2,1,0:T(8,128)(2,1)S(1)}, u32[]{:S(2)}, u32[]{:S(2)}) collective-permute-start(bf16[2,48,512]{2,1,0:T(8,128)(2,1)S(1)} %get-tuple-element.92), channel_id=1, source_target_pairs={{0,4},{1,5},{2,6},{3,7},{4,0},{5,1},{6,2},{7,3},{8,12},{9,13},{10,... | collective-permute-start | bytes 294920 | tf_op jit(solution)/shard_map/ppermute | solution.py:29
  75.8 1.5 %collective-permute-start.43 = (bf16[2,48,512]{2,1,0:T(8,128)(2,1)S(1)}, bf16[2,48,512]{2,1,0:T(8,128)(2,1)S(1)}, u32[]{:S(2)}, u32[]{:S(2)}) collective-permute-start(bf16[2,48,512]{2,1,0:T(8,128)(2,1)S(1)} %get-tuple-element.93), channel_id=1, source_target_pairs={{0,6},{1,7},{2,4},{3,5},{4,2},{5,3},{6,0},{7,1},{8,14},{9,15},{10,... | collective-permute-start | bytes 294920 | tf_op jit(solution)/shard_map/ppermute | solution.py:29
  77.4 1.4 %collective-permute-done.38.refs_3_ = bf16[2,48,512]{2,1,0:T(8,128)(2,1)S(1)} collective-permute-done((bf16[2,48,512]{2,1,0:T(8,128)(2,1)S(1)}, bf16[2,48,512]{2,1,0:T(8,128)(2,1)S(1)}, u32[]{:S(2)}, u32[]{:S(2)}) %collective-permute-start.38) | collective-permute-done | bytes 98336 | tf_op jit(solution)/shard_map/ppermute | solution.py:29
  78.8 0.6 collective-permute-start.39
  79.4 0.8 collective-permute-done.41.refs_1_
  80.2 1.7 %collective-permute-done.42.refs_2_ = bf16[2,48,512]{2,1,0:T(8,128)(2,1)S(1)} collective-permute-done((bf16[2,48,512]{2,1,0:T(8,128)(2,1)S(1)}, bf16[2,48,512]{2,1,0:T(8,128)(2,1)S(1)}, u32[]{:S(2)}, u32[]{:S(2)}) %collective-permute-start.42) | collective-permute-done | bytes 98336 | tf_op jit(solution)/shard_map/ppermute | solution.py:29
  81.9 0.7 collective-permute-start.44
  82.7 2.2 %collective-permute-start.45 = (bf16[2,24,512]{2,1,0:T(8,128)(2,1)S(1)}, bf16[2,24,512]{2,1,0:T(8,128)(2,1)S(1)}, u32[]{:S(2)}, u32[]{:S(2)}) collective-permute-start(bf16[2,24,512]{2,1,0:T(8,128)(2,1)S(1)} %get-tuple-element.95), channel_id=1, source_target_pairs={{0,24},{8,16},{16,8},{24,0},{1,25},{9,17},{17,9},{25,1},{2,26},{10... | collective-permute-start | bytes 147464 | tf_op jit(solution)/shard_map/ppermute | solution.py:29
  84.9 2.1 %shard_map.247 = (f32[64,16,64]{2,1,0:T(8,128)}, f32[64,16,64]{2,1,0:T(8,128)}) custom-call(bf16[64,256]{1,0:T(8,128)(2,1)S(1)} %get-tuple-element.96.driven, f32[64,1024]{1,0:T(8,128)S(1)} %get-tuple-element.97.dec_r, f32[64,1024]{1,0:T(8,128)S(1)} %get-tuple-element.98.dec_i, bf16[256,512]{1,0:T(8,128)(2,1)S(1)} %get-tuple-element.99.bt_r, ...), custom_call_target="tpu_custom_call" | custom-call | flops 10000000 | bytes 1000000 | tf_op jit(solution)/shard_map/pallas_call | solution.py:499
  87.1 0.5 collective-permute-done.44.refs_5_
  87.5 1.1 %collective-permute-done.45.refs_6_ = bf16[2,24,512]{2,1,0:T(8,128)(2,1)S(1)} collective-permute-done((bf16[2,24,512]{2,1,0:T(8,128)(2,1)S(1)}, bf16[2,24,512]{2,1,0:T(8,128)(2,1)S(1)}, u32[]{:S(2)}, u32[]{:S(2)}) %collective-permute-start.45) | collective-permute-done | bytes 49184 | tf_op jit(solution)/shard_map/ppermute | solution.py:29
  88.6 0.9 shard_map.246
  (49 shorter events, 0.6 us)
Async XLA Ops:
  0.6 5.8 %collective-permute-start.1 = (bf16[64,512]{1,0:T(8,128)(2,1)}, bf16[64,512]{1,0:T(8,128)(2,1)S(1)}, u32[]{:S(2)}, u32[]{:S(2)}) collective-permute-start(bf16[64,512]{1,0:T(8,128)(2,1)} %refs_15_.1), channel_id=1, source_target_pairs={{0,2},{1,3},{2,0},{3,1},{4,6},{5,7},{6,4},{7,5},{8,10},{9,11},{10,... | collective-permute-start | bytes 196616 | tf_op jit(solution)/shard_map/ppermute | solution.py:29
  3.7 5.4 %collective-permute-start.5 = (bf16[64,512]{1,0:T(8,128)(2,1)}, bf16[64,512]{1,0:T(8,128)(2,1)S(1)}, u32[]{:S(2)}, u32[]{:S(2)}) collective-permute-start(bf16[64,512]{1,0:T(8,128)(2,1)} %refs_15_.1), channel_id=1, source_target_pairs={{0,6},{1,7},{2,4},{3,5},{4,2},{5,3},{6,0},{7,1},{8,14},{9,15},{10,... | collective-permute-start | bytes 196616 | tf_op jit(solution)/shard_map/ppermute | solution.py:29
  5.2 4.7 %collective-permute-start.3 = (bf16[64,512]{1,0:T(8,128)(2,1)}, bf16[64,512]{1,0:T(8,128)(2,1)S(1)}, u32[]{:S(2)}, u32[]{:S(2)}) collective-permute-start(bf16[64,512]{1,0:T(8,128)(2,1)} %refs_15_.1), channel_id=1, source_target_pairs={{0,4},{1,5},{2,6},{3,7},{4,0},{5,1},{6,2},{7,3},{8,12},{9,13},{10,... | collective-permute-start | bytes 196616 | tf_op jit(solution)/shard_map/ppermute | solution.py:29
  5.2 8.4 %collective-permute-start = (bf16[64,512]{1,0:T(8,128)(2,1)}, bf16[64,512]{1,0:T(8,128)(2,1)S(1)}, u32[]{:S(2)}, u32[]{:S(2)}) collective-permute-start(bf16[64,512]{1,0:T(8,128)(2,1)} %refs_15_.1), channel_id=1, source_target_pairs={{0,1},{1,0},{2,3},{3,2},{4,5},{5,4},{6,7},{7,6},{8,9},{9,8},{10,11... | collective-permute-start | bytes 196616 | tf_op jit(solution)/shard_map/ppermute | solution.py:29
  6.4 7.3 %collective-permute-start.2 = (bf16[64,512]{1,0:T(8,128)(2,1)S(1)}, bf16[64,512]{1,0:T(8,128)(2,1)S(1)}, u32[]{:S(2)}, u32[]{:S(2)}) collective-permute-start(bf16[64,512]{1,0:T(8,128)(2,1)S(1)} %collective-permute-done.1.refs_2_), channel_id=1, source_target_pairs={{0,1},{1,0},{2,3},{3,2},{4,5},{5,4},{6,7},{7,6},{8,9},{9,8},{10,11... | collective-permute-start | bytes 196616 | tf_op jit(solution)/shard_map/ppermute | solution.py:29
  9.1 4.5 %collective-permute-start.6 = (bf16[64,512]{1,0:T(8,128)(2,1)S(1)}, bf16[64,512]{1,0:T(8,128)(2,1)S(1)}, u32[]{:S(2)}, u32[]{:S(2)}) collective-permute-start(bf16[64,512]{1,0:T(8,128)(2,1)S(1)} %collective-permute-done.5.refs_6_), channel_id=1, source_target_pairs={{0,1},{1,0},{2,3},{3,2},{4,5},{5,4},{6,7},{7,6},{8,9},{9,8},{10,11... | collective-permute-start | bytes 196616 | tf_op jit(solution)/shard_map/ppermute | solution.py:29
  9.9 3.8 %collective-permute-start.4 = (bf16[64,512]{1,0:T(8,128)(2,1)S(1)}, bf16[64,512]{1,0:T(8,128)(2,1)S(1)}, u32[]{:S(2)}, u32[]{:S(2)}) collective-permute-start(bf16[64,512]{1,0:T(8,128)(2,1)S(1)} %collective-permute-done.3.refs_4_), channel_id=1, source_target_pairs={{0,1},{1,0},{2,3},{3,2},{4,5},{5,4},{6,7},{7,6},{8,9},{9,8},{10,11... | collective-permute-start | bytes 196616 | tf_op jit(solution)/shard_map/ppermute | solution.py:29
  14.6 4.9 %collective-permute-start.12 = (bf16[64,256]{1,0:T(8,128)(2,1)S(1)}, bf16[64,256]{1,0:T(8,128)(2,1)S(1)}, u32[]{:S(2)}, u32[]{:S(2)}) collective-permute-start(bf16[64,256]{1,0:T(8,128)(2,1)S(1)} %get-tuple-element.59.refs_0_), channel_id=1, source_target_pairs={{0,6},{1,7},{2,4},{3,5},{4,2},{5,3},{6,0},{7,1},{8,14},{9,15},{10,... | collective-permute-start | bytes 98312 | tf_op jit(solution)/shard_map/ppermute | solution.py:29
  16.2 3.9 %collective-permute-start.10 = (bf16[64,256]{1,0:T(8,128)(2,1)S(1)}, bf16[64,256]{1,0:T(8,128)(2,1)S(1)}, u32[]{:S(2)}, u32[]{:S(2)}) collective-permute-start(bf16[64,256]{1,0:T(8,128)(2,1)S(1)} %get-tuple-element.59.refs_0_), channel_id=1, source_target_pairs={{0,4},{1,5},{2,6},{3,7},{4,0},{5,1},{6,2},{7,3},{8,12},{9,13},{10,... | collective-permute-start | bytes 98312 | tf_op jit(solution)/shard_map/ppermute | solution.py:29
  17.4 3.9 %collective-permute-start.8 = (bf16[64,256]{1,0:T(8,128)(2,1)S(1)}, bf16[64,256]{1,0:T(8,128)(2,1)S(1)}, u32[]{:S(2)}, u32[]{:S(2)}) collective-permute-start(bf16[64,256]{1,0:T(8,128)(2,1)S(1)} %get-tuple-element.59.refs_0_), channel_id=1, source_target_pairs={{0,2},{1,3},{2,0},{3,1},{4,6},{5,7},{6,4},{7,5},{8,10},{9,11},{10,... | collective-permute-start | bytes 98312 | tf_op jit(solution)/shard_map/ppermute | solution.py:29
  18.2 5.2 %collective-permute-start.7 = (bf16[64,256]{1,0:T(8,128)(2,1)S(1)}, bf16[64,256]{1,0:T(8,128)(2,1)S(1)}, u32[]{:S(2)}, u32[]{:S(2)}) collective-permute-start(bf16[64,256]{1,0:T(8,128)(2,1)S(1)} %get-tuple-element.59.refs_0_), channel_id=1, source_target_pairs={{0,1},{1,0},{2,3},{3,2},{4,5},{5,4},{6,7},{7,6},{8,9},{9,8},{10,11... | collective-permute-start | bytes 98312 | tf_op jit(solution)/shard_map/ppermute | solution.py:29
  19.5 3.9 %collective-permute-start.13 = (bf16[64,256]{1,0:T(8,128)(2,1)S(1)}, bf16[64,256]{1,0:T(8,128)(2,1)S(1)}, u32[]{:S(2)}, u32[]{:S(2)}) collective-permute-start(bf16[64,256]{1,0:T(8,128)(2,1)S(1)} %collective-permute-done.12.refs_6_), channel_id=1, source_target_pairs={{0,1},{1,0},{2,3},{3,2},{4,5},{5,4},{6,7},{7,6},{8,9},{9,8},{10,11... | collective-permute-start | bytes 98312 | tf_op jit(solution)/shard_map/ppermute | solution.py:29
  20.1 3.3 %collective-permute-start.11 = (bf16[64,256]{1,0:T(8,128)(2,1)S(1)}, bf16[64,256]{1,0:T(8,128)(2,1)S(1)}, u32[]{:S(2)}, u32[]{:S(2)}) collective-permute-start(bf16[64,256]{1,0:T(8,128)(2,1)S(1)} %collective-permute-done.10.refs_4_), channel_id=1, source_target_pairs={{0,1},{1,0},{2,3},{3,2},{4,5},{5,4},{6,7},{7,6},{8,9},{9,8},{10,11... | collective-permute-start | bytes 98312 | tf_op jit(solution)/shard_map/ppermute | solution.py:29
  21.3 2.1 %collective-permute-start.9 = (bf16[64,256]{1,0:T(8,128)(2,1)S(1)}, bf16[64,256]{1,0:T(8,128)(2,1)S(1)}, u32[]{:S(2)}, u32[]{:S(2)}) collective-permute-start(bf16[64,256]{1,0:T(8,128)(2,1)S(1)} %collective-permute-done.8.refs_2_), channel_id=1, source_target_pairs={{0,1},{1,0},{2,3},{3,2},{4,5},{5,4},{6,7},{7,6},{8,9},{9,8},{10,11... | collective-permute-start | bytes 98312 | tf_op jit(solution)/shard_map/ppermute | solution.py:29
  24.4 1.7 %collective-permute-start.14 = (bf16[4,64,512]{2,1,0:T(8,128)(2,1)S(1)}, bf16[4,64,512]{2,1,0:T(8,128)(2,1)S(1)}, u32[]{:S(2)}, u32[]{:S(2)}) collective-permute-start(bf16[4,64,512]{2,1,0:T(8,128)(2,1)S(1)} %get-tuple-element.64), channel_id=1, source_target_pairs={{0,1},{1,0},{2,3},{3,2},{4,5},{5,4},{6,7},{7,6},{8,9},{9,8},{10,11... | collective-permute-start | bytes 786440 | tf_op jit(solution)/shard_map/ppermute | solution.py:29
  26.2 4.4 %collective-permute-start.15 = (bf16[64,512]{1,0:T(8,128)(2,1)S(1)}, bf16[64,512]{1,0:T(8,128)(2,1)S(1)}, u32[]{:S(2)}, u32[]{:S(2)}) collective-permute-start(bf16[64,512]{1,0:T(8,128)(2,1)S(1)} %get-tuple-element.66), channel_id=1, source_target_pairs={{0,2},{1,3},{2,0},{3,1},{4,6},{5,7},{6,4},{7,5},{8,10},{9,11},{10,... | collective-permute-start | bytes 196616 | tf_op jit(solution)/shard_map/ppermute | solution.py:29
  27.0 4.3 %collective-permute-start.16 = (bf16[64,512]{1,0:T(8,128)(2,1)S(1)}, bf16[64,512]{1,0:T(8,128)(2,1)S(1)}, u32[]{:S(2)}, u32[]{:S(2)}) collective-permute-start(bf16[64,512]{1,0:T(8,128)(2,1)S(1)} %get-tuple-element.67), channel_id=1, source_target_pairs={{0,4},{1,5},{2,6},{3,7},{4,0},{5,1},{6,2},{7,3},{8,12},{9,13},{10,... | collective-permute-start | bytes 196616 | tf_op jit(solution)/shard_map/ppermute | solution.py:29
  28.2 5.2 %collective-permute-start.17 = (bf16[64,512]{1,0:T(8,128)(2,1)S(1)}, bf16[64,512]{1,0:T(8,128)(2,1)S(1)}, u32[]{:S(2)}, u32[]{:S(2)}) collective-permute-start(bf16[64,512]{1,0:T(8,128)(2,1)S(1)} %get-tuple-element.68), channel_id=1, source_target_pairs={{0,6},{1,7},{2,4},{3,5},{4,2},{5,3},{6,0},{7,1},{8,14},{9,15},{10,... | collective-permute-start | bytes 196616 | tf_op jit(solution)/shard_map/ppermute | solution.py:29
  33.6 5.4 %collective-permute-start.26 = (bf16[2,24,512]{2,1,0:T(8,128)(2,1)S(1)}, bf16[2,24,512]{2,1,0:T(8,128)(2,1)S(1)}, u32[]{:S(2)}, u32[]{:S(2)}) collective-permute-start(bf16[2,24,512]{2,1,0:T(8,128)(2,1)S(1)} %get-tuple-element.74), channel_id=1, source_target_pairs={{0,16},{8,24},{16,0},{24,8},{1,17},{9,25},{17,1},{25,9},{2,18},{10... | collective-permute-start | bytes 147464 | tf_op jit(solution)/shard_map/ppermute | solution.py:29
  36.3 5.9 %collective-permute-start.27 = (bf16[2,24,512]{2,1,0:T(8,128)(2,1)S(1)}, bf16[2,24,512]{2,1,0:T(8,128)(2,1)S(1)}, u32[]{:S(2)}, u32[]{:S(2)}) collective-permute-start(bf16[2,24,512]{2,1,0:T(8,128)(2,1)S(1)} %get-tuple-element.75), channel_id=1, source_target_pairs={{0,24},{8,16},{16,8},{24,0},{1,25},{9,17},{17,9},{25,1},{2,26},{10... | collective-permute-start | bytes 147464 | tf_op jit(solution)/shard_map/ppermute | solution.py:29
  42.2 9.2 %collective-permute-start.33 = (bf16[2,48,512]{2,1,0:T(8,128)(2,1)S(1)}, bf16[2,48,512]{2,1,0:T(8,128)(2,1)S(1)}, u32[]{:S(2)}, u32[]{:S(2)}) collective-permute-start(bf16[2,48,512]{2,1,0:T(8,128)(2,1)S(1)} %shard_map.237.refs_8_), channel_id=1, source_target_pairs={{0,6},{1,7},{2,4},{3,5},{4,2},{5,3},{6,0},{7,1},{8,14},{9,15},{10,... | collective-permute-start | bytes 294920 | tf_op jit(solution)/shard_map/ppermute | solution.py:29
  43.7 8.5 %collective-permute-start.31 = (bf16[2,48,512]{2,1,0:T(8,128)(2,1)S(1)}, bf16[2,48,512]{2,1,0:T(8,128)(2,1)S(1)}, u32[]{:S(2)}, u32[]{:S(2)}) collective-permute-start(bf16[2,48,512]{2,1,0:T(8,128)(2,1)S(1)} %shard_map.237.refs_8_), channel_id=1, source_target_pairs={{0,4},{1,5},{2,6},{3,7},{4,0},{5,1},{6,2},{7,3},{8,12},{9,13},{10,... | collective-permute-start | bytes 294920 | tf_op jit(solution)/shard_map/ppermute | solution.py:29
  44.5 9.0 %collective-permute-start.29 = (bf16[2,48,512]{2,1,0:T(8,128)(2,1)S(1)}, bf16[2,48,512]{2,1,0:T(8,128)(2,1)S(1)}, u32[]{:S(2)}, u32[]{:S(2)}) collective-permute-start(bf16[2,48,512]{2,1,0:T(8,128)(2,1)S(1)} %shard_map.237.refs_8_), channel_id=1, source_target_pairs={{0,2},{1,3},{2,0},{3,1},{4,6},{5,7},{6,4},{7,5},{8,10},{9,11},{10,... | collective-permute-start | bytes 294920 | tf_op jit(solution)/shard_map/ppermute | solution.py:29
  45.8 7.7 %collective-permute-start.28 = (bf16[2,48,512]{2,1,0:T(8,128)(2,1)S(1)}, bf16[2,48,512]{2,1,0:T(8,128)(2,1)S(1)}, u32[]{:S(2)}, u32[]{:S(2)}) collective-permute-start(bf16[2,48,512]{2,1,0:T(8,128)(2,1)S(1)} %shard_map.237.refs_8_), channel_id=1, source_target_pairs={{0,1},{1,0},{2,3},{3,2},{4,5},{5,4},{6,7},{7,6},{8,9},{9,8},{10,11... | collective-permute-start | bytes 294920 | tf_op jit(solution)/shard_map/ppermute | solution.py:29
  45.8 4.2 %collective-permute-start.18 = (bf16[2,24,512]{2,1,0:T(8,128)(2,1)S(1)}, bf16[2,24,512]{2,1,0:T(8,128)(2,1)S(1)}, u32[]{:S(2)}, u32[]{:S(2)}) collective-permute-start(bf16[2,24,512]{2,1,0:T(8,128)(2,1)S(1)} %get-tuple-element.73), channel_id=1, source_target_pairs={{0,8},{8,0},{16,24},{24,16},{1,9},{9,1},{17,25},{25,17},{2,10},{10... | collective-permute-start | bytes 147464 | tf_op jit(solution)/shard_map/ppermute | solution.py:29
  50.0 6.5 %collective-permute-start.24 = (bf16[2,48,512]{2,1,0:T(8,128)(2,1)S(1)}, bf16[2,48,512]{2,1,0:T(8,128)(2,1)S(1)}, u32[]{:S(2)}, u32[]{:S(2)}) collective-permute-start(bf16[2,48,512]{2,1,0:T(8,128)(2,1)S(1)} %shard_map.236.refs_0_), channel_id=1, source_target_pairs={{0,6},{1,7},{2,4},{3,5},{4,2},{5,3},{6,0},{7,1},{8,14},{9,15},{10,... | collective-permute-start | bytes 294920 | tf_op jit(solution)/shard_map/ppermute | solution.py:29
  51.4 5.9 %collective-permute-start.22 = (bf16[2,48,512]{2,1,0:T(8,128)(2,1)S(1)}, bf16[2,48,512]{2,1,0:T(8,128)(2,1)S(1)}, u32[]{:S(2)}, u32[]{:S(2)}) collective-permute-start(bf16[2,48,512]{2,1,0:T(8,128)(2,1)S(1)} %shard_map.236.refs_0_), channel_id=1, source_target_pairs={{0,4},{1,5},{2,6},{3,7},{4,0},{5,1},{6,2},{7,3},{8,12},{9,13},{10,... | collective-permute-start | bytes 294920 | tf_op jit(solution)/shard_map/ppermute | solution.py:29
  52.2 5.1 %collective-permute-start.20 = (bf16[2,48,512]{2,1,0:T(8,128)(2,1)S(1)}, bf16[2,48,512]{2,1,0:T(8,128)(2,1)S(1)}, u32[]{:S(2)}, u32[]{:S(2)}) collective-permute-start(bf16[2,48,512]{2,1,0:T(8,128)(2,1)S(1)} %shard_map.236.refs_0_), channel_id=1, source_target_pairs={{0,2},{1,3},{2,0},{3,1},{4,6},{5,7},{6,4},{7,5},{8,10},{9,11},{10,... | collective-permute-start | bytes 294920 | tf_op jit(solution)/shard_map/ppermute | solution.py:29
  53.5 4.4 %collective-permute-start.19 = (bf16[2,48,512]{2,1,0:T(8,128)(2,1)S(1)}, bf16[2,48,512]{2,1,0:T(8,128)(2,1)S(1)}, u32[]{:S(2)}, u32[]{:S(2)}) collective-permute-start(bf16[2,48,512]{2,1,0:T(8,128)(2,1)S(1)} %shard_map.236.refs_0_), channel_id=1, source_target_pairs={{0,1},{1,0},{2,3},{3,2},{4,5},{5,4},{6,7},{7,6},{8,9},{9,8},{10,11... | collective-permute-start | bytes 294920 | tf_op jit(solution)/shard_map/ppermute | solution.py:29
  53.5 4.4 %collective-permute-start.34 = (bf16[2,48,512]{2,1,0:T(8,128)(2,1)S(1)}, bf16[2,48,512]{2,1,0:T(8,128)(2,1)S(1)}, u32[]{:S(2)}, u32[]{:S(2)}) collective-permute-start(bf16[2,48,512]{2,1,0:T(8,128)(2,1)S(1)} %collective-permute-done.33.refs_14_), channel_id=1, source_target_pairs={{0,1},{1,0},{2,3},{3,2},{4,5},{5,4},{6,7},{7,6},{8,9},{9,8},{10,11... | collective-permute-start | bytes 294920 | tf_op jit(solution)/shard_map/ppermute | solution.py:29
  56.5 7.8 %collective-permute-start.32 = (bf16[2,48,512]{2,1,0:T(8,128)(2,1)S(1)}, bf16[2,48,512]{2,1,0:T(8,128)(2,1)S(1)}, u32[]{:S(2)}, u32[]{:S(2)}) collective-permute-start(bf16[2,48,512]{2,1,0:T(8,128)(2,1)S(1)} %collective-permute-done.31.refs_12_), channel_id=1, source_target_pairs={{0,1},{1,0},{2,3},{3,2},{4,5},{5,4},{6,7},{7,6},{8,9},{9,8},{10,11... | collective-permute-start | bytes 294920 | tf_op jit(solution)/shard_map/ppermute | solution.py:29
  57.4 6.9 %collective-permute-start.30 = (bf16[2,48,512]{2,1,0:T(8,128)(2,1)S(1)}, bf16[2,48,512]{2,1,0:T(8,128)(2,1)S(1)}, u32[]{:S(2)}, u32[]{:S(2)}) collective-permute-start(bf16[2,48,512]{2,1,0:T(8,128)(2,1)S(1)} %collective-permute-done.29.refs_10_), channel_id=1, source_target_pairs={{0,1},{1,0},{2,3},{3,2},{4,5},{5,4},{6,7},{7,6},{8,9},{9,8},{10,11... | collective-permute-start | bytes 294920 | tf_op jit(solution)/shard_map/ppermute | solution.py:29
  57.4 6.9 %collective-permute-start.25 = (bf16[2,48,512]{2,1,0:T(8,128)(2,1)S(1)}, bf16[2,48,512]{2,1,0:T(8,128)(2,1)S(1)}, u32[]{:S(2)}, u32[]{:S(2)}) collective-permute-start(bf16[2,48,512]{2,1,0:T(8,128)(2,1)S(1)} %collective-permute-done.24.refs_6_), channel_id=1, source_target_pairs={{0,1},{1,0},{2,3},{3,2},{4,5},{5,4},{6,7},{7,6},{8,9},{9,8},{10,11... | collective-permute-start | bytes 294920 | tf_op jit(solution)/shard_map/ppermute | solution.py:29
  57.9 6.4 %collective-permute-start.23 = (bf16[2,48,512]{2,1,0:T(8,128)(2,1)S(1)}, bf16[2,48,512]{2,1,0:T(8,128)(2,1)S(1)}, u32[]{:S(2)}, u32[]{:S(2)}) collective-permute-start(bf16[2,48,512]{2,1,0:T(8,128)(2,1)S(1)} %collective-permute-done.22.refs_4_), channel_id=1, source_target_pairs={{0,1},{1,0},{2,3},{3,2},{4,5},{5,4},{6,7},{7,6},{8,9},{9,8},{10,11... | collective-permute-start | bytes 294920 | tf_op jit(solution)/shard_map/ppermute | solution.py:29
  58.0 6.3 %collective-permute-start.21 = (bf16[2,48,512]{2,1,0:T(8,128)(2,1)S(1)}, bf16[2,48,512]{2,1,0:T(8,128)(2,1)S(1)}, u32[]{:S(2)}, u32[]{:S(2)}) collective-permute-start(bf16[2,48,512]{2,1,0:T(8,128)(2,1)S(1)} %collective-permute-done.20.refs_2_), channel_id=1, source_target_pairs={{0,1},{1,0},{2,3},{3,2},{4,5},{5,4},{6,7},{7,6},{8,9},{9,8},{10,11... | collective-permute-start | bytes 294920 | tf_op jit(solution)/shard_map/ppermute | solution.py:29
  67.1 21.5 %copy-start = (f32[64,2]{0,1:T(2,128)S(1)}, f32[64,2]{0,1:T(2,128)}, u32[]{:S(2)}) copy-start(f32[64,2]{0,1:T(2,128)} %param.40) | copy-start | bytes 1540
  68.3 1.8 %collective-permute-start.35 = (bf16[4,2,48,512]{3,2,1,0:T(8,128)(2,1)S(1)}, bf16[4,2,48,512]{3,2,1,0:T(8,128)(2,1)S(1)}, u32[]{:S(2)}, u32[]{:S(2)}) collective-permute-start(bf16[4,2,48,512]{3,2,1,0:T(8,128)(2,1)S(1)} %get-tuple-element.81), channel_id=1, source_target_pairs={{0,1},{1,0},{2,3},{3,2},{4,5},{5,4},{6,7},{7,6},{8,9},{9,8},{10,11... | collective-permute-start | bytes 1179656 | tf_op jit(solution)/shard_map/ppermute | solution.py:29
  68.4 5.3 %collective-permute-start.40 = (bf16[4,2,48,512]{3,2,1,0:T(8,128)(2,1)S(1)}, bf16[4,2,48,512]{3,2,1,0:T(8,128)(2,1)S(1)}, u32[]{:S(2)}, u32[]{:S(2)}) collective-permute-start(bf16[4,2,48,512]{3,2,1,0:T(8,128)(2,1)S(1)} %get-tuple-element.89), channel_id=1, source_target_pairs={{0,1},{1,0},{2,3},{3,2},{4,5},{5,4},{6,7},{7,6},{8,9},{9,8},{10,11... | collective-permute-start | bytes 1179656 | tf_op jit(solution)/shard_map/ppermute | solution.py:29
  70.1 5.7 %collective-permute-start.36 = (bf16[2,48,512]{2,1,0:T(8,128)(2,1)S(1)}, bf16[2,48,512]{2,1,0:T(8,128)(2,1)S(1)}, u32[]{:S(2)}, u32[]{:S(2)}) collective-permute-start(bf16[2,48,512]{2,1,0:T(8,128)(2,1)S(1)} %get-tuple-element.83), channel_id=1, source_target_pairs={{0,2},{1,3},{2,0},{3,1},{4,6},{5,7},{6,4},{7,5},{8,10},{9,11},{10,... | collective-permute-start | bytes 294920 | tf_op jit(solution)/shard_map/ppermute | solution.py:29
  71.0 6.4 %collective-permute-start.37 = (bf16[2,48,512]{2,1,0:T(8,128)(2,1)S(1)}, bf16[2,48,512]{2,1,0:T(8,128)(2,1)S(1)}, u32[]{:S(2)}, u32[]{:S(2)}) collective-permute-start(bf16[2,48,512]{2,1,0:T(8,128)(2,1)S(1)} %get-tuple-element.84), channel_id=1, source_target_pairs={{0,4},{1,5},{2,6},{3,7},{4,0},{5,1},{6,2},{7,3},{8,12},{9,13},{10,... | collective-permute-start | bytes 294920 | tf_op jit(solution)/shard_map/ppermute | solution.py:29
  72.2 6.6 %collective-permute-start.38 = (bf16[2,48,512]{2,1,0:T(8,128)(2,1)S(1)}, bf16[2,48,512]{2,1,0:T(8,128)(2,1)S(1)}, u32[]{:S(2)}, u32[]{:S(2)}) collective-permute-start(bf16[2,48,512]{2,1,0:T(8,128)(2,1)S(1)} %get-tuple-element.85), channel_id=1, source_target_pairs={{0,6},{1,7},{2,4},{3,5},{4,2},{5,3},{6,0},{7,1},{8,14},{9,15},{10,... | collective-permute-start | bytes 294920 | tf_op jit(solution)/shard_map/ppermute | solution.py:29
  73.8 6.4 %collective-permute-start.41 = (bf16[2,48,512]{2,1,0:T(8,128)(2,1)S(1)}, bf16[2,48,512]{2,1,0:T(8,128)(2,1)S(1)}, u32[]{:S(2)}, u32[]{:S(2)}) collective-permute-start(bf16[2,48,512]{2,1,0:T(8,128)(2,1)S(1)} %get-tuple-element.91), channel_id=1, source_target_pairs={{0,2},{1,3},{2,0},{3,1},{4,6},{5,7},{6,4},{7,5},{8,10},{9,11},{10,... | collective-permute-start | bytes 294920 | tf_op jit(solution)/shard_map/ppermute | solution.py:29
  74.6 7.3 %collective-permute-start.42 = (bf16[2,48,512]{2,1,0:T(8,128)(2,1)S(1)}, bf16[2,48,512]{2,1,0:T(8,128)(2,1)S(1)}, u32[]{:S(2)}, u32[]{:S(2)}) collective-permute-start(bf16[2,48,512]{2,1,0:T(8,128)(2,1)S(1)} %get-tuple-element.92), channel_id=1, source_target_pairs={{0,4},{1,5},{2,6},{3,7},{4,0},{5,1},{6,2},{7,3},{8,12},{9,13},{10,... | collective-permute-start | bytes 294920 | tf_op jit(solution)/shard_map/ppermute | solution.py:29
  75.8 6.1 %collective-permute-start.43 = (bf16[2,48,512]{2,1,0:T(8,128)(2,1)S(1)}, bf16[2,48,512]{2,1,0:T(8,128)(2,1)S(1)}, u32[]{:S(2)}, u32[]{:S(2)}) collective-permute-start(bf16[2,48,512]{2,1,0:T(8,128)(2,1)S(1)} %get-tuple-element.93), channel_id=1, source_target_pairs={{0,6},{1,7},{2,4},{3,5},{4,2},{5,3},{6,0},{7,1},{8,14},{9,15},{10,... | collective-permute-start | bytes 294920 | tf_op jit(solution)/shard_map/ppermute | solution.py:29
  78.8 8.3 %collective-permute-start.39 = (bf16[2,24,512]{2,1,0:T(8,128)(2,1)S(1)}, bf16[2,24,512]{2,1,0:T(8,128)(2,1)S(1)}, u32[]{:S(2)}, u32[]{:S(2)}) collective-permute-start(bf16[2,24,512]{2,1,0:T(8,128)(2,1)S(1)} %get-tuple-element.87), channel_id=1, source_target_pairs={{0,8},{8,0},{16,24},{24,16},{1,9},{9,1},{17,25},{25,17},{2,10},{10... | collective-permute-start | bytes 147464 | tf_op jit(solution)/shard_map/ppermute | solution.py:29
  81.9 5.6 %collective-permute-start.44 = (bf16[2,24,512]{2,1,0:T(8,128)(2,1)S(1)}, bf16[2,24,512]{2,1,0:T(8,128)(2,1)S(1)}, u32[]{:S(2)}, u32[]{:S(2)}) collective-permute-start(bf16[2,24,512]{2,1,0:T(8,128)(2,1)S(1)} %get-tuple-element.94), channel_id=1, source_target_pairs={{0,16},{8,24},{16,0},{24,8},{1,17},{9,25},{17,1},{25,9},{2,18},{10... | collective-permute-start | bytes 147464 | tf_op jit(solution)/shard_map/ppermute | solution.py:29
  82.7 5.9 %collective-permute-start.45 = (bf16[2,24,512]{2,1,0:T(8,128)(2,1)S(1)}, bf16[2,24,512]{2,1,0:T(8,128)(2,1)S(1)}, u32[]{:S(2)}, u32[]{:S(2)}) collective-permute-start(bf16[2,24,512]{2,1,0:T(8,128)(2,1)S(1)} %get-tuple-element.95), channel_id=1, source_target_pairs={{0,24},{8,16},{16,8},{24,0},{1,25},{9,17},{17,9},{25,1},{2,26},{10... | collective-permute-start | bytes 147464 | tf_op jit(solution)/shard_map/ppermute | solution.py:29

commit v2 on v1

--- a/solution.py
+++ b/solution.py
@@ -71,6 +71,13 @@
         compiler_params=pltpu.CompilerParams(vmem_limit_bytes=limit),
         cost_estimate=pl.CostEstimate(flops=flops, bytes_accessed=10**6, transcendentals=0),
     )
+
+
+def fold(x):
+    total = x[:, :LANES]
+    for c in range(LANES, x.shape[1], LANES):
+        total = total + x[:, c : c + LANES]
+    return total
 
 
 def column(row):
@@ -201,14 +208,17 @@
     square = 0.0
     for k in range(n):
         x = pieces[k][...].astype(f32)
-        square = square + jnp.sum(x * x, axis=1, keepdims=True)
-    scale = lax.rsqrt(square / (n * width) + norm_eps)
-    total = 0.0
+        square = square + fold(x * x)
+    scale = lax.rsqrt(jnp.sum(square, axis=1, keepdims=True) / (n * width) + norm_eps)
+    total, turned = 0.0, 0.0
     for k in range(n):
         part = gain[:, place(k, width)]
-        normed = (pieces[k][...].astype(f32) * scale * part).astype(bf16)
-        total = total + dot(normed, weight[k], NT)
-    driven = total.astype(bf16)
+        normed = (pieces[k][...].astype(f32) * part).astype(bf16)
+        if k % 2:
+            turned = turned + dot(weight[k], normed, NT)
+        else:
+            total = total + dot(normed, weight[k], NT)
+    driven = ((total + turned.T) * scale).astype(bf16)
     driven_ref[...] = driven
     for b in range(driven.shape[1] // LANES):
         lanes = slice(b * LANES, (b + 1) * LANES)
@@ -229,42 +239,62 @@
                 out[:, b * pack + g, :] = new[:, g * entries : (g + 1) * entries]
 
 
-def fetch_body(n, count, *refs):
+PARTS = 8
+
+
+def fetch_body(spans, *refs):
+    count = len(spans)
     copies = []
-    for i in range(count):
+    for i, (low, high) in enumerate(spans):
         src, dst, sems = refs[i], refs[count + i], refs[2 * count + i]
-        copies += load(src, dst, sems, n, dst.shape[-1])
+        step = (high - low) // PARTS
+        for p in range(PARTS):
+            copies.append(
+                pltpu.make_async_copy(
+                    src.at[pl.ds(low + p * step, step)], dst.at[pl.ds(p * step, step)], sems.at[p]
+                )
+            )
+            copies[-1].start()
     for copy in copies:
         copy.wait()
 
 
-def fetch(n, *sources):
-    shapes = [(n, *x.shape[:-1], x.shape[-1] // n) for x in sources]
+def fetch(*sources):
+    sources = [x if isinstance(x, tuple) else (x, 0, x.shape[0]) for x in sources]
     return call(
-        functools.partial(fetch_body, n, len(sources)),
-        [pltpu.VMEM(x, bf16) for x in shapes],
+        functools.partial(fetch_body, [x[1:] for x in sources]),
+        [pltpu.VMEM((high - low, x.shape[1]), bf16) for x, low, high in sources],
         [FAR] * len(sources),
-        [pltpu.SemaphoreType.DMA((n,))] * len(sources),
+        [pltpu.SemaphoreType.DMA((PARTS,))] * len(sources),
         limit=2**20,
-    )(*[stay(x) for x in sources])
+    )(*[stay(x) for x, _, _ in sources])
+
+
+def rows_of(weight, i, experts):
+    height = weight.shape[0] // experts
+    return slice(i * height, (i + 1) * height)
 
 
 def glu_body(n, *refs):
     pieces = refs[:n]
     glu, bias, out_w = refs[n : n + 3]
     glued_ref, partner = refs[n + 3 :]
-    gate = bias[...]
+    gate, turned = bias[...], 0.0
     for k in range(n):
-        gate = gate + dot(pieces[k][...], glu[k], NT)
-    glued = (pieces[0][...].astype(f32) * jax.nn.sigmoid(gate)).astype(bf16)
+        block = glu[:, place(k, pieces[k].shape[1])]
+        if k % 2:
+            turned = turned + dot(block, pieces[k][...], NT)
+        else:
+            gate = gate + dot(pieces[k][...], block, NT)
+    glued = (pieces[0][...].astype(f32) * jax.nn.sigmoid(gate + turned.T)).astype(bf16)
     glued_ref[...] = glued
     for k in range(1, n, 2):
-        partner[k // 2] = dot(glued, out_w[k], NN).astype(bf16)
+        partner[k // 2] = dot(glued, out_w[:, place(k, partner.shape[2])], NN).astype(bf16)
 
 
 def out_body(n, glued, out_w, own):
     for k in range(0, n, 2):
-        own[k // 2] = dot(glued[...], out_w[k], NN).astype(bf16)
+        own[k // 2] = dot(glued[...], out_w[:, place(k, own.shape[2])], NN).astype(bf16)
 
 
 def merge_body(*refs):
@@ -295,36 +325,40 @@
 
 def up_body(n, *refs):
     near, far = refs[:n], refs[n : 2 * n]
-    gain, gate_w, up_w, down_w = refs[2 * n : 2 * n + 4]
-    later, partner = refs[2 * n + 4 :]
+    gain, gate_w, up_low, up_high, down_w = refs[2 * n : 2 * n + 5]
+    later, partner = refs[2 * n + 5 :]
     experts, count, width = near[0].shape
     g, u, square = [0.0] * experts, [0.0] * experts, [0.0] * experts
     for k in range(n):
         part = gain[:, place(k, width)]
         for i in range(experts):
             x = jnp.concatenate([near[k][i], far[k][i]], axis=0).astype(f32)
-            square[i] = square[i] + jnp.sum(x * x, axis=1, keepdims=True)
+            square[i] = square[i] + fold(x * x)
             x = (x * part).astype(bf16)
-            g[i] = g[i] + dot(gate_w[k, i], x, NT)
-            u[i] = u[i] + dot(up_w[k, i], x, NT)
+            g[i] = g[i] + dot(x, gate_w[rows_of(gate_w, i, experts), place(k, width)], NT)
+            height = gate_w.shape[0] // experts
+            held = up_low.shape[0] // height
+            up_w, at = (up_low, i) if i < held else (up_high, i - held)
+            u[i] = u[i] + dot(up_w[at * height : (at + 1) * height, place(k, width)], x, NT)
     for i in range(experts):
-        scale = lax.rsqrt(square[i] / (n * width) + norm_eps)
-        hidden = (jax.nn.silu(g[i].T * scale) * (u[i].T * scale)).astype(bf16)
+        scale = lax.rsqrt(jnp.sum(square[i], axis=1, keepdims=True) / (n * width) + norm_eps)
+        hidden = (jax.nn.silu(g[i] * scale) * (u[i].T * scale)).astype(bf16)
         later[i] = hidden
         for k in range(1, n, 2):
-            partner[k // 2, i] = dot(hidden[count:], down_w[k, i], NN).astype(bf16)
+            partner[k // 2, i] = dot(hidden[count:], down_w[rows_of(down_w, i, experts), place(k, width)], NN).astype(bf16)
 
 
 def down_body(n, hidden, down_w, far_own, own, partner):
-    count = own.shape[2]
-    for i in range(hidden.shape[0]):
+    count, width = own.shape[2:]
+    experts = hidden.shape[0]
+    for i in range(experts):
         near, far = hidden[i, :count], hidden[i, count:]
         for k in range(0, n, 2):
-            far_own[k // 2, i] = dot(far, down_w[k, i], NN).astype(bf16)
+            far_own[k // 2, i] = dot(far, down_w[rows_of(down_w, i, experts), place(k, width)], NN).astype(bf16)
         for k in range(1, n, 2):
-            partner[k // 2, i] = dot(near, down_w[k, i], NN).astype(bf16)
+            partner[k // 2, i] = dot(near, down_w[rows_of(down_w, i, experts), place(k, width)], NN).astype(bf16)
         for k in range(0, n, 2):
-            own[k // 2, i] = dot(near, down_w[k, i], NN).astype(bf16)
+            own[k // 2, i] = dot(near, down_w[rows_of(down_w, i, experts), place(k, width)], NN).astype(bf16)
 
 
 def total_body(m, terms, *refs):
@@ -441,7 +475,7 @@
     )(*pieces, gain1, in_w, base, mix, skip)
 
     acts = gather_swaps(activated, n)
-    glu_w, out_w = fetch(n, glu_weight, out_weight)
+    glu_w, out_w = fetch(glu_weight, out_weight)
     block = jax.ShapeDtypeStruct((n // 2, count, wide), bf16)
     glued, partner = call(
         functools.partial(glu_body, n),
@@ -453,8 +487,11 @@
 
     terms = reduce_swaps(sums, partner, n)
     hidden = gate_weight.shape[1]
-    gate_w, up_w = fetch(n, gate_weight, up_weight)
-    (down_w,) = fetch(n, down_weight)
+    flat_up = up_weight.reshape(-1, full)
+    held = (exp_dev + 1) // 2 * hidden
+    gate_w, up_low = fetch(gate_weight.reshape(-1, full), (flat_up, 0, held))
+    (up_high,) = fetch((flat_up, held, exp_dev * hidden))
+    (down_w,) = fetch(down_weight.reshape(-1, full))
     resid, *packed = call(
         functools.partial(dispatch_body, m, len(terms)),
         [jax.ShapeDtypeStruct((count, wide), bf16)]
@@ -478,9 +515,9 @@
     later, far_partner = call(
         functools.partial(up_body, n),
         [jax.ShapeDtypeStruct((exp_dev, 2 * half * cap, hidden), bf16), part],
-        [WHOLE] * (2 * n + 4),
+        [WHOLE] * (2 * n + 5),
         limit=16 * 2**20,
-    )(*fragments, gain2, gate_w, up_w, down_w)
+    )(*fragments, gain2, gate_w, up_low, up_high, down_w)
     far_own, *near_outs = call(
         functools.partial(down_body, n), [part] * 3, [WHOLE] * 2, limit=8 * 2**20
     )(later, down_w)

time: 89.6 us -> 90 us (level)
    pallas_call x3 -> x4, Pallas kernels: 7.87 us -> 8.7 us  [fetch(): call(functools.partial(fetch_body, [x[1:] for x in sources]), [pltpu.VMEM...]
  transfers between devices with their start and end apart: 46 -> 46, of which waited for: 21 -> 21; matrix products, arithmetic and copies ran while one was open for 0% -> 0% of each run, Pallas kernels for 16% -> 17%
where the time goes in v2:
time: 90 us; the launch traced here: 89.8 us
  starting transfers between devices  36.3 us (40%)
  waiting for transfers between devices  31 us (34%)
  Pallas kernels  21.6 us (24%)
    ppermute x46, starting transfers between devices, swap(): lax.ppermute(x, axis, [(i, i ^ k) for i in range(lax.axis_size(axis))])  36.3 us
    ppermute x46, waiting for transfers between devices, swap(): lax.ppermute(x, axis, [(i, i ^ k) for i in range(lax.axis_size(axis))])  31 us
    pallas_call x4, Pallas kernels, fetch(): call(functools.partial(fetch_body, [x[1:] for x in sources]), [pltpu.VMEM...  8.7 us
    pallas_call x1, Pallas kernels, local_swaps(): call(functools.partial(prep_body, n, cap), [jax.ShapeDtypeStruct((count,...  3.73 us
    pallas_call x1, Pallas kernels, local_swaps(): call(functools.partial(up_body, n), [jax.ShapeDtypeStruct((exp_dev, 2 * h...  2.54 us
    pallas_call x1, Pallas kernels, local_swaps(): call(state_body, [jax.ShapeDtypeStruct((count, groups, entries), f32)] *...  2.13 us
  transfers between devices with their start and end apart: 46, of which 21 were waited for; matrix products, arithmetic and copies ran while one was open for 0% of the time, Pallas kernels for 17%

profile of v2, /device:TPU:0, one launch (start us, length us, event | category | flops | bytes accessed | tf_op | source)
XLA Modules:
  0.0 89.8 jit_solution(9446972511203370403)
XLA Ops:
  0.6 3.0 %collective-permute-start.1 = (bf16[64,512]{1,0:T(8,128)(2,1)}, bf16[64,512]{1,0:T(8,128)(2,1)S(1)}, u32[]{:S(2)}, u32[]{:S(2)}) collective-permute-start(bf16[64,512]{1,0:T(8,128)(2,1)} %refs_15_.1), channel_id=1, source_target_pairs={{0,2},{1,3},{2,0},{3,1},{4,6},{5,7},{6,4},{7,5},{8,10},{9,11},{10,... | collective-permute-start | bytes 196616 | tf_op jit(solution)/shard_map/ppermute | solution.py:29
  3.7 1.5 %collective-permute-start.5 = (bf16[64,512]{1,0:T(8,128)(2,1)}, bf16[64,512]{1,0:T(8,128)(2,1)S(1)}, u32[]{:S(2)}, u32[]{:S(2)}) collective-permute-start(bf16[64,512]{1,0:T(8,128)(2,1)} %refs_15_.1), channel_id=1, source_target_pairs={{0,6},{1,7},{2,4},{3,5},{4,2},{5,3},{6,0},{7,1},{8,14},{9,15},{10,... | collective-permute-start | bytes 196616 | tf_op jit(solution)/shard_map/ppermute | solution.py:29
  5.2 1.2 %collective-permute-done.1.refs_2_ = bf16[64,512]{1,0:T(8,128)(2,1)S(1)} collective-permute-done((bf16[64,512]{1,0:T(8,128)(2,1)}, bf16[64,512]{1,0:T(8,128)(2,1)S(1)}, u32[]{:S(2)}, u32[]{:S(2)}) %collective-permute-start.1) | collective-permute-done | bytes 65568 | tf_op jit(solution)/shard_map/ppermute | solution.py:29
  6.4 2.7 %collective-permute-done.5.refs_6_ = bf16[64,512]{1,0:T(8,128)(2,1)S(1)} collective-permute-done((bf16[64,512]{1,0:T(8,128)(2,1)}, bf16[64,512]{1,0:T(8,128)(2,1)S(1)}, u32[]{:S(2)}, u32[]{:S(2)}) %collective-permute-start.5) | collective-permute-done | bytes 65568 | tf_op jit(solution)/shard_map/ppermute | solution.py:29
  9.1 0.8 collective-permute-done.3.refs_4_
  9.9 3.7 %shard_map.229 = (f32[64,1024]{1,0:T(8,128)S(1)}, f32[64,1024]{1,0:T(8,128)S(1)}, bf16[256,512]{1,0:T(8,128)(2,1)S(1)}, bf16[256,512]{1,0:T(8,128)(2,1)S(1)}, f3...) custom-call(bf16[256,4096]{1,0:T(8,128)(2,1)} %refs_0_.2, ...), custom_call_target="tpu_custom_call" | custom-call | flops 10000000 | bytes 1000000 | tf_op jit(solution)/shard_map/pallas_call | solution.py:449
  13.7 0.9 shard_map.230
  14.6 1.5 %collective-permute-start.12 = (bf16[64,256]{1,0:T(8,128)(2,1)S(1)}, bf16[64,256]{1,0:T(8,128)(2,1)S(1)}, u32[]{:S(2)}, u32[]{:S(2)}) collective-permute-start(bf16[64,256]{1,0:T(8,128)(2,1)S(1)} %get-tuple-element.59.refs_0_), channel_id=1, source_target_pairs={{0,6},{1,7},{2,4},{3,5},{4,2},{5,3},{6,0},{7,1},{8,14},{9,15},{10,... | collective-permute-start | bytes 98312 | tf_op jit(solution)/shard_map/ppermute | solution.py:29
  16.1 1.2 %collective-permute-start.10 = (bf16[64,256]{1,0:T(8,128)(2,1)S(1)}, bf16[64,256]{1,0:T(8,128)(2,1)S(1)}, u32[]{:S(2)}, u32[]{:S(2)}) collective-permute-start(bf16[64,256]{1,0:T(8,128)(2,1)S(1)} %get-tuple-element.59.refs_0_), channel_id=1, source_target_pairs={{0,4},{1,5},{2,6},{3,7},{4,0},{5,1},{6,2},{7,3},{8,12},{9,13},{10,... | collective-permute-start | bytes 98312 | tf_op jit(solution)/shard_map/ppermute | solution.py:29
  17.3 0.8 collective-permute-start.8
  18.1 1.3 %collective-permute-done.12.refs_6_ = bf16[64,256]{1,0:T(8,128)(2,1)S(1)} collective-permute-done((bf16[64,256]{1,0:T(8,128)(2,1)S(1)}, bf16[64,256]{1,0:T(8,128)(2,1)S(1)}, u32[]{:S(2)}, u32[]{:S(2)}) %collective-permute-start.12) | collective-permute-done | bytes 32800 | tf_op jit(solution)/shard_map/ppermute | solution.py:29
  19.5 0.6 collective-permute-done.10.refs_4_
  20.0 1.2 %collective-permute-done.8.refs_2_ = bf16[64,256]{1,0:T(8,128)(2,1)S(1)} collective-permute-done((bf16[64,256]{1,0:T(8,128)(2,1)S(1)}, bf16[64,256]{1,0:T(8,128)(2,1)S(1)}, u32[]{:S(2)}, u32[]{:S(2)}) %collective-permute-start.8) | collective-permute-done | bytes 32800 | tf_op jit(solution)/shard_map/ppermute | solution.py:29
  21.3 2.0 %shard_map.231 = (bf16[256,2048]{1,0:T(8,128)(2,1)S(1)}, bf16[256,4096]{1,0:T(8,128)(2,1)S(1)}) custom-call(bf16[256,2048]{1,0:T(8,128)(2,1)} %refs_0_.3, bf16[256,4096]{1,0:T(8,128)(2,1)} %refs_1_.3), custom_call_target="tpu_custom_call" | custom-call | flops 10000000 | bytes 1000000 | tf_op jit(solution)/shard_map/pallas_call | solution.py:264
  23.3 0.7 shard_map.232
  24.1 0.6 collective-permute-start.14
  24.6 0.3 shard_map.233.own
  24.9 0.9 collective-permute-done.14.other
  25.8 0.9 collective-permute-start.15
  26.7 1.2 %collective-permute-start.16 = (bf16[64,512]{1,0:T(8,128)(2,1)S(1)}, bf16[64,512]{1,0:T(8,128)(2,1)S(1)}, u32[]{:S(2)}, u32[]{:S(2)}) collective-permute-start(bf16[64,512]{1,0:T(8,128)(2,1)S(1)} %get-tuple-element.67), channel_id=1, source_target_pairs={{0,4},{1,5},{2,6},{3,7},{4,0},{5,1},{6,2},{7,3},{8,12},{9,13},{10,... | collective-permute-start | bytes 196616 | tf_op jit(solution)/shard_map/ppermute | solution.py:29
  27.9 1.5 %collective-permute-start.17 = (bf16[64,512]{1,0:T(8,128)(2,1)S(1)}, bf16[64,512]{1,0:T(8,128)(2,1)S(1)}, u32[]{:S(2)}, u32[]{:S(2)}) collective-permute-start(bf16[64,512]{1,0:T(8,128)(2,1)S(1)} %get-tuple-element.68), channel_id=1, source_target_pairs={{0,6},{1,7},{2,4},{3,5},{4,2},{5,3},{6,0},{7,1},{8,14},{9,15},{10,... | collective-permute-start | bytes 196616 | tf_op jit(solution)/shard_map/ppermute | solution.py:29
  29.4 0.9 collective-permute-done.15.refs_2_
  30.3 0.7 collective-permute-done.16.refs_3_
  31.0 2.1 %collective-permute-done.17.refs_4_ = bf16[64,512]{1,0:T(8,128)(2,1)S(1)} collective-permute-done((bf16[64,512]{1,0:T(8,128)(2,1)S(1)}, bf16[64,512]{1,0:T(8,128)(2,1)S(1)}, u32[]{:S(2)}, u32[]{:S(2)}) %collective-permute-start.17) | collective-permute-done | bytes 65568 | tf_op jit(solution)/shard_map/ppermute | solution.py:29
  33.0 0.2 shard_map.235
  33.3 2.7 %collective-permute-start.26 = (bf16[2,24,512]{2,1,0:T(8,128)(2,1)S(1)}, bf16[2,24,512]{2,1,0:T(8,128)(2,1)S(1)}, u32[]{:S(2)}, u32[]{:S(2)}) collective-permute-start(bf16[2,24,512]{2,1,0:T(8,128)(2,1)S(1)} %get-tuple-element.74), channel_id=1, source_target_pairs={{0,16},{8,24},{16,0},{24,8},{1,17},{9,25},{17,1},{25,9},{2,18},{10... | collective-permute-start | bytes 147464 | tf_op jit(solution)/shard_map/ppermute | solution.py:29
  36.0 1.3 %collective-permute-start.27 = (bf16[2,24,512]{2,1,0:T(8,128)(2,1)S(1)}, bf16[2,24,512]{2,1,0:T(8,128)(2,1)S(1)}, u32[]{:S(2)}, u32[]{:S(2)}) collective-permute-start(bf16[2,24,512]{2,1,0:T(8,128)(2,1)S(1)} %get-tuple-element.75), channel_id=1, source_target_pairs={{0,24},{8,16},{16,8},{24,0},{1,25},{9,17},{17,9},{25,1},{2,26},{10... | collective-permute-start | bytes 147464 | tf_op jit(solution)/shard_map/ppermute | solution.py:29
  37.4 1.3 %collective-permute-done.26.refs_0_ = bf16[2,24,512]{2,1,0:T(8,128)(2,1)S(1)} collective-permute-done((bf16[2,24,512]{2,1,0:T(8,128)(2,1)S(1)}, bf16[2,24,512]{2,1,0:T(8,128)(2,1)S(1)}, u32[]{:S(2)}, u32[]{:S(2)}) %collective-permute-start.26) | collective-permute-done | bytes 49184 | tf_op jit(solution)/shard_map/ppermute | solution.py:29
  38.6 3.3 %collective-permute-done.27.refs_1_ = bf16[2,24,512]{2,1,0:T(8,128)(2,1)S(1)} collective-permute-done((bf16[2,24,512]{2,1,0:T(8,128)(2,1)S(1)}, bf16[2,24,512]{2,1,0:T(8,128)(2,1)S(1)}, u32[]{:S(2)}, u32[]{:S(2)}) %collective-permute-start.27) | collective-permute-done | bytes 49184 | tf_op jit(solution)/shard_map/ppermute | solution.py:29
  41.9 1.5 %collective-permute-start.33 = (bf16[2,48,512]{2,1,0:T(8,128)(2,1)S(1)}, bf16[2,48,512]{2,1,0:T(8,128)(2,1)S(1)}, u32[]{:S(2)}, u32[]{:S(2)}) collective-permute-start(bf16[2,48,512]{2,1,0:T(8,128)(2,1)S(1)} %shard_map.237.refs_8_), channel_id=1, source_target_pairs={{0,6},{1,7},{2,4},{3,5},{4,2},{5,3},{6,0},{7,1},{8,14},{9,15},{10,... | collective-permute-start | bytes 294920 | tf_op jit(solution)/shard_map/ppermute | solution.py:29
  43.4 0.8 collective-permute-start.31
  44.2 1.3 %collective-permute-start.29 = (bf16[2,48,512]{2,1,0:T(8,128)(2,1)S(1)}, bf16[2,48,512]{2,1,0:T(8,128)(2,1)S(1)}, u32[]{:S(2)}, u32[]{:S(2)}) collective-permute-start(bf16[2,48,512]{2,1,0:T(8,128)(2,1)S(1)} %shard_map.237.refs_8_), channel_id=1, source_target_pairs={{0,2},{1,3},{2,0},{3,1},{4,6},{5,7},{6,4},{7,5},{8,10},{9,11},{10,... | collective-permute-start | bytes 294920 | tf_op jit(solution)/shard_map/ppermute | solution.py:29
  45.5 4.2 %collective-permute-done.18.refs_1_ = bf16[2,24,512]{2,1,0:T(8,128)(2,1)S(1)} collective-permute-done((bf16[2,24,512]{2,1,0:T(8,128)(2,1)S(1)}, bf16[2,24,512]{2,1,0:T(8,128)(2,1)S(1)}, u32[]{:S(2)}, u32[]{:S(2)}) %collective-permute-start.18) | collective-permute-done | bytes 49184 | tf_op jit(solution)/shard_map/ppermute | solution.py:29
  49.7 1.5 %collective-permute-start.24 = (bf16[2,48,512]{2,1,0:T(8,128)(2,1)S(1)}, bf16[2,48,512]{2,1,0:T(8,128)(2,1)S(1)}, u32[]{:S(2)}, u32[]{:S(2)}) collective-permute-start(bf16[2,48,512]{2,1,0:T(8,128)(2,1)S(1)} %shard_map.236.refs_0_), channel_id=1, source_target_pairs={{0,6},{1,7},{2,4},{3,5},{4,2},{5,3},{6,0},{7,1},{8,14},{9,15},{10,... | collective-permute-start | bytes 294920 | tf_op jit(solution)/shard_map/ppermute | solution.py:29
  51.1 0.8 collective-permute-start.22
  51.9 1.3 %collective-permute-start.20 = (bf16[2,48,512]{2,1,0:T(8,128)(2,1)S(1)}, bf16[2,48,512]{2,1,0:T(8,128)(2,1)S(1)}, u32[]{:S(2)}, u32[]{:S(2)}) collective-permute-start(bf16[2,48,512]{2,1,0:T(8,128)(2,1)S(1)} %shard_map.236.refs_0_), channel_id=1, source_target_pairs={{0,2},{1,3},{2,0},{3,1},{4,6},{5,7},{6,4},{7,5},{8,10},{9,11},{10,... | collective-permute-start | bytes 294920 | tf_op jit(solution)/shard_map/ppermute | solution.py:29
  53.2 0.5 collective-permute-start.34
  53.7 2.4 %collective-permute-done.24.refs_6_ = bf16[2,48,512]{2,1,0:T(8,128)(2,1)S(1)} collective-permute-done((bf16[2,48,512]{2,1,0:T(8,128)(2,1)S(1)}, bf16[2,48,512]{2,1,0:T(8,128)(2,1)S(1)}, u32[]{:S(2)}, u32[]{:S(2)}) %collective-permute-start.24) | collective-permute-done | bytes 98336 | tf_op jit(solution)/shard_map/ppermute | solution.py:29
  56.2 0.9 collective-permute-done.22.refs_4_
  57.1 0.5 collective-permute-start.25
  57.7 0.4 collective-permute-start.21
  58.1 1.6 %shard_map.239.refs_19_ = bf16[256,4096]{1,0:T(8,128)(2,1)S(1)} custom-call(bf16[512,4096]{1,0:T(8,128)(2,1)} %bitcast.13), custom_call_target="tpu_custom_call" | custom-call | flops 10000000 | bytes 1000000 | tf_op jit(solution)/shard_map/pallas_call | solution.py:264
  59.7 2.2 %shard_map.240.refs_20_.down_w = bf16[512,4096]{1,0:T(8,128)(2,1)S(1)} custom-call(bf16[512,4096]{1,0:T(8,128)(2,1)} %bitcast.15), custom_call_target="tpu_custom_call" | custom-call | flops 10000000 | bytes 1000000 | tf_op jit(solution)/shard_map/pallas_call | solution.py:264
  61.9 2.9 %shard_map.238 = (bf16[512,4096]{1,0:T(8,128)(2,1)S(1)}, bf16[256,4096]{1,0:T(8,128)(2,1)S(1)}) custom-call(bf16[512,4096]{1,0:T(8,128)(2,1)} %bitcast.16, bf16[512,4096]{1,0:T(8,128)(2,1)} %bitcast.14), custom_call_target="tpu_custom_call" | custom-call | flops 10000000 | bytes 1000000 | tf_op jit(solution)/shard_map/pallas_call | solution.py:264
  64.9 2.5 %shard_map.241 = (bf16[2,96,256]{2,1,0:T(8,128)(2,1)S(1)}, bf16[4,2,48,512]{3,2,1,0:T(8,128)(2,1)S(1)}) custom-call(bf16[2,48,512]{2,1,0:T(8,128)(2,1)S(1)} %shard_map.236.refs_0_, bf16[2,48,512]{2,1,0:T(8,128)(2,1)S(1)} %collective-permute-done.19.refs_1_, bf16[2,48,512]{2,1,0:T(8,128)(2,1)S(1)} %collective-permute-done.20.refs_2_, ...), custom_call_target="tpu_custom_call" | custom-call | flops 10000000 | bytes 1000000 | tf_op jit(solution)/shard_map/pallas_call | solution.py:515
  67.4 1.2 %shard_map.242 = (bf16[4,2,48,512]{3,2,1,0:T(8,128)(2,1)S(1)}, bf16[4,2,48,512]{3,2,1,0:T(8,128)(2,1)S(1)}, bf16[4,2,48,512]{3,2,1,0:T(8,128)(2,1)S(1)}) custom-call(bf16[2,96,256]{2,1,0:T(8,128)(2,1)S(1)} %get-tuple-element.79.hidden, bf16[512,4096]{1,0:T(8,128)(2,1)S(1)} %shard_map.240.refs_20_.down_w), custom_call_target="tpu_custom_call" | custom-call | flops 10000000 | bytes 1000000 | tf_op jit(solution)/shard_map/pallas_call | solution.py:521
  68.8 0.4 collective-permute-start.40
  69.2 1.2 %collective-permute-done.35.other = bf16[4,2,48,512]{3,2,1,0:T(8,128)(2,1)S(1)} collective-permute-done((bf16[4,2,48,512]{3,2,1,0:T(8,128)(2,1)S(1)}, bf16[4,2,48,512]{3,2,1,0:T(8,128)(2,1)S(1)}, u32[]{:S(2)}, u32[]{:S(2)}) %collective-permute-start.35) | collective-permute-done | bytes 393248 | tf_op jit(solution)/shard_map/ppermute | solution.py:29
  70.5 0.8 collective-permute-start.36
  71.3 1.2 %collective-permute-start.37 = (bf16[2,48,512]{2,1,0:T(8,128)(2,1)S(1)}, bf16[2,48,512]{2,1,0:T(8,128)(2,1)S(1)}, u32[]{:S(2)}, u32[]{:S(2)}) collective-permute-start(bf16[2,48,512]{2,1,0:T(8,128)(2,1)S(1)} %get-tuple-element.84), channel_id=1, source_target_pairs={{0,4},{1,5},{2,6},{3,7},{4,0},{5,1},{6,2},{7,3},{8,12},{9,13},{10,... | collective-permute-start | bytes 294920 | tf_op jit(solution)/shard_map/ppermute | solution.py:29
  72.6 1.5 %collective-permute-start.38 = (bf16[2,48,512]{2,1,0:T(8,128)(2,1)S(1)}, bf16[2,48,512]{2,1,0:T(8,128)(2,1)S(1)}, u32[]{:S(2)}, u32[]{:S(2)}) collective-permute-start(bf16[2,48,512]{2,1,0:T(8,128)(2,1)S(1)} %get-tuple-element.85), channel_id=1, source_target_pairs={{0,6},{1,7},{2,4},{3,5},{4,2},{5,3},{6,0},{7,1},{8,14},{9,15},{10,... | collective-permute-start | bytes 294920 | tf_op jit(solution)/shard_map/ppermute | solution.py:29
  74.2 0.8 collective-permute-start.41
  75.0 1.2 %collective-permute-start.42 = (bf16[2,48,512]{2,1,0:T(8,128)(2,1)S(1)}, bf16[2,48,512]{2,1,0:T(8,128)(2,1)S(1)}, u32[]{:S(2)}, u32[]{:S(2)}) collective-permute-start(bf16[2,48,512]{2,1,0:T(8,128)(2,1)S(1)} %get-tuple-element.92), channel_id=1, source_target_pairs={{0,4},{1,5},{2,6},{3,7},{4,0},{5,1},{6,2},{7,3},{8,12},{9,13},{10,... | collective-permute-start | bytes 294920 | tf_op jit(solution)/shard_map/ppermute | solution.py:29
  76.2 1.5 %collective-permute-start.43 = (bf16[2,48,512]{2,1,0:T(8,128)(2,1)S(1)}, bf16[2,48,512]{2,1,0:T(8,128)(2,1)S(1)}, u32[]{:S(2)}, u32[]{:S(2)}) collective-permute-start(bf16[2,48,512]{2,1,0:T(8,128)(2,1)S(1)} %get-tuple-element.93), channel_id=1, source_target_pairs={{0,6},{1,7},{2,4},{3,5},{4,2},{5,3},{6,0},{7,1},{8,14},{9,15},{10,... | collective-permute-start | bytes 294920 | tf_op jit(solution)/shard_map/ppermute | solution.py:29
  77.7 1.4 %collective-permute-done.38.refs_3_ = bf16[2,48,512]{2,1,0:T(8,128)(2,1)S(1)} collective-permute-done((bf16[2,48,512]{2,1,0:T(8,128)(2,1)S(1)}, bf16[2,48,512]{2,1,0:T(8,128)(2,1)S(1)}, u32[]{:S(2)}, u32[]{:S(2)}) %collective-permute-start.38) | collective-permute-done | bytes 98336 | tf_op jit(solution)/shard_map/ppermute | solution.py:29
  79.2 0.6 collective-permute-start.39
  79.8 0.8 collective-permute-done.41.refs_1_
  80.6 1.7 %collective-permute-done.42.refs_2_ = bf16[2,48,512]{2,1,0:T(8,128)(2,1)S(1)} collective-permute-done((bf16[2,48,512]{2,1,0:T(8,128)(2,1)S(1)}, bf16[2,48,512]{2,1,0:T(8,128)(2,1)S(1)}, u32[]{:S(2)}, u32[]{:S(2)}) %collective-permute-start.42) | collective-permute-done | bytes 98336 | tf_op jit(solution)/shard_map/ppermute | solution.py:29
  82.3 0.7 collective-permute-start.44
  83.1 2.2 %collective-permute-start.45 = (bf16[2,24,512]{2,1,0:T(8,128)(2,1)S(1)}, bf16[2,24,512]{2,1,0:T(8,128)(2,1)S(1)}, u32[]{:S(2)}, u32[]{:S(2)}) collective-permute-start(bf16[2,24,512]{2,1,0:T(8,128)(2,1)S(1)} %get-tuple-element.95), channel_id=1, source_target_pairs={{0,24},{8,16},{16,8},{24,0},{1,25},{9,17},{17,9},{25,1},{2,26},{10... | collective-permute-start | bytes 147464 | tf_op jit(solution)/shard_map/ppermute | solution.py:29
  85.3 2.1 %shard_map.248 = (f32[64,16,64]{2,1,0:T(8,128)}, f32[64,16,64]{2,1,0:T(8,128)}) custom-call(bf16[64,256]{1,0:T(8,128)(2,1)S(1)} %get-tuple-element.96.driven, f32[64,1024]{1,0:T(8,128)S(1)} %get-tuple-element.97.dec_r, f32[64,1024]{1,0:T(8,128)S(1)} %get-tuple-element.98.dec_i, bf16[256,512]{1,0:T(8,128)(2,1)S(1)} %get-tuple-element.99.bt_r, ...), custom_call_target="tpu_custom_call" | custom-call | flops 10000000 | bytes 1000000 | tf_op jit(solution)/shard_map/pallas_call | solution.py:536
  87.5 0.5 collective-permute-done.44.refs_5_
  87.9 1.1 %collective-permute-done.45.refs_6_ = bf16[2,24,512]{2,1,0:T(8,128)(2,1)S(1)} collective-permute-done((bf16[2,24,512]{2,1,0:T(8,128)(2,1)S(1)}, bf16[2,24,512]{2,1,0:T(8,128)(2,1)S(1)}, u32[]{:S(2)}, u32[]{:S(2)}) %collective-permute-start.45) | collective-permute-done | bytes 49184 | tf_op jit(solution)/shard_map/ppermute | solution.py:29
  89.0 0.9 shard_map.247
  (50 shorter events, 0.7 us)
Async XLA Ops:
  0.6 5.8 %collective-permute-start.1 = (bf16[64,512]{1,0:T(8,128)(2,1)}, bf16[64,512]{1,0:T(8,128)(2,1)S(1)}, u32[]{:S(2)}, u32[]{:S(2)}) collective-permute-start(bf16[64,512]{1,0:T(8,128)(2,1)} %refs_15_.1), channel_id=1, source_target_pairs={{0,2},{1,3},{2,0},{3,1},{4,6},{5,7},{6,4},{7,5},{8,10},{9,11},{10,... | collective-permute-start | bytes 196616 | tf_op jit(solution)/shard_map/ppermute | solution.py:29
  3.7 5.4 %collective-permute-start.5 = (bf16[64,512]{1,0:T(8,128)(2,1)}, bf16[64,512]{1,0:T(8,128)(2,1)S(1)}, u32[]{:S(2)}, u32[]{:S(2)}) collective-permute-start(bf16[64,512]{1,0:T(8,128)(2,1)} %refs_15_.1), channel_id=1, source_target_pairs={{0,6},{1,7},{2,4},{3,5},{4,2},{5,3},{6,0},{7,1},{8,14},{9,15},{10,... | collective-permute-start | bytes 196616 | tf_op jit(solution)/shard_map/ppermute | solution.py:29
  5.2 4.7 %collective-permute-start.3 = (bf16[64,512]{1,0:T(8,128)(2,1)}, bf16[64,512]{1,0:T(8,128)(2,1)S(1)}, u32[]{:S(2)}, u32[]{:S(2)}) collective-permute-start(bf16[64,512]{1,0:T(8,128)(2,1)} %refs_15_.1), channel_id=1, source_target_pairs={{0,4},{1,5},{2,6},{3,7},{4,0},{5,1},{6,2},{7,3},{8,12},{9,13},{10,... | collective-permute-start | bytes 196616 | tf_op jit(solution)/shard_map/ppermute | solution.py:29
  5.2 8.4 %collective-permute-start = (bf16[64,512]{1,0:T(8,128)(2,1)}, bf16[64,512]{1,0:T(8,128)(2,1)S(1)}, u32[]{:S(2)}, u32[]{:S(2)}) collective-permute-start(bf16[64,512]{1,0:T(8,128)(2,1)} %refs_15_.1), channel_id=1, source_target_pairs={{0,1},{1,0},{2,3},{3,2},{4,5},{5,4},{6,7},{7,6},{8,9},{9,8},{10,11... | collective-permute-start | bytes 196616 | tf_op jit(solution)/shard_map/ppermute | solution.py:29
  6.4 7.3 %collective-permute-start.2 = (bf16[64,512]{1,0:T(8,128)(2,1)S(1)}, bf16[64,512]{1,0:T(8,128)(2,1)S(1)}, u32[]{:S(2)}, u32[]{:S(2)}) collective-permute-start(bf16[64,512]{1,0:T(8,128)(2,1)S(1)} %collective-permute-done.1.refs_2_), channel_id=1, source_target_pairs={{0,1},{1,0},{2,3},{3,2},{4,5},{5,4},{6,7},{7,6},{8,9},{9,8},{10,11... | collective-permute-start | bytes 196616 | tf_op jit(solution)/shard_map/ppermute | solution.py:29
  9.1 4.5 %collective-permute-start.6 = (bf16[64,512]{1,0:T(8,128)(2,1)S(1)}, bf16[64,512]{1,0:T(8,128)(2,1)S(1)}, u32[]{:S(2)}, u32[]{:S(2)}) collective-permute-start(bf16[64,512]{1,0:T(8,128)(2,1)S(1)} %collective-permute-done.5.refs_6_), channel_id=1, source_target_pairs={{0,1},{1,0},{2,3},{3,2},{4,5},{5,4},{6,7},{7,6},{8,9},{9,8},{10,11... | collective-permute-start | bytes 196616 | tf_op jit(solution)/shard_map/ppermute | solution.py:29
  9.9 3.8 %collective-permute-start.4 = (bf16[64,512]{1,0:T(8,128)(2,1)S(1)}, bf16[64,512]{1,0:T(8,128)(2,1)S(1)}, u32[]{:S(2)}, u32[]{:S(2)}) collective-permute-start(bf16[64,512]{1,0:T(8,128)(2,1)S(1)} %collective-permute-done.3.refs_4_), channel_id=1, source_target_pairs={{0,1},{1,0},{2,3},{3,2},{4,5},{5,4},{6,7},{7,6},{8,9},{9,8},{10,11... | collective-permute-start | bytes 196616 | tf_op jit(solution)/shard_map/ppermute | solution.py:29
  14.6 4.9 %collective-permute-start.12 = (bf16[64,256]{1,0:T(8,128)(2,1)S(1)}, bf16[64,256]{1,0:T(8,128)(2,1)S(1)}, u32[]{:S(2)}, u32[]{:S(2)}) collective-permute-start(bf16[64,256]{1,0:T(8,128)(2,1)S(1)} %get-tuple-element.59.refs_0_), channel_id=1, source_target_pairs={{0,6},{1,7},{2,4},{3,5},{4,2},{5,3},{6,0},{7,1},{8,14},{9,15},{10,... | collective-permute-start | bytes 98312 | tf_op jit(solution)/shard_map/ppermute | solution.py:29
  16.1 3.9 %collective-permute-start.10 = (bf16[64,256]{1,0:T(8,128)(2,1)S(1)}, bf16[64,256]{1,0:T(8,128)(2,1)S(1)}, u32[]{:S(2)}, u32[]{:S(2)}) collective-permute-start(bf16[64,256]{1,0:T(8,128)(2,1)S(1)} %get-tuple-element.59.refs_0_), channel_id=1, source_target_pairs={{0,4},{1,5},{2,6},{3,7},{4,0},{5,1},{6,2},{7,3},{8,12},{9,13},{10,... | collective-permute-start | bytes 98312 | tf_op jit(solution)/shard_map/ppermute | solution.py:29
  17.3 3.9 %collective-permute-start.8 = (bf16[64,256]{1,0:T(8,128)(2,1)S(1)}, bf16[64,256]{1,0:T(8,128)(2,1)S(1)}, u32[]{:S(2)}, u32[]{:S(2)}) collective-permute-start(bf16[64,256]{1,0:T(8,128)(2,1)S(1)} %get-tuple-element.59.refs_0_), channel_id=1, source_target_pairs={{0,2},{1,3},{2,0},{3,1},{4,6},{5,7},{6,4},{7,5},{8,10},{9,11},{10,... | collective-permute-start | bytes 98312 | tf_op jit(solution)/shard_map/ppermute | solution.py:29
  18.1 5.2 %collective-permute-start.7 = (bf16[64,256]{1,0:T(8,128)(2,1)S(1)}, bf16[64,256]{1,0:T(8,128)(2,1)S(1)}, u32[]{:S(2)}, u32[]{:S(2)}) collective-permute-start(bf16[64,256]{1,0:T(8,128)(2,1)S(1)} %get-tuple-element.59.refs_0_), channel_id=1, source_target_pairs={{0,1},{1,0},{2,3},{3,2},{4,5},{5,4},{6,7},{7,6},{8,9},{9,8},{10,11... | collective-permute-start | bytes 98312 | tf_op jit(solution)/shard_map/ppermute | solution.py:29
  19.5 3.8 %collective-permute-start.13 = (bf16[64,256]{1,0:T(8,128)(2,1)S(1)}, bf16[64,256]{1,0:T(8,128)(2,1)S(1)}, u32[]{:S(2)}, u32[]{:S(2)}) collective-permute-start(bf16[64,256]{1,0:T(8,128)(2,1)S(1)} %collective-permute-done.12.refs_6_), channel_id=1, source_target_pairs={{0,1},{1,0},{2,3},{3,2},{4,5},{5,4},{6,7},{7,6},{8,9},{9,8},{10,11... | collective-permute-start | bytes 98312 | tf_op jit(solution)/shard_map/ppermute | solution.py:29
  20.0 3.3 %collective-permute-start.11 = (bf16[64,256]{1,0:T(8,128)(2,1)S(1)}, bf16[64,256]{1,0:T(8,128)(2,1)S(1)}, u32[]{:S(2)}, u32[]{:S(2)}) collective-permute-start(bf16[64,256]{1,0:T(8,128)(2,1)S(1)} %collective-permute-done.10.refs_4_), channel_id=1, source_target_pairs={{0,1},{1,0},{2,3},{3,2},{4,5},{5,4},{6,7},{7,6},{8,9},{9,8},{10,11... | collective-permute-start | bytes 98312 | tf_op jit(solution)/shard_map/ppermute | solution.py:29
  21.3 2.1 %collective-permute-start.9 = (bf16[64,256]{1,0:T(8,128)(2,1)S(1)}, bf16[64,256]{1,0:T(8,128)(2,1)S(1)}, u32[]{:S(2)}, u32[]{:S(2)}) collective-permute-start(bf16[64,256]{1,0:T(8,128)(2,1)S(1)} %collective-permute-done.8.refs_2_), channel_id=1, source_target_pairs={{0,1},{1,0},{2,3},{3,2},{4,5},{5,4},{6,7},{7,6},{8,9},{9,8},{10,11... | collective-permute-start | bytes 98312 | tf_op jit(solution)/shard_map/ppermute | solution.py:29
  24.1 1.7 %collective-permute-start.14 = (bf16[4,64,512]{2,1,0:T(8,128)(2,1)S(1)}, bf16[4,64,512]{2,1,0:T(8,128)(2,1)S(1)}, u32[]{:S(2)}, u32[]{:S(2)}) collective-permute-start(bf16[4,64,512]{2,1,0:T(8,128)(2,1)S(1)} %get-tuple-element.64), channel_id=1, source_target_pairs={{0,1},{1,0},{2,3},{3,2},{4,5},{5,4},{6,7},{7,6},{8,9},{9,8},{10,11... | collective-permute-start | bytes 786440 | tf_op jit(solution)/shard_map/ppermute | solution.py:29
  25.8 4.4 %collective-permute-start.15 = (bf16[64,512]{1,0:T(8,128)(2,1)S(1)}, bf16[64,512]{1,0:T(8,128)(2,1)S(1)}, u32[]{:S(2)}, u32[]{:S(2)}) collective-permute-start(bf16[64,512]{1,0:T(8,128)(2,1)S(1)} %get-tuple-element.66), channel_id=1, source_target_pairs={{0,2},{1,3},{2,0},{3,1},{4,6},{5,7},{6,4},{7,5},{8,10},{9,11},{10,... | collective-permute-start | bytes 196616 | tf_op jit(solution)/shard_map/ppermute | solution.py:29
  26.7 4.3 %collective-permute-start.16 = (bf16[64,512]{1,0:T(8,128)(2,1)S(1)}, bf16[64,512]{1,0:T(8,128)(2,1)S(1)}, u32[]{:S(2)}, u32[]{:S(2)}) collective-permute-start(bf16[64,512]{1,0:T(8,128)(2,1)S(1)} %get-tuple-element.67), channel_id=1, source_target_pairs={{0,4},{1,5},{2,6},{3,7},{4,0},{5,1},{6,2},{7,3},{8,12},{9,13},{10,... | collective-permute-start | bytes 196616 | tf_op jit(solution)/shard_map/ppermute | solution.py:29
  27.9 5.2 %collective-permute-start.17 = (bf16[64,512]{1,0:T(8,128)(2,1)S(1)}, bf16[64,512]{1,0:T(8,128)(2,1)S(1)}, u32[]{:S(2)}, u32[]{:S(2)}) collective-permute-start(bf16[64,512]{1,0:T(8,128)(2,1)S(1)} %get-tuple-element.68), channel_id=1, source_target_pairs={{0,6},{1,7},{2,4},{3,5},{4,2},{5,3},{6,0},{7,1},{8,14},{9,15},{10,... | collective-permute-start | bytes 196616 | tf_op jit(solution)/shard_map/ppermute | solution.py:29
  33.3 5.4 %collective-permute-start.26 = (bf16[2,24,512]{2,1,0:T(8,128)(2,1)S(1)}, bf16[2,24,512]{2,1,0:T(8,128)(2,1)S(1)}, u32[]{:S(2)}, u32[]{:S(2)}) collective-permute-start(bf16[2,24,512]{2,1,0:T(8,128)(2,1)S(1)} %get-tuple-element.74), channel_id=1, source_target_pairs={{0,16},{8,24},{16,0},{24,8},{1,17},{9,25},{17,1},{25,9},{2,18},{10... | collective-permute-start | bytes 147464 | tf_op jit(solution)/shard_map/ppermute | solution.py:29
  36.0 5.9 %collective-permute-start.27 = (bf16[2,24,512]{2,1,0:T(8,128)(2,1)S(1)}, bf16[2,24,512]{2,1,0:T(8,128)(2,1)S(1)}, u32[]{:S(2)}, u32[]{:S(2)}) collective-permute-start(bf16[2,24,512]{2,1,0:T(8,128)(2,1)S(1)} %get-tuple-element.75), channel_id=1, source_target_pairs={{0,24},{8,16},{16,8},{24,0},{1,25},{9,17},{17,9},{25,1},{2,26},{10... | collective-permute-start | bytes 147464 | tf_op jit(solution)/shard_map/ppermute | solution.py:29
  41.9 9.2 %collective-permute-start.33 = (bf16[2,48,512]{2,1,0:T(8,128)(2,1)S(1)}, bf16[2,48,512]{2,1,0:T(8,128)(2,1)S(1)}, u32[]{:S(2)}, u32[]{:S(2)}) collective-permute-start(bf16[2,48,512]{2,1,0:T(8,128)(2,1)S(1)} %shard_map.237.refs_8_), channel_id=1, source_target_pairs={{0,6},{1,7},{2,4},{3,5},{4,2},{5,3},{6,0},{7,1},{8,14},{9,15},{10,... | collective-permute-start | bytes 294920 | tf_op jit(solution)/shard_map/ppermute | solution.py:29
  43.4 8.5 %collective-permute-start.31 = (bf16[2,48,512]{2,1,0:T(8,128)(2,1)S(1)}, bf16[2,48,512]{2,1,0:T(8,128)(2,1)S(1)}, u32[]{:S(2)}, u32[]{:S(2)}) collective-permute-start(bf16[2,48,512]{2,1,0:T(8,128)(2,1)S(1)} %shard_map.237.refs_8_), channel_id=1, source_target_pairs={{0,4},{1,5},{2,6},{3,7},{4,0},{5,1},{6,2},{7,3},{8,12},{9,13},{10,... | collective-permute-start | bytes 294920 | tf_op jit(solution)/shard_map/ppermute | solution.py:29
  44.2 9.0 %collective-permute-start.29 = (bf16[2,48,512]{2,1,0:T(8,128)(2,1)S(1)}, bf16[2,48,512]{2,1,0:T(8,128)(2,1)S(1)}, u32[]{:S(2)}, u32[]{:S(2)}) collective-permute-start(bf16[2,48,512]{2,1,0:T(8,128)(2,1)S(1)} %shard_map.237.refs_8_), channel_id=1, source_target_pairs={{0,2},{1,3},{2,0},{3,1},{4,6},{5,7},{6,4},{7,5},{8,10},{9,11},{10,... | collective-permute-start | bytes 294920 | tf_op jit(solution)/shard_map/ppermute | solution.py:29
  45.5 7.7 %collective-permute-start.28 = (bf16[2,48,512]{2,1,0:T(8,128)(2,1)S(1)}, bf16[2,48,512]{2,1,0:T(8,128)(2,1)S(1)}, u32[]{:S(2)}, u32[]{:S(2)}) collective-permute-start(bf16[2,48,512]{2,1,0:T(8,128)(2,1)S(1)} %shard_map.237.refs_8_), channel_id=1, source_target_pairs={{0,1},{1,0},{2,3},{3,2},{4,5},{5,4},{6,7},{7,6},{8,9},{9,8},{10,11... | collective-permute-start | bytes 294920 | tf_op jit(solution)/shard_map/ppermute | solution.py:29
  45.5 4.2 %collective-permute-start.18 = (bf16[2,24,512]{2,1,0:T(8,128)(2,1)S(1)}, bf16[2,24,512]{2,1,0:T(8,128)(2,1)S(1)}, u32[]{:S(2)}, u32[]{:S(2)}) collective-permute-start(bf16[2,24,512]{2,1,0:T(8,128)(2,1)S(1)} %get-tuple-element.73), channel_id=1, source_target_pairs={{0,8},{8,0},{16,24},{24,16},{1,9},{9,1},{17,25},{25,17},{2,10},{10... | collective-permute-start | bytes 147464 | tf_op jit(solution)/shard_map/ppermute | solution.py:29
  49.7 6.5 %collective-permute-start.24 = (bf16[2,48,512]{2,1,0:T(8,128)(2,1)S(1)}, bf16[2,48,512]{2,1,0:T(8,128)(2,1)S(1)}, u32[]{:S(2)}, u32[]{:S(2)}) collective-permute-start(bf16[2,48,512]{2,1,0:T(8,128)(2,1)S(1)} %shard_map.236.refs_0_), channel_id=1, source_target_pairs={{0,6},{1,7},{2,4},{3,5},{4,2},{5,3},{6,0},{7,1},{8,14},{9,15},{10,... | collective-permute-start | bytes 294920 | tf_op jit(solution)/shard_map/ppermute | solution.py:29
  51.1 5.9 %collective-permute-start.22 = (bf16[2,48,512]{2,1,0:T(8,128)(2,1)S(1)}, bf16[2,48,512]{2,1,0:T(8,128)(2,1)S(1)}, u32[]{:S(2)}, u32[]{:S(2)}) collective-permute-start(bf16[2,48,512]{2,1,0:T(8,128)(2,1)S(1)} %shard_map.236.refs_0_), channel_id=1, source_target_pairs={{0,4},{1,5},{2,6},{3,7},{4,0},{5,1},{6,2},{7,3},{8,12},{9,13},{10,... | collective-permute-start | bytes 294920 | tf_op jit(solution)/shard_map/ppermute | solution.py:29
  51.9 5.1 %collective-permute-start.20 = (bf16[2,48,512]{2,1,0:T(8,128)(2,1)S(1)}, bf16[2,48,512]{2,1,0:T(8,128)(2,1)S(1)}, u32[]{:S(2)}, u32[]{:S(2)}) collective-permute-start(bf16[2,48,512]{2,1,0:T(8,128)(2,1)S(1)} %shard_map.236.refs_0_), channel_id=1, source_target_pairs={{0,2},{1,3},{2,0},{3,1},{4,6},{5,7},{6,4},{7,5},{8,10},{9,11},{10,... | collective-permute-start | bytes 294920 | tf_op jit(solution)/shard_map/ppermute | solution.py:29
  53.2 4.4 %collective-permute-start.19 = (bf16[2,48,512]{2,1,0:T(8,128)(2,1)S(1)}, bf16[2,48,512]{2,1,0:T(8,128)(2,1)S(1)}, u32[]{:S(2)}, u32[]{:S(2)}) collective-permute-start(bf16[2,48,512]{2,1,0:T(8,128)(2,1)S(1)} %shard_map.236.refs_0_), channel_id=1, source_target_pairs={{0,1},{1,0},{2,3},{3,2},{4,5},{5,4},{6,7},{7,6},{8,9},{9,8},{10,11... | collective-permute-start | bytes 294920 | tf_op jit(solution)/shard_map/ppermute | solution.py:29
  53.2 4.4 %collective-permute-start.34 = (bf16[2,48,512]{2,1,0:T(8,128)(2,1)S(1)}, bf16[2,48,512]{2,1,0:T(8,128)(2,1)S(1)}, u32[]{:S(2)}, u32[]{:S(2)}) collective-permute-start(bf16[2,48,512]{2,1,0:T(8,128)(2,1)S(1)} %collective-permute-done.33.refs_14_), channel_id=1, source_target_pairs={{0,1},{1,0},{2,3},{3,2},{4,5},{5,4},{6,7},{7,6},{8,9},{9,8},{10,11... | collective-permute-start | bytes 294920 | tf_op jit(solution)/shard_map/ppermute | solution.py:29
  56.2 8.6 %collective-permute-start.32 = (bf16[2,48,512]{2,1,0:T(8,128)(2,1)S(1)}, bf16[2,48,512]{2,1,0:T(8,128)(2,1)S(1)}, u32[]{:S(2)}, u32[]{:S(2)}) collective-permute-start(bf16[2,48,512]{2,1,0:T(8,128)(2,1)S(1)} %collective-permute-done.31.refs_12_), channel_id=1, source_target_pairs={{0,1},{1,0},{2,3},{3,2},{4,5},{5,4},{6,7},{7,6},{8,9},{9,8},{10,11... | collective-permute-start | bytes 294920 | tf_op jit(solution)/shard_map/ppermute | solution.py:29
  57.1 7.8 %collective-permute-start.30 = (bf16[2,48,512]{2,1,0:T(8,128)(2,1)S(1)}, bf16[2,48,512]{2,1,0:T(8,128)(2,1)S(1)}, u32[]{:S(2)}, u32[]{:S(2)}) collective-permute-start(bf16[2,48,512]{2,1,0:T(8,128)(2,1)S(1)} %collective-permute-done.29.refs_10_), channel_id=1, source_target_pairs={{0,1},{1,0},{2,3},{3,2},{4,5},{5,4},{6,7},{7,6},{8,9},{9,8},{10,11... | collective-permute-start | bytes 294920 | tf_op jit(solution)/shard_map/ppermute | solution.py:29
  57.1 7.8 %collective-permute-start.25 = (bf16[2,48,512]{2,1,0:T(8,128)(2,1)S(1)}, bf16[2,48,512]{2,1,0:T(8,128)(2,1)S(1)}, u32[]{:S(2)}, u32[]{:S(2)}) collective-permute-start(bf16[2,48,512]{2,1,0:T(8,128)(2,1)S(1)} %collective-permute-done.24.refs_6_), channel_id=1, source_target_pairs={{0,1},{1,0},{2,3},{3,2},{4,5},{5,4},{6,7},{7,6},{8,9},{9,8},{10,11... | collective-permute-start | bytes 294920 | tf_op jit(solution)/shard_map/ppermute | solution.py:29
  57.6 7.3 %collective-permute-start.23 = (bf16[2,48,512]{2,1,0:T(8,128)(2,1)S(1)}, bf16[2,48,512]{2,1,0:T(8,128)(2,1)S(1)}, u32[]{:S(2)}, u32[]{:S(2)}) collective-permute-start(bf16[2,48,512]{2,1,0:T(8,128)(2,1)S(1)} %collective-permute-done.22.refs_4_), channel_id=1, source_target_pairs={{0,1},{1,0},{2,3},{3,2},{4,5},{5,4},{6,7},{7,6},{8,9},{9,8},{10,11... | collective-permute-start | bytes 294920 | tf_op jit(solution)/shard_map/ppermute | solution.py:29
  57.7 7.2 %collective-permute-start.21 = (bf16[2,48,512]{2,1,0:T(8,128)(2,1)S(1)}, bf16[2,48,512]{2,1,0:T(8,128)(2,1)S(1)}, u32[]{:S(2)}, u32[]{:S(2)}) collective-permute-start(bf16[2,48,512]{2,1,0:T(8,128)(2,1)S(1)} %collective-permute-done.20.refs_2_), channel_id=1, source_target_pairs={{0,1},{1,0},{2,3},{3,2},{4,5},{5,4},{6,7},{7,6},{8,9},{9,8},{10,11... | collective-permute-start | bytes 294920 | tf_op jit(solution)/shard_map/ppermute | solution.py:29
  68.6 20.3 %copy-start = (f32[64,2]{0,1:T(2,128)S(1)}, f32[64,2]{0,1:T(2,128)}, u32[]{:S(2)}) copy-start(f32[64,2]{0,1:T(2,128)} %param.40) | copy-start | bytes 1540
  68.6 1.8 %collective-permute-start.35 = (bf16[4,2,48,512]{3,2,1,0:T(8,128)(2,1)S(1)}, bf16[4,2,48,512]{3,2,1,0:T(8,128)(2,1)S(1)}, u32[]{:S(2)}, u32[]{:S(2)}) collective-permute-start(bf16[4,2,48,512]{3,2,1,0:T(8,128)(2,1)S(1)} %get-tuple-element.81), channel_id=1, source_target_pairs={{0,1},{1,0},{2,3},{3,2},{4,5},{5,4},{6,7},{7,6},{8,9},{9,8},{10,11... | collective-permute-start | bytes 1179656 | tf_op jit(solution)/shard_map/ppermute | solution.py:29
  68.8 5.3 %collective-permute-start.40 = (bf16[4,2,48,512]{3,2,1,0:T(8,128)(2,1)S(1)}, bf16[4,2,48,512]{3,2,1,0:T(8,128)(2,1)S(1)}, u32[]{:S(2)}, u32[]{:S(2)}) collective-permute-start(bf16[4,2,48,512]{3,2,1,0:T(8,128)(2,1)S(1)} %get-tuple-element.89), channel_id=1, source_target_pairs={{0,1},{1,0},{2,3},{3,2},{4,5},{5,4},{6,7},{7,6},{8,9},{9,8},{10,11... | collective-permute-start | bytes 1179656 | tf_op jit(solution)/shard_map/ppermute | solution.py:29
  70.5 5.7 %collective-permute-start.36 = (bf16[2,48,512]{2,1,0:T(8,128)(2,1)S(1)}, bf16[2,48,512]{2,1,0:T(8,128)(2,1)S(1)}, u32[]{:S(2)}, u32[]{:S(2)}) collective-permute-start(bf16[2,48,512]{2,1,0:T(8,128)(2,1)S(1)} %get-tuple-element.83), channel_id=1, source_target_pairs={{0,2},{1,3},{2,0},{3,1},{4,6},{5,7},{6,4},{7,5},{8,10},{9,11},{10,... | collective-permute-start | bytes 294920 | tf_op jit(solution)/shard_map/ppermute | solution.py:29
  71.3 6.4 %collective-permute-start.37 = (bf16[2,48,512]{2,1,0:T(8,128)(2,1)S(1)}, bf16[2,48,512]{2,1,0:T(8,128)(2,1)S(1)}, u32[]{:S(2)}, u32[]{:S(2)}) collective-permute-start(bf16[2,48,512]{2,1,0:T(8,128)(2,1)S(1)} %get-tuple-element.84), channel_id=1, source_target_pairs={{0,4},{1,5},{2,6},{3,7},{4,0},{5,1},{6,2},{7,3},{8,12},{9,13},{10,... | collective-permute-start | bytes 294920 | tf_op jit(solution)/shard_map/ppermute | solution.py:29
  72.6 6.6 %collective-permute-start.38 = (bf16[2,48,512]{2,1,0:T(8,128)(2,1)S(1)}, bf16[2,48,512]{2,1,0:T(8,128)(2,1)S(1)}, u32[]{:S(2)}, u32[]{:S(2)}) collective-permute-start(bf16[2,48,512]{2,1,0:T(8,128)(2,1)S(1)} %get-tuple-element.85), channel_id=1, source_target_pairs={{0,6},{1,7},{2,4},{3,5},{4,2},{5,3},{6,0},{7,1},{8,14},{9,15},{10,... | collective-permute-start | bytes 294920 | tf_op jit(solution)/shard_map/ppermute | solution.py:29
  74.2 6.4 %collective-permute-start.41 = (bf16[2,48,512]{2,1,0:T(8,128)(2,1)S(1)}, bf16[2,48,512]{2,1,0:T(8,128)(2,1)S(1)}, u32[]{:S(2)}, u32[]{:S(2)}) collective-permute-start(bf16[2,48,512]{2,1,0:T(8,128)(2,1)S(1)} %get-tuple-element.91), channel_id=1, source_target_pairs={{0,2},{1,3},{2,0},{3,1},{4,6},{5,7},{6,4},{7,5},{8,10},{9,11},{10,... | collective-permute-start | bytes 294920 | tf_op jit(solution)/shard_map/ppermute | solution.py:29
  75.0 7.3 %collective-permute-start.42 = (bf16[2,48,512]{2,1,0:T(8,128)(2,1)S(1)}, bf16[2,48,512]{2,1,0:T(8,128)(2,1)S(1)}, u32[]{:S(2)}, u32[]{:S(2)}) collective-permute-start(bf16[2,48,512]{2,1,0:T(8,128)(2,1)S(1)} %get-tuple-element.92), channel_id=1, source_target_pairs={{0,4},{1,5},{2,6},{3,7},{4,0},{5,1},{6,2},{7,3},{8,12},{9,13},{10,... | collective-permute-start | bytes 294920 | tf_op jit(solution)/shard_map/ppermute | solution.py:29
  76.2 6.1 %collective-permute-start.43 = (bf16[2,48,512]{2,1,0:T(8,128)(2,1)S(1)}, bf16[2,48,512]{2,1,0:T(8,128)(2,1)S(1)}, u32[]{:S(2)}, u32[]{:S(2)}) collective-permute-start(bf16[2,48,512]{2,1,0:T(8,128)(2,1)S(1)} %get-tuple-element.93), channel_id=1, source_target_pairs={{0,6},{1,7},{2,4},{3,5},{4,2},{5,3},{6,0},{7,1},{8,14},{9,15},{10,... | collective-permute-start | bytes 294920 | tf_op jit(solution)/shard_map/ppermute | solution.py:29
  79.2 8.3 %collective-permute-start.39 = (bf16[2,24,512]{2,1,0:T(8,128)(2,1)S(1)}, bf16[2,24,512]{2,1,0:T(8,128)(2,1)S(1)}, u32[]{:S(2)}, u32[]{:S(2)}) collective-permute-start(bf16[2,24,512]{2,1,0:T(8,128)(2,1)S(1)} %get-tuple-element.87), channel_id=1, source_target_pairs={{0,8},{8,0},{16,24},{24,16},{1,9},{9,1},{17,25},{25,17},{2,10},{10... | collective-permute-start | bytes 147464 | tf_op jit(solution)/shard_map/ppermute | solution.py:29
  82.3 5.6 %collective-permute-start.44 = (bf16[2,24,512]{2,1,0:T(8,128)(2,1)S(1)}, bf16[2,24,512]{2,1,0:T(8,128)(2,1)S(1)}, u32[]{:S(2)}, u32[]{:S(2)}) collective-permute-start(bf16[2,24,512]{2,1,0:T(8,128)(2,1)S(1)} %get-tuple-element.94), channel_id=1, source_target_pairs={{0,16},{8,24},{16,0},{24,8},{1,17},{9,25},{17,1},{25,9},{2,18},{10... | collective-permute-start | bytes 147464 | tf_op jit(solution)/shard_map/ppermute | solution.py:29
  83.1 5.9 %collective-permute-start.45 = (bf16[2,24,512]{2,1,0:T(8,128)(2,1)S(1)}, bf16[2,24,512]{2,1,0:T(8,128)(2,1)S(1)}, u32[]{:S(2)}, u32[]{:S(2)}) collective-permute-start(bf16[2,24,512]{2,1,0:T(8,128)(2,1)S(1)} %get-tuple-element.95), channel_id=1, source_target_pairs={{0,24},{8,16},{16,8},{24,0},{1,25},{9,17},{17,9},{25,1},{2,26},{10... | collective-permute-start | bytes 147464 | tf_op jit(solution)/shard_map/ppermute | solution.py:29

commit v3 on v2

--- a/solution.py
+++ b/solution.py
@@ -200,24 +200,36 @@
     return copies
 
 
+def mixer_sums(odd, pieces, gain, weight, start):
+    total, turned, square = start
+    width = pieces[0].shape[1]
+    for at, piece in enumerate(pieces):
+        k = 2 * at + odd
+        x = piece[...].astype(f32)
+        square = square + fold(x * x)
+        x = (x * gain[:, place(k, width)]).astype(bf16)
+        if at % 2:
+            turned = turned + dot(weight[k], x, NT)
+        else:
+            total = total + dot(x, weight[k], NT)
+    return total, turned, square
+
+
+def first_body(n, *refs):
+    pieces = refs[: n // 2]
+    gain, weight = refs[n // 2 : n // 2 + 2]
+    for out, value in zip(refs[n // 2 + 2 :], mixer_sums(0, pieces, gain, weight, (0.0, 0.0, 0.0))):
+        out[...] = value
+
+
 def mixer_body(n, *refs):
-    pieces = refs[:n]
-    gain, weight, base, mix, skip = refs[n : n + 5]
-    driven_ref, act_ref = refs[n + 5 :]
+    pieces = refs[: n // 2]
+    gain, weight, base, mix, skip, total, turned, square = refs[n // 2 : n // 2 + 8]
+    driven_ref, act_ref = refs[n // 2 + 8 :]
+    start = (total[...], turned[...], square[...])
+    total, turned, square = mixer_sums(1, pieces, gain, weight, start)
     width = pieces[0].shape[1]
-    square = 0.0
-    for k in range(n):
-        x = pieces[k][...].astype(f32)
-        square = square + fold(x * x)
     scale = lax.rsqrt(jnp.sum(square, axis=1, keepdims=True) / (n * width) + norm_eps)
-    total, turned = 0.0, 0.0
-    for k in range(n):
-        part = gain[:, place(k, width)]
-        normed = (pieces[k][...].astype(f32) * part).astype(bf16)
-        if k % 2:
-            turned = turned + dot(weight[k], normed, NT)
-        else:
-            total = total + dot(normed, weight[k], NT)
     driven = ((total + turned.T) * scale).astype(bf16)
     driven_ref[...] = driven
     for b in range(driven.shape[1] // LANES):
@@ -275,18 +287,29 @@
     return slice(i * height, (i + 1) * height)
 
 
+def glu_sums(odd, pieces, glu, gate, turned):
+    width = pieces[0].shape[1]
+    for at, piece in enumerate(pieces):
+        block = glu[:, place(2 * at + odd, width)]
+        if at % 2:
+            turned = turned + dot(block, piece[...], NT)
+        else:
+            gate = gate + dot(piece[...], block, NT)
+    return gate, turned
+
+
+def gate_body(n, *refs):
+    pieces = refs[: n // 2]
+    glu, bias, gate_ref, turned_ref = refs[n // 2 :]
+    gate_ref[...], turned_ref[...] = glu_sums(0, pieces, glu, bias[...], 0.0)
+
+
 def glu_body(n, *refs):
-    pieces = refs[:n]
-    glu, bias, out_w = refs[n : n + 3]
-    glued_ref, partner = refs[n + 3 :]
-    gate, turned = bias[...], 0.0
-    for k in range(n):
-        block = glu[:, place(k, pieces[k].shape[1])]
-        if k % 2:
-            turned = turned + dot(block, pieces[k][...], NT)
-        else:
-            gate = gate + dot(pieces[k][...], block, NT)
-    glued = (pieces[0][...].astype(f32) * jax.nn.sigmoid(gate + turned.T)).astype(bf16)
+    pieces = refs[: n // 2]
+    own, glu, gate, turned, out_w = refs[n // 2 : n // 2 + 5]
+    glued_ref, partner = refs[n // 2 + 5 :]
+    gate, turned = glu_sums(1, pieces, glu, gate[...], turned[...])
+    glued = (own[...].astype(f32) * jax.nn.sigmoid(gate + turned.T)).astype(bf16)
     glued_ref[...] = glued
     for k in range(1, n, 2):
         partner[k // 2] = dot(glued, out_w[:, place(k, partner.shape[2])], NN).astype(bf16)
@@ -323,26 +346,41 @@
         outs[j][...] = picked.reshape(experts, cap, wide)
 
 
+def expert_sums(odd, near, far, gain, gate_w, up_low, up_high, i, start):
+    g, u, square = start
+    experts, _, width = near[0].shape
+    height = gate_w.shape[0] // experts
+    held = up_low.shape[0] // height
+    up_w, row = (up_low, i) if i < held else (up_high, i - held)
+    for at in range(len(near)):
+        k = 2 * at + odd
+        x = jnp.concatenate([near[at][i], far[at][i]], axis=0).astype(f32)
+        square = square + fold(x * x)
+        x = (x * gain[:, place(k, width)]).astype(bf16)
+        g = g + dot(x, gate_w[rows_of(gate_w, i, experts), place(k, width)], NT)
+        u = u + dot(up_w[row * height : (row + 1) * height, place(k, width)], x, NT)
+    return g, u, square
+
+
+def even_body(n, *refs):
+    near, far = refs[: n // 2], refs[n // 2 : n]
+    gain, gate_w, up_low, up_high, g_ref, u_ref, square_ref = refs[n:]
+    for i in range(near[0].shape[0]):
+        g_ref[i], u_ref[i], square_ref[i] = expert_sums(
+            0, near, far, gain, gate_w, up_low, up_high, i, (0.0, 0.0, 0.0)
+        )
+
+
 def up_body(n, *refs):
-    near, far = refs[:n], refs[n : 2 * n]
-    gain, gate_w, up_low, up_high, down_w = refs[2 * n : 2 * n + 5]
-    later, partner = refs[2 * n + 5 :]
+    near, far = refs[: n // 2], refs[n // 2 : n]
+    gain, gate_w, up_low, up_high, down_w, g_ref, u_ref, square_ref = refs[n : n + 8]
+    later, partner = refs[n + 8 :]
     experts, count, width = near[0].shape
-    g, u, square = [0.0] * experts, [0.0] * experts, [0.0] * experts
-    for k in range(n):
-        part = gain[:, place(k, width)]
-        for i in range(experts):
-            x = jnp.concatenate([near[k][i], far[k][i]], axis=0).astype(f32)
-            square[i] = square[i] + fold(x * x)
-            x = (x * part).astype(bf16)
-            g[i] = g[i] + dot(x, gate_w[rows_of(gate_w, i, experts), place(k, width)], NT)
-            height = gate_w.shape[0] // experts
-            held = up_low.shape[0] // height
-            up_w, at = (up_low, i) if i < held else (up_high, i - held)
-            u[i] = u[i] + dot(up_w[at * height : (at + 1) * height, place(k, width)], x, NT)
     for i in range(experts):
-        scale = lax.rsqrt(jnp.sum(square[i], axis=1, keepdims=True) / (n * width) + norm_eps)
-        hidden = (jax.nn.silu(g[i] * scale) * (u[i].T * scale)).astype(bf16)
+        start = (g_ref[i], u_ref[i], square_ref[i])
+        g, u, square = expert_sums(1, near, far, gain, gate_w, up_low, up_high, i, start)
+        scale = lax.rsqrt(jnp.sum(square, axis=1, keepdims=True) / (n * width) + norm_eps)
+        hidden = (jax.nn.silu(g * scale) * (u.T * scale)).astype(bf16)
         later[i] = hidden
         for k in range(1, n, 2):
             partner[k // 2, i] = dot(hidden[count:], down_w[rows_of(down_w, i, experts), place(k, width)], NN).astype(bf16)
@@ -467,22 +505,34 @@
     )(*[stay(x) for x in [in_weight] + far])
     pieces[0] = own
 
+    partial = call(
+        functools.partial(first_body, n),
+        [jax.ShapeDtypeStruct(x, f32) for x in ((count, channels), (channels, count), (count, LANES))],
+        [WHOLE] * (n // 2 + 2),
+        limit=8 * 2**20,
+    )(*pieces[::2], gain1, in_w)
     driven, activated = call(
         functools.partial(mixer_body, n),
         [jax.ShapeDtypeStruct((count, channels), bf16)] * 2,
-        [WHOLE] * (n + 5),
+        [WHOLE] * (n // 2 + 8),
         limit=12 * 2**20,
-    )(*pieces, gain1, in_w, base, mix, skip)
+    )(*pieces[1::2], gain1, in_w, base, mix, skip, *partial)
 
     acts = gather_swaps(activated, n)
     glu_w, out_w = fetch(glu_weight, out_weight)
     block = jax.ShapeDtypeStruct((n // 2, count, wide), bf16)
+    partial = call(
+        functools.partial(gate_body, n),
+        [jax.ShapeDtypeStruct(x, f32) for x in ((count, channels), (channels, count))],
+        [WHOLE] * (n // 2 + 2),
+        limit=8 * 2**20,
+    )(*acts[::2], glu_w, bias)
     glued, partner = call(
         functools.partial(glu_body, n),
         [jax.ShapeDtypeStruct((count, channels), bf16), block],
-        [WHOLE] * (n + 3),
+        [WHOLE] * (n // 2 + 5),
         limit=12 * 2**20,
-    )(*acts, glu_w, bias, out_w)
+    )(*acts[1::2], acts[0], glu_w, *partial, out_w)
     sums = call(functools.partial(out_body, n), block, [WHOLE] * 2, limit=8 * 2**20)(glued, out_w)
 
     terms = reduce_swaps(sums, partner, n)
@@ -512,12 +562,21 @@
         )(*group)
         fragments += gather_swaps(merged, n)
     part = jax.ShapeDtypeStruct((n // 2, exp_dev, half * cap, wide), bf16)
+    near, far = fragments[:n], fragments[n:]
+    rows = 2 * half * cap
+    weights = (gain2, gate_w, up_low, up_high)
+    partial = call(
+        functools.partial(even_body, n),
+        [jax.ShapeDtypeStruct((exp_dev, *x), f32) for x in ((rows, hidden), (hidden, rows), (rows, LANES))],
+        [WHOLE] * (n + 4),
+        limit=8 * 2**20,
+    )(*near[::2], *far[::2], *weights)
     later, far_partner = call(
         functools.partial(up_body, n),
-        [jax.ShapeDtypeStruct((exp_dev, 2 * half * cap, hidden), bf16), part],
-        [WHOLE] * (2 * n + 5),
+        [jax.ShapeDtypeStruct((exp_dev, rows, hidden), bf16), part],
+        [WHOLE] * (n + 8),
         limit=16 * 2**20,
-    )(*fragments, gain2, gate_w, up_low, up_high, down_w)
+    )(*near[1::2], *far[1::2], *weights, down_w, *partial)
     far_own, *near_outs = call(
         functools.partial(down_body, n), [part] * 3, [WHOLE] * 2, limit=8 * 2**20
     )(later, down_w)

time: 90 us -> 84.2 us (0.936)
  waiting for transfers between devices: 31 us -> 24.1 us
  Pallas kernels: 21.6 us -> 22.6 us
    ppermute x46, waiting for transfers between devices: 31 us -> 24.1 us  [swap(): lax.ppermute(x, axis, [(i, i ^ k) for i in range(lax.axis_size(axis))])]
    pallas_call x1 -> x4, Pallas kernels: 2.54 us -> 3.95 us  [the longest x1 1.99 us: local_swaps(): call(functools.partial(up_body, n), [jax.ShapeDtypeStruct((exp_dev, rows,...]
  transfers between devices with their start and end apart: 46 -> 46, of which waited for: 21 -> 21; matrix products, arithmetic and copies ran while one was open for 0% -> 0% of each run, Pallas kernels for 17% -> 22%
where the time goes in v3:
time: 84.2 us; the launch traced here: 84 us
  starting transfers between devices  36.3 us (43%)
  waiting for transfers between devices  24.1 us (29%)
  Pallas kernels  22.6 us (27%)
  between operations  0.91 us (1%)
    ppermute x46, starting transfers between devices, swap(): lax.ppermute(x, axis, [(i, i ^ k) for i in range(lax.axis_size(axis))])  36.3 us
    ppermute x46, waiting for transfers between devices, swap(): lax.ppermute(x, axis, [(i, i ^ k) for i in range(lax.axis_size(axis))])  24.1 us
    pallas_call x4, Pallas kernels, fetch(): call(functools.partial(fetch_body, [x[1:] for x in sources]), [pltpu.VMEM...  8.7 us
    pallas_call x1, Pallas kernels, local_swaps(): call(functools.partial(prep_body, n, cap), [jax.ShapeDtypeStruct((count,...  3.72 us
    pallas_call x1, Pallas kernels, local_swaps(): call(state_body, [jax.ShapeDtypeStruct((count, groups, entries), f32)] *...  2.13 us
    pallas_call x1, Pallas kernels, local_swaps(): call(functools.partial(up_body, n), [jax.ShapeDtypeStruct((exp_dev, rows,...  1.99 us
  transfers between devices with their start and end apart: 46, of which 21 were waited for; matrix products, arithmetic and copies ran while one was open for 0% of the time, Pallas kernels for 22%

profile of v3, /device:TPU:0, one launch (start us, length us, event | category | flops | bytes accessed | tf_op | source)
XLA Modules:
  0.0 84.0 jit_solution(16115125803652667086)
XLA Ops:
  0.6 3.0 %collective-permute-start.1 = (bf16[64,512]{1,0:T(8,128)(2,1)}, bf16[64,512]{1,0:T(8,128)(2,1)S(1)}, u32[]{:S(2)}, u32[]{:S(2)}) collective-permute-start(bf16[64,512]{1,0:T(8,128)(2,1)} %refs_15_.1), channel_id=1, source_target_pairs={{0,2},{1,3},{2,0},{3,1},{4,6},{5,7},{6,4},{7,5},{8,10},{9,11},{10,... | collective-permute-start | bytes 196616 | tf_op jit(solution)/shard_map/ppermute | solution.py:29
  3.7 1.5 %collective-permute-start.3 = (bf16[64,512]{1,0:T(8,128)(2,1)}, bf16[64,512]{1,0:T(8,128)(2,1)S(1)}, u32[]{:S(2)}, u32[]{:S(2)}) collective-permute-start(bf16[64,512]{1,0:T(8,128)(2,1)} %refs_15_.1), channel_id=1, source_target_pairs={{0,4},{1,5},{2,6},{3,7},{4,0},{5,1},{6,2},{7,3},{8,12},{9,13},{10,... | collective-permute-start | bytes 196616 | tf_op jit(solution)/shard_map/ppermute | solution.py:29
  5.2 1.1 %collective-permute-done.1.refs_1_ = bf16[64,512]{1,0:T(8,128)(2,1)S(1)} collective-permute-done((bf16[64,512]{1,0:T(8,128)(2,1)}, bf16[64,512]{1,0:T(8,128)(2,1)S(1)}, u32[]{:S(2)}, u32[]{:S(2)}) %collective-permute-start.1) | collective-permute-done | bytes 65568 | tf_op jit(solution)/shard_map/ppermute | solution.py:29
  6.3 1.8 %collective-permute-done.3.refs_2_ = bf16[64,512]{1,0:T(8,128)(2,1)S(1)} collective-permute-done((bf16[64,512]{1,0:T(8,128)(2,1)}, bf16[64,512]{1,0:T(8,128)(2,1)S(1)}, u32[]{:S(2)}, u32[]{:S(2)}) %collective-permute-start.3) | collective-permute-done | bytes 65568 | tf_op jit(solution)/shard_map/ppermute | solution.py:29
  8.1 2.4 %collective-permute-done.5.refs_3_ = bf16[64,512]{1,0:T(8,128)(2,1)S(1)} collective-permute-done((bf16[64,512]{1,0:T(8,128)(2,1)}, bf16[64,512]{1,0:T(8,128)(2,1)S(1)}, u32[]{:S(2)}, u32[]{:S(2)}) %collective-permute-start.5) | collective-permute-done | bytes 65568 | tf_op jit(solution)/shard_map/ppermute | solution.py:29
  10.6 3.7 %shard_map.229 = (f32[64,1024]{1,0:T(8,128)S(1)}, f32[64,1024]{1,0:T(8,128)S(1)}, bf16[256,512]{1,0:T(8,128)(2,1)S(1)}, bf16[256,512]{1,0:T(8,128)(2,1)S(1)}, f3...) custom-call(bf16[256,4096]{1,0:T(8,128)(2,1)} %refs_0_.2, ...), custom_call_target="tpu_custom_call" | custom-call | flops 10000000 | bytes 1000000 | tf_op jit(solution)/shard_map/pallas_call | solution.py:487
  14.3 0.4 shard_map.230
  14.8 0.6 shard_map.231
  15.4 0.6 collective-permute-start.10
  16.0 1.5 %collective-permute-start.12 = (bf16[64,256]{1,0:T(8,128)(2,1)S(1)}, bf16[64,256]{1,0:T(8,128)(2,1)S(1)}, u32[]{:S(2)}, u32[]{:S(2)}) collective-permute-start(bf16[64,256]{1,0:T(8,128)(2,1)S(1)} %get-tuple-element.70.refs_0_.refs_4_), channel_id=1, source_target_pairs={{0,6},{1,7},{2,4},{3,5},{4,2},{5,3},{6,0},{7,1},{8,14},{9,15},{10,... | collective-permute-start | bytes 98312 | tf_op jit(solution)/shard_map/ppermute | solution.py:29
  17.5 1.5 %collective-permute-start.8 = (bf16[64,256]{1,0:T(8,128)(2,1)S(1)}, bf16[64,256]{1,0:T(8,128)(2,1)S(1)}, u32[]{:S(2)}, u32[]{:S(2)}) collective-permute-start(bf16[64,256]{1,0:T(8,128)(2,1)S(1)} %get-tuple-element.70.refs_0_.refs_4_), channel_id=1, source_target_pairs={{0,2},{1,3},{2,0},{3,1},{4,6},{5,7},{6,4},{7,5},{8,10},{9,11},{10,... | collective-permute-start | bytes 98312 | tf_op jit(solution)/shard_map/ppermute | solution.py:29
  18.9 0.4 collective-permute-done.10.refs_2_
  19.5 1.3 %collective-permute-done.12.refs_3_ = bf16[64,256]{1,0:T(8,128)(2,1)S(1)} collective-permute-done((bf16[64,256]{1,0:T(8,128)(2,1)S(1)}, bf16[64,256]{1,0:T(8,128)(2,1)S(1)}, u32[]{:S(2)}, u32[]{:S(2)}) %collective-permute-start.12) | collective-permute-done | bytes 32800 | tf_op jit(solution)/shard_map/ppermute | solution.py:29
  20.8 0.6 collective-permute-done.8.refs_1_
  21.4 2.0 %shard_map.232 = (bf16[256,2048]{1,0:T(8,128)(2,1)S(1)}, bf16[256,4096]{1,0:T(8,128)(2,1)S(1)}) custom-call(bf16[256,2048]{1,0:T(8,128)(2,1)} %refs_0_.3, bf16[256,4096]{1,0:T(8,128)(2,1)} %refs_1_.3), custom_call_target="tpu_custom_call" | custom-call | flops 10000000 | bytes 1000000 | tf_op jit(solution)/shard_map/pallas_call | solution.py:276
  23.7 0.6 shard_map.234
  24.3 0.6 collective-permute-start.14
  24.9 0.3 shard_map.235.own
  25.2 0.9 %collective-permute-done.14.other = bf16[4,64,512]{2,1,0:T(8,128)(2,1)S(1)} collective-permute-done((bf16[4,64,512]{2,1,0:T(8,128)(2,1)S(1)}, bf16[4,64,512]{2,1,0:T(8,128)(2,1)S(1)}, u32[]{:S(2)}, u32[]{:S(2)}) %collective-permute-start.14) | collective-permute-done | bytes 262176 | tf_op jit(solution)/shard_map/ppermute | solution.py:29
  26.1 1.6 %collective-permute-start.15 = (bf16[64,512]{1,0:T(8,128)(2,1)S(1)}, bf16[64,512]{1,0:T(8,128)(2,1)S(1)}, u32[]{:S(2)}, u32[]{:S(2)}) collective-permute-start(bf16[64,512]{1,0:T(8,128)(2,1)S(1)} %get-tuple-element.79), channel_id=1, source_target_pairs={{0,2},{1,3},{2,0},{3,1},{4,6},{5,7},{6,4},{7,5},{8,10},{9,11},{10,... | collective-permute-start | bytes 196616 | tf_op jit(solution)/shard_map/ppermute | solution.py:29
  27.7 0.5 collective-permute-start.16
  28.2 1.5 %collective-permute-start.17 = (bf16[64,512]{1,0:T(8,128)(2,1)S(1)}, bf16[64,512]{1,0:T(8,128)(2,1)S(1)}, u32[]{:S(2)}, u32[]{:S(2)}) collective-permute-start(bf16[64,512]{1,0:T(8,128)(2,1)S(1)} %get-tuple-element.81), channel_id=1, source_target_pairs={{0,6},{1,7},{2,4},{3,5},{4,2},{5,3},{6,0},{7,1},{8,14},{9,15},{10,... | collective-permute-start | bytes 196616 | tf_op jit(solution)/shard_map/ppermute | solution.py:29
  29.7 0.9 %collective-permute-done.15.refs_2_ = bf16[64,512]{1,0:T(8,128)(2,1)S(1)} collective-permute-done((bf16[64,512]{1,0:T(8,128)(2,1)S(1)}, bf16[64,512]{1,0:T(8,128)(2,1)S(1)}, u32[]{:S(2)}, u32[]{:S(2)}) %collective-permute-start.15) | collective-permute-done | bytes 65568 | tf_op jit(solution)/shard_map/ppermute | solution.py:29
  30.5 2.1 %collective-permute-done.16.refs_3_ = bf16[64,512]{1,0:T(8,128)(2,1)S(1)} collective-permute-done((bf16[64,512]{1,0:T(8,128)(2,1)S(1)}, bf16[64,512]{1,0:T(8,128)(2,1)S(1)}, u32[]{:S(2)}, u32[]{:S(2)}) %collective-permute-start.16) | collective-permute-done | bytes 65568 | tf_op jit(solution)/shard_map/ppermute | solution.py:29
  32.6 0.7 collective-permute-done.17.refs_4_
  33.6 2.7 %collective-permute-start.26 = (bf16[2,24,512]{2,1,0:T(8,128)(2,1)S(1)}, bf16[2,24,512]{2,1,0:T(8,128)(2,1)S(1)}, u32[]{:S(2)}, u32[]{:S(2)}) collective-permute-start(bf16[2,24,512]{2,1,0:T(8,128)(2,1)S(1)} %get-tuple-element.87), channel_id=1, source_target_pairs={{0,16},{8,24},{16,0},{24,8},{1,17},{9,25},{17,1},{25,9},{2,18},{10... | collective-permute-start | bytes 147464 | tf_op jit(solution)/shard_map/ppermute | solution.py:29
  36.2 1.3 %collective-permute-start.27 = (bf16[2,24,512]{2,1,0:T(8,128)(2,1)S(1)}, bf16[2,24,512]{2,1,0:T(8,128)(2,1)S(1)}, u32[]{:S(2)}, u32[]{:S(2)}) collective-permute-start(bf16[2,24,512]{2,1,0:T(8,128)(2,1)S(1)} %get-tuple-element.88), channel_id=1, source_target_pairs={{0,24},{8,16},{16,8},{24,0},{1,25},{9,17},{17,9},{25,1},{2,26},{10... | collective-permute-start | bytes 147464 | tf_op jit(solution)/shard_map/ppermute | solution.py:29
  37.8 1.1 %collective-permute-done.26.refs_0_ = bf16[2,24,512]{2,1,0:T(8,128)(2,1)S(1)} collective-permute-done((bf16[2,24,512]{2,1,0:T(8,128)(2,1)S(1)}, bf16[2,24,512]{2,1,0:T(8,128)(2,1)S(1)}, u32[]{:S(2)}, u32[]{:S(2)}) %collective-permute-start.26) | collective-permute-done | bytes 49184 | tf_op jit(solution)/shard_map/ppermute | solution.py:29
  38.9 3.3 %collective-permute-done.27.refs_1_ = bf16[2,24,512]{2,1,0:T(8,128)(2,1)S(1)} collective-permute-done((bf16[2,24,512]{2,1,0:T(8,128)(2,1)S(1)}, bf16[2,24,512]{2,1,0:T(8,128)(2,1)S(1)}, u32[]{:S(2)}, u32[]{:S(2)}) %collective-permute-start.27) | collective-permute-done | bytes 49184 | tf_op jit(solution)/shard_map/ppermute | solution.py:29
  42.2 1.4 %collective-permute-start.29 = (bf16[2,48,512]{2,1,0:T(8,128)(2,1)S(1)}, bf16[2,48,512]{2,1,0:T(8,128)(2,1)S(1)}, u32[]{:S(2)}, u32[]{:S(2)}) collective-permute-start(bf16[2,48,512]{2,1,0:T(8,128)(2,1)S(1)} %shard_map.239.refs_4_), channel_id=1, source_target_pairs={{0,2},{1,3},{2,0},{3,1},{4,6},{5,7},{6,4},{7,5},{8,10},{9,11},{10,... | collective-permute-start | bytes 294920 | tf_op jit(solution)/shard_map/ppermute | solution.py:29
  43.6 0.7 collective-permute-start.31
  44.3 1.4 %collective-permute-start.33 = (bf16[2,48,512]{2,1,0:T(8,128)(2,1)S(1)}, bf16[2,48,512]{2,1,0:T(8,128)(2,1)S(1)}, u32[]{:S(2)}, u32[]{:S(2)}) collective-permute-start(bf16[2,48,512]{2,1,0:T(8,128)(2,1)S(1)} %shard_map.239.refs_4_), channel_id=1, source_target_pairs={{0,6},{1,7},{2,4},{3,5},{4,2},{5,3},{6,0},{7,1},{8,14},{9,15},{10,... | collective-permute-start | bytes 294920 | tf_op jit(solution)/shard_map/ppermute | solution.py:29
  45.8 1.4 %collective-permute-start.20 = (bf16[2,48,512]{2,1,0:T(8,128)(2,1)S(1)}, bf16[2,48,512]{2,1,0:T(8,128)(2,1)S(1)}, u32[]{:S(2)}, u32[]{:S(2)}) collective-permute-start(bf16[2,48,512]{2,1,0:T(8,128)(2,1)S(1)} %shard_map.238.refs_0_), channel_id=1, source_target_pairs={{0,2},{1,3},{2,0},{3,1},{4,6},{5,7},{6,4},{7,5},{8,10},{9,11},{10,... | collective-permute-start | bytes 294920 | tf_op jit(solution)/shard_map/ppermute | solution.py:29
  47.2 0.7 collective-permute-start.22
  47.9 1.5 %collective-permute-start.24 = (bf16[2,48,512]{2,1,0:T(8,128)(2,1)S(1)}, bf16[2,48,512]{2,1,0:T(8,128)(2,1)S(1)}, u32[]{:S(2)}, u32[]{:S(2)}) collective-permute-start(bf16[2,48,512]{2,1,0:T(8,128)(2,1)S(1)} %shard_map.238.refs_0_), channel_id=1, source_target_pairs={{0,6},{1,7},{2,4},{3,5},{4,2},{5,3},{6,0},{7,1},{8,14},{9,15},{10,... | collective-permute-start | bytes 294920 | tf_op jit(solution)/shard_map/ppermute | solution.py:29
  49.4 1.0 %collective-permute-done.33.refs_7_ = bf16[2,48,512]{2,1,0:T(8,128)(2,1)S(1)} collective-permute-done((bf16[2,48,512]{2,1,0:T(8,128)(2,1)S(1)}, bf16[2,48,512]{2,1,0:T(8,128)(2,1)S(1)}, u32[]{:S(2)}, u32[]{:S(2)}) %collective-permute-start.33) | collective-permute-done | bytes 98336 | tf_op jit(solution)/shard_map/ppermute | solution.py:29
  50.4 0.3 collective-permute-done.20.refs_1_
  50.9 0.8 collective-permute-done.22.refs_2_
  51.8 1.7 %collective-permute-done.24.refs_3_ = bf16[2,48,512]{2,1,0:T(8,128)(2,1)S(1)} collective-permute-done((bf16[2,48,512]{2,1,0:T(8,128)(2,1)S(1)}, bf16[2,48,512]{2,1,0:T(8,128)(2,1)S(1)}, u32[]{:S(2)}, u32[]{:S(2)}) %collective-permute-start.24) | collective-permute-done | bytes 98336 | tf_op jit(solution)/shard_map/ppermute | solution.py:29
  53.5 0.5 collective-permute-start.21
  54.0 0.4 collective-permute-start.25
  54.5 1.6 %shard_map.241.refs_11_ = bf16[256,4096]{1,0:T(8,128)(2,1)S(1)} custom-call(bf16[512,4096]{1,0:T(8,128)(2,1)} %bitcast.13), custom_call_target="tpu_custom_call" | custom-call | flops 10000000 | bytes 1000000 | tf_op jit(solution)/shard_map/pallas_call | solution.py:276
  56.1 2.9 %shard_map.240 = (bf16[512,4096]{1,0:T(8,128)(2,1)S(1)}, bf16[256,4096]{1,0:T(8,128)(2,1)S(1)}) custom-call(bf16[512,4096]{1,0:T(8,128)(2,1)} %bitcast.15, bf16[512,4096]{1,0:T(8,128)(2,1)} %bitcast.14), custom_call_target="tpu_custom_call" | custom-call | flops 10000000 | bytes 1000000 | tf_op jit(solution)/shard_map/pallas_call | solution.py:276
  59.0 2.2 %shard_map.242.refs_12_.down_w = bf16[512,4096]{1,0:T(8,128)(2,1)S(1)} custom-call(bf16[512,4096]{1,0:T(8,128)(2,1)} %bitcast.16), custom_call_target="tpu_custom_call" | custom-call | flops 10000000 | bytes 1000000 | tf_op jit(solution)/shard_map/pallas_call | solution.py:276
  61.2 1.3 %shard_map.243 = (f32[2,96,256]{2,1,0:T(8,128)S(1)}, f32[2,256,96]{2,1,0:T(8,128)S(1)}, f32[2,96,128]{2,1,0:T(8,128)S(1)}) custom-call(bf16[2,48,512]{2,1,0:T(8,128)(2,1)S(1)} %shard_map.238.refs_0_, bf16[2,48,512]{2,1,0:T(8,128)(2,1)S(1)} %collective-permute-done.20.refs_1_, bf16[2,48,512]{2,1,0:T(8,128)(2,1)S(1)} %collective-permute-done.22.refs_2_, ...), custom_call_target="tpu_custom_call" | custom-call | flops 10000000 | bytes 1000000 | tf_op jit(solution)/shard_map/pallas_call | solution.py:568
  62.5 2.0 %shard_map.244 = (bf16[2,96,256]{2,1,0:T(8,128)(2,1)S(1)}, bf16[4,2,48,512]{3,2,1,0:T(8,128)(2,1)S(1)}) custom-call(bf16[2,48,512]{2,1,0:T(8,128)(2,1)S(1)} %collective-permute-done.19.refs_0_, bf16[2,48,512]{2,1,0:T(8,128)(2,1)S(1)} %collective-permute-done.21.refs_1_, bf16[2,48,512]{2,1,0:T(8,128)(2,1)S(1)} %collective-permute-done.23.refs_2_, ...), custom_call_target="tpu_custom_call" | custom-call | flops 10000000 | bytes 1000000 | tf_op jit(solution)/shard_map/pallas_call | solution.py:574
  64.6 1.2 %shard_map.245 = (bf16[4,2,48,512]{3,2,1,0:T(8,128)(2,1)S(1)}, bf16[4,2,48,512]{3,2,1,0:T(8,128)(2,1)S(1)}, bf16[4,2,48,512]{3,2,1,0:T(8,128)(2,1)S(1)}) custom-call(bf16[2,96,256]{2,1,0:T(8,128)(2,1)S(1)} %get-tuple-element.95.hidden, bf16[512,4096]{1,0:T(8,128)(2,1)S(1)} %shard_map.242.refs_12_.down_w), custom_call_target="tpu_custom_call" | custom-call | flops 10000000 | bytes 1000000 | tf_op jit(solution)/shard_map/pallas_call | solution.py:580
  65.8 0.5 collective-permute-start.35
  66.5 1.5 %collective-permute-start.41 = (bf16[2,48,512]{2,1,0:T(8,128)(2,1)S(1)}, bf16[2,48,512]{2,1,0:T(8,128)(2,1)S(1)}, u32[]{:S(2)}, u32[]{:S(2)}) collective-permute-start(bf16[2,48,512]{2,1,0:T(8,128)(2,1)S(1)} %get-tuple-element.107), channel_id=1, source_target_pairs={{0,2},{1,3},{2,0},{3,1},{4,6},{5,7},{6,4},{7,5},{8,10},{9,11},{10,... | collective-permute-start | bytes 294920 | tf_op jit(solution)/shard_map/ppermute | solution.py:29
  68.0 0.6 collective-permute-start.42
  68.6 1.4 %collective-permute-start.43 = (bf16[2,48,512]{2,1,0:T(8,128)(2,1)S(1)}, bf16[2,48,512]{2,1,0:T(8,128)(2,1)S(1)}, u32[]{:S(2)}, u32[]{:S(2)}) collective-permute-start(bf16[2,48,512]{2,1,0:T(8,128)(2,1)S(1)} %get-tuple-element.109), channel_id=1, source_target_pairs={{0,6},{1,7},{2,4},{3,5},{4,2},{5,3},{6,0},{7,1},{8,14},{9,15},{10,... | collective-permute-start | bytes 294920 | tf_op jit(solution)/shard_map/ppermute | solution.py:29
  70.1 1.5 %collective-permute-start.36 = (bf16[2,48,512]{2,1,0:T(8,128)(2,1)S(1)}, bf16[2,48,512]{2,1,0:T(8,128)(2,1)S(1)}, u32[]{:S(2)}, u32[]{:S(2)}) collective-permute-start(bf16[2,48,512]{2,1,0:T(8,128)(2,1)S(1)} %get-tuple-element.99), channel_id=1, source_target_pairs={{0,2},{1,3},{2,0},{3,1},{4,6},{5,7},{6,4},{7,5},{8,10},{9,11},{10,... | collective-permute-start | bytes 294920 | tf_op jit(solution)/shard_map/ppermute | solution.py:29
  71.6 0.6 collective-permute-start.37
  72.2 1.4 %collective-permute-start.38 = (bf16[2,48,512]{2,1,0:T(8,128)(2,1)S(1)}, bf16[2,48,512]{2,1,0:T(8,128)(2,1)S(1)}, u32[]{:S(2)}, u32[]{:S(2)}) collective-permute-start(bf16[2,48,512]{2,1,0:T(8,128)(2,1)S(1)} %get-tuple-element.101), channel_id=1, source_target_pairs={{0,6},{1,7},{2,4},{3,5},{4,2},{5,3},{6,0},{7,1},{8,14},{9,15},{10,... | collective-permute-start | bytes 294920 | tf_op jit(solution)/shard_map/ppermute | solution.py:29
  73.7 1.1 %collective-permute-done.42.refs_2_ = bf16[2,48,512]{2,1,0:T(8,128)(2,1)S(1)} collective-permute-done((bf16[2,48,512]{2,1,0:T(8,128)(2,1)S(1)}, bf16[2,48,512]{2,1,0:T(8,128)(2,1)S(1)}, u32[]{:S(2)}, u32[]{:S(2)}) %collective-permute-start.42) | collective-permute-done | bytes 98336 | tf_op jit(solution)/shard_map/ppermute | solution.py:29
  74.8 0.3 collective-permute-done.43.refs_3_
  75.2 0.7 collective-permute-start.44
  75.9 2.6 %collective-permute-start.45 = (bf16[2,24,512]{2,1,0:T(8,128)(2,1)S(1)}, bf16[2,24,512]{2,1,0:T(8,128)(2,1)S(1)}, u32[]{:S(2)}, u32[]{:S(2)}) collective-permute-start(bf16[2,24,512]{2,1,0:T(8,128)(2,1)S(1)} %get-tuple-element.111), channel_id=1, source_target_pairs={{0,24},{8,16},{16,8},{24,0},{1,25},{9,17},{17,9},{25,1},{2,26},{10... | collective-permute-start | bytes 147464 | tf_op jit(solution)/shard_map/ppermute | solution.py:29
  78.4 0.5 collective-permute-done.37.refs_2_
  79.0 0.3 collective-permute-start.39
  79.3 2.1 %shard_map.251 = (f32[64,16,64]{2,1,0:T(8,128)}, f32[64,16,64]{2,1,0:T(8,128)}) custom-call(bf16[64,256]{1,0:T(8,128)(2,1)S(1)} %get-tuple-element.112.driven, f32[64,1024]{1,0:T(8,128)S(1)} %get-tuple-element.113.dec_r, f32[64,1024]{1,0:T(8,128)S(1)} %get-tuple-element.114.dec_i, bf16[256,512]{1,0:T(8,128)(2,1)S(1)} %get-tuple-element.115.bt_r, ...), custom_call_target="tpu_custom_call" | custom-call | flops 10000000 | bytes 1000000 | tf_op jit(solution)/shard_map/pallas_call | solution.py:595
  81.4 0.8 collective-permute-done.45.refs_6_
  82.2 0.9 %collective-permute-done.39.refs_4_ = bf16[2,24,512]{2,1,0:T(8,128)(2,1)S(1)} collective-permute-done((bf16[2,24,512]{2,1,0:T(8,128)(2,1)S(1)}, bf16[2,24,512]{2,1,0:T(8,128)(2,1)S(1)}, u32[]{:S(2)}, u32[]{:S(2)}) %collective-permute-start.39) | collective-permute-done | bytes 49184 | tf_op jit(solution)/shard_map/ppermute | solution.py:29
  83.1 0.9 %shard_map.250 = bf16[64,512]{1,0:T(8,128)(2,1)} custom-call(bf16[64,512]{1,0:T(8,128)(2,1)S(1)} %get-tuple-element.83.refs_0_, bf16[2,64,192]{2,1,0:T(8,128)(2,1)S(1)} %get-tuple-element.84.refs_1_, f32[2,64]{1,0:T(2,128)S(1)} %bitcast.12, bf16[2,24,512]{2,1,0:T(8,128)(2,1)S(1)} %get-tuple-element.102.refs_3_, ...), custom_call_target="tpu_custom_call" | custom-call | flops 10000000 | bytes 1000000 | tf_op jit(solution)/shard_map/pallas_call | solution.py:601
  (53 shorter events, 1.8 us)
Async XLA Ops:
  0.6 5.7 %collective-permute-start.1 = (bf16[64,512]{1,0:T(8,128)(2,1)}, bf16[64,512]{1,0:T(8,128)(2,1)S(1)}, u32[]{:S(2)}, u32[]{:S(2)}) collective-permute-start(bf16[64,512]{1,0:T(8,128)(2,1)} %refs_15_.1), channel_id=1, source_target_pairs={{0,2},{1,3},{2,0},{3,1},{4,6},{5,7},{6,4},{7,5},{8,10},{9,11},{10,... | collective-permute-start | bytes 196616 | tf_op jit(solution)/shard_map/ppermute | solution.py:29
  3.7 4.5 %collective-permute-start.3 = (bf16[64,512]{1,0:T(8,128)(2,1)}, bf16[64,512]{1,0:T(8,128)(2,1)S(1)}, u32[]{:S(2)}, u32[]{:S(2)}) collective-permute-start(bf16[64,512]{1,0:T(8,128)(2,1)} %refs_15_.1), channel_id=1, source_target_pairs={{0,4},{1,5},{2,6},{3,7},{4,0},{5,1},{6,2},{7,3},{8,12},{9,13},{10,... | collective-permute-start | bytes 196616 | tf_op jit(solution)/shard_map/ppermute | solution.py:29
  5.2 5.4 %collective-permute-start.5 = (bf16[64,512]{1,0:T(8,128)(2,1)}, bf16[64,512]{1,0:T(8,128)(2,1)S(1)}, u32[]{:S(2)}, u32[]{:S(2)}) collective-permute-start(bf16[64,512]{1,0:T(8,128)(2,1)} %refs_15_.1), channel_id=1, source_target_pairs={{0,6},{1,7},{2,4},{3,5},{4,2},{5,3},{6,0},{7,1},{8,14},{9,15},{10,... | collective-permute-start | bytes 196616 | tf_op jit(solution)/shard_map/ppermute | solution.py:29
  5.2 9.5 %collective-permute-start = (bf16[64,512]{1,0:T(8,128)(2,1)}, bf16[64,512]{1,0:T(8,128)(2,1)S(1)}, u32[]{:S(2)}, u32[]{:S(2)}) collective-permute-start(bf16[64,512]{1,0:T(8,128)(2,1)} %refs_15_.1), channel_id=1, source_target_pairs={{0,1},{1,0},{2,3},{3,2},{4,5},{5,4},{6,7},{7,6},{8,9},{9,8},{10,11... | collective-permute-start | bytes 196616 | tf_op jit(solution)/shard_map/ppermute | solution.py:29
  6.3 8.4 %collective-permute-start.2 = (bf16[64,512]{1,0:T(8,128)(2,1)S(1)}, bf16[64,512]{1,0:T(8,128)(2,1)S(1)}, u32[]{:S(2)}, u32[]{:S(2)}) collective-permute-start(bf16[64,512]{1,0:T(8,128)(2,1)S(1)} %collective-permute-done.1.refs_1_), channel_id=1, source_target_pairs={{0,1},{1,0},{2,3},{3,2},{4,5},{5,4},{6,7},{7,6},{8,9},{9,8},{10,11... | collective-permute-start | bytes 196616 | tf_op jit(solution)/shard_map/ppermute | solution.py:29
  8.1 6.6 %collective-permute-start.4 = (bf16[64,512]{1,0:T(8,128)(2,1)S(1)}, bf16[64,512]{1,0:T(8,128)(2,1)S(1)}, u32[]{:S(2)}, u32[]{:S(2)}) collective-permute-start(bf16[64,512]{1,0:T(8,128)(2,1)S(1)} %collective-permute-done.3.refs_2_), channel_id=1, source_target_pairs={{0,1},{1,0},{2,3},{3,2},{4,5},{5,4},{6,7},{7,6},{8,9},{9,8},{10,11... | collective-permute-start | bytes 196616 | tf_op jit(solution)/shard_map/ppermute | solution.py:29
  10.6 4.2 %collective-permute-start.6 = (bf16[64,512]{1,0:T(8,128)(2,1)S(1)}, bf16[64,512]{1,0:T(8,128)(2,1)S(1)}, u32[]{:S(2)}, u32[]{:S(2)}) collective-permute-start(bf16[64,512]{1,0:T(8,128)(2,1)S(1)} %collective-permute-done.5.refs_3_), channel_id=1, source_target_pairs={{0,1},{1,0},{2,3},{3,2},{4,5},{5,4},{6,7},{7,6},{8,9},{9,8},{10,11... | collective-permute-start | bytes 196616 | tf_op jit(solution)/shard_map/ppermute | solution.py:29
  15.4 4.0 %collective-permute-start.10 = (bf16[64,256]{1,0:T(8,128)(2,1)S(1)}, bf16[64,256]{1,0:T(8,128)(2,1)S(1)}, u32[]{:S(2)}, u32[]{:S(2)}) collective-permute-start(bf16[64,256]{1,0:T(8,128)(2,1)S(1)} %get-tuple-element.70.refs_0_.refs_4_), channel_id=1, source_target_pairs={{0,4},{1,5},{2,6},{3,7},{4,0},{5,1},{6,2},{7,3},{8,12},{9,13},{10,... | collective-permute-start | bytes 98312 | tf_op jit(solution)/shard_map/ppermute | solution.py:29
  16.0 4.8 %collective-permute-start.12 = (bf16[64,256]{1,0:T(8,128)(2,1)S(1)}, bf16[64,256]{1,0:T(8,128)(2,1)S(1)}, u32[]{:S(2)}, u32[]{:S(2)}) collective-permute-start(bf16[64,256]{1,0:T(8,128)(2,1)S(1)} %get-tuple-element.70.refs_0_.refs_4_), channel_id=1, source_target_pairs={{0,6},{1,7},{2,4},{3,5},{4,2},{5,3},{6,0},{7,1},{8,14},{9,15},{10,... | collective-permute-start | bytes 98312 | tf_op jit(solution)/shard_map/ppermute | solution.py:29
  17.5 3.9 %collective-permute-start.8 = (bf16[64,256]{1,0:T(8,128)(2,1)S(1)}, bf16[64,256]{1,0:T(8,128)(2,1)S(1)}, u32[]{:S(2)}, u32[]{:S(2)}) collective-permute-start(bf16[64,256]{1,0:T(8,128)(2,1)S(1)} %get-tuple-element.70.refs_0_.refs_4_), channel_id=1, source_target_pairs={{0,2},{1,3},{2,0},{3,1},{4,6},{5,7},{6,4},{7,5},{8,10},{9,11},{10,... | collective-permute-start | bytes 98312 | tf_op jit(solution)/shard_map/ppermute | solution.py:29
  18.9 4.7 %collective-permute-start.7 = (bf16[64,256]{1,0:T(8,128)(2,1)S(1)}, bf16[64,256]{1,0:T(8,128)(2,1)S(1)}, u32[]{:S(2)}, u32[]{:S(2)}) collective-permute-start(bf16[64,256]{1,0:T(8,128)(2,1)S(1)} %get-tuple-element.70.refs_0_.refs_4_), channel_id=1, source_target_pairs={{0,1},{1,0},{2,3},{3,2},{4,5},{5,4},{6,7},{7,6},{8,9},{9,8},{10,11... | collective-permute-start | bytes 98312 | tf_op jit(solution)/shard_map/ppermute | solution.py:29
  19.4 4.3 %collective-permute-start.11 = (bf16[64,256]{1,0:T(8,128)(2,1)S(1)}, bf16[64,256]{1,0:T(8,128)(2,1)S(1)}, u32[]{:S(2)}, u32[]{:S(2)}) collective-permute-start(bf16[64,256]{1,0:T(8,128)(2,1)S(1)} %collective-permute-done.10.refs_2_), channel_id=1, source_target_pairs={{0,1},{1,0},{2,3},{3,2},{4,5},{5,4},{6,7},{7,6},{8,9},{9,8},{10,11... | collective-permute-start | bytes 98312 | tf_op jit(solution)/shard_map/ppermute | solution.py:29
  20.8 2.9 %collective-permute-start.13 = (bf16[64,256]{1,0:T(8,128)(2,1)S(1)}, bf16[64,256]{1,0:T(8,128)(2,1)S(1)}, u32[]{:S(2)}, u32[]{:S(2)}) collective-permute-start(bf16[64,256]{1,0:T(8,128)(2,1)S(1)} %collective-permute-done.12.refs_3_), channel_id=1, source_target_pairs={{0,1},{1,0},{2,3},{3,2},{4,5},{5,4},{6,7},{7,6},{8,9},{9,8},{10,11... | collective-permute-start | bytes 98312 | tf_op jit(solution)/shard_map/ppermute | solution.py:29
  21.4 2.3 %collective-permute-start.9 = (bf16[64,256]{1,0:T(8,128)(2,1)S(1)}, bf16[64,256]{1,0:T(8,128)(2,1)S(1)}, u32[]{:S(2)}, u32[]{:S(2)}) collective-permute-start(bf16[64,256]{1,0:T(8,128)(2,1)S(1)} %collective-permute-done.8.refs_1_), channel_id=1, source_target_pairs={{0,1},{1,0},{2,3},{3,2},{4,5},{5,4},{6,7},{7,6},{8,9},{9,8},{10,11... | collective-permute-start | bytes 98312 | tf_op jit(solution)/shard_map/ppermute | solution.py:29
  24.3 1.7 %collective-permute-start.14 = (bf16[4,64,512]{2,1,0:T(8,128)(2,1)S(1)}, bf16[4,64,512]{2,1,0:T(8,128)(2,1)S(1)}, u32[]{:S(2)}, u32[]{:S(2)}) collective-permute-start(bf16[4,64,512]{2,1,0:T(8,128)(2,1)S(1)} %get-tuple-element.77), channel_id=1, source_target_pairs={{0,1},{1,0},{2,3},{3,2},{4,5},{5,4},{6,7},{7,6},{8,9},{9,8},{10,11... | collective-permute-start | bytes 786440 | tf_op jit(solution)/shard_map/ppermute | solution.py:29
  26.1 4.4 %collective-permute-start.15 = (bf16[64,512]{1,0:T(8,128)(2,1)S(1)}, bf16[64,512]{1,0:T(8,128)(2,1)S(1)}, u32[]{:S(2)}, u32[]{:S(2)}) collective-permute-start(bf16[64,512]{1,0:T(8,128)(2,1)S(1)} %get-tuple-element.79), channel_id=1, source_target_pairs={{0,2},{1,3},{2,0},{3,1},{4,6},{5,7},{6,4},{7,5},{8,10},{9,11},{10,... | collective-permute-start | bytes 196616 | tf_op jit(solution)/shard_map/ppermute | solution.py:29
  27.7 5.0 %collective-permute-start.16 = (bf16[64,512]{1,0:T(8,128)(2,1)S(1)}, bf16[64,512]{1,0:T(8,128)(2,1)S(1)}, u32[]{:S(2)}, u32[]{:S(2)}) collective-permute-start(bf16[64,512]{1,0:T(8,128)(2,1)S(1)} %get-tuple-element.80), channel_id=1, source_target_pairs={{0,4},{1,5},{2,6},{3,7},{4,0},{5,1},{6,2},{7,3},{8,12},{9,13},{10,... | collective-permute-start | bytes 196616 | tf_op jit(solution)/shard_map/ppermute | solution.py:29
  28.2 5.2 %collective-permute-start.17 = (bf16[64,512]{1,0:T(8,128)(2,1)S(1)}, bf16[64,512]{1,0:T(8,128)(2,1)S(1)}, u32[]{:S(2)}, u32[]{:S(2)}) collective-permute-start(bf16[64,512]{1,0:T(8,128)(2,1)S(1)} %get-tuple-element.81), channel_id=1, source_target_pairs={{0,6},{1,7},{2,4},{3,5},{4,2},{5,3},{6,0},{7,1},{8,14},{9,15},{10,... | collective-permute-start | bytes 196616 | tf_op jit(solution)/shard_map/ppermute | solution.py:29
  33.6 5.4 %collective-permute-start.26 = (bf16[2,24,512]{2,1,0:T(8,128)(2,1)S(1)}, bf16[2,24,512]{2,1,0:T(8,128)(2,1)S(1)}, u32[]{:S(2)}, u32[]{:S(2)}) collective-permute-start(bf16[2,24,512]{2,1,0:T(8,128)(2,1)S(1)} %get-tuple-element.87), channel_id=1, source_target_pairs={{0,16},{8,24},{16,0},{24,8},{1,17},{9,25},{17,1},{25,9},{2,18},{10... | collective-permute-start | bytes 147464 | tf_op jit(solution)/shard_map/ppermute | solution.py:29
  36.2 6.0 %collective-permute-start.27 = (bf16[2,24,512]{2,1,0:T(8,128)(2,1)S(1)}, bf16[2,24,512]{2,1,0:T(8,128)(2,1)S(1)}, u32[]{:S(2)}, u32[]{:S(2)}) collective-permute-start(bf16[2,24,512]{2,1,0:T(8,128)(2,1)S(1)} %get-tuple-element.88), channel_id=1, source_target_pairs={{0,24},{8,16},{16,8},{24,0},{1,25},{9,17},{17,9},{25,1},{2,26},{10... | collective-permute-start | bytes 147464 | tf_op jit(solution)/shard_map/ppermute | solution.py:29
  37.6 8.2 %collective-permute-start.18 = (bf16[2,24,512]{2,1,0:T(8,128)(2,1)S(1)}, bf16[2,24,512]{2,1,0:T(8,128)(2,1)S(1)}, u32[]{:S(2)}, u32[]{:S(2)}) collective-permute-start(bf16[2,24,512]{2,1,0:T(8,128)(2,1)S(1)} %get-tuple-element.86), channel_id=1, source_target_pairs={{0,8},{8,0},{16,24},{24,16},{1,9},{9,1},{17,25},{25,17},{2,10},{10... | collective-permute-start | bytes 147464 | tf_op jit(solution)/shard_map/ppermute | solution.py:29
  42.2 5.7 %collective-permute-start.29 = (bf16[2,48,512]{2,1,0:T(8,128)(2,1)S(1)}, bf16[2,48,512]{2,1,0:T(8,128)(2,1)S(1)}, u32[]{:S(2)}, u32[]{:S(2)}) collective-permute-start(bf16[2,48,512]{2,1,0:T(8,128)(2,1)S(1)} %shard_map.239.refs_4_), channel_id=1, source_target_pairs={{0,2},{1,3},{2,0},{3,1},{4,6},{5,7},{6,4},{7,5},{8,10},{9,11},{10,... | collective-permute-start | bytes 294920 | tf_op jit(solution)/shard_map/ppermute | solution.py:29
  43.6 5.8 %collective-permute-start.31 = (bf16[2,48,512]{2,1,0:T(8,128)(2,1)S(1)}, bf16[2,48,512]{2,1,0:T(8,128)(2,1)S(1)}, u32[]{:S(2)}, u32[]{:S(2)}) collective-permute-start(bf16[2,48,512]{2,1,0:T(8,128)(2,1)S(1)} %shard_map.239.refs_4_), channel_id=1, source_target_pairs={{0,4},{1,5},{2,6},{3,7},{4,0},{5,1},{6,2},{7,3},{8,12},{9,13},{10,... | collective-permute-start | bytes 294920 | tf_op jit(solution)/shard_map/ppermute | solution.py:29
  44.3 6.1 %collective-permute-start.33 = (bf16[2,48,512]{2,1,0:T(8,128)(2,1)S(1)}, bf16[2,48,512]{2,1,0:T(8,128)(2,1)S(1)}, u32[]{:S(2)}, u32[]{:S(2)}) collective-permute-start(bf16[2,48,512]{2,1,0:T(8,128)(2,1)S(1)} %shard_map.239.refs_4_), channel_id=1, source_target_pairs={{0,6},{1,7},{2,4},{3,5},{4,2},{5,3},{6,0},{7,1},{8,14},{9,15},{10,... | collective-permute-start | bytes 294920 | tf_op jit(solution)/shard_map/ppermute | solution.py:29
  45.8 5.0 %collective-permute-start.20 = (bf16[2,48,512]{2,1,0:T(8,128)(2,1)S(1)}, bf16[2,48,512]{2,1,0:T(8,128)(2,1)S(1)}, u32[]{:S(2)}, u32[]{:S(2)}) collective-permute-start(bf16[2,48,512]{2,1,0:T(8,128)(2,1)S(1)} %shard_map.238.refs_0_), channel_id=1, source_target_pairs={{0,2},{1,3},{2,0},{3,1},{4,6},{5,7},{6,4},{7,5},{8,10},{9,11},{10,... | collective-permute-start | bytes 294920 | tf_op jit(solution)/shard_map/ppermute | solution.py:29
  47.2 4.6 %collective-permute-start.22 = (bf16[2,48,512]{2,1,0:T(8,128)(2,1)S(1)}, bf16[2,48,512]{2,1,0:T(8,128)(2,1)S(1)}, u32[]{:S(2)}, u32[]{:S(2)}) collective-permute-start(bf16[2,48,512]{2,1,0:T(8,128)(2,1)S(1)} %shard_map.238.refs_0_), channel_id=1, source_target_pairs={{0,4},{1,5},{2,6},{3,7},{4,0},{5,1},{6,2},{7,3},{8,12},{9,13},{10,... | collective-permute-start | bytes 294920 | tf_op jit(solution)/shard_map/ppermute | solution.py:29
  47.9 5.5 %collective-permute-start.24 = (bf16[2,48,512]{2,1,0:T(8,128)(2,1)S(1)}, bf16[2,48,512]{2,1,0:T(8,128)(2,1)S(1)}, u32[]{:S(2)}, u32[]{:S(2)}) collective-permute-start(bf16[2,48,512]{2,1,0:T(8,128)(2,1)S(1)} %shard_map.238.refs_0_), channel_id=1, source_target_pairs={{0,6},{1,7},{2,4},{3,5},{4,2},{5,3},{6,0},{7,1},{8,14},{9,15},{10,... | collective-permute-start | bytes 294920 | tf_op jit(solution)/shard_map/ppermute | solution.py:29
  49.4 4.0 %collective-permute-start.28 = (bf16[2,48,512]{2,1,0:T(8,128)(2,1)S(1)}, bf16[2,48,512]{2,1,0:T(8,128)(2,1)S(1)}, u32[]{:S(2)}, u32[]{:S(2)}) collective-permute-start(bf16[2,48,512]{2,1,0:T(8,128)(2,1)S(1)} %shard_map.239.refs_4_), channel_id=1, source_target_pairs={{0,1},{1,0},{2,3},{3,2},{4,5},{5,4},{6,7},{7,6},{8,9},{9,8},{10,11... | collective-permute-start | bytes 294920 | tf_op jit(solution)/shard_map/ppermute | solution.py:29
  50.4 3.5 %collective-permute-start.19 = (bf16[2,48,512]{2,1,0:T(8,128)(2,1)S(1)}, bf16[2,48,512]{2,1,0:T(8,128)(2,1)S(1)}, u32[]{:S(2)}, u32[]{:S(2)}) collective-permute-start(bf16[2,48,512]{2,1,0:T(8,128)(2,1)S(1)} %shard_map.238.refs_0_), channel_id=1, source_target_pairs={{0,1},{1,0},{2,3},{3,2},{4,5},{5,4},{6,7},{7,6},{8,9},{9,8},{10,11... | collective-permute-start | bytes 294920 | tf_op jit(solution)/shard_map/ppermute | solution.py:29
  50.7 3.3 %collective-permute-start.30 = (bf16[2,48,512]{2,1,0:T(8,128)(2,1)S(1)}, bf16[2,48,512]{2,1,0:T(8,128)(2,1)S(1)}, u32[]{:S(2)}, u32[]{:S(2)}) collective-permute-start(bf16[2,48,512]{2,1,0:T(8,128)(2,1)S(1)} %collective-permute-done.29.refs_5_), channel_id=1, source_target_pairs={{0,1},{1,0},{2,3},{3,2},{4,5},{5,4},{6,7},{7,6},{8,9},{9,8},{10,11... | collective-permute-start | bytes 294920 | tf_op jit(solution)/shard_map/ppermute | solution.py:29
  51.8 10.7 %collective-permute-start.32 = (bf16[2,48,512]{2,1,0:T(8,128)(2,1)S(1)}, bf16[2,48,512]{2,1,0:T(8,128)(2,1)S(1)}, u32[]{:S(2)}, u32[]{:S(2)}) collective-permute-start(bf16[2,48,512]{2,1,0:T(8,128)(2,1)S(1)} %collective-permute-done.31.refs_6_), channel_id=1, source_target_pairs={{0,1},{1,0},{2,3},{3,2},{4,5},{5,4},{6,7},{7,6},{8,9},{9,8},{10,11... | collective-permute-start | bytes 294920 | tf_op jit(solution)/shard_map/ppermute | solution.py:29
  53.4 9.0 %collective-permute-start.34 = (bf16[2,48,512]{2,1,0:T(8,128)(2,1)S(1)}, bf16[2,48,512]{2,1,0:T(8,128)(2,1)S(1)}, u32[]{:S(2)}, u32[]{:S(2)}) collective-permute-start(bf16[2,48,512]{2,1,0:T(8,128)(2,1)S(1)} %collective-permute-done.33.refs_7_), channel_id=1, source_target_pairs={{0,1},{1,0},{2,3},{3,2},{4,5},{5,4},{6,7},{7,6},{8,9},{9,8},{10,11... | collective-permute-start | bytes 294920 | tf_op jit(solution)/shard_map/ppermute | solution.py:29
  53.5 9.0 %collective-permute-start.21 = (bf16[2,48,512]{2,1,0:T(8,128)(2,1)S(1)}, bf16[2,48,512]{2,1,0:T(8,128)(2,1)S(1)}, u32[]{:S(2)}, u32[]{:S(2)}) collective-permute-start(bf16[2,48,512]{2,1,0:T(8,128)(2,1)S(1)} %collective-permute-done.20.refs_1_), channel_id=1, source_target_pairs={{0,1},{1,0},{2,3},{3,2},{4,5},{5,4},{6,7},{7,6},{8,9},{9,8},{10,11... | collective-permute-start | bytes 294920 | tf_op jit(solution)/shard_map/ppermute | solution.py:29
  54.0 8.5 %collective-permute-start.23 = (bf16[2,48,512]{2,1,0:T(8,128)(2,1)S(1)}, bf16[2,48,512]{2,1,0:T(8,128)(2,1)S(1)}, u32[]{:S(2)}, u32[]{:S(2)}) collective-permute-start(bf16[2,48,512]{2,1,0:T(8,128)(2,1)S(1)} %collective-permute-done.22.refs_2_), channel_id=1, source_target_pairs={{0,1},{1,0},{2,3},{3,2},{4,5},{5,4},{6,7},{7,6},{8,9},{9,8},{10,11... | collective-permute-start | bytes 294920 | tf_op jit(solution)/shard_map/ppermute | solution.py:29
  54.0 8.5 %collective-permute-start.25 = (bf16[2,48,512]{2,1,0:T(8,128)(2,1)S(1)}, bf16[2,48,512]{2,1,0:T(8,128)(2,1)S(1)}, u32[]{:S(2)}, u32[]{:S(2)}) collective-permute-start(bf16[2,48,512]{2,1,0:T(8,128)(2,1)S(1)} %collective-permute-done.24.refs_3_), channel_id=1, source_target_pairs={{0,1},{1,0},{2,3},{3,2},{4,5},{5,4},{6,7},{7,6},{8,9},{9,8},{10,11... | collective-permute-start | bytes 294920 | tf_op jit(solution)/shard_map/ppermute | solution.py:29
  64.5 1.9 %collective-permute-start.40 = (bf16[4,2,48,512]{3,2,1,0:T(8,128)(2,1)S(1)}, bf16[4,2,48,512]{3,2,1,0:T(8,128)(2,1)S(1)}, u32[]{:S(2)}, u32[]{:S(2)}) collective-permute-start(bf16[4,2,48,512]{3,2,1,0:T(8,128)(2,1)S(1)} %get-tuple-element.105), channel_id=1, source_target_pairs={{0,1},{1,0},{2,3},{3,2},{4,5},{5,4},{6,7},{7,6},{8,9},{9,8},{10,11... | collective-permute-start | bytes 1179656 | tf_op jit(solution)/shard_map/ppermute | solution.py:29
  65.8 17.3 %copy-start = (f32[64,2]{0,1:T(2,128)S(1)}, f32[64,2]{0,1:T(2,128)}, u32[]{:S(2)}) copy-start(f32[64,2]{0,1:T(2,128)} %param.40) | copy-start | bytes 1540
  65.8 4.2 %collective-permute-start.35 = (bf16[4,2,48,512]{3,2,1,0:T(8,128)(2,1)S(1)}, bf16[4,2,48,512]{3,2,1,0:T(8,128)(2,1)S(1)}, u32[]{:S(2)}, u32[]{:S(2)}) collective-permute-start(bf16[4,2,48,512]{3,2,1,0:T(8,128)(2,1)S(1)} %get-tuple-element.97), channel_id=1, source_target_pairs={{0,1},{1,0},{2,3},{3,2},{4,5},{5,4},{6,7},{7,6},{8,9},{9,8},{10,11... | collective-permute-start | bytes 1179656 | tf_op jit(solution)/shard_map/ppermute | solution.py:29
  66.5 5.8 %collective-permute-start.41 = (bf16[2,48,512]{2,1,0:T(8,128)(2,1)S(1)}, bf16[2,48,512]{2,1,0:T(8,128)(2,1)S(1)}, u32[]{:S(2)}, u32[]{:S(2)}) collective-permute-start(bf16[2,48,512]{2,1,0:T(8,128)(2,1)S(1)} %get-tuple-element.107), channel_id=1, source_target_pairs={{0,2},{1,3},{2,0},{3,1},{4,6},{5,7},{6,4},{7,5},{8,10},{9,11},{10,... | collective-permute-start | bytes 294920 | tf_op jit(solution)/shard_map/ppermute | solution.py:29
  68.0 6.8 %collective-permute-start.42 = (bf16[2,48,512]{2,1,0:T(8,128)(2,1)S(1)}, bf16[2,48,512]{2,1,0:T(8,128)(2,1)S(1)}, u32[]{:S(2)}, u32[]{:S(2)}) collective-permute-start(bf16[2,48,512]{2,1,0:T(8,128)(2,1)S(1)} %get-tuple-element.108), channel_id=1, source_target_pairs={{0,4},{1,5},{2,6},{3,7},{4,0},{5,1},{6,2},{7,3},{8,12},{9,13},{10,... | collective-permute-start | bytes 294920 | tf_op jit(solution)/shard_map/ppermute | solution.py:29
  68.6 6.6 %collective-permute-start.43 = (bf16[2,48,512]{2,1,0:T(8,128)(2,1)S(1)}, bf16[2,48,512]{2,1,0:T(8,128)(2,1)S(1)}, u32[]{:S(2)}, u32[]{:S(2)}) collective-permute-start(bf16[2,48,512]{2,1,0:T(8,128)(2,1)S(1)} %get-tuple-element.109), channel_id=1, source_target_pairs={{0,6},{1,7},{2,4},{3,5},{4,2},{5,3},{6,0},{7,1},{8,14},{9,15},{10,... | collective-permute-start | bytes 294920 | tf_op jit(solution)/shard_map/ppermute | solution.py:29
  70.1 8.3 %collective-permute-start.36 = (bf16[2,48,512]{2,1,0:T(8,128)(2,1)S(1)}, bf16[2,48,512]{2,1,0:T(8,128)(2,1)S(1)}, u32[]{:S(2)}, u32[]{:S(2)}) collective-permute-start(bf16[2,48,512]{2,1,0:T(8,128)(2,1)S(1)} %get-tuple-element.99), channel_id=1, source_target_pairs={{0,2},{1,3},{2,0},{3,1},{4,6},{5,7},{6,4},{7,5},{8,10},{9,11},{10,... | collective-permute-start | bytes 294920 | tf_op jit(solution)/shard_map/ppermute | solution.py:29
  71.6 7.3 %collective-permute-start.37 = (bf16[2,48,512]{2,1,0:T(8,128)(2,1)S(1)}, bf16[2,48,512]{2,1,0:T(8,128)(2,1)S(1)}, u32[]{:S(2)}, u32[]{:S(2)}) collective-permute-start(bf16[2,48,512]{2,1,0:T(8,128)(2,1)S(1)} %get-tuple-element.100), channel_id=1, source_target_pairs={{0,4},{1,5},{2,6},{3,7},{4,0},{5,1},{6,2},{7,3},{8,12},{9,13},{10,... | collective-permute-start | bytes 294920 | tf_op jit(solution)/shard_map/ppermute | solution.py:29
  72.2 6.7 %collective-permute-start.38 = (bf16[2,48,512]{2,1,0:T(8,128)(2,1)S(1)}, bf16[2,48,512]{2,1,0:T(8,128)(2,1)S(1)}, u32[]{:S(2)}, u32[]{:S(2)}) collective-permute-start(bf16[2,48,512]{2,1,0:T(8,128)(2,1)S(1)} %get-tuple-element.101), channel_id=1, source_target_pairs={{0,6},{1,7},{2,4},{3,5},{4,2},{5,3},{6,0},{7,1},{8,14},{9,15},{10,... | collective-permute-start | bytes 294920 | tf_op jit(solution)/shard_map/ppermute | solution.py:29
  75.2 6.2 %collective-permute-start.44 = (bf16[2,24,512]{2,1,0:T(8,128)(2,1)S(1)}, bf16[2,24,512]{2,1,0:T(8,128)(2,1)S(1)}, u32[]{:S(2)}, u32[]{:S(2)}) collective-permute-start(bf16[2,24,512]{2,1,0:T(8,128)(2,1)S(1)} %get-tuple-element.110), channel_id=1, source_target_pairs={{0,16},{8,24},{16,0},{24,8},{1,17},{9,25},{17,1},{25,9},{2,18},{10... | collective-permute-start | bytes 147464 | tf_op jit(solution)/shard_map/ppermute | solution.py:29
  75.9 6.4 %collective-permute-start.45 = (bf16[2,24,512]{2,1,0:T(8,128)(2,1)S(1)}, bf16[2,24,512]{2,1,0:T(8,128)(2,1)S(1)}, u32[]{:S(2)}, u32[]{:S(2)}) collective-permute-start(bf16[2,24,512]{2,1,0:T(8,128)(2,1)S(1)} %get-tuple-element.111), channel_id=1, source_target_pairs={{0,24},{8,16},{16,8},{24,0},{1,25},{9,17},{17,9},{25,1},{2,26},{10... | collective-permute-start | bytes 147464 | tf_op jit(solution)/shard_map/ppermute | solution.py:29
  79.0 4.2 %collective-permute-start.39 = (bf16[2,24,512]{2,1,0:T(8,128)(2,1)S(1)}, bf16[2,24,512]{2,1,0:T(8,128)(2,1)S(1)}, u32[]{:S(2)}, u32[]{:S(2)}) collective-permute-start(bf16[2,24,512]{2,1,0:T(8,128)(2,1)S(1)} %get-tuple-element.103), channel_id=1, source_target_pairs={{0,8},{8,0},{16,24},{24,16},{1,9},{9,1},{17,25},{25,17},{2,10},{10... | collective-permute-start | bytes 147464 | tf_op jit(solution)/shard_map/ppermute | solution.py:29

commit v4 on v3

--- a/solution.py
+++ b/solution.py
@@ -29,12 +29,16 @@
     return lax.ppermute(x, axis, [(i, i ^ k) for i in range(lax.axis_size(axis))])
 
 
+def crossings(n):
+    return [0] + [k + 1 for k in range(2, n, 2)]
+
+
 def gather_swaps(x, n):
     pieces = [None] * n
     pieces[0] = x
-    for k in range(2, n, 2):
+    for k in crossings(n)[1:]:
         pieces[k] = swap(x, "tp", k)
-    for k in range(0, n, 2):
+    for k in crossings(n):
         pieces[k ^ 1] = swap(pieces[k], "tp", 1)
     return pieces
 
@@ -52,7 +56,7 @@
 
 def reduce_swaps(own, partner, n):
     first, *rest = pair_swaps(own, partner, n)
-    return [first] + [swap(x, "tp", k) for x, k in zip(rest, range(2, n, 2))]
+    return [first] + [swap(x, "tp", k) for x, k in zip(rest, crossings(n)[1:])]
 
 
 def pair_body(own, other, *outs):
@@ -200,11 +204,11 @@
     return copies
 
 
-def mixer_sums(odd, pieces, gain, weight, start):
+def mixer_sums(n, odd, pieces, gain, weight, start):
     total, turned, square = start
     width = pieces[0].shape[1]
-    for at, piece in enumerate(pieces):
-        k = 2 * at + odd
+    for at, (k, piece) in enumerate(zip(crossings(n), pieces)):
+        k = k ^ odd
         x = piece[...].astype(f32)
         square = square + fold(x * x)
         x = (x * gain[:, place(k, width)]).astype(bf16)
@@ -218,7 +222,7 @@
 def first_body(n, *refs):
     pieces = refs[: n // 2]
     gain, weight = refs[n // 2 : n // 2 + 2]
-    for out, value in zip(refs[n // 2 + 2 :], mixer_sums(0, pieces, gain, weight, (0.0, 0.0, 0.0))):
+    for out, value in zip(refs[n // 2 + 2 :], mixer_sums(n, 0, pieces, gain, weight, (0.0, 0.0, 0.0))):
         out[...] = value
 
 
@@ -227,7 +231,7 @@
     gain, weight, base, mix, skip, total, turned, square = refs[n // 2 : n // 2 + 8]
     driven_ref, act_ref = refs[n // 2 + 8 :]
     start = (total[...], turned[...], square[...])
-    total, turned, square = mixer_sums(1, pieces, gain, weight, start)
+    total, turned, square = mixer_sums(n, 1, pieces, gain, weight, start)
     width = pieces[0].shape[1]
     scale = lax.rsqrt(jnp.sum(square, axis=1, keepdims=True) / (n * width) + norm_eps)
     driven = ((total + turned.T) * scale).astype(bf16)
@@ -289,8 +293,8 @@
 
 def glu_sums(odd, pieces, glu, gate, turned):
     width = pieces[0].shape[1]
-    for at, piece in enumerate(pieces):
-        block = glu[:, place(2 * at + odd, width)]
+    for at, (k, piece) in enumerate(zip(crossings(2 * len(pieces)), pieces)):
+        block = glu[:, place(k ^ odd, width)]
         if at % 2:
             turned = turned + dot(block, piece[...], NT)
         else:
@@ -311,13 +315,13 @@
     gate, turned = glu_sums(1, pieces, glu, gate[...], turned[...])
     glued = (own[...].astype(f32) * jax.nn.sigmoid(gate + turned.T)).astype(bf16)
     glued_ref[...] = glued
-    for k in range(1, n, 2):
-        partner[k // 2] = dot(glued, out_w[:, place(k, partner.shape[2])], NN).astype(bf16)
+    for at, k in enumerate(crossings(n)):
+        partner[at] = dot(glued, out_w[:, place(k ^ 1, partner.shape[2])], NN).astype(bf16)
 
 
 def out_body(n, glued, out_w, own):
-    for k in range(0, n, 2):
-        own[k // 2] = dot(glued[...], out_w[:, place(k, own.shape[2])], NN).astype(bf16)
+    for at, k in enumerate(crossings(n)):
+        own[at] = dot(glued[...], out_w[:, place(k, own.shape[2])], NN).astype(bf16)
 
 
 def merge_body(*refs):
@@ -352,8 +356,8 @@
     height = gate_w.shape[0] // experts
     held = up_low.shape[0] // height
     up_w, row = (up_low, i) if i < held else (up_high, i - held)
-    for at in range(len(near)):
-        k = 2 * at + odd
+    for at, k in enumerate(crossings(2 * len(near))):
+        k = k ^ odd
         x = jnp.concatenate([near[at][i], far[at][i]], axis=0).astype(f32)
         square = square + fold(x * x)
         x = (x * gain[:, place(k, width)]).astype(bf16)
@@ -382,8 +386,9 @@
         scale = lax.rsqrt(jnp.sum(square, axis=1, keepdims=True) / (n * width) + norm_eps)
         hidden = (jax.nn.silu(g * scale) * (u.T * scale)).astype(bf16)
         later[i] = hidden
-        for k in range(1, n, 2):
-            partner[k // 2, i] = dot(hidden[count:], down_w[rows_of(down_w, i, experts), place(k, width)], NN).astype(bf16)
+        for at, k in enumerate(crossings(n)):
+            block = down_w[rows_of(down_w, i, experts), place(k ^ 1, width)]
+            partner[at, i] = dot(hidden[count:], block, NN).astype(bf16)
 
 
 def down_body(n, hidden, down_w, far_own, own, partner):
@@ -391,12 +396,13 @@
     experts = hidden.shape[0]
     for i in range(experts):
         near, far = hidden[i, :count], hidden[i, count:]
-        for k in range(0, n, 2):
-            far_own[k // 2, i] = dot(far, down_w[rows_of(down_w, i, experts), place(k, width)], NN).astype(bf16)
-        for k in range(1, n, 2):
-            partner[k // 2, i] = dot(near, down_w[rows_of(down_w, i, experts), place(k, width)], NN).astype(bf16)
-        for k in range(0, n, 2):
-            own[k // 2, i] = dot(near, down_w[rows_of(down_w, i, experts), place(k, width)], NN).astype(bf16)
+        for at, k in enumerate(crossings(n)):
+            block = down_w[rows_of(down_w, i, experts), place(k, width)]
+            far_own[at, i] = dot(far, block, NN).astype(bf16)
+            own[at, i] = dot(near, block, NN).astype(bf16)
+        for at, k in enumerate(crossings(n)):
+            block = down_w[rows_of(down_w, i, experts), place(k ^ 1, width)]
+            partner[at, i] = dot(near, block, NN).astype(bf16)
 
 
 def total_body(m, terms, *refs):
@@ -510,13 +516,13 @@
         [jax.ShapeDtypeStruct(x, f32) for x in ((count, channels), (channels, count), (count, LANES))],
         [WHOLE] * (n // 2 + 2),
         limit=8 * 2**20,
-    )(*pieces[::2], gain1, in_w)
+    )(*[pieces[k] for k in crossings(n)], gain1, in_w)
     driven, activated = call(
         functools.partial(mixer_body, n),
         [jax.ShapeDtypeStruct((count, channels), bf16)] * 2,
         [WHOLE] * (n // 2 + 8),
         limit=12 * 2**20,
-    )(*pieces[1::2], gain1, in_w, base, mix, skip, *partial)
+    )(*[pieces[k ^ 1] for k in crossings(n)], gain1, in_w, base, mix, skip, *partial)
 
     acts = gather_swaps(activated, n)
     glu_w, out_w = fetch(glu_weight, out_weight)
@@ -526,13 +532,13 @@
         [jax.ShapeDtypeStruct(x, f32) for x in ((count, channels), (channels, count))],
         [WHOLE] * (n // 2 + 2),
         limit=8 * 2**20,
-    )(*acts[::2], glu_w, bias)
+    )(*[acts[k] for k in crossings(n)], glu_w, bias)
     glued, partner = call(
         functools.partial(glu_body, n),
         [jax.ShapeDtypeStruct((count, channels), bf16), block],
         [WHOLE] * (n // 2 + 5),
         limit=12 * 2**20,
-    )(*acts[1::2], acts[0], glu_w, *partial, out_w)
+    )(*[acts[k ^ 1] for k in crossings(n)], acts[0], glu_w, *partial, out_w)
     sums = call(functools.partial(out_body, n), block, [WHOLE] * 2, limit=8 * 2**20)(glued, out_w)
 
     terms = reduce_swaps(sums, partner, n)
@@ -570,13 +576,13 @@
         [jax.ShapeDtypeStruct((exp_dev, *x), f32) for x in ((rows, hidden), (hidden, rows), (rows, LANES))],
         [WHOLE] * (n + 4),
         limit=8 * 2**20,
-    )(*near[::2], *far[::2], *weights)
+    )(*[near[k] for k in crossings(n)], *[far[k] for k in crossings(n)], *weights)
     later, far_partner = call(
         functools.partial(up_body, n),
         [jax.ShapeDtypeStruct((exp_dev, rows, hidden), bf16), part],
         [WHOLE] * (n + 8),
         limit=16 * 2**20,
-    )(*near[1::2], *far[1::2], *weights, down_w, *partial)
+    )(*[near[k ^ 1] for k in crossings(n)], *[far[k ^ 1] for k in crossings(n)], *weights, down_w, *partial)
     far_own, *near_outs = call(
         functools.partial(down_body, n), [part] * 3, [WHOLE] * 2, limit=8 * 2**20
     )(later, down_w)

time: 84.2 us -> 84 us (level)
  starting transfers between devices: 36.3 us -> 34.7 us
  waiting for transfers between devices: 24.1 us -> 25.6 us
    ppermute x46, starting transfers between devices: 36.3 us -> 34.7 us  [swap(): lax.ppermute(x, axis, [(i, i ^ k) for i in range(lax.axis_size(axis))])]
    ppermute x46, waiting for transfers between devices: 24.1 us -> 25.6 us  [swap(): lax.ppermute(x, axis, [(i, i ^ k) for i in range(lax.axis_size(axis))])]
where the time goes in v4:
time: 84 us; the launch traced here: 83.8 us
  starting transfers between devices  34.7 us (41%)
  waiting for transfers between devices  25.6 us (30%)
  Pallas kernels  22.6 us (27%)
  between operations  0.91 us (1%)
    ppermute x46, starting transfers between devices, swap(): lax.ppermute(x, axis, [(i, i ^ k) for i in range(lax.axis_size(axis))])  34.7 us
    ppermute x46, waiting for transfers between devices, swap(): lax.ppermute(x, axis, [(i, i ^ k) for i in range(lax.axis_size(axis))])  25.6 us
    pallas_call x4, Pallas kernels, fetch(): call(functools.partial(fetch_body, [x[1:] for x in sources]), [pltpu.VMEM...  8.7 us
    pallas_call x1, Pallas kernels, local_swaps(): call(functools.partial(prep_body, n, cap), [jax.ShapeDtypeStruct((count,...  3.73 us
    pallas_call x1, Pallas kernels, local_swaps(): call(state_body, [jax.ShapeDtypeStruct((count, groups, entries), f32)] *...  2.13 us
    pallas_call x1, Pallas kernels, local_swaps(): call(functools.partial(up_body, n), [jax.ShapeDtypeStruct((exp_dev, rows,...  1.98 us
  transfers between devices with their start and end apart: 46, of which 21 were waited for; matrix products, arithmetic and copies ran while one was open for 0% of the time, Pallas kernels for 22%

profile of v4, /device:TPU:0, one launch (start us, length us, event | category | flops | bytes accessed | tf_op | source)
XLA Modules:
  0.0 83.8 jit_solution(7354354493593795542)
XLA Ops:
  0.6 2.5 %collective-permute-start.1 = (bf16[64,512]{1,0:T(8,128)(2,1)}, bf16[64,512]{1,0:T(8,128)(2,1)S(1)}, u32[]{:S(2)}, u32[]{:S(2)}) collective-permute-start(bf16[64,512]{1,0:T(8,128)(2,1)} %refs_15_.1), channel_id=1, source_target_pairs={{0,3},{1,2},{2,1},{3,0},{4,7},{5,6},{6,5},{7,4},{8,11},{9,10},{10,... | collective-permute-start | bytes 196616 | tf_op jit(solution)/shard_map/ppermute | solution.py:29
  3.1 1.8 %collective-permute-start.3 = (bf16[64,512]{1,0:T(8,128)(2,1)}, bf16[64,512]{1,0:T(8,128)(2,1)S(1)}, u32[]{:S(2)}, u32[]{:S(2)}) collective-permute-start(bf16[64,512]{1,0:T(8,128)(2,1)} %refs_15_.1), channel_id=1, source_target_pairs={{0,5},{1,4},{2,7},{3,6},{4,1},{5,0},{6,3},{7,2},{8,13},{9,12},{10,... | collective-permute-start | bytes 196616 | tf_op jit(solution)/shard_map/ppermute | solution.py:29
  4.9 1.0 %collective-permute-done.1.refs_1_ = bf16[64,512]{1,0:T(8,128)(2,1)S(1)} collective-permute-done((bf16[64,512]{1,0:T(8,128)(2,1)}, bf16[64,512]{1,0:T(8,128)(2,1)S(1)}, u32[]{:S(2)}, u32[]{:S(2)}) %collective-permute-start.1) | collective-permute-done | bytes 65568 | tf_op jit(solution)/shard_map/ppermute | solution.py:29
  6.0 1.1 %collective-permute-done.3.refs_2_ = bf16[64,512]{1,0:T(8,128)(2,1)S(1)} collective-permute-done((bf16[64,512]{1,0:T(8,128)(2,1)}, bf16[64,512]{1,0:T(8,128)(2,1)S(1)}, u32[]{:S(2)}, u32[]{:S(2)}) %collective-permute-start.3) | collective-permute-done | bytes 65568 | tf_op jit(solution)/shard_map/ppermute | solution.py:29
  7.1 0.6 collective-permute-start.4
  7.7 2.7 %collective-permute-done.5.refs_3_ = bf16[64,512]{1,0:T(8,128)(2,1)S(1)} collective-permute-done((bf16[64,512]{1,0:T(8,128)(2,1)}, bf16[64,512]{1,0:T(8,128)(2,1)S(1)}, u32[]{:S(2)}, u32[]{:S(2)}) %collective-permute-start.5) | collective-permute-done | bytes 65568 | tf_op jit(solution)/shard_map/ppermute | solution.py:29
  10.5 3.7 %shard_map.229 = (f32[64,1024]{1,0:T(8,128)S(1)}, f32[64,1024]{1,0:T(8,128)S(1)}, bf16[256,512]{1,0:T(8,128)(2,1)S(1)}, bf16[256,512]{1,0:T(8,128)(2,1)S(1)}, f3...) custom-call(bf16[256,4096]{1,0:T(8,128)(2,1)} %refs_0_.2, ...), custom_call_target="tpu_custom_call" | custom-call | flops 10000000 | bytes 1000000 | tf_op jit(solution)/shard_map/pallas_call | solution.py:493
  14.2 0.4 shard_map.230
  14.7 0.6 shard_map.231
  15.3 0.5 collective-permute-start.10
  15.8 1.2 %collective-permute-start.12 = (bf16[64,256]{1,0:T(8,128)(2,1)S(1)}, bf16[64,256]{1,0:T(8,128)(2,1)S(1)}, u32[]{:S(2)}, u32[]{:S(2)}) collective-permute-start(bf16[64,256]{1,0:T(8,128)(2,1)S(1)} %get-tuple-element.70.refs_0_.refs_4_), channel_id=1, source_target_pairs={{0,7},{1,6},{2,5},{3,4},{4,3},{5,2},{6,1},{7,0},{8,15},{9,14},{10,... | collective-permute-start | bytes 98312 | tf_op jit(solution)/shard_map/ppermute | solution.py:29
  17.0 1.6 %collective-permute-start.8 = (bf16[64,256]{1,0:T(8,128)(2,1)S(1)}, bf16[64,256]{1,0:T(8,128)(2,1)S(1)}, u32[]{:S(2)}, u32[]{:S(2)}) collective-permute-start(bf16[64,256]{1,0:T(8,128)(2,1)S(1)} %get-tuple-element.70.refs_0_.refs_4_), channel_id=1, source_target_pairs={{0,3},{1,2},{2,1},{3,0},{4,7},{5,6},{6,5},{7,4},{8,11},{9,10},{10,... | collective-permute-start | bytes 98312 | tf_op jit(solution)/shard_map/ppermute | solution.py:29
  18.7 0.4 collective-permute-start.11
  19.1 1.0 %collective-permute-done.12.refs_3_ = bf16[64,256]{1,0:T(8,128)(2,1)S(1)} collective-permute-done((bf16[64,256]{1,0:T(8,128)(2,1)S(1)}, bf16[64,256]{1,0:T(8,128)(2,1)S(1)}, u32[]{:S(2)}, u32[]{:S(2)}) %collective-permute-start.12) | collective-permute-done | bytes 32800 | tf_op jit(solution)/shard_map/ppermute | solution.py:29
  20.1 0.4 collective-permute-start.13
  20.6 0.4 collective-permute-done.8.refs_1_
  21.1 2.0 %shard_map.232 = (bf16[256,2048]{1,0:T(8,128)(2,1)S(1)}, bf16[256,4096]{1,0:T(8,128)(2,1)S(1)}) custom-call(bf16[256,2048]{1,0:T(8,128)(2,1)} %refs_0_.3, bf16[256,4096]{1,0:T(8,128)(2,1)} %refs_1_.3), custom_call_target="tpu_custom_call" | custom-call | flops 10000000 | bytes 1000000 | tf_op jit(solution)/shard_map/pallas_call | solution.py:280
  23.4 0.6 shard_map.234
  24.0 0.5 collective-permute-start.14
  24.8 0.9 %collective-permute-done.14.other = bf16[4,64,512]{2,1,0:T(8,128)(2,1)S(1)} collective-permute-done((bf16[4,64,512]{2,1,0:T(8,128)(2,1)S(1)}, bf16[4,64,512]{2,1,0:T(8,128)(2,1)S(1)}, u32[]{:S(2)}, u32[]{:S(2)}) %collective-permute-start.14) | collective-permute-done | bytes 262176 | tf_op jit(solution)/shard_map/ppermute | solution.py:29
  25.7 1.1 %collective-permute-start.15 = (bf16[64,512]{1,0:T(8,128)(2,1)S(1)}, bf16[64,512]{1,0:T(8,128)(2,1)S(1)}, u32[]{:S(2)}, u32[]{:S(2)}) collective-permute-start(bf16[64,512]{1,0:T(8,128)(2,1)S(1)} %get-tuple-element.79), channel_id=1, source_target_pairs={{0,3},{1,2},{2,1},{3,0},{4,7},{5,6},{6,5},{7,4},{8,11},{9,10},{10,... | collective-permute-start | bytes 196616 | tf_op jit(solution)/shard_map/ppermute | solution.py:29
  26.8 0.4 collective-permute-start.16
  27.2 1.8 %collective-permute-start.17 = (bf16[64,512]{1,0:T(8,128)(2,1)S(1)}, bf16[64,512]{1,0:T(8,128)(2,1)S(1)}, u32[]{:S(2)}, u32[]{:S(2)}) collective-permute-start(bf16[64,512]{1,0:T(8,128)(2,1)S(1)} %get-tuple-element.81), channel_id=1, source_target_pairs={{0,7},{1,6},{2,5},{3,4},{4,3},{5,2},{6,1},{7,0},{8,15},{9,14},{10,... | collective-permute-start | bytes 196616 | tf_op jit(solution)/shard_map/ppermute | solution.py:29
  28.9 0.7 collective-permute-done.15.refs_2_
  29.6 1.0 %collective-permute-done.16.refs_3_ = bf16[64,512]{1,0:T(8,128)(2,1)S(1)} collective-permute-done((bf16[64,512]{1,0:T(8,128)(2,1)S(1)}, bf16[64,512]{1,0:T(8,128)(2,1)S(1)}, u32[]{:S(2)}, u32[]{:S(2)}) %collective-permute-start.16) | collective-permute-done | bytes 65568 | tf_op jit(solution)/shard_map/ppermute | solution.py:29
  30.6 1.6 %collective-permute-done.17.refs_4_ = bf16[64,512]{1,0:T(8,128)(2,1)S(1)} collective-permute-done((bf16[64,512]{1,0:T(8,128)(2,1)S(1)}, bf16[64,512]{1,0:T(8,128)(2,1)S(1)}, u32[]{:S(2)}, u32[]{:S(2)}) %collective-permute-start.17) | collective-permute-done | bytes 65568 | tf_op jit(solution)/shard_map/ppermute | solution.py:29
  32.5 2.7 %collective-permute-start.26 = (bf16[2,24,512]{2,1,0:T(8,128)(2,1)S(1)}, bf16[2,24,512]{2,1,0:T(8,128)(2,1)S(1)}, u32[]{:S(2)}, u32[]{:S(2)}) collective-permute-start(bf16[2,24,512]{2,1,0:T(8,128)(2,1)S(1)} %get-tuple-element.87), channel_id=1, source_target_pairs={{0,16},{8,24},{16,0},{24,8},{1,17},{9,25},{17,1},{25,9},{2,18},{10... | collective-permute-start | bytes 147464 | tf_op jit(solution)/shard_map/ppermute | solution.py:29
  35.1 1.3 %collective-permute-start.27 = (bf16[2,24,512]{2,1,0:T(8,128)(2,1)S(1)}, bf16[2,24,512]{2,1,0:T(8,128)(2,1)S(1)}, u32[]{:S(2)}, u32[]{:S(2)}) collective-permute-start(bf16[2,24,512]{2,1,0:T(8,128)(2,1)S(1)} %get-tuple-element.88), channel_id=1, source_target_pairs={{0,24},{8,16},{16,8},{24,0},{1,25},{9,17},{17,9},{25,1},{2,26},{10... | collective-permute-start | bytes 147464 | tf_op jit(solution)/shard_map/ppermute | solution.py:29
  36.7 1.9 %collective-permute-done.26.refs_0_ = bf16[2,24,512]{2,1,0:T(8,128)(2,1)S(1)} collective-permute-done((bf16[2,24,512]{2,1,0:T(8,128)(2,1)S(1)}, bf16[2,24,512]{2,1,0:T(8,128)(2,1)S(1)}, u32[]{:S(2)}, u32[]{:S(2)}) %collective-permute-start.26) | collective-permute-done | bytes 49184 | tf_op jit(solution)/shard_map/ppermute | solution.py:29
  38.6 2.5 %collective-permute-done.27.refs_1_ = bf16[2,24,512]{2,1,0:T(8,128)(2,1)S(1)} collective-permute-done((bf16[2,24,512]{2,1,0:T(8,128)(2,1)S(1)}, bf16[2,24,512]{2,1,0:T(8,128)(2,1)S(1)}, u32[]{:S(2)}, u32[]{:S(2)}) %collective-permute-start.27) | collective-permute-done | bytes 49184 | tf_op jit(solution)/shard_map/ppermute | solution.py:29
  41.2 1.9 %collective-permute-start.31 = (bf16[2,48,512]{2,1,0:T(8,128)(2,1)S(1)}, bf16[2,48,512]{2,1,0:T(8,128)(2,1)S(1)}, u32[]{:S(2)}, u32[]{:S(2)}) collective-permute-start(bf16[2,48,512]{2,1,0:T(8,128)(2,1)S(1)} %shard_map.239.refs_4_), channel_id=1, source_target_pairs={{0,5},{1,4},{2,7},{3,6},{4,1},{5,0},{6,3},{7,2},{8,13},{9,12},{10,... | collective-permute-start | bytes 294920 | tf_op jit(solution)/shard_map/ppermute | solution.py:29
  43.0 0.8 collective-permute-start.33
  43.9 1.6 %collective-permute-start.20 = (bf16[2,48,512]{2,1,0:T(8,128)(2,1)S(1)}, bf16[2,48,512]{2,1,0:T(8,128)(2,1)S(1)}, u32[]{:S(2)}, u32[]{:S(2)}) collective-permute-start(bf16[2,48,512]{2,1,0:T(8,128)(2,1)S(1)} %shard_map.238.refs_0_), channel_id=1, source_target_pairs={{0,3},{1,2},{2,1},{3,0},{4,7},{5,6},{6,5},{7,4},{8,11},{9,10},{10,... | collective-permute-start | bytes 294920 | tf_op jit(solution)/shard_map/ppermute | solution.py:29
  45.8 0.4 collective-permute-done.29.refs_5_
  46.1 1.3 %collective-permute-start.24 = (bf16[2,48,512]{2,1,0:T(8,128)(2,1)S(1)}, bf16[2,48,512]{2,1,0:T(8,128)(2,1)S(1)}, u32[]{:S(2)}, u32[]{:S(2)}) collective-permute-start(bf16[2,48,512]{2,1,0:T(8,128)(2,1)S(1)} %shard_map.238.refs_0_), channel_id=1, source_target_pairs={{0,7},{1,6},{2,5},{3,4},{4,3},{5,2},{6,1},{7,0},{8,15},{9,14},{10,... | collective-permute-start | bytes 294920 | tf_op jit(solution)/shard_map/ppermute | solution.py:29
  47.4 0.5 collective-permute-start.28
  48.0 1.2 %collective-permute-done.33.refs_7_ = bf16[2,48,512]{2,1,0:T(8,128)(2,1)S(1)} collective-permute-done((bf16[2,48,512]{2,1,0:T(8,128)(2,1)S(1)}, bf16[2,48,512]{2,1,0:T(8,128)(2,1)S(1)}, u32[]{:S(2)}, u32[]{:S(2)}) %collective-permute-start.33) | collective-permute-done | bytes 98336 | tf_op jit(solution)/shard_map/ppermute | solution.py:29
  49.1 1.4 %collective-permute-done.20.refs_1_ = bf16[2,48,512]{2,1,0:T(8,128)(2,1)S(1)} collective-permute-done((bf16[2,48,512]{2,1,0:T(8,128)(2,1)S(1)}, bf16[2,48,512]{2,1,0:T(8,128)(2,1)S(1)}, u32[]{:S(2)}, u32[]{:S(2)}) %collective-permute-start.20) | collective-permute-done | bytes 98336 | tf_op jit(solution)/shard_map/ppermute | solution.py:29
  50.5 0.6 collective-permute-done.22.refs_2_
  51.2 2.0 %collective-permute-done.24.refs_3_ = bf16[2,48,512]{2,1,0:T(8,128)(2,1)S(1)} collective-permute-done((bf16[2,48,512]{2,1,0:T(8,128)(2,1)S(1)}, bf16[2,48,512]{2,1,0:T(8,128)(2,1)S(1)}, u32[]{:S(2)}, u32[]{:S(2)}) %collective-permute-start.24) | collective-permute-done | bytes 98336 | tf_op jit(solution)/shard_map/ppermute | solution.py:29
  53.3 0.4 collective-permute-start.21
  53.9 0.4 collective-permute-start.25
  54.3 1.6 %shard_map.241.refs_11_ = bf16[256,4096]{1,0:T(8,128)(2,1)S(1)} custom-call(bf16[512,4096]{1,0:T(8,128)(2,1)} %bitcast.13), custom_call_target="tpu_custom_call" | custom-call | flops 10000000 | bytes 1000000 | tf_op jit(solution)/shard_map/pallas_call | solution.py:280
  55.8 2.9 %shard_map.240 = (bf16[512,4096]{1,0:T(8,128)(2,1)S(1)}, bf16[256,4096]{1,0:T(8,128)(2,1)S(1)}) custom-call(bf16[512,4096]{1,0:T(8,128)(2,1)} %bitcast.15, bf16[512,4096]{1,0:T(8,128)(2,1)} %bitcast.14), custom_call_target="tpu_custom_call" | custom-call | flops 10000000 | bytes 1000000 | tf_op jit(solution)/shard_map/pallas_call | solution.py:280
  58.7 2.2 %shard_map.242.refs_12_.down_w = bf16[512,4096]{1,0:T(8,128)(2,1)S(1)} custom-call(bf16[512,4096]{1,0:T(8,128)(2,1)} %bitcast.16), custom_call_target="tpu_custom_call" | custom-call | flops 10000000 | bytes 1000000 | tf_op jit(solution)/shard_map/pallas_call | solution.py:280
  61.0 1.3 %shard_map.243 = (f32[2,96,256]{2,1,0:T(8,128)S(1)}, f32[2,256,96]{2,1,0:T(8,128)S(1)}, f32[2,96,128]{2,1,0:T(8,128)S(1)}) custom-call(bf16[2,48,512]{2,1,0:T(8,128)(2,1)S(1)} %shard_map.238.refs_0_, bf16[2,48,512]{2,1,0:T(8,128)(2,1)S(1)} %collective-permute-done.20.refs_1_, bf16[2,48,512]{2,1,0:T(8,128)(2,1)S(1)} %collective-permute-done.22.refs_2_, ...), custom_call_target="tpu_custom_call" | custom-call | flops 10000000 | bytes 1000000 | tf_op jit(solution)/shard_map/pallas_call | solution.py:574
  62.3 2.0 %shard_map.244 = (bf16[2,96,256]{2,1,0:T(8,128)(2,1)S(1)}, bf16[4,2,48,512]{3,2,1,0:T(8,128)(2,1)S(1)}) custom-call(bf16[2,48,512]{2,1,0:T(8,128)(2,1)S(1)} %collective-permute-done.19.refs_0_, bf16[2,48,512]{2,1,0:T(8,128)(2,1)S(1)} %collective-permute-done.21.refs_1_, bf16[2,48,512]{2,1,0:T(8,128)(2,1)S(1)} %collective-permute-done.23.refs_2_, ...), custom_call_target="tpu_custom_call" | custom-call | flops 10000000 | bytes 1000000 | tf_op jit(solution)/shard_map/pallas_call | solution.py:580
  64.5 1.2 %shard_map.245 = (bf16[4,2,48,512]{3,2,1,0:T(8,128)(2,1)S(1)}, bf16[4,2,48,512]{3,2,1,0:T(8,128)(2,1)S(1)}, bf16[4,2,48,512]{3,2,1,0:T(8,128)(2,1)S(1)}) custom-call(bf16[2,96,256]{2,1,0:T(8,128)(2,1)S(1)} %get-tuple-element.95.hidden, bf16[512,4096]{1,0:T(8,128)(2,1)S(1)} %shard_map.242.refs_12_.down_w), custom_call_target="tpu_custom_call" | custom-call | flops 10000000 | bytes 1000000 | tf_op jit(solution)/shard_map/pallas_call | solution.py:586
  65.7 0.5 collective-permute-start.35
  66.2 0.6 collective-permute-start.41
  66.9 1.2 %collective-permute-start.42 = (bf16[2,48,512]{2,1,0:T(8,128)(2,1)S(1)}, bf16[2,48,512]{2,1,0:T(8,128)(2,1)S(1)}, u32[]{:S(2)}, u32[]{:S(2)}) collective-permute-start(bf16[2,48,512]{2,1,0:T(8,128)(2,1)S(1)} %get-tuple-element.108), channel_id=1, source_target_pairs={{0,5},{1,4},{2,7},{3,6},{4,1},{5,0},{6,3},{7,2},{8,13},{9,12},{10,... | collective-permute-start | bytes 294920 | tf_op jit(solution)/shard_map/ppermute | solution.py:29
  68.1 1.1 %collective-permute-start.43 = (bf16[2,48,512]{2,1,0:T(8,128)(2,1)S(1)}, bf16[2,48,512]{2,1,0:T(8,128)(2,1)S(1)}, u32[]{:S(2)}, u32[]{:S(2)}) collective-permute-start(bf16[2,48,512]{2,1,0:T(8,128)(2,1)S(1)} %get-tuple-element.109), channel_id=1, source_target_pairs={{0,7},{1,6},{2,5},{3,4},{4,3},{5,2},{6,1},{7,0},{8,15},{9,14},{10,... | collective-permute-start | bytes 294920 | tf_op jit(solution)/shard_map/ppermute | solution.py:29
  69.3 0.9 %collective-permute-start.36 = (bf16[2,48,512]{2,1,0:T(8,128)(2,1)S(1)}, bf16[2,48,512]{2,1,0:T(8,128)(2,1)S(1)}, u32[]{:S(2)}, u32[]{:S(2)}) collective-permute-start(bf16[2,48,512]{2,1,0:T(8,128)(2,1)S(1)} %get-tuple-element.99), channel_id=1, source_target_pairs={{0,3},{1,2},{2,1},{3,0},{4,7},{5,6},{6,5},{7,4},{8,11},{9,10},{10,... | collective-permute-start | bytes 294920 | tf_op jit(solution)/shard_map/ppermute | solution.py:29
  70.3 0.9 %collective-permute-start.37 = (bf16[2,48,512]{2,1,0:T(8,128)(2,1)S(1)}, bf16[2,48,512]{2,1,0:T(8,128)(2,1)S(1)}, u32[]{:S(2)}, u32[]{:S(2)}) collective-permute-start(bf16[2,48,512]{2,1,0:T(8,128)(2,1)S(1)} %get-tuple-element.100), channel_id=1, source_target_pairs={{0,5},{1,4},{2,7},{3,6},{4,1},{5,0},{6,3},{7,2},{8,13},{9,12},{10,... | collective-permute-start | bytes 294920 | tf_op jit(solution)/shard_map/ppermute | solution.py:29
  71.1 1.5 %collective-permute-start.38 = (bf16[2,48,512]{2,1,0:T(8,128)(2,1)S(1)}, bf16[2,48,512]{2,1,0:T(8,128)(2,1)S(1)}, u32[]{:S(2)}, u32[]{:S(2)}) collective-permute-start(bf16[2,48,512]{2,1,0:T(8,128)(2,1)S(1)} %get-tuple-element.101), channel_id=1, source_target_pairs={{0,7},{1,6},{2,5},{3,4},{4,3},{5,2},{6,1},{7,0},{8,15},{9,14},{10,... | collective-permute-start | bytes 294920 | tf_op jit(solution)/shard_map/ppermute | solution.py:29
  72.7 1.2 %collective-permute-done.43.refs_3_ = bf16[2,48,512]{2,1,0:T(8,128)(2,1)S(1)} collective-permute-done((bf16[2,48,512]{2,1,0:T(8,128)(2,1)S(1)}, bf16[2,48,512]{2,1,0:T(8,128)(2,1)S(1)}, u32[]{:S(2)}, u32[]{:S(2)}) %collective-permute-start.43) | collective-permute-done | bytes 98336 | tf_op jit(solution)/shard_map/ppermute | solution.py:29
  73.9 2.0 %collective-permute-start.44 = (bf16[2,24,512]{2,1,0:T(8,128)(2,1)S(1)}, bf16[2,24,512]{2,1,0:T(8,128)(2,1)S(1)}, u32[]{:S(2)}, u32[]{:S(2)}) collective-permute-start(bf16[2,24,512]{2,1,0:T(8,128)(2,1)S(1)} %get-tuple-element.110), channel_id=1, source_target_pairs={{0,16},{8,24},{16,0},{24,8},{1,17},{9,25},{17,1},{25,9},{2,18},{10... | collective-permute-start | bytes 147464 | tf_op jit(solution)/shard_map/ppermute | solution.py:29
  75.9 0.6 collective-permute-start.45
  76.6 1.5 %collective-permute-done.38.refs_3_ = bf16[2,48,512]{2,1,0:T(8,128)(2,1)S(1)} collective-permute-done((bf16[2,48,512]{2,1,0:T(8,128)(2,1)S(1)}, bf16[2,48,512]{2,1,0:T(8,128)(2,1)S(1)}, u32[]{:S(2)}, u32[]{:S(2)}) %collective-permute-start.38) | collective-permute-done | bytes 98336 | tf_op jit(solution)/shard_map/ppermute | solution.py:29
  78.1 0.3 collective-permute-start.39
  78.4 2.1 %shard_map.251 = (f32[64,16,64]{2,1,0:T(8,128)}, f32[64,16,64]{2,1,0:T(8,128)}) custom-call(bf16[64,256]{1,0:T(8,128)(2,1)S(1)} %get-tuple-element.112.driven, f32[64,1024]{1,0:T(8,128)S(1)} %get-tuple-element.113.dec_r, f32[64,1024]{1,0:T(8,128)S(1)} %get-tuple-element.114.dec_i, bf16[256,512]{1,0:T(8,128)(2,1)S(1)} %get-tuple-element.115.bt_r, ...), custom_call_target="tpu_custom_call" | custom-call | flops 10000000 | bytes 1000000 | tf_op jit(solution)/shard_map/pallas_call | solution.py:601
  80.6 1.8 %collective-permute-done.45.refs_6_ = bf16[2,24,512]{2,1,0:T(8,128)(2,1)S(1)} collective-permute-done((bf16[2,24,512]{2,1,0:T(8,128)(2,1)S(1)}, bf16[2,24,512]{2,1,0:T(8,128)(2,1)S(1)}, u32[]{:S(2)}, u32[]{:S(2)}) %collective-permute-start.45) | collective-permute-done | bytes 49184 | tf_op jit(solution)/shard_map/ppermute | solution.py:29
  82.4 0.6 collective-permute-done.39.refs_4_
  83.0 0.9 %shard_map.250 = bf16[64,512]{1,0:T(8,128)(2,1)} custom-call(bf16[64,512]{1,0:T(8,128)(2,1)S(1)} %get-tuple-element.83.refs_0_, bf16[2,64,192]{2,1,0:T(8,128)(2,1)S(1)} %get-tuple-element.84.refs_1_, f32[2,64]{1,0:T(2,128)S(1)} %bitcast.12, bf16[2,24,512]{2,1,0:T(8,128)(2,1)S(1)} %get-tuple-element.102.refs_3_, ...), custom_call_target="tpu_custom_call" | custom-call | flops 10000000 | bytes 1000000 | tf_op jit(solution)/shard_map/pallas_call | solution.py:607
  (53 shorter events, 2.9 us)
Async XLA Ops:
  0.6 5.3 %collective-permute-start.1 = (bf16[64,512]{1,0:T(8,128)(2,1)}, bf16[64,512]{1,0:T(8,128)(2,1)S(1)}, u32[]{:S(2)}, u32[]{:S(2)}) collective-permute-start(bf16[64,512]{1,0:T(8,128)(2,1)} %refs_15_.1), channel_id=1, source_target_pairs={{0,3},{1,2},{2,1},{3,0},{4,7},{5,6},{6,5},{7,4},{8,11},{9,10},{10,... | collective-permute-start | bytes 196616 | tf_op jit(solution)/shard_map/ppermute | solution.py:29
  3.1 4.0 %collective-permute-start.3 = (bf16[64,512]{1,0:T(8,128)(2,1)}, bf16[64,512]{1,0:T(8,128)(2,1)S(1)}, u32[]{:S(2)}, u32[]{:S(2)}) collective-permute-start(bf16[64,512]{1,0:T(8,128)(2,1)} %refs_15_.1), channel_id=1, source_target_pairs={{0,5},{1,4},{2,7},{3,6},{4,1},{5,0},{6,3},{7,2},{8,13},{9,12},{10,... | collective-permute-start | bytes 196616 | tf_op jit(solution)/shard_map/ppermute | solution.py:29
  4.9 5.5 %collective-permute-start.5 = (bf16[64,512]{1,0:T(8,128)(2,1)}, bf16[64,512]{1,0:T(8,128)(2,1)S(1)}, u32[]{:S(2)}, u32[]{:S(2)}) collective-permute-start(bf16[64,512]{1,0:T(8,128)(2,1)} %refs_15_.1), channel_id=1, source_target_pairs={{0,7},{1,6},{2,5},{3,4},{4,3},{5,2},{6,1},{7,0},{8,15},{9,14},{10,... | collective-permute-start | bytes 196616 | tf_op jit(solution)/shard_map/ppermute | solution.py:29
  4.9 9.7 %collective-permute-start = (bf16[64,512]{1,0:T(8,128)(2,1)}, bf16[64,512]{1,0:T(8,128)(2,1)S(1)}, u32[]{:S(2)}, u32[]{:S(2)}) collective-permute-start(bf16[64,512]{1,0:T(8,128)(2,1)} %refs_15_.1), channel_id=1, source_target_pairs={{0,1},{1,0},{2,3},{3,2},{4,5},{5,4},{6,7},{7,6},{8,9},{9,8},{10,11... | collective-permute-start | bytes 196616 | tf_op jit(solution)/shard_map/ppermute | solution.py:29
  5.9 8.8 %collective-permute-start.2 = (bf16[64,512]{1,0:T(8,128)(2,1)S(1)}, bf16[64,512]{1,0:T(8,128)(2,1)S(1)}, u32[]{:S(2)}, u32[]{:S(2)}) collective-permute-start(bf16[64,512]{1,0:T(8,128)(2,1)S(1)} %collective-permute-done.1.refs_1_), channel_id=1, source_target_pairs={{0,1},{1,0},{2,3},{3,2},{4,5},{5,4},{6,7},{7,6},{8,9},{9,8},{10,11... | collective-permute-start | bytes 196616 | tf_op jit(solution)/shard_map/ppermute | solution.py:29
  7.1 7.6 %collective-permute-start.4 = (bf16[64,512]{1,0:T(8,128)(2,1)S(1)}, bf16[64,512]{1,0:T(8,128)(2,1)S(1)}, u32[]{:S(2)}, u32[]{:S(2)}) collective-permute-start(bf16[64,512]{1,0:T(8,128)(2,1)S(1)} %collective-permute-done.3.refs_2_), channel_id=1, source_target_pairs={{0,1},{1,0},{2,3},{3,2},{4,5},{5,4},{6,7},{7,6},{8,9},{9,8},{10,11... | collective-permute-start | bytes 196616 | tf_op jit(solution)/shard_map/ppermute | solution.py:29
  10.4 4.3 %collective-permute-start.6 = (bf16[64,512]{1,0:T(8,128)(2,1)S(1)}, bf16[64,512]{1,0:T(8,128)(2,1)S(1)}, u32[]{:S(2)}, u32[]{:S(2)}) collective-permute-start(bf16[64,512]{1,0:T(8,128)(2,1)S(1)} %collective-permute-done.5.refs_3_), channel_id=1, source_target_pairs={{0,1},{1,0},{2,3},{3,2},{4,5},{5,4},{6,7},{7,6},{8,9},{9,8},{10,11... | collective-permute-start | bytes 196616 | tf_op jit(solution)/shard_map/ppermute | solution.py:29
  15.3 3.4 %collective-permute-start.10 = (bf16[64,256]{1,0:T(8,128)(2,1)S(1)}, bf16[64,256]{1,0:T(8,128)(2,1)S(1)}, u32[]{:S(2)}, u32[]{:S(2)}) collective-permute-start(bf16[64,256]{1,0:T(8,128)(2,1)S(1)} %get-tuple-element.70.refs_0_.refs_4_), channel_id=1, source_target_pairs={{0,5},{1,4},{2,7},{3,6},{4,1},{5,0},{6,3},{7,2},{8,13},{9,12},{10,... | collective-permute-start | bytes 98312 | tf_op jit(solution)/shard_map/ppermute | solution.py:29
  15.8 4.3 %collective-permute-start.12 = (bf16[64,256]{1,0:T(8,128)(2,1)S(1)}, bf16[64,256]{1,0:T(8,128)(2,1)S(1)}, u32[]{:S(2)}, u32[]{:S(2)}) collective-permute-start(bf16[64,256]{1,0:T(8,128)(2,1)S(1)} %get-tuple-element.70.refs_0_.refs_4_), channel_id=1, source_target_pairs={{0,7},{1,6},{2,5},{3,4},{4,3},{5,2},{6,1},{7,0},{8,15},{9,14},{10,... | collective-permute-start | bytes 98312 | tf_op jit(solution)/shard_map/ppermute | solution.py:29
  17.0 3.9 %collective-permute-start.8 = (bf16[64,256]{1,0:T(8,128)(2,1)S(1)}, bf16[64,256]{1,0:T(8,128)(2,1)S(1)}, u32[]{:S(2)}, u32[]{:S(2)}) collective-permute-start(bf16[64,256]{1,0:T(8,128)(2,1)S(1)} %get-tuple-element.70.refs_0_.refs_4_), channel_id=1, source_target_pairs={{0,3},{1,2},{2,1},{3,0},{4,7},{5,6},{6,5},{7,4},{8,11},{9,10},{10,... | collective-permute-start | bytes 98312 | tf_op jit(solution)/shard_map/ppermute | solution.py:29
  18.6 4.8 %collective-permute-start.7 = (bf16[64,256]{1,0:T(8,128)(2,1)S(1)}, bf16[64,256]{1,0:T(8,128)(2,1)S(1)}, u32[]{:S(2)}, u32[]{:S(2)}) collective-permute-start(bf16[64,256]{1,0:T(8,128)(2,1)S(1)} %get-tuple-element.70.refs_0_.refs_4_), channel_id=1, source_target_pairs={{0,1},{1,0},{2,3},{3,2},{4,5},{5,4},{6,7},{7,6},{8,9},{9,8},{10,11... | collective-permute-start | bytes 98312 | tf_op jit(solution)/shard_map/ppermute | solution.py:29
  18.7 4.7 %collective-permute-start.11 = (bf16[64,256]{1,0:T(8,128)(2,1)S(1)}, bf16[64,256]{1,0:T(8,128)(2,1)S(1)}, u32[]{:S(2)}, u32[]{:S(2)}) collective-permute-start(bf16[64,256]{1,0:T(8,128)(2,1)S(1)} %collective-permute-done.10.refs_2_), channel_id=1, source_target_pairs={{0,1},{1,0},{2,3},{3,2},{4,5},{5,4},{6,7},{7,6},{8,9},{9,8},{10,11... | collective-permute-start | bytes 98312 | tf_op jit(solution)/shard_map/ppermute | solution.py:29
  20.1 3.3 %collective-permute-start.13 = (bf16[64,256]{1,0:T(8,128)(2,1)S(1)}, bf16[64,256]{1,0:T(8,128)(2,1)S(1)}, u32[]{:S(2)}, u32[]{:S(2)}) collective-permute-start(bf16[64,256]{1,0:T(8,128)(2,1)S(1)} %collective-permute-done.12.refs_3_), channel_id=1, source_target_pairs={{0,1},{1,0},{2,3},{3,2},{4,5},{5,4},{6,7},{7,6},{8,9},{9,8},{10,11... | collective-permute-start | bytes 98312 | tf_op jit(solution)/shard_map/ppermute | solution.py:29
  21.0 2.5 %collective-permute-start.9 = (bf16[64,256]{1,0:T(8,128)(2,1)S(1)}, bf16[64,256]{1,0:T(8,128)(2,1)S(1)}, u32[]{:S(2)}, u32[]{:S(2)}) collective-permute-start(bf16[64,256]{1,0:T(8,128)(2,1)S(1)} %collective-permute-done.8.refs_1_), channel_id=1, source_target_pairs={{0,1},{1,0},{2,3},{3,2},{4,5},{5,4},{6,7},{7,6},{8,9},{9,8},{10,11... | collective-permute-start | bytes 98312 | tf_op jit(solution)/shard_map/ppermute | solution.py:29
  24.0 1.6 %collective-permute-start.14 = (bf16[4,64,512]{2,1,0:T(8,128)(2,1)S(1)}, bf16[4,64,512]{2,1,0:T(8,128)(2,1)S(1)}, u32[]{:S(2)}, u32[]{:S(2)}) collective-permute-start(bf16[4,64,512]{2,1,0:T(8,128)(2,1)S(1)} %get-tuple-element.77), channel_id=1, source_target_pairs={{0,1},{1,0},{2,3},{3,2},{4,5},{5,4},{6,7},{7,6},{8,9},{9,8},{10,11... | collective-permute-start | bytes 786440 | tf_op jit(solution)/shard_map/ppermute | solution.py:29
  25.7 3.9 %collective-permute-start.15 = (bf16[64,512]{1,0:T(8,128)(2,1)S(1)}, bf16[64,512]{1,0:T(8,128)(2,1)S(1)}, u32[]{:S(2)}, u32[]{:S(2)}) collective-permute-start(bf16[64,512]{1,0:T(8,128)(2,1)S(1)} %get-tuple-element.79), channel_id=1, source_target_pairs={{0,3},{1,2},{2,1},{3,0},{4,7},{5,6},{6,5},{7,4},{8,11},{9,10},{10,... | collective-permute-start | bytes 196616 | tf_op jit(solution)/shard_map/ppermute | solution.py:29
  26.8 3.8 %collective-permute-start.16 = (bf16[64,512]{1,0:T(8,128)(2,1)S(1)}, bf16[64,512]{1,0:T(8,128)(2,1)S(1)}, u32[]{:S(2)}, u32[]{:S(2)}) collective-permute-start(bf16[64,512]{1,0:T(8,128)(2,1)S(1)} %get-tuple-element.80), channel_id=1, source_target_pairs={{0,5},{1,4},{2,7},{3,6},{4,1},{5,0},{6,3},{7,2},{8,13},{9,12},{10,... | collective-permute-start | bytes 196616 | tf_op jit(solution)/shard_map/ppermute | solution.py:29
  27.2 5.1 %collective-permute-start.17 = (bf16[64,512]{1,0:T(8,128)(2,1)S(1)}, bf16[64,512]{1,0:T(8,128)(2,1)S(1)}, u32[]{:S(2)}, u32[]{:S(2)}) collective-permute-start(bf16[64,512]{1,0:T(8,128)(2,1)S(1)} %get-tuple-element.81), channel_id=1, source_target_pairs={{0,7},{1,6},{2,5},{3,4},{4,3},{5,2},{6,1},{7,0},{8,15},{9,14},{10,... | collective-permute-start | bytes 196616 | tf_op jit(solution)/shard_map/ppermute | solution.py:29
  32.5 6.1 %collective-permute-start.26 = (bf16[2,24,512]{2,1,0:T(8,128)(2,1)S(1)}, bf16[2,24,512]{2,1,0:T(8,128)(2,1)S(1)}, u32[]{:S(2)}, u32[]{:S(2)}) collective-permute-start(bf16[2,24,512]{2,1,0:T(8,128)(2,1)S(1)} %get-tuple-element.87), channel_id=1, source_target_pairs={{0,16},{8,24},{16,0},{24,8},{1,17},{9,25},{17,1},{25,9},{2,18},{10... | collective-permute-start | bytes 147464 | tf_op jit(solution)/shard_map/ppermute | solution.py:29
  35.1 6.0 %collective-permute-start.27 = (bf16[2,24,512]{2,1,0:T(8,128)(2,1)S(1)}, bf16[2,24,512]{2,1,0:T(8,128)(2,1)S(1)}, u32[]{:S(2)}, u32[]{:S(2)}) collective-permute-start(bf16[2,24,512]{2,1,0:T(8,128)(2,1)S(1)} %get-tuple-element.88), channel_id=1, source_target_pairs={{0,24},{8,16},{16,8},{24,0},{1,25},{9,17},{17,9},{25,1},{2,26},{10... | collective-permute-start | bytes 147464 | tf_op jit(solution)/shard_map/ppermute | solution.py:29
  36.5 7.4 %collective-permute-start.18 = (bf16[2,24,512]{2,1,0:T(8,128)(2,1)S(1)}, bf16[2,24,512]{2,1,0:T(8,128)(2,1)S(1)}, u32[]{:S(2)}, u32[]{:S(2)}) collective-permute-start(bf16[2,24,512]{2,1,0:T(8,128)(2,1)S(1)} %get-tuple-element.86), channel_id=1, source_target_pairs={{0,8},{8,0},{16,24},{24,16},{1,9},{9,1},{17,25},{25,17},{2,10},{10... | collective-permute-start | bytes 147464 | tf_op jit(solution)/shard_map/ppermute | solution.py:29
  41.1 5.0 %collective-permute-start.29 = (bf16[2,48,512]{2,1,0:T(8,128)(2,1)S(1)}, bf16[2,48,512]{2,1,0:T(8,128)(2,1)S(1)}, u32[]{:S(2)}, u32[]{:S(2)}) collective-permute-start(bf16[2,48,512]{2,1,0:T(8,128)(2,1)S(1)} %shard_map.239.refs_4_), channel_id=1, source_target_pairs={{0,3},{1,2},{2,1},{3,0},{4,7},{5,6},{6,5},{7,4},{8,11},{9,10},{10,... | collective-permute-start | bytes 294920 | tf_op jit(solution)/shard_map/ppermute | solution.py:29
  41.2 6.3 %collective-permute-start.31 = (bf16[2,48,512]{2,1,0:T(8,128)(2,1)S(1)}, bf16[2,48,512]{2,1,0:T(8,128)(2,1)S(1)}, u32[]{:S(2)}, u32[]{:S(2)}) collective-permute-start(bf16[2,48,512]{2,1,0:T(8,128)(2,1)S(1)} %shard_map.239.refs_4_), channel_id=1, source_target_pairs={{0,5},{1,4},{2,7},{3,6},{4,1},{5,0},{6,3},{7,2},{8,13},{9,12},{10,... | collective-permute-start | bytes 294920 | tf_op jit(solution)/shard_map/ppermute | solution.py:29
  43.0 6.1 %collective-permute-start.33 = (bf16[2,48,512]{2,1,0:T(8,128)(2,1)S(1)}, bf16[2,48,512]{2,1,0:T(8,128)(2,1)S(1)}, u32[]{:S(2)}, u32[]{:S(2)}) collective-permute-start(bf16[2,48,512]{2,1,0:T(8,128)(2,1)S(1)} %shard_map.239.refs_4_), channel_id=1, source_target_pairs={{0,7},{1,6},{2,5},{3,4},{4,3},{5,2},{6,1},{7,0},{8,15},{9,14},{10,... | collective-permute-start | bytes 294920 | tf_op jit(solution)/shard_map/ppermute | solution.py:29
  43.9 6.6 %collective-permute-start.20 = (bf16[2,48,512]{2,1,0:T(8,128)(2,1)S(1)}, bf16[2,48,512]{2,1,0:T(8,128)(2,1)S(1)}, u32[]{:S(2)}, u32[]{:S(2)}) collective-permute-start(bf16[2,48,512]{2,1,0:T(8,128)(2,1)S(1)} %shard_map.238.refs_0_), channel_id=1, source_target_pairs={{0,3},{1,2},{2,1},{3,0},{4,7},{5,6},{6,5},{7,4},{8,11},{9,10},{10,... | collective-permute-start | bytes 294920 | tf_op jit(solution)/shard_map/ppermute | solution.py:29
  45.5 5.7 %collective-permute-start.22 = (bf16[2,48,512]{2,1,0:T(8,128)(2,1)S(1)}, bf16[2,48,512]{2,1,0:T(8,128)(2,1)S(1)}, u32[]{:S(2)}, u32[]{:S(2)}) collective-permute-start(bf16[2,48,512]{2,1,0:T(8,128)(2,1)S(1)} %shard_map.238.refs_0_), channel_id=1, source_target_pairs={{0,5},{1,4},{2,7},{3,6},{4,1},{5,0},{6,3},{7,2},{8,13},{9,12},{10,... | collective-permute-start | bytes 294920 | tf_op jit(solution)/shard_map/ppermute | solution.py:29
  46.1 7.1 %collective-permute-start.24 = (bf16[2,48,512]{2,1,0:T(8,128)(2,1)S(1)}, bf16[2,48,512]{2,1,0:T(8,128)(2,1)S(1)}, u32[]{:S(2)}, u32[]{:S(2)}) collective-permute-start(bf16[2,48,512]{2,1,0:T(8,128)(2,1)S(1)} %shard_map.238.refs_0_), channel_id=1, source_target_pairs={{0,7},{1,6},{2,5},{3,4},{4,3},{5,2},{6,1},{7,0},{8,15},{9,14},{10,... | collective-permute-start | bytes 294920 | tf_op jit(solution)/shard_map/ppermute | solution.py:29
  47.4 5.9 %collective-permute-start.28 = (bf16[2,48,512]{2,1,0:T(8,128)(2,1)S(1)}, bf16[2,48,512]{2,1,0:T(8,128)(2,1)S(1)}, u32[]{:S(2)}, u32[]{:S(2)}) collective-permute-start(bf16[2,48,512]{2,1,0:T(8,128)(2,1)S(1)} %shard_map.239.refs_4_), channel_id=1, source_target_pairs={{0,1},{1,0},{2,3},{3,2},{4,5},{5,4},{6,7},{7,6},{8,9},{9,8},{10,11... | collective-permute-start | bytes 294920 | tf_op jit(solution)/shard_map/ppermute | solution.py:29
  49.1 4.6 %collective-permute-start.19 = (bf16[2,48,512]{2,1,0:T(8,128)(2,1)S(1)}, bf16[2,48,512]{2,1,0:T(8,128)(2,1)S(1)}, u32[]{:S(2)}, u32[]{:S(2)}) collective-permute-start(bf16[2,48,512]{2,1,0:T(8,128)(2,1)S(1)} %shard_map.238.refs_0_), channel_id=1, source_target_pairs={{0,1},{1,0},{2,3},{3,2},{4,5},{5,4},{6,7},{7,6},{8,9},{9,8},{10,11... | collective-permute-start | bytes 294920 | tf_op jit(solution)/shard_map/ppermute | solution.py:29
  50.5 3.4 %collective-permute-start.30 = (bf16[2,48,512]{2,1,0:T(8,128)(2,1)S(1)}, bf16[2,48,512]{2,1,0:T(8,128)(2,1)S(1)}, u32[]{:S(2)}, u32[]{:S(2)}) collective-permute-start(bf16[2,48,512]{2,1,0:T(8,128)(2,1)S(1)} %collective-permute-done.29.refs_5_), channel_id=1, source_target_pairs={{0,1},{1,0},{2,3},{3,2},{4,5},{5,4},{6,7},{7,6},{8,9},{9,8},{10,11... | collective-permute-start | bytes 294920 | tf_op jit(solution)/shard_map/ppermute | solution.py:29
  51.1 11.1 %collective-permute-start.32 = (bf16[2,48,512]{2,1,0:T(8,128)(2,1)S(1)}, bf16[2,48,512]{2,1,0:T(8,128)(2,1)S(1)}, u32[]{:S(2)}, u32[]{:S(2)}) collective-permute-start(bf16[2,48,512]{2,1,0:T(8,128)(2,1)S(1)} %collective-permute-done.31.refs_6_), channel_id=1, source_target_pairs={{0,1},{1,0},{2,3},{3,2},{4,5},{5,4},{6,7},{7,6},{8,9},{9,8},{10,11... | collective-permute-start | bytes 294920 | tf_op jit(solution)/shard_map/ppermute | solution.py:29
  53.2 9.0 %collective-permute-start.34 = (bf16[2,48,512]{2,1,0:T(8,128)(2,1)S(1)}, bf16[2,48,512]{2,1,0:T(8,128)(2,1)S(1)}, u32[]{:S(2)}, u32[]{:S(2)}) collective-permute-start(bf16[2,48,512]{2,1,0:T(8,128)(2,1)S(1)} %collective-permute-done.33.refs_7_), channel_id=1, source_target_pairs={{0,1},{1,0},{2,3},{3,2},{4,5},{5,4},{6,7},{7,6},{8,9},{9,8},{10,11... | collective-permute-start | bytes 294920 | tf_op jit(solution)/shard_map/ppermute | solution.py:29
  53.3 8.9 %collective-permute-start.21 = (bf16[2,48,512]{2,1,0:T(8,128)(2,1)S(1)}, bf16[2,48,512]{2,1,0:T(8,128)(2,1)S(1)}, u32[]{:S(2)}, u32[]{:S(2)}) collective-permute-start(bf16[2,48,512]{2,1,0:T(8,128)(2,1)S(1)} %collective-permute-done.20.refs_1_), channel_id=1, source_target_pairs={{0,1},{1,0},{2,3},{3,2},{4,5},{5,4},{6,7},{7,6},{8,9},{9,8},{10,11... | collective-permute-start | bytes 294920 | tf_op jit(solution)/shard_map/ppermute | solution.py:29
  53.7 8.5 %collective-permute-start.23 = (bf16[2,48,512]{2,1,0:T(8,128)(2,1)S(1)}, bf16[2,48,512]{2,1,0:T(8,128)(2,1)S(1)}, u32[]{:S(2)}, u32[]{:S(2)}) collective-permute-start(bf16[2,48,512]{2,1,0:T(8,128)(2,1)S(1)} %collective-permute-done.22.refs_2_), channel_id=1, source_target_pairs={{0,1},{1,0},{2,3},{3,2},{4,5},{5,4},{6,7},{7,6},{8,9},{9,8},{10,11... | collective-permute-start | bytes 294920 | tf_op jit(solution)/shard_map/ppermute | solution.py:29
  53.9 8.4 %collective-permute-start.25 = (bf16[2,48,512]{2,1,0:T(8,128)(2,1)S(1)}, bf16[2,48,512]{2,1,0:T(8,128)(2,1)S(1)}, u32[]{:S(2)}, u32[]{:S(2)}) collective-permute-start(bf16[2,48,512]{2,1,0:T(8,128)(2,1)S(1)} %collective-permute-done.24.refs_3_), channel_id=1, source_target_pairs={{0,1},{1,0},{2,3},{3,2},{4,5},{5,4},{6,7},{7,6},{8,9},{9,8},{10,11... | collective-permute-start | bytes 294920 | tf_op jit(solution)/shard_map/ppermute | solution.py:29
  64.3 1.9 %collective-permute-start.40 = (bf16[4,2,48,512]{3,2,1,0:T(8,128)(2,1)S(1)}, bf16[4,2,48,512]{3,2,1,0:T(8,128)(2,1)S(1)}, u32[]{:S(2)}, u32[]{:S(2)}) collective-permute-start(bf16[4,2,48,512]{3,2,1,0:T(8,128)(2,1)S(1)} %get-tuple-element.105), channel_id=1, source_target_pairs={{0,1},{1,0},{2,3},{3,2},{4,5},{5,4},{6,7},{7,6},{8,9},{9,8},{10,11... | collective-permute-start | bytes 1179656 | tf_op jit(solution)/shard_map/ppermute | solution.py:29
  65.7 17.3 %copy-start = (f32[64,2]{0,1:T(2,128)S(1)}, f32[64,2]{0,1:T(2,128)}, u32[]{:S(2)}) copy-start(f32[64,2]{0,1:T(2,128)} %param.40) | copy-start | bytes 1540
  65.7 3.6 %collective-permute-start.35 = (bf16[4,2,48,512]{3,2,1,0:T(8,128)(2,1)S(1)}, bf16[4,2,48,512]{3,2,1,0:T(8,128)(2,1)S(1)}, u32[]{:S(2)}, u32[]{:S(2)}) collective-permute-start(bf16[4,2,48,512]{3,2,1,0:T(8,128)(2,1)S(1)} %get-tuple-element.97), channel_id=1, source_target_pairs={{0,1},{1,0},{2,3},{3,2},{4,5},{5,4},{6,7},{7,6},{8,9},{9,8},{10,11... | collective-permute-start | bytes 1179656 | tf_op jit(solution)/shard_map/ppermute | solution.py:29
  66.2 4.9 %collective-permute-start.41 = (bf16[2,48,512]{2,1,0:T(8,128)(2,1)S(1)}, bf16[2,48,512]{2,1,0:T(8,128)(2,1)S(1)}, u32[]{:S(2)}, u32[]{:S(2)}) collective-permute-start(bf16[2,48,512]{2,1,0:T(8,128)(2,1)S(1)} %get-tuple-element.107), channel_id=1, source_target_pairs={{0,3},{1,2},{2,1},{3,0},{4,7},{5,6},{6,5},{7,4},{8,11},{9,10},{10,... | collective-permute-start | bytes 294920 | tf_op jit(solution)/shard_map/ppermute | solution.py:29
  66.9 5.9 %collective-permute-start.42 = (bf16[2,48,512]{2,1,0:T(8,128)(2,1)S(1)}, bf16[2,48,512]{2,1,0:T(8,128)(2,1)S(1)}, u32[]{:S(2)}, u32[]{:S(2)}) collective-permute-start(bf16[2,48,512]{2,1,0:T(8,128)(2,1)S(1)} %get-tuple-element.108), channel_id=1, source_target_pairs={{0,5},{1,4},{2,7},{3,6},{4,1},{5,0},{6,3},{7,2},{8,13},{9,12},{10,... | collective-permute-start | bytes 294920 | tf_op jit(solution)/shard_map/ppermute | solution.py:29
  68.1 5.8 %collective-permute-start.43 = (bf16[2,48,512]{2,1,0:T(8,128)(2,1)S(1)}, bf16[2,48,512]{2,1,0:T(8,128)(2,1)S(1)}, u32[]{:S(2)}, u32[]{:S(2)}) collective-permute-start(bf16[2,48,512]{2,1,0:T(8,128)(2,1)S(1)} %get-tuple-element.109), channel_id=1, source_target_pairs={{0,7},{1,6},{2,5},{3,4},{4,3},{5,2},{6,1},{7,0},{8,15},{9,14},{10,... | collective-permute-start | bytes 294920 | tf_op jit(solution)/shard_map/ppermute | solution.py:29
  69.3 7.2 %collective-permute-start.36 = (bf16[2,48,512]{2,1,0:T(8,128)(2,1)S(1)}, bf16[2,48,512]{2,1,0:T(8,128)(2,1)S(1)}, u32[]{:S(2)}, u32[]{:S(2)}) collective-permute-start(bf16[2,48,512]{2,1,0:T(8,128)(2,1)S(1)} %get-tuple-element.99), channel_id=1, source_target_pairs={{0,3},{1,2},{2,1},{3,0},{4,7},{5,6},{6,5},{7,4},{8,11},{9,10},{10,... | collective-permute-start | bytes 294920 | tf_op jit(solution)/shard_map/ppermute | solution.py:29
  70.3 6.3 %collective-permute-start.37 = (bf16[2,48,512]{2,1,0:T(8,128)(2,1)S(1)}, bf16[2,48,512]{2,1,0:T(8,128)(2,1)S(1)}, u32[]{:S(2)}, u32[]{:S(2)}) collective-permute-start(bf16[2,48,512]{2,1,0:T(8,128)(2,1)S(1)} %get-tuple-element.100), channel_id=1, source_target_pairs={{0,5},{1,4},{2,7},{3,6},{4,1},{5,0},{6,3},{7,2},{8,13},{9,12},{10,... | collective-permute-start | bytes 294920 | tf_op jit(solution)/shard_map/ppermute | solution.py:29
  71.1 6.9 %collective-permute-start.38 = (bf16[2,48,512]{2,1,0:T(8,128)(2,1)S(1)}, bf16[2,48,512]{2,1,0:T(8,128)(2,1)S(1)}, u32[]{:S(2)}, u32[]{:S(2)}) collective-permute-start(bf16[2,48,512]{2,1,0:T(8,128)(2,1)S(1)} %get-tuple-element.101), channel_id=1, source_target_pairs={{0,7},{1,6},{2,5},{3,4},{4,3},{5,2},{6,1},{7,0},{8,15},{9,14},{10,... | collective-permute-start | bytes 294920 | tf_op jit(solution)/shard_map/ppermute | solution.py:29
  73.9 6.6 %collective-permute-start.44 = (bf16[2,24,512]{2,1,0:T(8,128)(2,1)S(1)}, bf16[2,24,512]{2,1,0:T(8,128)(2,1)S(1)}, u32[]{:S(2)}, u32[]{:S(2)}) collective-permute-start(bf16[2,24,512]{2,1,0:T(8,128)(2,1)S(1)} %get-tuple-element.110), channel_id=1, source_target_pairs={{0,16},{8,24},{16,0},{24,8},{1,17},{9,25},{17,1},{25,9},{2,18},{10... | collective-permute-start | bytes 147464 | tf_op jit(solution)/shard_map/ppermute | solution.py:29
  75.9 6.5 %collective-permute-start.45 = (bf16[2,24,512]{2,1,0:T(8,128)(2,1)S(1)}, bf16[2,24,512]{2,1,0:T(8,128)(2,1)S(1)}, u32[]{:S(2)}, u32[]{:S(2)}) collective-permute-start(bf16[2,24,512]{2,1,0:T(8,128)(2,1)S(1)} %get-tuple-element.111), channel_id=1, source_target_pairs={{0,24},{8,16},{16,8},{24,0},{1,25},{9,17},{17,9},{25,1},{2,26},{10... | collective-permute-start | bytes 147464 | tf_op jit(solution)/shard_map/ppermute | solution.py:29
  78.1 4.9 %collective-permute-start.39 = (bf16[2,24,512]{2,1,0:T(8,128)(2,1)S(1)}, bf16[2,24,512]{2,1,0:T(8,128)(2,1)S(1)}, u32[]{:S(2)}, u32[]{:S(2)}) collective-permute-start(bf16[2,24,512]{2,1,0:T(8,128)(2,1)S(1)} %get-tuple-element.103), channel_id=1, source_target_pairs={{0,8},{8,0},{16,24},{24,16},{1,9},{9,1},{17,25},{25,17},{2,10},{10... | collective-permute-start | bytes 147464 | tf_op jit(solution)/shard_map/ppermute | solution.py:29

commit v5 on v4

--- a/solution.py
+++ b/solution.py
@@ -27,6 +27,12 @@
 
 def swap(x, axis, k):
     return lax.ppermute(x, axis, [(i, i ^ k) for i in range(lax.axis_size(axis))])
+
+
+def far_swap(x, j):
+    n = lax.axis_size("tp")
+    total = n * lax.axis_size("ep")
+    return lax.ppermute(x, ("ep", "tp"), [(i, i ^ (j * n + 1)) for i in range(total)])
 
 
 def crossings(n):
@@ -371,7 +377,7 @@
     gain, gate_w, up_low, up_high, g_ref, u_ref, square_ref = refs[n:]
     for i in range(near[0].shape[0]):
         g_ref[i], u_ref[i], square_ref[i] = expert_sums(
-            0, near, far, gain, gate_w, up_low, up_high, i, (0.0, 0.0, 0.0)
+            1, near, far, gain, gate_w, up_low, up_high, i, (0.0, 0.0, 0.0)
         )
 
 
@@ -382,7 +388,7 @@
     experts, count, width = near[0].shape
     for i in range(experts):
         start = (g_ref[i], u_ref[i], square_ref[i])
-        g, u, square = expert_sums(1, near, far, gain, gate_w, up_low, up_high, i, start)
+        g, u, square = expert_sums(0, near, far, gain, gate_w, up_low, up_high, i, start)
         scale = lax.rsqrt(jnp.sum(square, axis=1, keepdims=True) / (n * width) + norm_eps)
         hidden = (jax.nn.silu(g * scale) * (u.T * scale)).astype(bf16)
         later[i] = hidden
@@ -556,8 +562,9 @@
         limit=8 * 2**20,
     )(own, *terms, table)
 
-    arrived = [packed[0]] + [swap(packed[j], "ep", j) for j in range(1, m)]
     half = m // 2
+    arrived = [packed[0]] + [swap(packed[j], "ep", j) for j in range(1, half)]
+    arrived += [far_swap(packed[j], j) for j in range(half, m)]
     fragments = []
     for group in (arrived[:half], arrived[half:]):
         merged = call(
@@ -568,7 +575,8 @@
         )(*group)
         fragments += gather_swaps(merged, n)
     part = jax.ShapeDtypeStruct((n // 2, exp_dev, half * cap, wide), bf16)
-    near, far = fragments[:n], fragments[n:]
+    near = fragments[:n]
+    far = [fragments[n + (k ^ 1)] for k in range(n)]
     rows = 2 * half * cap
     weights = (gain2, gate_w, up_low, up_high)
     partial = call(
@@ -576,13 +584,13 @@
         [jax.ShapeDtypeStruct((exp_dev, *x), f32) for x in ((rows, hidden), (hidden, rows), (rows, LANES))],
         [WHOLE] * (n + 4),
         limit=8 * 2**20,
-    )(*[near[k] for k in crossings(n)], *[far[k] for k in crossings(n)], *weights)
+    )(*[near[k ^ 1] for k in crossings(n)], *[far[k ^ 1] for k in crossings(n)], *weights)
     later, far_partner = call(
         functools.partial(up_body, n),
         [jax.ShapeDtypeStruct((exp_dev, rows, hidden), bf16), part],
         [WHOLE] * (n + 8),
         limit=16 * 2**20,
-    )(*[near[k ^ 1] for k in crossings(n)], *[far[k ^ 1] for k in crossings(n)], *weights, down_w, *partial)
+    )(*[near[k] for k in crossings(n)], *[far[k] for k in crossings(n)], *weights, down_w, *partial)
     far_own, *near_outs = call(
         functools.partial(down_body, n), [part] * 3, [WHOLE] * 2, limit=8 * 2**20
     )(later, down_w)

time: 84 us -> 84.5 us (level)
  starting transfers between devices: 34.7 us -> 36.3 us
  waiting for transfers between devices: 25.6 us -> 24.5 us
    ppermute x46 -> x44, waiting for transfers between devices: 25.6 us -> 20.6 us  [swap(): lax.ppermute(x, axis, [(i, i ^ k) for i in range(lax.axis_size(axis))])]
    ppermute x0 -> x2, waiting for transfers between devices: none -> 3.94 us  [far_swap(): lax.ppermute(x, ('ep', 'tp'), [(i, i ^ j * n + 1) for i in range(total)])]
    ppermute x0 -> x2, starting transfers between devices: none -> 3.72 us  [far_swap(): lax.ppermute(x, ('ep', 'tp'), [(i, i ^ j * n + 1) for i in range(total)])]
    ppermute x46 -> x44, starting transfers between devices: 34.7 us -> 32.6 us  [swap(): lax.ppermute(x, axis, [(i, i ^ k) for i in range(lax.axis_size(axis))])]
  transfers between devices with their start and end apart: 46 -> 46, of which waited for: 21 -> 19; matrix products, arithmetic and copies ran while one was open for 0% -> 0% of each run, Pallas kernels for 22% -> 22%
where the time goes in v5:
time: 84.5 us; the launch traced here: 84.4 us
  starting transfers between devices  36.3 us (43%)
  waiting for transfers between devices  24.5 us (29%)
  Pallas kernels  22.6 us (27%)
  between operations  0.91 us (1%)
    ppermute x44, starting transfers between devices, swap(): lax.ppermute(x, axis, [(i, i ^ k) for i in range(lax.axis_size(axis))])  32.6 us
    ppermute x44, waiting for transfers between devices, swap(): lax.ppermute(x, axis, [(i, i ^ k) for i in range(lax.axis_size(axis))])  20.6 us
    pallas_call x4, Pallas kernels, fetch(): call(functools.partial(fetch_body, [x[1:] for x in sources]), [pltpu.VMEM...  8.7 us
    ppermute x2, waiting for transfers between devices, far_swap(): lax.ppermute(x, ('ep', 'tp'), [(i, i ^ j * n + 1) for i in range(total)])  3.94 us
    pallas_call x1, Pallas kernels, local_swaps(): call(functools.partial(prep_body, n, cap), [jax.ShapeDtypeStruct((count,...  3.73 us
    ppermute x2, starting transfers between devices, far_swap(): lax.ppermute(x, ('ep', 'tp'), [(i, i ^ j * n + 1) for i in range(total)])  3.72 us
    pallas_call x1, Pallas kernels, local_swaps(): call(state_body, [jax.ShapeDtypeStruct((count, groups, entries), f32)] *...  2.13 us
    pallas_call x1, Pallas kernels, local_swaps(): call(functools.partial(up_body, n), [jax.ShapeDtypeStruct((exp_dev, rows,...  1.98 us
  transfers between devices with their start and end apart: 46, of which 19 were waited for; matrix products, arithmetic and copies ran while one was open for 0% of the time, Pallas kernels for 22%

profile of v5, /device:TPU:0, one launch (start us, length us, event | category | flops | bytes accessed | tf_op | source)
XLA Modules:
  0.0 84.4 jit_solution(3235244053729715776)
XLA Ops:
  0.6 2.5 %collective-permute-start.1 = (bf16[64,512]{1,0:T(8,128)(2,1)}, bf16[64,512]{1,0:T(8,128)(2,1)S(1)}, u32[]{:S(2)}, u32[]{:S(2)}) collective-permute-start(bf16[64,512]{1,0:T(8,128)(2,1)} %refs_15_.1), channel_id=1, source_target_pairs={{0,3},{1,2},{2,1},{3,0},{4,7},{5,6},{6,5},{7,4},{8,11},{9,10},{10,... | collective-permute-start | bytes 196616 | tf_op jit(solution)/shard_map/ppermute | solution.py:29
  3.1 1.8 %collective-permute-start.3 = (bf16[64,512]{1,0:T(8,128)(2,1)}, bf16[64,512]{1,0:T(8,128)(2,1)S(1)}, u32[]{:S(2)}, u32[]{:S(2)}) collective-permute-start(bf16[64,512]{1,0:T(8,128)(2,1)} %refs_15_.1), channel_id=1, source_target_pairs={{0,5},{1,4},{2,7},{3,6},{4,1},{5,0},{6,3},{7,2},{8,13},{9,12},{10,... | collective-permute-start | bytes 196616 | tf_op jit(solution)/shard_map/ppermute | solution.py:29
  4.9 1.0 %collective-permute-done.1.refs_1_ = bf16[64,512]{1,0:T(8,128)(2,1)S(1)} collective-permute-done((bf16[64,512]{1,0:T(8,128)(2,1)}, bf16[64,512]{1,0:T(8,128)(2,1)S(1)}, u32[]{:S(2)}, u32[]{:S(2)}) %collective-permute-start.1) | collective-permute-done | bytes 65568 | tf_op jit(solution)/shard_map/ppermute | solution.py:29
  6.0 1.1 %collective-permute-done.3.refs_2_ = bf16[64,512]{1,0:T(8,128)(2,1)S(1)} collective-permute-done((bf16[64,512]{1,0:T(8,128)(2,1)}, bf16[64,512]{1,0:T(8,128)(2,1)S(1)}, u32[]{:S(2)}, u32[]{:S(2)}) %collective-permute-start.3) | collective-permute-done | bytes 65568 | tf_op jit(solution)/shard_map/ppermute | solution.py:29
  7.1 0.6 collective-permute-start.4
  7.7 2.7 %collective-permute-done.5.refs_3_ = bf16[64,512]{1,0:T(8,128)(2,1)S(1)} collective-permute-done((bf16[64,512]{1,0:T(8,128)(2,1)}, bf16[64,512]{1,0:T(8,128)(2,1)S(1)}, u32[]{:S(2)}, u32[]{:S(2)}) %collective-permute-start.5) | collective-permute-done | bytes 65568 | tf_op jit(solution)/shard_map/ppermute | solution.py:29
  10.5 3.7 %shard_map.229 = (f32[64,1024]{1,0:T(8,128)S(1)}, f32[64,1024]{1,0:T(8,128)S(1)}, bf16[256,512]{1,0:T(8,128)(2,1)S(1)}, bf16[256,512]{1,0:T(8,128)(2,1)S(1)}, f3...) custom-call(bf16[256,4096]{1,0:T(8,128)(2,1)} %refs_0_.2, ...), custom_call_target="tpu_custom_call" | custom-call | flops 10000000 | bytes 1000000 | tf_op jit(solution)/shard_map/pallas_call | solution.py:499
  14.2 0.4 shard_map.230
  14.7 0.6 shard_map.231
  15.3 0.5 collective-permute-start.10
  15.8 1.2 %collective-permute-start.12 = (bf16[64,256]{1,0:T(8,128)(2,1)S(1)}, bf16[64,256]{1,0:T(8,128)(2,1)S(1)}, u32[]{:S(2)}, u32[]{:S(2)}) collective-permute-start(bf16[64,256]{1,0:T(8,128)(2,1)S(1)} %get-tuple-element.70.refs_0_.refs_4_), channel_id=1, source_target_pairs={{0,7},{1,6},{2,5},{3,4},{4,3},{5,2},{6,1},{7,0},{8,15},{9,14},{10,... | collective-permute-start | bytes 98312 | tf_op jit(solution)/shard_map/ppermute | solution.py:29
  17.0 1.6 %collective-permute-start.8 = (bf16[64,256]{1,0:T(8,128)(2,1)S(1)}, bf16[64,256]{1,0:T(8,128)(2,1)S(1)}, u32[]{:S(2)}, u32[]{:S(2)}) collective-permute-start(bf16[64,256]{1,0:T(8,128)(2,1)S(1)} %get-tuple-element.70.refs_0_.refs_4_), channel_id=1, source_target_pairs={{0,3},{1,2},{2,1},{3,0},{4,7},{5,6},{6,5},{7,4},{8,11},{9,10},{10,... | collective-permute-start | bytes 98312 | tf_op jit(solution)/shard_map/ppermute | solution.py:29
  18.7 0.4 collective-permute-start.11
  19.1 1.0 %collective-permute-done.12.refs_3_ = bf16[64,256]{1,0:T(8,128)(2,1)S(1)} collective-permute-done((bf16[64,256]{1,0:T(8,128)(2,1)S(1)}, bf16[64,256]{1,0:T(8,128)(2,1)S(1)}, u32[]{:S(2)}, u32[]{:S(2)}) %collective-permute-start.12) | collective-permute-done | bytes 32800 | tf_op jit(solution)/shard_map/ppermute | solution.py:29
  20.1 0.4 collective-permute-start.13
  20.5 0.4 collective-permute-done.8.refs_1_
  21.1 2.0 %shard_map.232 = (bf16[256,2048]{1,0:T(8,128)(2,1)S(1)}, bf16[256,4096]{1,0:T(8,128)(2,1)S(1)}) custom-call(bf16[256,2048]{1,0:T(8,128)(2,1)} %refs_0_.3, bf16[256,4096]{1,0:T(8,128)(2,1)} %refs_1_.3), custom_call_target="tpu_custom_call" | custom-call | flops 10000000 | bytes 1000000 | tf_op jit(solution)/shard_map/pallas_call | solution.py:286
  23.4 0.6 shard_map.234
  24.0 0.5 collective-permute-start.14
  24.5 0.3 shard_map.235.own
  24.8 0.9 %collective-permute-done.14.other = bf16[4,64,512]{2,1,0:T(8,128)(2,1)S(1)} collective-permute-done((bf16[4,64,512]{2,1,0:T(8,128)(2,1)S(1)}, bf16[4,64,512]{2,1,0:T(8,128)(2,1)S(1)}, u32[]{:S(2)}, u32[]{:S(2)}) %collective-permute-start.14) | collective-permute-done | bytes 262176 | tf_op jit(solution)/shard_map/ppermute | solution.py:29
  25.7 1.1 %collective-permute-start.15 = (bf16[64,512]{1,0:T(8,128)(2,1)S(1)}, bf16[64,512]{1,0:T(8,128)(2,1)S(1)}, u32[]{:S(2)}, u32[]{:S(2)}) collective-permute-start(bf16[64,512]{1,0:T(8,128)(2,1)S(1)} %get-tuple-element.79), channel_id=1, source_target_pairs={{0,3},{1,2},{2,1},{3,0},{4,7},{5,6},{6,5},{7,4},{8,11},{9,10},{10,... | collective-permute-start | bytes 196616 | tf_op jit(solution)/shard_map/ppermute | solution.py:29
  26.7 0.4 collective-permute-start.16
  27.2 1.8 %collective-permute-start.17 = (bf16[64,512]{1,0:T(8,128)(2,1)S(1)}, bf16[64,512]{1,0:T(8,128)(2,1)S(1)}, u32[]{:S(2)}, u32[]{:S(2)}) collective-permute-start(bf16[64,512]{1,0:T(8,128)(2,1)S(1)} %get-tuple-element.81), channel_id=1, source_target_pairs={{0,7},{1,6},{2,5},{3,4},{4,3},{5,2},{6,1},{7,0},{8,15},{9,14},{10,... | collective-permute-start | bytes 196616 | tf_op jit(solution)/shard_map/ppermute | solution.py:29
  28.9 0.7 collective-permute-done.15.refs_2_
  29.6 1.0 %collective-permute-done.16.refs_3_ = bf16[64,512]{1,0:T(8,128)(2,1)S(1)} collective-permute-done((bf16[64,512]{1,0:T(8,128)(2,1)S(1)}, bf16[64,512]{1,0:T(8,128)(2,1)S(1)}, u32[]{:S(2)}, u32[]{:S(2)}) %collective-permute-start.16) | collective-permute-done | bytes 65568 | tf_op jit(solution)/shard_map/ppermute | solution.py:29
  30.6 1.6 %collective-permute-done.17.refs_4_ = bf16[64,512]{1,0:T(8,128)(2,1)S(1)} collective-permute-done((bf16[64,512]{1,0:T(8,128)(2,1)S(1)}, bf16[64,512]{1,0:T(8,128)(2,1)S(1)}, u32[]{:S(2)}, u32[]{:S(2)}) %collective-permute-start.17) | collective-permute-done | bytes 65568 | tf_op jit(solution)/shard_map/ppermute | solution.py:29
  32.5 2.4 %collective-permute-start.22 = (bf16[2,24,512]{2,1,0:T(8,128)(2,1)S(1)}, bf16[2,24,512]{2,1,0:T(8,128)(2,1)S(1)}, u32[]{:S(2)}, u32[]{:S(2)}) collective-permute-start(bf16[2,24,512]{2,1,0:T(8,128)(2,1)S(1)} %get-tuple-element.87), channel_id=1, source_target_pairs={{0,17},{1,16},{2,19},{3,18},{4,21},{5,20},{6,23},{7,22},{8,25},{9,... | collective-permute-start | bytes 147464 | tf_op jit(solution)/shard_map/ppermute | solution.py:35
  34.9 1.3 %collective-permute-start.23 = (bf16[2,24,512]{2,1,0:T(8,128)(2,1)S(1)}, bf16[2,24,512]{2,1,0:T(8,128)(2,1)S(1)}, u32[]{:S(2)}, u32[]{:S(2)}) collective-permute-start(bf16[2,24,512]{2,1,0:T(8,128)(2,1)S(1)} %get-tuple-element.88), channel_id=1, source_target_pairs={{0,25},{1,24},{2,27},{3,26},{4,29},{5,28},{6,31},{7,30},{8,17},{9,... | collective-permute-start | bytes 147464 | tf_op jit(solution)/shard_map/ppermute | solution.py:35
  36.4 0.7 collective-permute-done.22.refs_0_
  37.1 3.2 %collective-permute-done.23.refs_1_ = bf16[2,24,512]{2,1,0:T(8,128)(2,1)S(1)} collective-permute-done((bf16[2,24,512]{2,1,0:T(8,128)(2,1)S(1)}, bf16[2,24,512]{2,1,0:T(8,128)(2,1)S(1)}, u32[]{:S(2)}, u32[]{:S(2)}) %collective-permute-start.23) | collective-permute-done | bytes 49184 | tf_op jit(solution)/shard_map/ppermute | solution.py:35
  40.4 1.5 %collective-permute-start.25 = (bf16[2,48,512]{2,1,0:T(8,128)(2,1)S(1)}, bf16[2,48,512]{2,1,0:T(8,128)(2,1)S(1)}, u32[]{:S(2)}, u32[]{:S(2)}) collective-permute-start(bf16[2,48,512]{2,1,0:T(8,128)(2,1)S(1)} %shard_map.239.refs_4_), channel_id=1, source_target_pairs={{0,3},{1,2},{2,1},{3,0},{4,7},{5,6},{6,5},{7,4},{8,11},{9,10},{10,... | collective-permute-start | bytes 294920 | tf_op jit(solution)/shard_map/ppermute | solution.py:29
  41.9 0.6 collective-permute-start.27
  42.6 1.5 %collective-permute-start.19 = (bf16[2,48,512]{2,1,0:T(8,128)(2,1)S(1)}, bf16[2,48,512]{2,1,0:T(8,128)(2,1)S(1)}, u32[]{:S(2)}, u32[]{:S(2)}) collective-permute-start(bf16[2,48,512]{2,1,0:T(8,128)(2,1)S(1)} %shard_map.238.refs_0_), channel_id=1, source_target_pairs={{0,3},{1,2},{2,1},{3,0},{4,7},{5,6},{6,5},{7,4},{8,11},{9,10},{10,... | collective-permute-start | bytes 294920 | tf_op jit(solution)/shard_map/ppermute | solution.py:29
  44.1 1.7 %collective-permute-start.21 = (bf16[2,48,512]{2,1,0:T(8,128)(2,1)S(1)}, bf16[2,48,512]{2,1,0:T(8,128)(2,1)S(1)}, u32[]{:S(2)}, u32[]{:S(2)}) collective-permute-start(bf16[2,48,512]{2,1,0:T(8,128)(2,1)S(1)} %shard_map.238.refs_0_), channel_id=1, source_target_pairs={{0,7},{1,6},{2,5},{3,4},{4,3},{5,2},{6,1},{7,0},{8,15},{9,14},{10,... | collective-permute-start | bytes 294920 | tf_op jit(solution)/shard_map/ppermute | solution.py:29
  45.8 1.8 %collective-permute-start.29 = (bf16[2,48,512]{2,1,0:T(8,128)(2,1)S(1)}, bf16[2,48,512]{2,1,0:T(8,128)(2,1)S(1)}, u32[]{:S(2)}, u32[]{:S(2)}) collective-permute-start(bf16[2,48,512]{2,1,0:T(8,128)(2,1)S(1)} %shard_map.239.refs_4_), channel_id=1, source_target_pairs={{0,7},{1,6},{2,5},{3,4},{4,3},{5,2},{6,1},{7,0},{8,15},{9,14},{10,... | collective-permute-start | bytes 294920 | tf_op jit(solution)/shard_map/ppermute | solution.py:29
  47.6 0.5 collective-permute-start.32
  48.1 5.2 %collective-permute-done.20.refs_2_ = bf16[2,48,512]{2,1,0:T(8,128)(2,1)S(1)} collective-permute-done((bf16[2,48,512]{2,1,0:T(8,128)(2,1)S(1)}, bf16[2,48,512]{2,1,0:T(8,128)(2,1)S(1)}, u32[]{:S(2)}, u32[]{:S(2)}) %collective-permute-start.20) | collective-permute-done | bytes 98336 | tf_op jit(solution)/shard_map/ppermute | solution.py:29
  53.5 0.4 collective-permute-start.34
  54.0 0.4 collective-permute-start.26
  54.9 1.6 %shard_map.241.refs_11_ = bf16[256,4096]{1,0:T(8,128)(2,1)S(1)} custom-call(bf16[512,4096]{1,0:T(8,128)(2,1)} %bitcast.13), custom_call_target="tpu_custom_call" | custom-call | flops 10000000 | bytes 1000000 | tf_op jit(solution)/shard_map/pallas_call | solution.py:286
  56.5 2.9 %shard_map.240 = (bf16[512,4096]{1,0:T(8,128)(2,1)S(1)}, bf16[256,4096]{1,0:T(8,128)(2,1)S(1)}) custom-call(bf16[512,4096]{1,0:T(8,128)(2,1)} %bitcast.15, bf16[512,4096]{1,0:T(8,128)(2,1)} %bitcast.14), custom_call_target="tpu_custom_call" | custom-call | flops 10000000 | bytes 1000000 | tf_op jit(solution)/shard_map/pallas_call | solution.py:286
  59.4 2.2 %shard_map.242.refs_12_.down_w = bf16[512,4096]{1,0:T(8,128)(2,1)S(1)} custom-call(bf16[512,4096]{1,0:T(8,128)(2,1)} %bitcast.16), custom_call_target="tpu_custom_call" | custom-call | flops 10000000 | bytes 1000000 | tf_op jit(solution)/shard_map/pallas_call | solution.py:286
  61.6 1.3 %shard_map.243 = (f32[2,96,256]{2,1,0:T(8,128)S(1)}, f32[2,256,96]{2,1,0:T(8,128)S(1)}, f32[2,96,128]{2,1,0:T(8,128)S(1)}) custom-call(bf16[2,48,512]{2,1,0:T(8,128)(2,1)S(1)} %collective-permute-done.31.refs_0_, bf16[2,48,512]{2,1,0:T(8,128)(2,1)S(1)} %collective-permute-done.32.refs_1_, bf16[2,48,512]{2,1,0:T(8,128)(2,1)S(1)} %collective-permute-done.33.refs_2_, ...), custom_call_target="tpu_custom_call" | custom-call | flops 10000000 | bytes 1000000 | tf_op jit(solution)/shard_map/pallas_call | solution.py:582
  62.9 2.0 %shard_map.244 = (bf16[2,96,256]{2,1,0:T(8,128)(2,1)S(1)}, bf16[4,2,48,512]{3,2,1,0:T(8,128)(2,1)S(1)}) custom-call(bf16[2,48,512]{2,1,0:T(8,128)(2,1)S(1)} %shard_map.238.refs_0_, bf16[2,48,512]{2,1,0:T(8,128)(2,1)S(1)} %collective-permute-done.19.refs_1_, bf16[2,48,512]{2,1,0:T(8,128)(2,1)S(1)} %collective-permute-done.20.refs_2_, ...), custom_call_target="tpu_custom_call" | custom-call | flops 10000000 | bytes 1000000 | tf_op jit(solution)/shard_map/pallas_call | solution.py:588
  64.9 0.3 collective-permute-start.40
  65.2 1.2 %shard_map.245 = (bf16[4,2,48,512]{3,2,1,0:T(8,128)(2,1)S(1)}, bf16[4,2,48,512]{3,2,1,0:T(8,128)(2,1)S(1)}, bf16[4,2,48,512]{3,2,1,0:T(8,128)(2,1)S(1)}) custom-call(bf16[2,96,256]{2,1,0:T(8,128)(2,1)S(1)} %get-tuple-element.95.hidden, bf16[512,4096]{1,0:T(8,128)(2,1)S(1)} %shard_map.242.refs_12_.down_w), custom_call_target="tpu_custom_call" | custom-call | flops 10000000 | bytes 1000000 | tf_op jit(solution)/shard_map/pallas_call | solution.py:594
  66.5 0.3 collective-permute-start.35
  66.9 0.7 collective-permute-start.41
  67.5 1.4 %collective-permute-start.42 = (bf16[2,48,512]{2,1,0:T(8,128)(2,1)S(1)}, bf16[2,48,512]{2,1,0:T(8,128)(2,1)S(1)}, u32[]{:S(2)}, u32[]{:S(2)}) collective-permute-start(bf16[2,48,512]{2,1,0:T(8,128)(2,1)S(1)} %get-tuple-element.108), channel_id=1, source_target_pairs={{0,5},{1,4},{2,7},{3,6},{4,1},{5,0},{6,3},{7,2},{8,13},{9,12},{10,... | collective-permute-start | bytes 294920 | tf_op jit(solution)/shard_map/ppermute | solution.py:29
  69.0 1.1 %collective-permute-start.43 = (bf16[2,48,512]{2,1,0:T(8,128)(2,1)S(1)}, bf16[2,48,512]{2,1,0:T(8,128)(2,1)S(1)}, u32[]{:S(2)}, u32[]{:S(2)}) collective-permute-start(bf16[2,48,512]{2,1,0:T(8,128)(2,1)S(1)} %get-tuple-element.109), channel_id=1, source_target_pairs={{0,7},{1,6},{2,5},{3,4},{4,3},{5,2},{6,1},{7,0},{8,15},{9,14},{10,... | collective-permute-start | bytes 294920 | tf_op jit(solution)/shard_map/ppermute | solution.py:29
  70.1 0.6 collective-permute-start.36
  70.8 1.4 %collective-permute-start.37 = (bf16[2,48,512]{2,1,0:T(8,128)(2,1)S(1)}, bf16[2,48,512]{2,1,0:T(8,128)(2,1)S(1)}, u32[]{:S(2)}, u32[]{:S(2)}) collective-permute-start(bf16[2,48,512]{2,1,0:T(8,128)(2,1)S(1)} %get-tuple-element.100), channel_id=1, source_target_pairs={{0,5},{1,4},{2,7},{3,6},{4,1},{5,0},{6,3},{7,2},{8,13},{9,12},{10,... | collective-permute-start | bytes 294920 | tf_op jit(solution)/shard_map/ppermute | solution.py:29
  72.2 1.7 %collective-permute-start.38 = (bf16[2,48,512]{2,1,0:T(8,128)(2,1)S(1)}, bf16[2,48,512]{2,1,0:T(8,128)(2,1)S(1)}, u32[]{:S(2)}, u32[]{:S(2)}) collective-permute-start(bf16[2,48,512]{2,1,0:T(8,128)(2,1)S(1)} %get-tuple-element.101), channel_id=1, source_target_pairs={{0,7},{1,6},{2,5},{3,4},{4,3},{5,2},{6,1},{7,0},{8,15},{9,14},{10,... | collective-permute-start | bytes 294920 | tf_op jit(solution)/shard_map/ppermute | solution.py:29
  73.9 0.3 collective-permute-done.42.refs_2_
  74.3 0.3 collective-permute-done.43.refs_3_
  74.6 1.9 %collective-permute-start.44 = (bf16[2,24,512]{2,1,0:T(8,128)(2,1)S(1)}, bf16[2,24,512]{2,1,0:T(8,128)(2,1)S(1)}, u32[]{:S(2)}, u32[]{:S(2)}) collective-permute-start(bf16[2,24,512]{2,1,0:T(8,128)(2,1)S(1)} %get-tuple-element.110), channel_id=1, source_target_pairs={{0,16},{8,24},{16,0},{24,8},{1,17},{9,25},{17,1},{25,9},{2,18},{10... | collective-permute-start | bytes 147464 | tf_op jit(solution)/shard_map/ppermute | solution.py:29
  76.6 0.5 collective-permute-start.45
  77.1 1.0 %collective-permute-done.37.refs_2_ = bf16[2,48,512]{2,1,0:T(8,128)(2,1)S(1)} collective-permute-done((bf16[2,48,512]{2,1,0:T(8,128)(2,1)S(1)}, bf16[2,48,512]{2,1,0:T(8,128)(2,1)S(1)}, u32[]{:S(2)}, u32[]{:S(2)}) %collective-permute-start.37) | collective-permute-done | bytes 98336 | tf_op jit(solution)/shard_map/ppermute | solution.py:29
  78.1 0.6 collective-permute-done.38.refs_3_
  78.9 2.1 %shard_map.251 = (f32[64,16,64]{2,1,0:T(8,128)}, f32[64,16,64]{2,1,0:T(8,128)}) custom-call(bf16[64,256]{1,0:T(8,128)(2,1)S(1)} %get-tuple-element.112.driven, f32[64,1024]{1,0:T(8,128)S(1)} %get-tuple-element.113.dec_r, f32[64,1024]{1,0:T(8,128)S(1)} %get-tuple-element.114.dec_i, bf16[256,512]{1,0:T(8,128)(2,1)S(1)} %get-tuple-element.115.bt_r, ...), custom_call_target="tpu_custom_call" | custom-call | flops 10000000 | bytes 1000000 | tf_op jit(solution)/shard_map/pallas_call | solution.py:609
  81.0 1.5 %collective-permute-done.45.refs_6_ = bf16[2,24,512]{2,1,0:T(8,128)(2,1)S(1)} collective-permute-done((bf16[2,24,512]{2,1,0:T(8,128)(2,1)S(1)}, bf16[2,24,512]{2,1,0:T(8,128)(2,1)S(1)}, u32[]{:S(2)}, u32[]{:S(2)}) %collective-permute-start.45) | collective-permute-done | bytes 49184 | tf_op jit(solution)/shard_map/ppermute | solution.py:29
  82.5 1.0 %collective-permute-done.39.refs_4_ = bf16[2,24,512]{2,1,0:T(8,128)(2,1)S(1)} collective-permute-done((bf16[2,24,512]{2,1,0:T(8,128)(2,1)S(1)}, bf16[2,24,512]{2,1,0:T(8,128)(2,1)S(1)}, u32[]{:S(2)}, u32[]{:S(2)}) %collective-permute-start.39) | collective-permute-done | bytes 49184 | tf_op jit(solution)/shard_map/ppermute | solution.py:29
  83.5 0.9 %shard_map.250 = bf16[64,512]{1,0:T(8,128)(2,1)} custom-call(bf16[64,512]{1,0:T(8,128)(2,1)S(1)} %get-tuple-element.83.refs_0_, bf16[2,64,192]{2,1,0:T(8,128)(2,1)S(1)} %get-tuple-element.84.refs_1_, f32[2,64]{1,0:T(2,128)S(1)} %bitcast.12, bf16[2,24,512]{2,1,0:T(8,128)(2,1)S(1)} %get-tuple-element.102.refs_3_, ...), custom_call_target="tpu_custom_call" | custom-call | flops 10000000 | bytes 1000000 | tf_op jit(solution)/shard_map/pallas_call | solution.py:615
  (53 shorter events, 2.5 us)
Async XLA Ops:
  0.6 5.3 %collective-permute-start.1 = (bf16[64,512]{1,0:T(8,128)(2,1)}, bf16[64,512]{1,0:T(8,128)(2,1)S(1)}, u32[]{:S(2)}, u32[]{:S(2)}) collective-permute-start(bf16[64,512]{1,0:T(8,128)(2,1)} %refs_15_.1), channel_id=1, source_target_pairs={{0,3},{1,2},{2,1},{3,0},{4,7},{5,6},{6,5},{7,4},{8,11},{9,10},{10,... | collective-permute-start | bytes 196616 | tf_op jit(solution)/shard_map/ppermute | solution.py:29
  3.1 4.0 %collective-permute-start.3 = (bf16[64,512]{1,0:T(8,128)(2,1)}, bf16[64,512]{1,0:T(8,128)(2,1)S(1)}, u32[]{:S(2)}, u32[]{:S(2)}) collective-permute-start(bf16[64,512]{1,0:T(8,128)(2,1)} %refs_15_.1), channel_id=1, source_target_pairs={{0,5},{1,4},{2,7},{3,6},{4,1},{5,0},{6,3},{7,2},{8,13},{9,12},{10,... | collective-permute-start | bytes 196616 | tf_op jit(solution)/shard_map/ppermute | solution.py:29
  4.9 5.5 %collective-permute-start.5 = (bf16[64,512]{1,0:T(8,128)(2,1)}, bf16[64,512]{1,0:T(8,128)(2,1)S(1)}, u32[]{:S(2)}, u32[]{:S(2)}) collective-permute-start(bf16[64,512]{1,0:T(8,128)(2,1)} %refs_15_.1), channel_id=1, source_target_pairs={{0,7},{1,6},{2,5},{3,4},{4,3},{5,2},{6,1},{7,0},{8,15},{9,14},{10,... | collective-permute-start | bytes 196616 | tf_op jit(solution)/shard_map/ppermute | solution.py:29
  4.9 9.7 %collective-permute-start = (bf16[64,512]{1,0:T(8,128)(2,1)}, bf16[64,512]{1,0:T(8,128)(2,1)S(1)}, u32[]{:S(2)}, u32[]{:S(2)}) collective-permute-start(bf16[64,512]{1,0:T(8,128)(2,1)} %refs_15_.1), channel_id=1, source_target_pairs={{0,1},{1,0},{2,3},{3,2},{4,5},{5,4},{6,7},{7,6},{8,9},{9,8},{10,11... | collective-permute-start | bytes 196616 | tf_op jit(solution)/shard_map/ppermute | solution.py:29
  5.9 8.8 %collective-permute-start.2 = (bf16[64,512]{1,0:T(8,128)(2,1)S(1)}, bf16[64,512]{1,0:T(8,128)(2,1)S(1)}, u32[]{:S(2)}, u32[]{:S(2)}) collective-permute-start(bf16[64,512]{1,0:T(8,128)(2,1)S(1)} %collective-permute-done.1.refs_1_), channel_id=1, source_target_pairs={{0,1},{1,0},{2,3},{3,2},{4,5},{5,4},{6,7},{7,6},{8,9},{9,8},{10,11... | collective-permute-start | bytes 196616 | tf_op jit(solution)/shard_map/ppermute | solution.py:29
  7.1 7.6 %collective-permute-start.4 = (bf16[64,512]{1,0:T(8,128)(2,1)S(1)}, bf16[64,512]{1,0:T(8,128)(2,1)S(1)}, u32[]{:S(2)}, u32[]{:S(2)}) collective-permute-start(bf16[64,512]{1,0:T(8,128)(2,1)S(1)} %collective-permute-done.3.refs_2_), channel_id=1, source_target_pairs={{0,1},{1,0},{2,3},{3,2},{4,5},{5,4},{6,7},{7,6},{8,9},{9,8},{10,11... | collective-permute-start | bytes 196616 | tf_op jit(solution)/shard_map/ppermute | solution.py:29
  10.4 4.3 %collective-permute-start.6 = (bf16[64,512]{1,0:T(8,128)(2,1)S(1)}, bf16[64,512]{1,0:T(8,128)(2,1)S(1)}, u32[]{:S(2)}, u32[]{:S(2)}) collective-permute-start(bf16[64,512]{1,0:T(8,128)(2,1)S(1)} %collective-permute-done.5.refs_3_), channel_id=1, source_target_pairs={{0,1},{1,0},{2,3},{3,2},{4,5},{5,4},{6,7},{7,6},{8,9},{9,8},{10,11... | collective-permute-start | bytes 196616 | tf_op jit(solution)/shard_map/ppermute | solution.py:29
  15.3 3.4 %collective-permute-start.10 = (bf16[64,256]{1,0:T(8,128)(2,1)S(1)}, bf16[64,256]{1,0:T(8,128)(2,1)S(1)}, u32[]{:S(2)}, u32[]{:S(2)}) collective-permute-start(bf16[64,256]{1,0:T(8,128)(2,1)S(1)} %get-tuple-element.70.refs_0_.refs_4_), channel_id=1, source_target_pairs={{0,5},{1,4},{2,7},{3,6},{4,1},{5,0},{6,3},{7,2},{8,13},{9,12},{10,... | collective-permute-start | bytes 98312 | tf_op jit(solution)/shard_map/ppermute | solution.py:29
  15.8 4.3 %collective-permute-start.12 = (bf16[64,256]{1,0:T(8,128)(2,1)S(1)}, bf16[64,256]{1,0:T(8,128)(2,1)S(1)}, u32[]{:S(2)}, u32[]{:S(2)}) collective-permute-start(bf16[64,256]{1,0:T(8,128)(2,1)S(1)} %get-tuple-element.70.refs_0_.refs_4_), channel_id=1, source_target_pairs={{0,7},{1,6},{2,5},{3,4},{4,3},{5,2},{6,1},{7,0},{8,15},{9,14},{10,... | collective-permute-start | bytes 98312 | tf_op jit(solution)/shard_map/ppermute | solution.py:29
  17.0 3.9 %collective-permute-start.8 = (bf16[64,256]{1,0:T(8,128)(2,1)S(1)}, bf16[64,256]{1,0:T(8,128)(2,1)S(1)}, u32[]{:S(2)}, u32[]{:S(2)}) collective-permute-start(bf16[64,256]{1,0:T(8,128)(2,1)S(1)} %get-tuple-element.70.refs_0_.refs_4_), channel_id=1, source_target_pairs={{0,3},{1,2},{2,1},{3,0},{4,7},{5,6},{6,5},{7,4},{8,11},{9,10},{10,... | collective-permute-start | bytes 98312 | tf_op jit(solution)/shard_map/ppermute | solution.py:29
  18.6 4.8 %collective-permute-start.7 = (bf16[64,256]{1,0:T(8,128)(2,1)S(1)}, bf16[64,256]{1,0:T(8,128)(2,1)S(1)}, u32[]{:S(2)}, u32[]{:S(2)}) collective-permute-start(bf16[64,256]{1,0:T(8,128)(2,1)S(1)} %get-tuple-element.70.refs_0_.refs_4_), channel_id=1, source_target_pairs={{0,1},{1,0},{2,3},{3,2},{4,5},{5,4},{6,7},{7,6},{8,9},{9,8},{10,11... | collective-permute-start | bytes 98312 | tf_op jit(solution)/shard_map/ppermute | solution.py:29
  18.7 4.7 %collective-permute-start.11 = (bf16[64,256]{1,0:T(8,128)(2,1)S(1)}, bf16[64,256]{1,0:T(8,128)(2,1)S(1)}, u32[]{:S(2)}, u32[]{:S(2)}) collective-permute-start(bf16[64,256]{1,0:T(8,128)(2,1)S(1)} %collective-permute-done.10.refs_2_), channel_id=1, source_target_pairs={{0,1},{1,0},{2,3},{3,2},{4,5},{5,4},{6,7},{7,6},{8,9},{9,8},{10,11... | collective-permute-start | bytes 98312 | tf_op jit(solution)/shard_map/ppermute | solution.py:29
  20.1 3.3 %collective-permute-start.13 = (bf16[64,256]{1,0:T(8,128)(2,1)S(1)}, bf16[64,256]{1,0:T(8,128)(2,1)S(1)}, u32[]{:S(2)}, u32[]{:S(2)}) collective-permute-start(bf16[64,256]{1,0:T(8,128)(2,1)S(1)} %collective-permute-done.12.refs_3_), channel_id=1, source_target_pairs={{0,1},{1,0},{2,3},{3,2},{4,5},{5,4},{6,7},{7,6},{8,9},{9,8},{10,11... | collective-permute-start | bytes 98312 | tf_op jit(solution)/shard_map/ppermute | solution.py:29
  21.0 2.5 %collective-permute-start.9 = (bf16[64,256]{1,0:T(8,128)(2,1)S(1)}, bf16[64,256]{1,0:T(8,128)(2,1)S(1)}, u32[]{:S(2)}, u32[]{:S(2)}) collective-permute-start(bf16[64,256]{1,0:T(8,128)(2,1)S(1)} %collective-permute-done.8.refs_1_), channel_id=1, source_target_pairs={{0,1},{1,0},{2,3},{3,2},{4,5},{5,4},{6,7},{7,6},{8,9},{9,8},{10,11... | collective-permute-start | bytes 98312 | tf_op jit(solution)/shard_map/ppermute | solution.py:29
  24.0 1.6 %collective-permute-start.14 = (bf16[4,64,512]{2,1,0:T(8,128)(2,1)S(1)}, bf16[4,64,512]{2,1,0:T(8,128)(2,1)S(1)}, u32[]{:S(2)}, u32[]{:S(2)}) collective-permute-start(bf16[4,64,512]{2,1,0:T(8,128)(2,1)S(1)} %get-tuple-element.77), channel_id=1, source_target_pairs={{0,1},{1,0},{2,3},{3,2},{4,5},{5,4},{6,7},{7,6},{8,9},{9,8},{10,11... | collective-permute-start | bytes 786440 | tf_op jit(solution)/shard_map/ppermute | solution.py:29
  25.7 3.9 %collective-permute-start.15 = (bf16[64,512]{1,0:T(8,128)(2,1)S(1)}, bf16[64,512]{1,0:T(8,128)(2,1)S(1)}, u32[]{:S(2)}, u32[]{:S(2)}) collective-permute-start(bf16[64,512]{1,0:T(8,128)(2,1)S(1)} %get-tuple-element.79), channel_id=1, source_target_pairs={{0,3},{1,2},{2,1},{3,0},{4,7},{5,6},{6,5},{7,4},{8,11},{9,10},{10,... | collective-permute-start | bytes 196616 | tf_op jit(solution)/shard_map/ppermute | solution.py:29
  26.7 3.8 %collective-permute-start.16 = (bf16[64,512]{1,0:T(8,128)(2,1)S(1)}, bf16[64,512]{1,0:T(8,128)(2,1)S(1)}, u32[]{:S(2)}, u32[]{:S(2)}) collective-permute-start(bf16[64,512]{1,0:T(8,128)(2,1)S(1)} %get-tuple-element.80), channel_id=1, source_target_pairs={{0,5},{1,4},{2,7},{3,6},{4,1},{5,0},{6,3},{7,2},{8,13},{9,12},{10,... | collective-permute-start | bytes 196616 | tf_op jit(solution)/shard_map/ppermute | solution.py:29
  27.2 5.1 %collective-permute-start.17 = (bf16[64,512]{1,0:T(8,128)(2,1)S(1)}, bf16[64,512]{1,0:T(8,128)(2,1)S(1)}, u32[]{:S(2)}, u32[]{:S(2)}) collective-permute-start(bf16[64,512]{1,0:T(8,128)(2,1)S(1)} %get-tuple-element.81), channel_id=1, source_target_pairs={{0,7},{1,6},{2,5},{3,4},{4,3},{5,2},{6,1},{7,0},{8,15},{9,14},{10,... | collective-permute-start | bytes 196616 | tf_op jit(solution)/shard_map/ppermute | solution.py:29
  32.5 4.7 %collective-permute-start.22 = (bf16[2,24,512]{2,1,0:T(8,128)(2,1)S(1)}, bf16[2,24,512]{2,1,0:T(8,128)(2,1)S(1)}, u32[]{:S(2)}, u32[]{:S(2)}) collective-permute-start(bf16[2,24,512]{2,1,0:T(8,128)(2,1)S(1)} %get-tuple-element.87), channel_id=1, source_target_pairs={{0,17},{1,16},{2,19},{3,18},{4,21},{5,20},{6,23},{7,22},{8,25},{9,... | collective-permute-start | bytes 147464 | tf_op jit(solution)/shard_map/ppermute | solution.py:35
  34.9 5.5 %collective-permute-start.23 = (bf16[2,24,512]{2,1,0:T(8,128)(2,1)S(1)}, bf16[2,24,512]{2,1,0:T(8,128)(2,1)S(1)}, u32[]{:S(2)}, u32[]{:S(2)}) collective-permute-start(bf16[2,24,512]{2,1,0:T(8,128)(2,1)S(1)} %get-tuple-element.88), channel_id=1, source_target_pairs={{0,25},{1,24},{2,27},{3,26},{4,29},{5,28},{6,31},{7,30},{8,17},{9,... | collective-permute-start | bytes 147464 | tf_op jit(solution)/shard_map/ppermute | solution.py:35
  36.2 6.4 %collective-permute-start.18 = (bf16[2,24,512]{2,1,0:T(8,128)(2,1)S(1)}, bf16[2,24,512]{2,1,0:T(8,128)(2,1)S(1)}, u32[]{:S(2)}, u32[]{:S(2)}) collective-permute-start(bf16[2,24,512]{2,1,0:T(8,128)(2,1)S(1)} %get-tuple-element.86), channel_id=1, source_target_pairs={{0,8},{8,0},{16,24},{24,16},{1,9},{9,1},{17,25},{25,17},{2,10},{10... | collective-permute-start | bytes 147464 | tf_op jit(solution)/shard_map/ppermute | solution.py:29
  40.4 5.4 %collective-permute-start.25 = (bf16[2,48,512]{2,1,0:T(8,128)(2,1)S(1)}, bf16[2,48,512]{2,1,0:T(8,128)(2,1)S(1)}, u32[]{:S(2)}, u32[]{:S(2)}) collective-permute-start(bf16[2,48,512]{2,1,0:T(8,128)(2,1)S(1)} %shard_map.239.refs_4_), channel_id=1, source_target_pairs={{0,3},{1,2},{2,1},{3,0},{4,7},{5,6},{6,5},{7,4},{8,11},{9,10},{10,... | collective-permute-start | bytes 294920 | tf_op jit(solution)/shard_map/ppermute | solution.py:29
  41.9 5.7 %collective-permute-start.27 = (bf16[2,48,512]{2,1,0:T(8,128)(2,1)S(1)}, bf16[2,48,512]{2,1,0:T(8,128)(2,1)S(1)}, u32[]{:S(2)}, u32[]{:S(2)}) collective-permute-start(bf16[2,48,512]{2,1,0:T(8,128)(2,1)S(1)} %shard_map.239.refs_4_), channel_id=1, source_target_pairs={{0,5},{1,4},{2,7},{3,6},{4,1},{5,0},{6,3},{7,2},{8,13},{9,12},{10,... | collective-permute-start | bytes 294920 | tf_op jit(solution)/shard_map/ppermute | solution.py:29
  42.6 5.1 %collective-permute-start.19 = (bf16[2,48,512]{2,1,0:T(8,128)(2,1)S(1)}, bf16[2,48,512]{2,1,0:T(8,128)(2,1)S(1)}, u32[]{:S(2)}, u32[]{:S(2)}) collective-permute-start(bf16[2,48,512]{2,1,0:T(8,128)(2,1)S(1)} %shard_map.238.refs_0_), channel_id=1, source_target_pairs={{0,3},{1,2},{2,1},{3,0},{4,7},{5,6},{6,5},{7,4},{8,11},{9,10},{10,... | collective-permute-start | bytes 294920 | tf_op jit(solution)/shard_map/ppermute | solution.py:29
  44.1 9.3 %collective-permute-start.20 = (bf16[2,48,512]{2,1,0:T(8,128)(2,1)S(1)}, bf16[2,48,512]{2,1,0:T(8,128)(2,1)S(1)}, u32[]{:S(2)}, u32[]{:S(2)}) collective-permute-start(bf16[2,48,512]{2,1,0:T(8,128)(2,1)S(1)} %shard_map.238.refs_0_), channel_id=1, source_target_pairs={{0,5},{1,4},{2,7},{3,6},{4,1},{5,0},{6,3},{7,2},{8,13},{9,12},{10,... | collective-permute-start | bytes 294920 | tf_op jit(solution)/shard_map/ppermute | solution.py:29
  44.1 9.4 %collective-permute-start.21 = (bf16[2,48,512]{2,1,0:T(8,128)(2,1)S(1)}, bf16[2,48,512]{2,1,0:T(8,128)(2,1)S(1)}, u32[]{:S(2)}, u32[]{:S(2)}) collective-permute-start(bf16[2,48,512]{2,1,0:T(8,128)(2,1)S(1)} %shard_map.238.refs_0_), channel_id=1, source_target_pairs={{0,7},{1,6},{2,5},{3,4},{4,3},{5,2},{6,1},{7,0},{8,15},{9,14},{10,... | collective-permute-start | bytes 294920 | tf_op jit(solution)/shard_map/ppermute | solution.py:29
  45.8 8.1 %collective-permute-start.29 = (bf16[2,48,512]{2,1,0:T(8,128)(2,1)S(1)}, bf16[2,48,512]{2,1,0:T(8,128)(2,1)S(1)}, u32[]{:S(2)}, u32[]{:S(2)}) collective-permute-start(bf16[2,48,512]{2,1,0:T(8,128)(2,1)S(1)} %shard_map.239.refs_4_), channel_id=1, source_target_pairs={{0,7},{1,6},{2,5},{3,4},{4,3},{5,2},{6,1},{7,0},{8,15},{9,14},{10,... | collective-permute-start | bytes 294920 | tf_op jit(solution)/shard_map/ppermute | solution.py:29
  47.6 6.4 %collective-permute-start.31 = (bf16[2,48,512]{2,1,0:T(8,128)(2,1)S(1)}, bf16[2,48,512]{2,1,0:T(8,128)(2,1)S(1)}, u32[]{:S(2)}, u32[]{:S(2)}) collective-permute-start(bf16[2,48,512]{2,1,0:T(8,128)(2,1)S(1)} %shard_map.238.refs_0_), channel_id=1, source_target_pairs={{0,1},{1,0},{2,3},{3,2},{4,5},{5,4},{6,7},{7,6},{8,9},{9,8},{10,11... | collective-permute-start | bytes 294920 | tf_op jit(solution)/shard_map/ppermute | solution.py:29
  47.6 6.8 %collective-permute-start.32 = (bf16[2,48,512]{2,1,0:T(8,128)(2,1)S(1)}, bf16[2,48,512]{2,1,0:T(8,128)(2,1)S(1)}, u32[]{:S(2)}, u32[]{:S(2)}) collective-permute-start(bf16[2,48,512]{2,1,0:T(8,128)(2,1)S(1)} %collective-permute-done.19.refs_1_), channel_id=1, source_target_pairs={{0,1},{1,0},{2,3},{3,2},{4,5},{5,4},{6,7},{7,6},{8,9},{9,8},{10,11... | collective-permute-start | bytes 294920 | tf_op jit(solution)/shard_map/ppermute | solution.py:29
  53.3 1.3 %collective-permute-start.33 = (bf16[2,48,512]{2,1,0:T(8,128)(2,1)S(1)}, bf16[2,48,512]{2,1,0:T(8,128)(2,1)S(1)}, u32[]{:S(2)}, u32[]{:S(2)}) collective-permute-start(bf16[2,48,512]{2,1,0:T(8,128)(2,1)S(1)} %collective-permute-done.20.refs_2_), channel_id=1, source_target_pairs={{0,1},{1,0},{2,3},{3,2},{4,5},{5,4},{6,7},{7,6},{8,9},{9,8},{10,11... | collective-permute-start | bytes 294920 | tf_op jit(solution)/shard_map/ppermute | solution.py:29
  53.5 8.1 %collective-permute-start.34 = (bf16[2,48,512]{2,1,0:T(8,128)(2,1)S(1)}, bf16[2,48,512]{2,1,0:T(8,128)(2,1)S(1)}, u32[]{:S(2)}, u32[]{:S(2)}) collective-permute-start(bf16[2,48,512]{2,1,0:T(8,128)(2,1)S(1)} %collective-permute-done.21.refs_3_), channel_id=1, source_target_pairs={{0,1},{1,0},{2,3},{3,2},{4,5},{5,4},{6,7},{7,6},{8,9},{9,8},{10,11... | collective-permute-start | bytes 294920 | tf_op jit(solution)/shard_map/ppermute | solution.py:29
  53.9 9.0 %collective-permute-start.24 = (bf16[2,48,512]{2,1,0:T(8,128)(2,1)S(1)}, bf16[2,48,512]{2,1,0:T(8,128)(2,1)S(1)}, u32[]{:S(2)}, u32[]{:S(2)}) collective-permute-start(bf16[2,48,512]{2,1,0:T(8,128)(2,1)S(1)} %shard_map.239.refs_4_), channel_id=1, source_target_pairs={{0,1},{1,0},{2,3},{3,2},{4,5},{5,4},{6,7},{7,6},{8,9},{9,8},{10,11... | collective-permute-start | bytes 294920 | tf_op jit(solution)/shard_map/ppermute | solution.py:29
  54.0 8.9 %collective-permute-start.26 = (bf16[2,48,512]{2,1,0:T(8,128)(2,1)S(1)}, bf16[2,48,512]{2,1,0:T(8,128)(2,1)S(1)}, u32[]{:S(2)}, u32[]{:S(2)}) collective-permute-start(bf16[2,48,512]{2,1,0:T(8,128)(2,1)S(1)} %collective-permute-done.25.refs_5_), channel_id=1, source_target_pairs={{0,1},{1,0},{2,3},{3,2},{4,5},{5,4},{6,7},{7,6},{8,9},{9,8},{10,11... | collective-permute-start | bytes 294920 | tf_op jit(solution)/shard_map/ppermute | solution.py:29
  54.4 8.5 %collective-permute-start.28 = (bf16[2,48,512]{2,1,0:T(8,128)(2,1)S(1)}, bf16[2,48,512]{2,1,0:T(8,128)(2,1)S(1)}, u32[]{:S(2)}, u32[]{:S(2)}) collective-permute-start(bf16[2,48,512]{2,1,0:T(8,128)(2,1)S(1)} %collective-permute-done.27.refs_6_), channel_id=1, source_target_pairs={{0,1},{1,0},{2,3},{3,2},{4,5},{5,4},{6,7},{7,6},{8,9},{9,8},{10,11... | collective-permute-start | bytes 294920 | tf_op jit(solution)/shard_map/ppermute | solution.py:29
  54.6 8.3 %collective-permute-start.30 = (bf16[2,48,512]{2,1,0:T(8,128)(2,1)S(1)}, bf16[2,48,512]{2,1,0:T(8,128)(2,1)S(1)}, u32[]{:S(2)}, u32[]{:S(2)}) collective-permute-start(bf16[2,48,512]{2,1,0:T(8,128)(2,1)S(1)} %collective-permute-done.29.refs_7_), channel_id=1, source_target_pairs={{0,1},{1,0},{2,3},{3,2},{4,5},{5,4},{6,7},{7,6},{8,9},{9,8},{10,11... | collective-permute-start | bytes 294920 | tf_op jit(solution)/shard_map/ppermute | solution.py:29
  64.9 1.9 %collective-permute-start.40 = (bf16[4,2,48,512]{3,2,1,0:T(8,128)(2,1)S(1)}, bf16[4,2,48,512]{3,2,1,0:T(8,128)(2,1)S(1)}, u32[]{:S(2)}, u32[]{:S(2)}) collective-permute-start(bf16[4,2,48,512]{3,2,1,0:T(8,128)(2,1)S(1)} %get-tuple-element.105), channel_id=1, source_target_pairs={{0,1},{1,0},{2,3},{3,2},{4,5},{5,4},{6,7},{7,6},{8,9},{9,8},{10,11... | collective-permute-start | bytes 1179656 | tf_op jit(solution)/shard_map/ppermute | solution.py:29
  66.5 17.1 %copy-start = (f32[64,2]{0,1:T(2,128)S(1)}, f32[64,2]{0,1:T(2,128)}, u32[]{:S(2)}) copy-start(f32[64,2]{0,1:T(2,128)} %param.40) | copy-start | bytes 1540
  66.5 3.6 %collective-permute-start.35 = (bf16[4,2,48,512]{3,2,1,0:T(8,128)(2,1)S(1)}, bf16[4,2,48,512]{3,2,1,0:T(8,128)(2,1)S(1)}, u32[]{:S(2)}, u32[]{:S(2)}) collective-permute-start(bf16[4,2,48,512]{3,2,1,0:T(8,128)(2,1)S(1)} %get-tuple-element.97), channel_id=1, source_target_pairs={{0,1},{1,0},{2,3},{3,2},{4,5},{5,4},{6,7},{7,6},{8,9},{9,8},{10,11... | collective-permute-start | bytes 1179656 | tf_op jit(solution)/shard_map/ppermute | solution.py:29
  66.9 5.3 %collective-permute-start.41 = (bf16[2,48,512]{2,1,0:T(8,128)(2,1)S(1)}, bf16[2,48,512]{2,1,0:T(8,128)(2,1)S(1)}, u32[]{:S(2)}, u32[]{:S(2)}) collective-permute-start(bf16[2,48,512]{2,1,0:T(8,128)(2,1)S(1)} %get-tuple-element.107), channel_id=1, source_target_pairs={{0,3},{1,2},{2,1},{3,0},{4,7},{5,6},{6,5},{7,4},{8,11},{9,10},{10,... | collective-permute-start | bytes 294920 | tf_op jit(solution)/shard_map/ppermute | solution.py:29
  67.5 6.7 %collective-permute-start.42 = (bf16[2,48,512]{2,1,0:T(8,128)(2,1)S(1)}, bf16[2,48,512]{2,1,0:T(8,128)(2,1)S(1)}, u32[]{:S(2)}, u32[]{:S(2)}) collective-permute-start(bf16[2,48,512]{2,1,0:T(8,128)(2,1)S(1)} %get-tuple-element.108), channel_id=1, source_target_pairs={{0,5},{1,4},{2,7},{3,6},{4,1},{5,0},{6,3},{7,2},{8,13},{9,12},{10,... | collective-permute-start | bytes 294920 | tf_op jit(solution)/shard_map/ppermute | solution.py:29
  69.0 5.6 %collective-permute-start.43 = (bf16[2,48,512]{2,1,0:T(8,128)(2,1)S(1)}, bf16[2,48,512]{2,1,0:T(8,128)(2,1)S(1)}, u32[]{:S(2)}, u32[]{:S(2)}) collective-permute-start(bf16[2,48,512]{2,1,0:T(8,128)(2,1)S(1)} %get-tuple-element.109), channel_id=1, source_target_pairs={{0,7},{1,6},{2,5},{3,4},{4,3},{5,2},{6,1},{7,0},{8,15},{9,14},{10,... | collective-permute-start | bytes 294920 | tf_op jit(solution)/shard_map/ppermute | solution.py:29
  70.1 7.0 %collective-permute-start.36 = (bf16[2,48,512]{2,1,0:T(8,128)(2,1)S(1)}, bf16[2,48,512]{2,1,0:T(8,128)(2,1)S(1)}, u32[]{:S(2)}, u32[]{:S(2)}) collective-permute-start(bf16[2,48,512]{2,1,0:T(8,128)(2,1)S(1)} %get-tuple-element.99), channel_id=1, source_target_pairs={{0,3},{1,2},{2,1},{3,0},{4,7},{5,6},{6,5},{7,4},{8,11},{9,10},{10,... | collective-permute-start | bytes 294920 | tf_op jit(solution)/shard_map/ppermute | solution.py:29
  70.8 7.3 %collective-permute-start.37 = (bf16[2,48,512]{2,1,0:T(8,128)(2,1)S(1)}, bf16[2,48,512]{2,1,0:T(8,128)(2,1)S(1)}, u32[]{:S(2)}, u32[]{:S(2)}) collective-permute-start(bf16[2,48,512]{2,1,0:T(8,128)(2,1)S(1)} %get-tuple-element.100), channel_id=1, source_target_pairs={{0,5},{1,4},{2,7},{3,6},{4,1},{5,0},{6,3},{7,2},{8,13},{9,12},{10,... | collective-permute-start | bytes 294920 | tf_op jit(solution)/shard_map/ppermute | solution.py:29
  72.2 6.5 %collective-permute-start.38 = (bf16[2,48,512]{2,1,0:T(8,128)(2,1)S(1)}, bf16[2,48,512]{2,1,0:T(8,128)(2,1)S(1)}, u32[]{:S(2)}, u32[]{:S(2)}) collective-permute-start(bf16[2,48,512]{2,1,0:T(8,128)(2,1)S(1)} %get-tuple-element.101), channel_id=1, source_target_pairs={{0,7},{1,6},{2,5},{3,4},{4,3},{5,2},{6,1},{7,0},{8,15},{9,14},{10,... | collective-permute-start | bytes 294920 | tf_op jit(solution)/shard_map/ppermute | solution.py:29
  74.6 6.4 %collective-permute-start.44 = (bf16[2,24,512]{2,1,0:T(8,128)(2,1)S(1)}, bf16[2,24,512]{2,1,0:T(8,128)(2,1)S(1)}, u32[]{:S(2)}, u32[]{:S(2)}) collective-permute-start(bf16[2,24,512]{2,1,0:T(8,128)(2,1)S(1)} %get-tuple-element.110), channel_id=1, source_target_pairs={{0,16},{8,24},{16,0},{24,8},{1,17},{9,25},{17,1},{25,9},{2,18},{10... | collective-permute-start | bytes 147464 | tf_op jit(solution)/shard_map/ppermute | solution.py:29
  76.6 6.0 %collective-permute-start.45 = (bf16[2,24,512]{2,1,0:T(8,128)(2,1)S(1)}, bf16[2,24,512]{2,1,0:T(8,128)(2,1)S(1)}, u32[]{:S(2)}, u32[]{:S(2)}) collective-permute-start(bf16[2,24,512]{2,1,0:T(8,128)(2,1)S(1)} %get-tuple-element.111), channel_id=1, source_target_pairs={{0,24},{8,16},{16,8},{24,0},{1,25},{9,17},{17,9},{25,1},{2,26},{10... | collective-permute-start | bytes 147464 | tf_op jit(solution)/shard_map/ppermute | solution.py:29
  78.8 4.7 %collective-permute-start.39 = (bf16[2,24,512]{2,1,0:T(8,128)(2,1)S(1)}, bf16[2,24,512]{2,1,0:T(8,128)(2,1)S(1)}, u32[]{:S(2)}, u32[]{:S(2)}) collective-permute-start(bf16[2,24,512]{2,1,0:T(8,128)(2,1)S(1)} %get-tuple-element.103), channel_id=1, source_target_pairs={{0,8},{8,0},{16,24},{24,16},{1,9},{9,1},{17,25},{25,17},{2,10},{10... | collective-permute-start | bytes 147464 | tf_op jit(solution)/shard_map/ppermute | solution.py:29
